TPU v7x, 128 devices: a whole 4x4x4 slice. The times are simulated.
128 devices in a mesh: fs: 16 (over z, y), tp: 8 (over x, core).
Axes of the slice: x: 4, y: 4, z: 4, core: 2. Of those that a mesh axis runs over, the one named last changes fastest.
Arguments:
- inputs: bfloat16 [49152, 2048], P('fs'), may hold values from -6 to 6
- cot_query: bfloat16 [49152, 2048], P('fs', 'tp'), may hold values from -0.0625 to 0.0625
- cot_value: bfloat16 [49152, 4096], P('fs', 'tp'), may hold values from -0.0625 to 0.0625
- proj_query: bfloat16 [2048, 256], replicated, may hold values from -0.375 to 0.375
- proj_value: bfloat16 [2048, 256], replicated, may hold values from -0.375 to 0.375
- w_query: float32 [2048, 2048], P('fs', 'tp'), may hold values from -6 to 6
- w_value: float32 [2048, 4096], P('fs', 'tp'), may hold values from -6 to 6
- m_query: float32 [256, 2048], P('fs', 'tp'), may hold values from -30 to 30
- m_value: float32 [256, 4096], P('fs', 'tp'), may hold values from -30 to 30
- v_query: float32 [256, 2048], P('fs', 'tp'), may hold values from 0.05 to 2
- v_value: float32 [256, 4096], P('fs', 'tp'), may hold values from 0.05 to 2
Outputs:
- new_query: float32 [2048, 2048], P('fs', 'tp')
- new_value: float32 [2048, 4096], P('fs', 'tp')
- copy_query: bfloat16 [2048, 2048], P(None, 'tp')
- copy_value: bfloat16 [2048, 4096], P(None, 'tp')
- first_query: float32 [256, 2048], P('fs', 'tp')
- first_value: float32 [256, 4096], P('fs', 'tp')
- second_query: float32 [256, 2048], P('fs', 'tp')
- second_value: float32 [256, 4096], P('fs', 'tp')
- step_query: float32 [2048, 2048], P('fs', 'tp')
- step_value: float32 [2048, 4096], P('fs', 'tp')
All inputs are finite; a program needn't handle non-finite values.
Results may differ from a plain program's by a relative error of at most 0.015.
Values may be sent and summed in bfloat16 or wider, within the bound.
No kernel may reach another device: no remote copies, remote signals or barrier semaphores. Data moves between devices by JAX's collectives and lax.ppermute only.
A program may use at most 128 MiB of HBM per device.

v0:
```python
import jax
import jax.numpy as jnp
from jax import lax
from jax.sharding import Mesh
from jax.sharding import PartitionSpec as P

RANK = 256
QK_W = 2048
V_W = 4096
FS = ("fs_0", "fs_1")
FS_TP = ("fs_0", "fs_1", "tp_0", "tp_1")
TP = ("tp_0", "tp_1")


beta_first = 0.9
beta_second = 0.95
adam_eps = 1e-08
norm_eps = 1e-06
step_rate = 0.05
decay_rate = 0.2


def cut_along(array, dim, length):
    lengths = array.shape
    pieces = array.reshape(*lengths[:dim], length, lengths[dim] // length, *lengths[dim + 1 :])
    return jnp.moveaxis(pieces, dim, 0)


def summed_on_arrival(array, axis, dim):
    length = lax.axis_size(axis)
    pieces = lax.all_to_all(cut_along(array, dim, length), axis, 0, 0, tiled=True)
    return jnp.sum(pieces, axis=0)


def by_axis(array, axes):
    for axis in axes:
        array = lax.psum(array, axis)
    return array


def sent_together(arrays, axis, dim, along):
    ends, at = ([], 0)
    for a in arrays[:-1]:
        at += a.shape[along]
        ends.append(at)
    both = jnp.concatenate(arrays, axis=along)
    return tuple(jnp.split(lax.all_gather(both, axis, axis=dim, tiled=True), ends, axis=along))


def moment_update(low, first, second):
    first_new = beta_first * first + (1.0 - beta_first) * low
    second_new = beta_second * second + (1.0 - beta_second) * low * low
    update = first_new / (jnp.sqrt(second_new) + adam_eps)
    return (first_new, second_new, update)


def lead_product(left, right):
    return lax.dot_general(
        left, right, (((0,), (0,)), ((), ())), preferred_element_type=jnp.float32
    )


def split_pair(values):
    upper = values.astype(jnp.bfloat16)
    lower = (values - upper.astype(jnp.float32)).astype(jnp.bfloat16)
    return (upper, lower)


def front_exact(factor, values):
    upper, lower = split_pair(values)
    return jnp.dot(factor, upper, preferred_element_type=jnp.float32) + jnp.dot(
        factor, lower, preferred_element_type=jnp.float32
    )


def on_device(
    inputs,
    cot_query,
    cot_value,
    proj_query,
    proj_value,
    w_query,
    w_value,
    m_query,
    m_value,
    v_query,
    v_value,
):
    rows = w_query.shape[0]
    width_query = cot_query.shape[1]
    offset = lax.axis_index(FS) * rows
    local_query = lax.dynamic_slice_in_dim(proj_query, offset, rows, 0)
    local_value = lax.dynamic_slice_in_dim(proj_value, offset, rows, 0)
    factor_query = proj_query
    factor_value = proj_value
    mixed_query = jnp.dot(inputs, factor_query, preferred_element_type=jnp.float32)
    mixed_value = jnp.dot(inputs, factor_value, preferred_element_type=jnp.float32)
    upper_query, lower_query = split_pair(mixed_query)
    upper_value, lower_value = split_pair(mixed_value)
    low = summed_on_arrival(
        jnp.concatenate(
            [
                lead_product(upper_query, cot_query) + lead_product(lower_query, cot_query),
                lead_product(upper_value, cot_value) + lead_product(lower_value, cot_value),
            ],
            axis=1,
        ),
        FS,
        0,
    )
    first_query, second_query, update_query = moment_update(low[:, :width_query], m_query, v_query)
    first_value, second_value, update_value = moment_update(low[:, width_query:], m_value, v_value)
    total = by_axis(
        jnp.sum(update_query * update_query) + jnp.sum(update_value * update_value), FS_TP
    )
    scale = lax.rsqrt(total / (RANK * (QK_W + V_W)) + norm_eps)
    pieces = sent_together((update_query, update_value), FS, 0, 1)
    factor_query = local_query
    factor_value = local_value
    back_query = front_exact(factor_query, pieces[0])
    back_value = front_exact(factor_value, pieces[1])
    step_query = scale * back_query + decay_rate * w_query
    step_value = scale * back_value + decay_rate * w_value
    new_query = w_query - step_rate * step_query
    new_value = w_value - step_rate * step_value
    copy_query, copy_value = sent_together(
        (new_query.astype(jnp.bfloat16), new_value.astype(jnp.bfloat16)), FS, 0, 1
    )
    return (
        new_query,
        new_value,
        copy_query,
        copy_value,
        first_query,
        first_value,
        second_query,
        second_value,
        step_query,
        step_value,
    )


def solution(mesh):
    finer = Mesh(mesh.devices.reshape(4, 4, 4, 2), ("fs_0", "fs_1", "tp_0", "tp_1"))
    placed = (
        P(FS, None),
        P(FS, TP),
        P(FS, TP),
        P(),
        P(),
        P(FS, TP),
        P(FS, TP),
        P(FS, TP),
        P(FS, TP),
        P(FS, TP),
        P(FS, TP),
    )
    return jax.shard_map(
        on_device,
        mesh=finer,
        in_specs=placed,
        out_specs=(
            P(FS, TP),
            P(FS, TP),
            P(None, TP),
            P(None, TP),
            P(FS, TP),
            P(FS, TP),
            P(FS, TP),
            P(FS, TP),
            P(FS, TP),
            P(FS, TP),
        ),
        check_vma=False,
    )
```

profile of v0, /device:TPU:1, one launch (start us, length us, event | category | flops | bytes accessed | tf_op | source)
XLA Modules:
  0.0 172.2 jit_solution(14548449293007263506)
XLA Ops:
  7.2 0.0 copy-start
  7.2 0.0 slice-start
  7.2 7.0 %fusion.31 = f32[3072,256]{1,0:T(8,128)S(1)} fusion(bf16[3072,2048]{1,0:T(8,128)(2,1)} %param.11, bf16[2048,256]{1,0:T(8,128)(2,1)} %param.15), kind=kOutput, calls=%fused_computation.50 | convolution fusion | flops 3221225472 | bytes 16777216 | tf_op jit(solution)/shard_map/dot_general | solution.py:97
  14.2 0.0 slice-start.2
  14.2 1.1 fusion.9
  15.3 1.9 %fusion.2 = f32[256,512]{1,0:T(8,128)} fusion(f32[256,512]{1,0:T(8,128)S(1)} %fusion.9, bf16[3072,512]{1,0:T(8,128)(2,1)S(1)} %copy-done, f32[3072,256]{1,0:T(8,128)S(1)} %fusion.31), kind=kOutput, calls=%fused_computation.4 | convolution fusion | flops 808583168 | bytes 7340032 | tf_op jit(solution)/shard_map/dot_general | solution.py:58
  17.1 0.0 copy-start.2
  17.2 3.6 %fusion.30 = f32[3072,256]{1,0:T(8,128)S(1)} fusion(bf16[3072,2048]{1,0:T(8,128)(2,1)S(1)} %bitcast.11, bf16[2048,256]{1,0:T(8,128)(2,1)S(1)} %copy-done.5), kind=kOutput, calls=%fused_computation.49 | convolution fusion | flops 3221225472 | bytes 16777216 | tf_op jit(solution)/shard_map/dot_general | solution.py:96
  20.8 0.7 fusion.12
  21.5 0.8 fusion.5
  22.3 0.8 copy.21
  23.2 2.0 %pad_maximum_fusion = f32[256,768]{1,0:T(8,128)} fusion(f32[256,512]{1,0:T(8,128)} %fusion.2, f32[256,256]{1,0:T(8,128)} %copy.21), kind=kLoop, calls=%fused_computation.12 | loop fusion | flops 196608 | bytes 1572864 | tf_op jit(solution)/shard_map/concatenate | solution.py:101
  25.2 8.6 %all-to-all-start = ((f32[16,16,768]{2,1,0:T(8,128)}), f32[16,16,768]{2,1,0:T(8,128)}, u32[]{:S(2)}, u32[]{:S(2)}) async-start(f32[16,16,768]{2,1,0:T(8,128)} %bitcast.9), calls=%async_computation | async-start | bytes 1572864 | tf_op jit(solution)/shard_map/all_to_all | solution.py:31
  33.9 0.0 all-gather.2.cloned.1.call-start
  33.9 13.2 %all-to-all-done = f32[16,16,768]{2,1,0:T(8,128)} async-done(((f32[16,16,768]{2,1,0:T(8,128)}), f32[16,16,768]{2,1,0:T(8,128)}, u32[]{:S(2)}, u32[]{:S(2)}) %all-to-all-start) | async-done | bytes 786464 | tf_op jit(solution)/shard_map/all_to_all | solution.py:31
  47.1 1.2 reduce_sum.27
  48.3 1.2 multiply_reduce_fusion.1
  49.6 1.2 multiply_reduce_fusion
  52.1 7.2 %psum.28 = f32[]{:T(128)} all-reduce(f32[]{:T(128)S(6)} %add.73), channel_id=1, replica_groups=mesh['fs_0'=4,'fs_1'=4,'tp_0'=4,'tp_1'=2] {'fs_0'}, use_global_device_ids=true, to_apply=%region_3.0 | all-reduce | flops 1 | bytes 8 | tf_op jit(solution)/shard_map/psum | solution.py:37
  59.3 7.4 %psum.29 = f32[]{:T(128)} all-reduce(f32[]{:T(128)} %psum.28), channel_id=1, replica_groups=mesh['fs_0'=4,'fs_1'=4,'tp_0'=4,'tp_1'=2] {'fs_1'}, use_global_device_ids=true, to_apply=%region_4.0 | all-reduce | flops 1 | bytes 8 | tf_op jit(solution)/shard_map/psum | solution.py:37
  66.7 9.1 %psum.30 = f32[]{:T(128)} all-reduce(f32[]{:T(128)} %psum.29), channel_id=1, replica_groups=mesh['fs_0'=4,'fs_1'=4,'tp_0'=4,'tp_1'=2] {'tp_0'}, use_global_device_ids=true, to_apply=%region_5.0 | all-reduce | flops 1 | bytes 8 | tf_op jit(solution)/shard_map/psum | solution.py:37
  75.8 17.5 %all_gather.6 = f32[256,768]{1,0:T(8,128)S(1)} all-gather(f32[16,768]{1,0:T(8,128)S(1)} %pad_maximum_fusion.2), channel_id=1, replica_groups=mesh['fs_0'=4,'fs_1'=4,'tp_0'=4,'tp_1'=2] {'fs_0','fs_1'}, dimensions={0}, use_global_device_ids=true | all-gather | bytes 835584 | tf_op jit(solution)/shard_map/all_gather | solution.py:47
  93.2 1.1 fusion.14
  94.3 1.0 fusion.18
  95.4 15.5 %psum.31 = f32[]{:T(128)} all-reduce(f32[]{:T(128)} %psum.30), channel_id=1, replica_groups=mesh['fs_0'=4,'fs_1'=4,'tp_0'=4,'tp_1'=2] {'tp_1'}, use_global_device_ids=true, to_apply=%region_6.0 | all-reduce | flops 1 | bytes 8 | tf_op jit(solution)/shard_map/psum | solution.py:37
  111.5 1.9 %fusion.26 = (bf16[128,256]{1,0:T(8,128)(2,1)S(1)}, f32[128,256]{1,0:T(8,128)}, f32[128,256]{1,0:T(8,128)}) fusion(f32[128,256]{1,0:T(8,128)} %param.16, f32[128,256]{1,0:T(8,128)S(1)} %fusion.18, f32[256,768]{1,0:T(8,128)} %copy-done.1, bf16[2048,256]{1,0:T(8,128)(2,1)} %param.14, s32[]{:T(128)S(6)} %select_n.4, f32[]{:T(128)S(6)} %rsqrt.3), kind=kOutput, calls=%fused_computation.47 | convolution fusion | flops 17268736 | bytes 917512 | tf_op jit(solution)/shard_map/dot_general | solution.py:71
  113.4 2.1 %fusion.27 = (bf16[128,512]{1,0:T(8,128)(2,1)S(1)}, f32[128,512]{1,0:T(8,128)}, f32[128,512]{1,0:T(8,128)}) fusion(f32[128,512]{1,0:T(8,128)} %param.17, f32[128,512]{1,0:T(8,128)S(1)} %fusion.14, f32[256,768]{1,0:T(8,128)} %copy-done.1, bf16[2048,256]{1,0:T(8,128)(2,1)} %param.15, s32[]{:T(128)S(6)} %select_n.4, f32[]{:T(128)S(6)} %rsqrt.3), kind=kOutput, calls=%fused_computation.48 | convolution fusion | flops 34537472 | bytes 1769480 | tf_op jit(solution)/shard_map/dot_general | solution.py:71
  115.5 0.7 pad_maximum_fusion.1
  116.2 0.0 all-gather.2.cloned.1.call-update
  116.3 43.8 %all-gather.2.cloned.1.call-done = bf16[2048,768]{1,0:T(8,128)(2,1)} async-done(((bf16[128,768]{1,0:T(8,128)(2,1)}), bf16[2048,768]{1,0:T(8,128)(2,1)}) %all-gather.2.cloned.1.call-update) | async-done | bytes 3145744 | tf_op jit(solution)/shard_map/all_gather | solution.py:47
  160.1 2.3 %split.18 = bf16[2048,256]{1,0:T(8,128)(2,1)} slice(bf16[2048,768]{1,0:T(8,128)(2,1)} %all-gather.2.cloned.1.call-done), slice={[0:2048], [0:256]} | slice | bytes 2097152 | tf_op jit(solution)/shard_map/split | solution.py:47
  162.3 3.0 %split.19 = bf16[2048,512]{1,0:T(8,128)(2,1)} slice(bf16[2048,768]{1,0:T(8,128)(2,1)} %all-gather.2.cloned.1.call-done), slice={[0:2048], [256:768]} | slice | bytes 4194304 | tf_op jit(solution)/shard_map/split | solution.py:47
  (20 shorter events, 0.1 us)
Async XLA Ops:
  7.2 7.0 %copy-start = (bf16[3072,512]{1,0:T(8,128)(2,1)S(1)}, bf16[3072,512]{1,0:T(8,128)(2,1)}, u32[]{:S(2)}) copy-start(bf16[3072,512]{1,0:T(8,128)(2,1)} %param.13) | copy-start | bytes 9437188
  7.2 9.9 %slice-start = ((s8[12582912]{0:T(1024)(128)(4,1)}), s8[4194304]{0:T(1024)(128)(4,1)S(1)}, s32[]{:S(2)}) async-start(s8[12582912]{0:T(1024)(128)(4,1)} %bitcast.10), calls=%async_computation.2 | async-start | bytes 8388608
  7.2 9.9 %slice-start.1 = ((s8[12582912]{0:T(1024)(128)(4,1)}), s8[4194304]{0:T(1024)(128)(4,1)S(1)}, s32[]{:S(2)}) async-start(s8[12582912]{0:T(1024)(128)(4,1)} %bitcast.10), calls=%async_computation.3 | async-start | bytes 8388608
  14.2 2.9 %slice-start.2 = ((s8[12582912]{0:T(1024)(128)(4,1)}), s8[4194304]{0:T(1024)(128)(4,1)S(1)}, s32[]{:S(2)}) async-start(s8[12582912]{0:T(1024)(128)(4,1)} %bitcast.10), calls=%async_computation.4 | async-start | bytes 8388608
  15.3 1.9 %copy-start.5 = (bf16[2048,256]{1,0:T(8,128)(2,1)S(1)}, bf16[2048,256]{1,0:T(8,128)(2,1)}, u32[]{:S(2)}) copy-start(bf16[2048,256]{1,0:T(8,128)(2,1)} %param.14) | copy-start | bytes 3145732
  17.1 3.6 %copy-start.2 = (bf16[3072,256]{1,0:T(8,128)(2,1)S(1)}, bf16[3072,256]{1,0:T(8,128)(2,1)}, u32[]{:S(2)}) copy-start(bf16[3072,256]{1,0:T(8,128)(2,1)} %param.12) | copy-start | bytes 4718596
  22.3 26.0 %copy-start.6 = (f32[16,256]{1,0:T(8,128)S(1)}, f32[16,256]{1,0:T(8,128)}, u32[]{:S(2)}) copy-start(f32[16,256]{1,0:T(8,128)} %param.20) | copy-start | bytes 49156
  22.3 26.0 %copy-start.7 = (f32[16,256]{1,0:T(8,128)S(1)}, f32[16,256]{1,0:T(8,128)}, u32[]{:S(2)}) copy-start(f32[16,256]{1,0:T(8,128)} %param.18) | copy-start | bytes 49156
  22.3 27.2 %copy-start.3 = (f32[16,512]{1,0:T(8,128)S(1)}, f32[16,512]{1,0:T(8,128)}, u32[]{:S(2)}) copy-start(f32[16,512]{1,0:T(8,128)} %param.21) | copy-start | bytes 98308
  22.3 27.2 %copy-start.4 = (f32[16,512]{1,0:T(8,128)S(1)}, f32[16,512]{1,0:T(8,128)}, u32[]{:S(2)}) copy-start(f32[16,512]{1,0:T(8,128)} %param.19) | copy-start | bytes 98308
  25.2 21.9 %all-to-all-start = ((f32[16,16,768]{2,1,0:T(8,128)}), f32[16,16,768]{2,1,0:T(8,128)}, u32[]{:S(2)}, u32[]{:S(2)}) async-start(f32[16,16,768]{2,1,0:T(8,128)} %bitcast.9), calls=%async_computation | async-start | bytes 1572864 | tf_op jit(solution)/shard_map/all_to_all | solution.py:31
  33.9 126.2 %all-gather.2.cloned.1.call-start = ((), (), s32[]{:S(2)}) async-start(), calls=%async_computation.1 | async-start | bytes 3342336 | tf_op jit(solution)/shard_map/all_gather | solution.py:47
  93.2 1.1 copy-start.1
Sparse Core Ops, SparseCore 0:
  116.4 43.6 all-gather.1
where the time goes:
time: 173 us; the launch traced here: 172 us
  waiting for transfers between devices  57.1 us (33%)
  blocking collectives  56.6 us (33%)
  matrix products  21.1 us (12%)
  between operations  16.2 us (9%)
  starting transfers between devices  8.67 us (5%)
  other arithmetic  6.36 us (4%)
  local copies, waits for them, and re-layouts  6.21 us (4%)
    all_gather x1, waiting for transfers between devices, sent_together(): lax.all_gather(both, axis, axis=dim, tiled=True)  43.8 us
    psum x4, blocking collectives, by_axis(): array = lax.psum(array, axis)  39.1 us
    all_gather x1, blocking collectives, sent_together(): lax.all_gather(both, axis, axis=dim, tiled=True)  17.5 us
    all_to_all x1, waiting for transfers between devices, summed_on_arrival(): lax.all_to_all(cut_along(array, dim, length), axis, 0, 0, tiled=True)  13.2 us
    all_to_all x1, starting transfers between devices, summed_on_arrival(): lax.all_to_all(cut_along(array, dim, length), axis, 0, 0, tiled=True)  8.63 us
    dot_general x1, matrix products, on_device(): jnp.dot(inputs, factor_value, preferred_element_type=jnp.float32)  6.95 us
    split x2, local copies, waits for them, and re-layouts, sent_together(): jnp.split(lax.all_gather(both, axis, axis=dim, tiled=True), ends, axis=al...  5.3 us
    dot_general x4, matrix products, lead_product(): lax.dot_general(left, right, (((0,), (0,)), ((), ())), preferred_element_...  4.44 us
  transfers between devices with their start and end apart: 2, of which 2 were waited for; matrix products, arithmetic and copies ran while one was open for 0% of the time, Pallas kernels for 0%

commit v1 on v0

v1 whole, which is shorter than its diff:
```python
import jax
import jax.numpy as jnp
from jax import lax
from jax.experimental import pallas as pl
from jax.experimental.pallas import tpu as pltpu
from jax.sharding import Mesh
from jax.sharding import PartitionSpec as P

RANK = 256
QK_W = 2048
V_W = 4096
AXES = ("z", "y", "x", "c")
SIZES = (4, 4, 4, 2)
FS = ("z", "y")
TP = ("x", "c")

beta_first = 0.9
beta_second = 0.95
adam_eps = 1e-08
norm_eps = 1e-06
step_rate = 0.05
decay_rate = 0.2

WQ = 256
WV = 512
W = WQ + WV
ROWS = 128
TOKEN_BLOCK = 512

F32 = jnp.float32
BF16 = jnp.bfloat16


def shift_pairs(kind, offset):
    pairs = []
    for z in range(4):
        for y in range(4):
            for x in range(4):
                for c in range(2):
                    to = [z, y, x, c]
                    if kind == "major":
                        axis = 0 if c == 0 else 1
                    elif kind == "minor":
                        axis = 1 if c == 0 else 0
                    elif kind == "x":
                        axis = 2
                    else:
                        axis = 3
                    to[axis] = (to[axis] + offset) % SIZES[axis]
                    source = ((z * 4 + y) * 4 + x) * 2 + c
                    target = ((to[0] * 4 + to[1]) * 4 + to[2]) * 2 + to[3]
                    pairs.append((source, target))
    return pairs


def shifted(array, kind, offset):
    return lax.ppermute(array, AXES, shift_pairs(kind, offset))


def own_place():
    z, y, c = lax.axis_index("z"), lax.axis_index("y"), lax.axis_index("c")
    first = c == 0
    major = jnp.where(first, z, y)
    minor = jnp.where(first, y, z)
    per_major = jnp.where(first, 4, 1)
    per_minor = jnp.where(first, 1, 4)
    return major, minor, per_major, per_minor


def gradient_kernel(x, cq, cv, pq, pv, wq, wv, own, to_1, to_2, to_3, w16, total):
    step = pl.program_id(0)

    @pl.when(step == 0)
    def _():
        total[...] = jnp.zeros_like(total)
        w16[:, :WQ] = wq[...].astype(BF16)
        w16[:, WQ:] = wv[...].astype(BF16)

    rows = x[...]
    mixed_q = jnp.dot(rows, pq[...], preferred_element_type=F32).astype(BF16)
    mixed_v = jnp.dot(rows, pv[...], preferred_element_type=F32).astype(BF16)
    lead = (((0,), (0,)), ((), ()))
    total[:, :WQ] += lax.dot_general(mixed_q, cq[...], lead, preferred_element_type=F32)
    total[:, WQ:] += lax.dot_general(mixed_v, cv[...], lead, preferred_element_type=F32)

    @pl.when(step == pl.num_programs(0) - 1)
    def _():
        major, _, per_major, per_minor = own_place()
        for offset, out in enumerate((own, to_1, to_2, to_3)):
            there = lax.rem(major + offset, 4)
            for minor in range(4):
                start = pl.multiple_of((there * per_major + minor * per_minor) * 16, 16)
                out[minor * 16 : (minor + 1) * 16, :] = total[pl.ds(start, 16), :].astype(out.dtype)


def projected_gradient(inputs, cq, cv, pq, pv, wq, wv):
    tokens, width = inputs.shape
    whole = lambda a: pl.BlockSpec(a.shape, lambda i: (0, 0))
    by_tokens = lambda a: pl.BlockSpec((TOKEN_BLOCK, a.shape[1]), lambda i: (i, 0))
    out = [
        jax.ShapeDtypeStruct((64, W), F32),
        jax.ShapeDtypeStruct((64, W), BF16),
        jax.ShapeDtypeStruct((64, W), BF16),
        jax.ShapeDtypeStruct((64, W), BF16),
        jax.ShapeDtypeStruct((ROWS, W), BF16),
    ]
    return pl.pallas_call(
        gradient_kernel,
        grid=(tokens // TOKEN_BLOCK,),
        in_specs=[by_tokens(inputs), by_tokens(cq), by_tokens(cv)]
        + [whole(a) for a in (pq, pv, wq, wv)],
        out_specs=[whole(a) for a in out],
        out_shape=out,
        scratch_shapes=[pltpu.VMEM((RANK, W), F32)],
        cost_estimate=pl.CostEstimate(
            flops=2 * tokens * RANK * (2 * width + W), bytes_accessed=20_000_000, transcendentals=0
        ),
        name="gradient",
    )(inputs, cq, cv, pq, pv, wq, wv)


def whole_call(body, out, operands, scratch=(), flops=1_000_000):
    vmem = pl.BlockSpec(memory_space=pltpu.VMEM)
    return pl.pallas_call(
        body,
        in_specs=[vmem] * len(operands),
        out_specs=[vmem] * len(out),
        out_shape=out,
        scratch_shapes=list(scratch),
        cost_estimate=pl.CostEstimate(flops=flops, bytes_accessed=1_000_000, transcendentals=0),
    )(*operands)


def partial_kernel(own, r1, r2, r3, mq, mv, vq, vv, out):
    out[:64, :] = (own[...] + r1[...].astype(F32) + (r2[...].astype(F32) + r3[...].astype(F32))).astype(BF16)
    out[64:80, :WQ] = mq[...].astype(BF16)
    out[64:80, WQ:] = mv[...].astype(BF16)
    out[80:96, :WQ] = vq[...].astype(BF16)
    out[80:96, WQ:] = vv[...].astype(BF16)


def moments(low, first, second):
    first_new = beta_first * first + (1.0 - beta_first) * low
    second_new = beta_second * second + (1.0 - beta_second) * low * low
    return first_new, second_new


def update_kernel(own, r1, r2, r3, mq, mv, vq, vv, u, fq, fv, sq, sv, low):
    low[...] = (own[:64, :].astype(F32) + r2[:64, :].astype(F32)) + (
        r1[:64, :].astype(F32) + r3[:64, :].astype(F32)
    )
    _, minor, _, _ = own_place()
    for offset, held in enumerate((own, r1, r2, r3)):
        there = lax.rem(minor + 4 - offset, 4)
        at = pl.ds(pl.multiple_of(there * 16, 16), 16)
        first, second = moments(low[at, :], held[64:80, :].astype(F32), held[80:96, :].astype(F32))
        u[at, :] = (first / (jnp.sqrt(second) + adam_eps)).astype(BF16)
    mine = low[pl.ds(pl.multiple_of(minor * 16, 16), 16), :]
    fq[...], sq[...] = moments(mine[:, :WQ], mq[...], vq[...])
    fv[...], sv[...] = moments(mine[:, WQ:], mv[...], vv[...])


def assemble_kernel(own, r1, r2, r3, u, squares):
    major, _, per_major, per_minor = own_place()
    for offset, held in enumerate((own, r1, r2, r3)):
        there = lax.rem(major + 4 - offset, 4)
        for minor in range(4):
            start = pl.multiple_of((there * per_major + minor * per_minor) * 16, 16)
            u[pl.ds(start, 16), :] = held[minor * 16 : (minor + 1) * 16, :]
    total = jnp.zeros((16, W), F32)
    for group in range(16):
        part = u[group * 16 : (group + 1) * 16, :].astype(F32)
        total += part * part
    total = total[:8, :] + total[8:, :]
    folded = total[:, :128]
    for lane in range(1, W // 128):
        folded += total[:, lane * 128 : (lane + 1) * 128]
    squares[...] = folded


def weight_kernel(
    s_own, s_other, u, pq, pv, g0, g1, g2, g3, wq, wv,
    nq, nv, tq, tv, cq, cv,
    pq_s, pv_s, w_s, cq_s, cv_s, p_sem, w_sem, c_sem,
):
    loads = [pltpu.make_async_copy(pq, pq_s, p_sem.at[0]), pltpu.make_async_copy(pv, pv_s, p_sem.at[1])]
    groups = [pltpu.make_async_copy(g, w_s.at[i], w_sem.at[i]) for i, g in enumerate((g0, g1, g2, g3))]
    for copy in loads + groups:
        copy.start()
    major, minor, per_major, per_minor = own_place()
    squares = jnp.sum(s_own[...] + s_other[...], axis=(0, 1), keepdims=True)
    scale = lax.rsqrt(squares / (RANK * (QK_W + V_W)) + norm_eps)
    uq, uv = u[:, :WQ], u[:, WQ:]
    for copy in loads:
        copy.wait()
    stores = []
    for i in range(4):
        groups[i].wait()
        b_there = lax.rem(minor + 4 - i, 4)
        for j in range(4):
            a_there = lax.rem(major + 4 - j, 4)
            block = a_there * per_major + b_there * per_minor
            at = pl.ds(pl.multiple_of(block * ROWS, ROWS), ROWS)
            back_q = scale * jnp.dot(pq_s[at, :], uq, preferred_element_type=F32)
            back_v = scale * jnp.dot(pv_s[at, :], uv, preferred_element_type=F32)
            held = w_s[i, j * ROWS : (j + 1) * ROWS, :].astype(F32)
            n = i * 4 + j
            keep = 1.0 - step_rate * decay_rate
            cq_s[n] = (keep * held[:, :WQ] - step_rate * back_q).astype(BF16)
            cv_s[n] = (keep * held[:, WQ:] - step_rate * back_v).astype(BF16)
            for part, (source, target) in enumerate(((cq_s, cq), (cv_s, cv))):
                copy = pltpu.make_async_copy(source.at[n], target.at[at, :], c_sem.at[n, part])
                copy.start()
                stores.append(copy)
            if n == 0:
                for back, w, t, new in ((back_q, wq, tq, nq), (back_v, wv, tv, nv)):
                    weight = w[...]
                    step = back + decay_rate * weight
                    t[...] = step
                    new[...] = weight - step_rate * step
    for copy in stores:
        copy.wait()


def new_weights(s_own, s_other, u, pq, pv, groups, wq, wv):
    vmem = pl.BlockSpec(memory_space=pltpu.VMEM)
    hbm = pl.BlockSpec(memory_space=pl.ANY)
    out = [
        jax.ShapeDtypeStruct((ROWS, WQ), F32),
        jax.ShapeDtypeStruct((ROWS, WV), F32),
        jax.ShapeDtypeStruct((ROWS, WQ), F32),
        jax.ShapeDtypeStruct((ROWS, WV), F32),
        jax.ShapeDtypeStruct((16 * ROWS, WQ), BF16),
        jax.ShapeDtypeStruct((16 * ROWS, WV), BF16),
    ]
    return pl.pallas_call(
        weight_kernel,
        in_specs=[vmem] * 3 + [hbm] * 6 + [vmem] * 2,
        out_specs=[vmem] * 4 + [hbm] * 2,
        out_shape=out,
        scratch_shapes=[
            pltpu.VMEM((16 * ROWS, RANK), BF16),
            pltpu.VMEM((16 * ROWS, RANK), BF16),
            pltpu.VMEM((4, 4 * ROWS, W), BF16),
            pltpu.VMEM((16, ROWS, WQ), BF16),
            pltpu.VMEM((16, ROWS, WV), BF16),
            pltpu.SemaphoreType.DMA((2,)),
            pltpu.SemaphoreType.DMA((4,)),
            pltpu.SemaphoreType.DMA((16, 2)),
        ],
        cost_estimate=pl.CostEstimate(
            flops=2 * 16 * ROWS * RANK * W, bytes_accessed=12_000_000, transcendentals=0
        ),
        name="weights",
    )(s_own, s_other, u, pq, pv, *groups, wq, wv)


def on_device(inputs, cq, cv, pq, pv, wq, wv, mq, mv, vq, vv):
    own, to_1, to_2, to_3, w16 = projected_gradient(inputs, cq, cv, pq, pv, wq, wv)
    parts = [shifted(a, "major", n) for n, a in ((2, to_2), (1, to_1), (3, to_3))]
    w_1, w_2, w_3 = (shifted(w16, "major", n) for n in (1, 2, 3))
    message, = whole_call(
        partial_kernel, [jax.ShapeDtypeStruct((96, W), BF16)], (own, *parts, mq, mv, vq, vv)
    )
    m_2, m_1, m_3 = (shifted(message, "minor", n) for n in (2, 1, 3))
    group = jnp.concatenate([w16, w_1, w_2, w_3], axis=0)
    g_1, g_2, g_3 = (shifted(group, "minor", n) for n in (1, 2, 3))
    small = lambda n: jax.ShapeDtypeStruct((16, n), F32)
    u_own, first_q, first_v, second_q, second_v = whole_call(
        update_kernel,
        [jax.ShapeDtypeStruct((64, W), BF16), small(WQ), small(WV), small(WQ), small(WV)],
        (message, m_1, m_2, m_3, mq, mv, vq, vv),
        [pltpu.VMEM((64, W), F32)],
    )
    u_2, u_1, u_3 = (shifted(u_own, "major", n) for n in (2, 1, 3))
    u, squares = whole_call(
        assemble_kernel,
        [jax.ShapeDtypeStruct((RANK, W), BF16), jax.ShapeDtypeStruct((8, 128), F32)],
        (u_own, u_1, u_2, u_3),
    )
    s_2, s_1, s_3 = (shifted(squares, "x", n) for n in (2, 1, 3))
    chips = (squares + s_2) + (s_1 + s_3)
    other = shifted(chips, "core", 1)
    new_q, new_v, step_q, step_v, copy_q, copy_v = new_weights(
        chips, other, u, pq, pv, (group, g_1, g_2, g_3), wq, wv
    )
    return (new_q, new_v, copy_q, copy_v, first_q, first_v, second_q, second_v, step_q, step_v)


def solution(mesh):
    finer = Mesh(mesh.devices.reshape(SIZES), AXES)
    both, tokens, columns = P(FS, TP), P(FS, None), P(None, TP)
    return jax.shard_map(
        on_device,
        mesh=finer,
        in_specs=(tokens, both, both, P(), P()) + (both,) * 6,
        out_specs=(both, both, columns, columns) + (both,) * 6,
        check_vma=False,
    )
```

time: 173 us -> 94.4 us (0.55)
  blocking collectives: 56.6 us -> 0 us
  Pallas kernels: 0 us -> 26.3 us
  waiting for transfers between devices: 57.1 us -> 32.4 us
  starting transfers between devices: 8.67 us -> 30.2 us
  matrix products: 21.1 us -> 0 us
  between operations: 16.2 us -> 0.79 us
  other arithmetic: 6.36 us -> 0.69 us
  local copies, waits for them, and re-layouts: 6.21 us -> 3.66 us
    all_gather x1 -> x0, waiting for transfers between devices: 43.8 us -> none  [sent_together(): lax.all_gather(both, axis, axis=dim, tiled=True)]
    psum x4 -> x0, blocking collectives: 39.1 us -> none  [by_axis(): array = lax.psum(array, axis)]
    ppermute x0 -> x19, waiting for transfers between devices: none -> 32.4 us  [shifted(): return lax.ppermute(array, AXES, shift_pairs(kind, offset))]
    ppermute x0 -> x19, starting transfers between devices: none -> 30.2 us  [shifted(): return lax.ppermute(array, AXES, shift_pairs(kind, offset))]
    pallas_call x0 -> x5, Pallas kernels: none -> 26.3 us  [the longest x1 13.4 us: projected_gradient(): pl.pallas_call(gradient_kernel, grid=(tokens // TOKEN_BLOCK,), in_specs=[...]
    dot_general x10 -> x0, matrix products: 21.1 us -> none  [the longest x1 6.95 us: on_device(): jnp.dot(inputs, factor_value, preferred_element_type=jnp.float32)]
    all_gather x1 -> x0, blocking collectives: 17.5 us -> none  [sent_together(): lax.all_gather(both, axis, axis=dim, tiled=True)]
    all_to_all x1 -> x0, waiting for transfers between devices: 13.2 us -> none  [summed_on_arrival(): lax.all_to_all(cut_along(array, dim, length), axis, 0, 0, tiled=True)]
  transfers between devices with their start and end apart: 2 -> 19, of which waited for: 2 -> 10; matrix products, arithmetic and copies ran while one was open for 0% -> 2% of each run, Pallas kernels for 0% -> 6%
where the time goes in v1:
time: 94.4 us; the launch traced here: 94 us
  waiting for transfers between devices  32.4 us (34%)
  starting transfers between devices  30.2 us (32%)
  Pallas kernels  26.3 us (28%)
  local copies, waits for them, and re-layouts  3.66 us (4%)
    ppermute x19, waiting for transfers between devices, shifted(): return lax.ppermute(array, AXES, shift_pairs(kind, offset))  32.4 us
    ppermute x19, starting transfers between devices, shifted(): return lax.ppermute(array, AXES, shift_pairs(kind, offset))  30.2 us
    pallas_call x1, Pallas kernels, projected_gradient(): pl.pallas_call(gradient_kernel, grid=(tokens // TOKEN_BLOCK,), in_specs=[...  13.4 us
    pallas_call x1, Pallas kernels, new_weights(): pl.pallas_call(weight_kernel, in_specs=[vmem] * 3 + [hbm] * 6 + [vmem] *...  7.21 us
    pallas_call x3, Pallas kernels, whole_call(): pl.pallas_call(body, in_specs=[vmem] * len(operands), out_specs=[vmem] *...  5.65 us
    unnamed x31, local copies, waits for them, and re-layouts  3.65 us
  transfers between devices with their start and end apart: 19, of which 10 were waited for; matrix products, arithmetic and copies ran while one was open for 2% of the time, Pallas kernels for 6%

profile of v1, /device:TPU:1, one launch (start us, length us, event | category | flops | bytes accessed | tf_op | source)
XLA Modules:
  0.0 94.0 jit_solution(6038765178781870376)
XLA Ops:
  0.6 13.4 %gradient.1 = (f32[64,768]{1,0:T(8,128)}, bf16[64,768]{1,0:T(8,128)(2,1)}, bf16[64,768]{1,0:T(8,128)(2,1)}, bf16[64,768]{1,0:T(8,128)(2,1)}, bf16[128,768]{1,0:T(8,128)(2,1)}) custom-call(bf16[3072,2048]{1,0:T(8,128)(2,1)} %x.1, bf16[3072,256]{1,0:T(8,128)(2,1)} %cq.1, bf16[3072,512]{1,0:T(8,128)(2,1)} %cv.1, bf16[2048,256]{1,0:T(8,128)(2,1)} %pq.3, ...), custom_call_target="tpu_custom_call" | custom-call | flops 7650410496 | bytes 20000000 | tf_op jit(solution)/shard_map/gradient/pallas_call | solution.py:107
  14.1 2.1 %collective-permute-start.13 = (bf16[128,768]{1,0:T(8,128)(2,1)}, bf16[128,768]{1,0:T(8,128)(2,1)S(1)}, u32[]{:S(2)}, u32[]{:S(2)}) collective-permute-start(bf16[128,768]{1,0:T(8,128)(2,1)} %get-tuple-element.35), channel_id=1, source_target_pairs={{0,32},{1,9},{2,34},{3,11},{4,36},{5,13},{6,38},{7,15},{8,40},{9,1... | collective-permute-start | bytes 589832 | tf_op jit(solution)/shard_map/ppermute | solution.py:57
  16.2 1.5 %collective-permute-start.15 = (bf16[128,768]{1,0:T(8,128)(2,1)}, bf16[128,768]{1,0:T(8,128)(2,1)S(1)}, u32[]{:S(2)}, u32[]{:S(2)}) collective-permute-start(bf16[128,768]{1,0:T(8,128)(2,1)} %get-tuple-element.35), channel_id=1, source_target_pairs={{0,96},{1,25},{2,98},{3,27},{4,100},{5,29},{6,102},{7,31},{8,104},... | collective-permute-start | bytes 589832 | tf_op jit(solution)/shard_map/ppermute | solution.py:57
  17.7 1.6 %collective-permute-start.14 = (bf16[128,768]{1,0:T(8,128)(2,1)}, bf16[128,768]{1,0:T(8,128)(2,1)S(1)}, u32[]{:S(2)}, u32[]{:S(2)}) collective-permute-start(bf16[128,768]{1,0:T(8,128)(2,1)} %get-tuple-element.35), channel_id=1, source_target_pairs={{0,64},{1,17},{2,66},{3,19},{4,68},{5,21},{6,70},{7,23},{8,72},{9,... | collective-permute-start | bytes 589832 | tf_op jit(solution)/shard_map/ppermute | solution.py:57
  19.3 1.4 %collective-permute-start = (bf16[64,768]{1,0:T(8,128)(2,1)}, bf16[64,768]{1,0:T(8,128)(2,1)S(1)}, u32[]{:S(2)}, u32[]{:S(2)}) collective-permute-start(bf16[64,768]{1,0:T(8,128)(2,1)} %get-tuple-element.29), channel_id=1, source_target_pairs={{0,64},{1,17},{2,66},{3,19},{4,68},{5,21},{6,70},{7,23},{8,72},{9,... | collective-permute-start | bytes 294920 | tf_op jit(solution)/shard_map/ppermute | solution.py:57
  20.7 0.9 %constant_dynamic-update-slice_fusion.3 = bf16[512,768]{1,0:T(8,128)(2,1)S(1)} fusion(bf16[128,768]{1,0:T(8,128)(2,1)} %get-tuple-element.35), kind=kLoop, calls=%fused_computation.3 | loop fusion | bytes 393216
  21.6 2.7 %collective-permute-start.2 = (bf16[64,768]{1,0:T(8,128)(2,1)}, bf16[64,768]{1,0:T(8,128)(2,1)S(1)}, u32[]{:S(2)}, u32[]{:S(2)}) collective-permute-start(bf16[64,768]{1,0:T(8,128)(2,1)} %get-tuple-element.31), channel_id=1, source_target_pairs={{0,96},{1,25},{2,98},{3,27},{4,100},{5,29},{6,102},{7,31},{8,104},... | collective-permute-start | bytes 294920 | tf_op jit(solution)/shard_map/ppermute | solution.py:57
  24.5 3.9 %collective-permute-start.18 = (bf16[512,768]{1,0:T(8,128)(2,1)S(1)}, bf16[512,768]{1,0:T(8,128)(2,1)S(1)}, u32[]{:S(2)}, u32[]{:S(2)}) collective-permute-start(bf16[512,768]{1,0:T(8,128)(2,1)S(1)} %constant_dynamic-update-slice_fusion.g0), channel_id=1, source_target_pairs={{0,24},{1,97},{2,26},{3,99},{4,28},{5,101},{6,30},{7,103},{8,0},{9... | collective-permute-start | bytes 2359304 | tf_op jit(solution)/shard_map/ppermute | solution.py:57
  28.4 0.7 collective-permute-start.16
  29.1 0.6 copy-done.10
  29.7 1.8 %shard_map.186.own = bf16[96,768]{1,0:T(8,128)(2,1)} custom-call(f32[64,768]{1,0:T(8,128)} %get-tuple-element.28.own, bf16[64,768]{1,0:T(8,128)(2,1)} %copy-done.9, bf16[64,768]{1,0:T(8,128)(2,1)} %copy-done.10, bf16[64,768]{1,0:T(8,128)(2,1)} %copy-done.11, f32[16,256]{1,0:T(8,128)} %mq.3, f32[16,512]{1,0:T(8,128)} %mv.3, f32[16,256]{1,0:T(8,128)} %vq.3, ...), custom_call_target="tpu_custom_call" | custom-call | flops 1000000 | bytes 1000000 | tf_op jit(solution)/shard_map/pallas_call | solution.py:124
  31.5 2.1 %collective-permute-start.5 = (bf16[96,768]{1,0:T(8,128)(2,1)}, bf16[96,768]{1,0:T(8,128)(2,1)S(1)}, u32[]{:S(2)}, u32[]{:S(2)}) collective-permute-start(bf16[96,768]{1,0:T(8,128)(2,1)} %shard_map.186.own), channel_id=1, source_target_pairs={{0,24},{1,97},{2,26},{3,99},{4,28},{5,101},{6,30},{7,103},{8,0},{9... | collective-permute-start | bytes 442376 | tf_op jit(solution)/shard_map/ppermute | solution.py:57
  33.6 1.7 %collective-permute-start.4 = (bf16[96,768]{1,0:T(8,128)(2,1)}, bf16[96,768]{1,0:T(8,128)(2,1)S(1)}, u32[]{:S(2)}, u32[]{:S(2)}) collective-permute-start(bf16[96,768]{1,0:T(8,128)(2,1)} %shard_map.186.own), channel_id=1, source_target_pairs={{0,16},{1,65},{2,18},{3,67},{4,20},{5,69},{6,22},{7,71},{8,24},{9,... | collective-permute-start | bytes 442376 | tf_op jit(solution)/shard_map/ppermute | solution.py:57
  35.3 14.2 %collective-permute-done.5.r3 = bf16[96,768]{1,0:T(8,128)(2,1)S(1)} collective-permute-done((bf16[96,768]{1,0:T(8,128)(2,1)}, bf16[96,768]{1,0:T(8,128)(2,1)S(1)}, u32[]{:S(2)}, u32[]{:S(2)}) %collective-permute-start.5) | collective-permute-done | bytes 147488 | tf_op jit(solution)/shard_map/ppermute | solution.py:57
  49.5 1.2 %collective-permute-done.4.r2 = bf16[96,768]{1,0:T(8,128)(2,1)S(1)} collective-permute-done((bf16[96,768]{1,0:T(8,128)(2,1)}, bf16[96,768]{1,0:T(8,128)(2,1)S(1)}, u32[]{:S(2)}, u32[]{:S(2)}) %collective-permute-start.4) | collective-permute-done | bytes 147488 | tf_op jit(solution)/shard_map/ppermute | solution.py:57
  50.8 4.9 %collective-permute-done.3.r1 = bf16[96,768]{1,0:T(8,128)(2,1)} collective-permute-done((bf16[96,768]{1,0:T(8,128)(2,1)}, bf16[96,768]{1,0:T(8,128)(2,1)}, u32[]{:S(2)}, u32[]{:S(2)}) %collective-permute-start.3) | collective-permute-done | bytes 147488 | tf_op jit(solution)/shard_map/ppermute | solution.py:57
  55.7 2.0 %shard_map.187 = (bf16[64,768]{1,0:T(8,128)(2,1)}, f32[16,256]{1,0:T(8,128)}, f32[16,512]{1,0:T(8,128)}, f32[16,256]{1,0:T(8,128)}, f32[16,512]{1,0:T(8,128)}) custom-call(bf16[96,768]{1,0:T(8,128)(2,1)} %shard_map.186.own, bf16[96,768]{1,0:T(8,128)(2,1)} %collective-permute-done.3.r1, bf16[96,768]{1,0:T(8,128)(2,1)} %copy-done.5, ...), custom_call_target="tpu_custom_call" | custom-call | flops 1000000 | bytes 1000000 | tf_op jit(solution)/shard_map/pallas_call | solution.py:124
  57.7 2.7 %collective-permute-start.8 = (bf16[64,768]{1,0:T(8,128)(2,1)}, bf16[64,768]{1,0:T(8,128)(2,1)S(1)}, u32[]{:S(2)}, u32[]{:S(2)}) collective-permute-start(bf16[64,768]{1,0:T(8,128)(2,1)} %get-tuple-element.32.own), channel_id=1, source_target_pairs={{0,96},{1,25},{2,98},{3,27},{4,100},{5,29},{6,102},{7,31},{8,104},... | collective-permute-start | bytes 294920 | tf_op jit(solution)/shard_map/ppermute | solution.py:57
  60.6 2.8 %collective-permute-done.8.r3 = bf16[64,768]{1,0:T(8,128)(2,1)S(1)} collective-permute-done((bf16[64,768]{1,0:T(8,128)(2,1)}, bf16[64,768]{1,0:T(8,128)(2,1)S(1)}, u32[]{:S(2)}, u32[]{:S(2)}) %collective-permute-start.8) | collective-permute-done | bytes 98336 | tf_op jit(solution)/shard_map/ppermute | solution.py:57
  63.4 2.2 %collective-permute-done.7.r2 = bf16[64,768]{1,0:T(8,128)(2,1)S(1)} collective-permute-done((bf16[64,768]{1,0:T(8,128)(2,1)}, bf16[64,768]{1,0:T(8,128)(2,1)S(1)}, u32[]{:S(2)}, u32[]{:S(2)}) %collective-permute-start.7) | collective-permute-done | bytes 98336 | tf_op jit(solution)/shard_map/ppermute | solution.py:57
  65.6 3.0 %collective-permute-done.6.r1 = bf16[64,768]{1,0:T(8,128)(2,1)S(1)} collective-permute-done((bf16[64,768]{1,0:T(8,128)(2,1)}, bf16[64,768]{1,0:T(8,128)(2,1)S(1)}, u32[]{:S(2)}, u32[]{:S(2)}) %collective-permute-start.6) | collective-permute-done | bytes 98336 | tf_op jit(solution)/shard_map/ppermute | solution.py:57
  68.6 0.6 copy-done.8
  69.2 1.8 %shard_map.188 = (bf16[256,768]{1,0:T(8,128)(2,1)}, f32[8,128]{1,0:T(8,128)}) custom-call(bf16[64,768]{1,0:T(8,128)(2,1)} %get-tuple-element.32.own, bf16[64,768]{1,0:T(8,128)(2,1)} %copy-done.8, bf16[64,768]{1,0:T(8,128)(2,1)} %copy-done.7, bf16[64,768]{1,0:T(8,128)(2,1)} %copy-done.6), custom_call_target="tpu_custom_call" | custom-call | flops 1000000 | bytes 1000000 | tf_op jit(solution)/shard_map/pallas_call | solution.py:124
  71.1 2.5 %collective-permute-start.11 = (f32[8,128]{1,0:T(8,128)}, f32[8,128]{1,0:T(8,128)S(1)}, u32[]{:S(2)}, u32[]{:S(2)}) collective-permute-start(f32[8,128]{1,0:T(8,128)} %get-tuple-element.33), channel_id=1, source_target_pairs={{0,6},{1,7},{2,0},{3,1},{4,2},{5,3},{6,4},{7,5},{8,14},{9,15},{10,... | collective-permute-start | bytes 12296 | tf_op jit(solution)/shard_map/ppermute | solution.py:57
  73.6 1.0 %collective-permute-done.11 = f32[8,128]{1,0:T(8,128)S(1)} collective-permute-done((f32[8,128]{1,0:T(8,128)}, f32[8,128]{1,0:T(8,128)S(1)}, u32[]{:S(2)}, u32[]{:S(2)}) %collective-permute-start.11) | collective-permute-done | bytes 4128 | tf_op jit(solution)/shard_map/ppermute | solution.py:57
  74.5 2.0 %collective-permute-start.9 = (f32[8,128]{1,0:T(8,128)}, f32[8,128]{1,0:T(8,128)S(1)}, u32[]{:S(2)}, u32[]{:S(2)}) collective-permute-start(f32[8,128]{1,0:T(8,128)} %get-tuple-element.33), channel_id=1, source_target_pairs={{0,4},{1,5},{2,6},{3,7},{4,0},{5,1},{6,2},{7,3},{8,12},{9,13},{10,... | collective-permute-start | bytes 12296 | tf_op jit(solution)/shard_map/ppermute | solution.py:57
  76.5 1.0 %collective-permute-done.10 = f32[8,128]{1,0:T(8,128)S(1)} collective-permute-done((f32[8,128]{1,0:T(8,128)}, f32[8,128]{1,0:T(8,128)S(1)}, u32[]{:S(2)}, u32[]{:S(2)}) %collective-permute-start.10) | collective-permute-done | bytes 4128 | tf_op jit(solution)/shard_map/ppermute | solution.py:57
  77.4 1.3 %collective-permute-done.9 = f32[8,128]{1,0:T(8,128)S(1)} collective-permute-done((f32[8,128]{1,0:T(8,128)}, f32[8,128]{1,0:T(8,128)S(1)}, u32[]{:S(2)}, u32[]{:S(2)}) %collective-permute-start.9) | collective-permute-done | bytes 4128 | tf_op jit(solution)/shard_map/ppermute | solution.py:57
  78.7 0.7 add_add_fusion.s_own
  79.4 5.2 %collective-permute-start.12 = (f32[8,128]{1,0:T(8,128)S(1)}, f32[8,128]{1,0:T(8,128)S(1)}, u32[]{:S(2)}, u32[]{:S(2)}) collective-permute-start(f32[8,128]{1,0:T(8,128)S(1)} %add_add_fusion.s_own), channel_id=1, source_target_pairs={{0,1},{1,0},{2,3},{3,2},{4,5},{5,4},{6,7},{7,6},{8,9},{9,8},{10,11... | collective-permute-start | bytes 12296 | tf_op jit(solution)/shard_map/ppermute | solution.py:57
  84.5 0.8 collective-permute-done.12.s_other
  86.8 7.2 %weights.1 = (f32[128,256]{1,0:T(8,128)}, f32[128,512]{1,0:T(8,128)}, f32[128,256]{1,0:T(8,128)}, f32[128,512]{1,0:T(8,128)}, bf16[2048,256]{1,0:T(8,128)(2,1)}, /*index=5*/bf16[2048,512]{1,0:T(8,128)(2,1)}) custom-call(f32[8,128]{1,0:T(8,128)} %copy-done.12, f32[8,128]{1,0:T(8,128)} %copy-done.13, bf16[256,768]{1,0:T(8,128)(2,1)} %get-tuple-element.34.u, ...), custom_call_target="tpu_custom_call" | custom-call | flops 805306368 | bytes 12000000 | tf_op jit(solution)/shard_map/weights/pallas_call | solution.py:236
  (44 shorter events, 1.7 us)
Async XLA Ops:
  14.1 7.5 %collective-permute-start.13 = (bf16[128,768]{1,0:T(8,128)(2,1)}, bf16[128,768]{1,0:T(8,128)(2,1)S(1)}, u32[]{:S(2)}, u32[]{:S(2)}) collective-permute-start(bf16[128,768]{1,0:T(8,128)(2,1)} %get-tuple-element.35), channel_id=1, source_target_pairs={{0,32},{1,9},{2,34},{3,11},{4,36},{5,13},{6,38},{7,15},{8,40},{9,1... | collective-permute-start | bytes 589832 | tf_op jit(solution)/shard_map/ppermute | solution.py:57
  16.2 8.2 %collective-permute-start.15 = (bf16[128,768]{1,0:T(8,128)(2,1)}, bf16[128,768]{1,0:T(8,128)(2,1)S(1)}, u32[]{:S(2)}, u32[]{:S(2)}) collective-permute-start(bf16[128,768]{1,0:T(8,128)(2,1)} %get-tuple-element.35), channel_id=1, source_target_pairs={{0,96},{1,25},{2,98},{3,27},{4,100},{5,29},{6,102},{7,31},{8,104},... | collective-permute-start | bytes 589832 | tf_op jit(solution)/shard_map/ppermute | solution.py:57
  17.7 6.7 %collective-permute-start.14 = (bf16[128,768]{1,0:T(8,128)(2,1)}, bf16[128,768]{1,0:T(8,128)(2,1)S(1)}, u32[]{:S(2)}, u32[]{:S(2)}) collective-permute-start(bf16[128,768]{1,0:T(8,128)(2,1)} %get-tuple-element.35), channel_id=1, source_target_pairs={{0,64},{1,17},{2,66},{3,19},{4,68},{5,21},{6,70},{7,23},{8,72},{9,... | collective-permute-start | bytes 589832 | tf_op jit(solution)/shard_map/ppermute | solution.py:57
  19.3 9.1 %collective-permute-start = (bf16[64,768]{1,0:T(8,128)(2,1)}, bf16[64,768]{1,0:T(8,128)(2,1)S(1)}, u32[]{:S(2)}, u32[]{:S(2)}) collective-permute-start(bf16[64,768]{1,0:T(8,128)(2,1)} %get-tuple-element.29), channel_id=1, source_target_pairs={{0,64},{1,17},{2,66},{3,19},{4,68},{5,21},{6,70},{7,23},{8,72},{9,... | collective-permute-start | bytes 294920 | tf_op jit(solution)/shard_map/ppermute | solution.py:57
  20.7 8.4 %collective-permute-start.1 = (bf16[64,768]{1,0:T(8,128)(2,1)}, bf16[64,768]{1,0:T(8,128)(2,1)S(1)}, u32[]{:S(2)}, u32[]{:S(2)}) collective-permute-start(bf16[64,768]{1,0:T(8,128)(2,1)} %get-tuple-element.30), channel_id=1, source_target_pairs={{0,32},{1,9},{2,34},{3,11},{4,36},{5,13},{6,38},{7,15},{8,40},{9,1... | collective-permute-start | bytes 294920 | tf_op jit(solution)/shard_map/ppermute | solution.py:57
  21.6 7.4 %collective-permute-start.2 = (bf16[64,768]{1,0:T(8,128)(2,1)}, bf16[64,768]{1,0:T(8,128)(2,1)S(1)}, u32[]{:S(2)}, u32[]{:S(2)}) collective-permute-start(bf16[64,768]{1,0:T(8,128)(2,1)} %get-tuple-element.31), channel_id=1, source_target_pairs={{0,96},{1,25},{2,98},{3,27},{4,100},{5,29},{6,102},{7,31},{8,104},... | collective-permute-start | bytes 294920 | tf_op jit(solution)/shard_map/ppermute | solution.py:57
  24.4 61.0 %copy-start = (bf16[512,768]{1,0:T(8,128)(2,1)}, bf16[512,768]{1,0:T(8,128)(2,1)S(1)}, u32[]{:S(2)}) copy-start(bf16[512,768]{1,0:T(8,128)(2,1)S(1)} %constant_dynamic-update-slice_fusion.g0) | copy-start | bytes 2359300
  24.5 60.9 %collective-permute-start.18 = (bf16[512,768]{1,0:T(8,128)(2,1)S(1)}, bf16[512,768]{1,0:T(8,128)(2,1)S(1)}, u32[]{:S(2)}, u32[]{:S(2)}) collective-permute-start(bf16[512,768]{1,0:T(8,128)(2,1)S(1)} %constant_dynamic-update-slice_fusion.g0), channel_id=1, source_target_pairs={{0,24},{1,97},{2,26},{3,99},{4,28},{5,101},{6,30},{7,103},{8,0},{9... | collective-permute-start | bytes 2359304 | tf_op jit(solution)/shard_map/ppermute | solution.py:57
  28.4 57.0 %collective-permute-start.17 = (bf16[512,768]{1,0:T(8,128)(2,1)S(1)}, bf16[512,768]{1,0:T(8,128)(2,1)S(1)}, u32[]{:S(2)}, u32[]{:S(2)}) collective-permute-start(bf16[512,768]{1,0:T(8,128)(2,1)S(1)} %constant_dynamic-update-slice_fusion.g0), channel_id=1, source_target_pairs={{0,16},{1,65},{2,18},{3,67},{4,20},{5,69},{6,22},{7,71},{8,24},{9,... | collective-permute-start | bytes 2359304 | tf_op jit(solution)/shard_map/ppermute | solution.py:57
  28.4 0.7 copy-start.9
  28.4 57.0 %collective-permute-start.16 = (bf16[512,768]{1,0:T(8,128)(2,1)S(1)}, bf16[512,768]{1,0:T(8,128)(2,1)S(1)}, u32[]{:S(2)}, u32[]{:S(2)}) collective-permute-start(bf16[512,768]{1,0:T(8,128)(2,1)S(1)} %constant_dynamic-update-slice_fusion.g0), channel_id=1, source_target_pairs={{0,8},{1,33},{2,10},{3,35},{4,12},{5,37},{6,14},{7,39},{8,16},{9,4... | collective-permute-start | bytes 2359304 | tf_op jit(solution)/shard_map/ppermute | solution.py:57
  29.0 0.6 copy-start.10
  29.1 0.7 copy-start.11
  31.5 18.0 %collective-permute-start.5 = (bf16[96,768]{1,0:T(8,128)(2,1)}, bf16[96,768]{1,0:T(8,128)(2,1)S(1)}, u32[]{:S(2)}, u32[]{:S(2)}) collective-permute-start(bf16[96,768]{1,0:T(8,128)(2,1)} %shard_map.186.own), channel_id=1, source_target_pairs={{0,24},{1,97},{2,26},{3,99},{4,28},{5,101},{6,30},{7,103},{8,0},{9... | collective-permute-start | bytes 442376 | tf_op jit(solution)/shard_map/ppermute | solution.py:57
  33.6 17.1 %collective-permute-start.4 = (bf16[96,768]{1,0:T(8,128)(2,1)}, bf16[96,768]{1,0:T(8,128)(2,1)S(1)}, u32[]{:S(2)}, u32[]{:S(2)}) collective-permute-start(bf16[96,768]{1,0:T(8,128)(2,1)} %shard_map.186.own), channel_id=1, source_target_pairs={{0,16},{1,65},{2,18},{3,67},{4,20},{5,69},{6,22},{7,71},{8,24},{9,... | collective-permute-start | bytes 442376 | tf_op jit(solution)/shard_map/ppermute | solution.py:57
  49.5 6.2 %copy-start.4 = (bf16[96,768]{1,0:T(8,128)(2,1)}, bf16[96,768]{1,0:T(8,128)(2,1)S(1)}, u32[]{:S(2)}) copy-start(bf16[96,768]{1,0:T(8,128)(2,1)S(1)} %collective-permute-done.5.r3) | copy-start | bytes 442372
  49.5 6.2 %collective-permute-start.3 = (bf16[96,768]{1,0:T(8,128)(2,1)}, bf16[96,768]{1,0:T(8,128)(2,1)}, u32[]{:S(2)}, u32[]{:S(2)}) collective-permute-start(bf16[96,768]{1,0:T(8,128)(2,1)} %shard_map.186.own), channel_id=1, source_target_pairs={{0,8},{1,33},{2,10},{3,35},{4,12},{5,37},{6,14},{7,39},{8,16},{9,4... | collective-permute-start | bytes 442376 | tf_op jit(solution)/shard_map/ppermute | solution.py:57
  50.8 4.9 %copy-start.5 = (bf16[96,768]{1,0:T(8,128)(2,1)}, bf16[96,768]{1,0:T(8,128)(2,1)S(1)}, u32[]{:S(2)}) copy-start(bf16[96,768]{1,0:T(8,128)(2,1)S(1)} %collective-permute-done.4.r2) | copy-start | bytes 442372
  57.7 5.7 %collective-permute-start.8 = (bf16[64,768]{1,0:T(8,128)(2,1)}, bf16[64,768]{1,0:T(8,128)(2,1)S(1)}, u32[]{:S(2)}, u32[]{:S(2)}) collective-permute-start(bf16[64,768]{1,0:T(8,128)(2,1)} %get-tuple-element.32.own), channel_id=1, source_target_pairs={{0,96},{1,25},{2,98},{3,27},{4,100},{5,29},{6,102},{7,31},{8,104},... | collective-permute-start | bytes 294920 | tf_op jit(solution)/shard_map/ppermute | solution.py:57
  60.4 5.2 %collective-permute-start.7 = (bf16[64,768]{1,0:T(8,128)(2,1)}, bf16[64,768]{1,0:T(8,128)(2,1)S(1)}, u32[]{:S(2)}, u32[]{:S(2)}) collective-permute-start(bf16[64,768]{1,0:T(8,128)(2,1)} %get-tuple-element.32.own), channel_id=1, source_target_pairs={{0,64},{1,17},{2,66},{3,19},{4,68},{5,21},{6,70},{7,23},{8,72},{9,... | collective-permute-start | bytes 294920 | tf_op jit(solution)/shard_map/ppermute | solution.py:57
  63.4 5.2 %copy-start.6 = (bf16[64,768]{1,0:T(8,128)(2,1)}, bf16[64,768]{1,0:T(8,128)(2,1)S(1)}, u32[]{:S(2)}) copy-start(bf16[64,768]{1,0:T(8,128)(2,1)S(1)} %collective-permute-done.8.r3) | copy-start | bytes 294916
  63.4 5.2 %collective-permute-start.6 = (bf16[64,768]{1,0:T(8,128)(2,1)}, bf16[64,768]{1,0:T(8,128)(2,1)S(1)}, u32[]{:S(2)}, u32[]{:S(2)}) collective-permute-start(bf16[64,768]{1,0:T(8,128)(2,1)} %get-tuple-element.32.own), channel_id=1, source_target_pairs={{0,32},{1,9},{2,34},{3,11},{4,36},{5,13},{6,38},{7,15},{8,40},{9,1... | collective-permute-start | bytes 294920 | tf_op jit(solution)/shard_map/ppermute | solution.py:57
  65.6 3.0 %copy-start.7 = (bf16[64,768]{1,0:T(8,128)(2,1)}, bf16[64,768]{1,0:T(8,128)(2,1)S(1)}, u32[]{:S(2)}) copy-start(bf16[64,768]{1,0:T(8,128)(2,1)S(1)} %collective-permute-done.7.r2) | copy-start | bytes 294916
  68.6 0.6 copy-start.8
  71.1 3.4 %collective-permute-start.11 = (f32[8,128]{1,0:T(8,128)}, f32[8,128]{1,0:T(8,128)S(1)}, u32[]{:S(2)}, u32[]{:S(2)}) collective-permute-start(f32[8,128]{1,0:T(8,128)} %get-tuple-element.33), channel_id=1, source_target_pairs={{0,6},{1,7},{2,0},{3,1},{4,2},{5,3},{6,4},{7,5},{8,14},{9,15},{10,... | collective-permute-start | bytes 12296 | tf_op jit(solution)/shard_map/ppermute | solution.py:57
  73.6 3.9 %collective-permute-start.10 = (f32[8,128]{1,0:T(8,128)}, f32[8,128]{1,0:T(8,128)S(1)}, u32[]{:S(2)}, u32[]{:S(2)}) collective-permute-start(f32[8,128]{1,0:T(8,128)} %get-tuple-element.33), channel_id=1, source_target_pairs={{0,2},{1,3},{2,4},{3,5},{4,6},{5,7},{6,0},{7,1},{8,10},{9,11},{10,... | collective-permute-start | bytes 12296 | tf_op jit(solution)/shard_map/ppermute | solution.py:57
  74.5 4.2 %collective-permute-start.9 = (f32[8,128]{1,0:T(8,128)}, f32[8,128]{1,0:T(8,128)S(1)}, u32[]{:S(2)}, u32[]{:S(2)}) collective-permute-start(f32[8,128]{1,0:T(8,128)} %get-tuple-element.33), channel_id=1, source_target_pairs={{0,4},{1,5},{2,6},{3,7},{4,0},{5,1},{6,2},{7,3},{8,12},{9,13},{10,... | collective-permute-start | bytes 12296 | tf_op jit(solution)/shard_map/ppermute | solution.py:57
  79.4 6.0 %copy-start.12 = (f32[8,128]{1,0:T(8,128)}, f32[8,128]{1,0:T(8,128)S(1)}, u32[]{:S(2)}) copy-start(f32[8,128]{1,0:T(8,128)S(1)} %add_add_fusion.s_own) | copy-start | bytes 12292
  79.4 6.0 %collective-permute-start.12 = (f32[8,128]{1,0:T(8,128)S(1)}, f32[8,128]{1,0:T(8,128)S(1)}, u32[]{:S(2)}, u32[]{:S(2)}) collective-permute-start(f32[8,128]{1,0:T(8,128)S(1)} %add_add_fusion.s_own), channel_id=1, source_target_pairs={{0,1},{1,0},{2,3},{3,2},{4,5},{5,4},{6,7},{7,6},{8,9},{9,8},{10,11... | collective-permute-start | bytes 12296 | tf_op jit(solution)/shard_map/ppermute | solution.py:57
  85.4 0.9 copy-start.1
  85.4 1.1 %copy-start.2 = (bf16[512,768]{1,0:T(8,128)(2,1)}, bf16[512,768]{1,0:T(8,128)(2,1)S(1)}, u32[]{:S(2)}) copy-start(bf16[512,768]{1,0:T(8,128)(2,1)S(1)} %collective-permute-done.17.g2) | copy-start | bytes 2359300
  85.4 1.4 %copy-start.3 = (bf16[512,768]{1,0:T(8,128)(2,1)}, bf16[512,768]{1,0:T(8,128)(2,1)S(1)}, u32[]{:S(2)}) copy-start(bf16[512,768]{1,0:T(8,128)(2,1)S(1)} %collective-permute-done.16.g1) | copy-start | bytes 2359300
  (1 other events, 0.6 us)

commit v2 on v1

--- a/solution.py
+++ b/solution.py
@@ -25,7 +25,7 @@
 WV = 512
 W = WQ + WV
 ROWS = 128
-TOKEN_BLOCK = 512
+TOKEN_BLOCK = 768
 
 F32 = jnp.float32
 BF16 = jnp.bfloat16
@@ -67,6 +67,10 @@
     return major, minor, per_major, per_minor
 
 
+def in_vmem(array):
+    return pltpu.with_memory_space_constraint(array, pltpu.VMEM)
+
+
 def gradient_kernel(x, cq, cv, pq, pv, wq, wv, own, to_1, to_2, to_3, w16, total):
     step = pl.program_id(0)
 
@@ -110,13 +114,14 @@
         in_specs=[by_tokens(inputs), by_tokens(cq), by_tokens(cv)]
         + [whole(a) for a in (pq, pv, wq, wv)],
         out_specs=[whole(a) for a in out],
-        out_shape=out,
+        out_shape=[pltpu.VMEM(o.shape, o.dtype) for o in out],
         scratch_shapes=[pltpu.VMEM((RANK, W), F32)],
         cost_estimate=pl.CostEstimate(
             flops=2 * tokens * RANK * (2 * width + W), bytes_accessed=20_000_000, transcendentals=0
         ),
+        compiler_params=pltpu.CompilerParams(vmem_limit_bytes=28 * 2**20),
         name="gradient",
-    )(inputs, cq, cv, pq, pv, wq, wv)
+    )(*(pltpu.with_memory_space_constraint(a, pltpu.HBM) for a in (inputs, cq, cv, pq, pv, wq, wv)))
 
 
 def whole_call(body, out, operands, scratch=(), flops=1_000_000):
@@ -125,10 +130,11 @@
         body,
         in_specs=[vmem] * len(operands),
         out_specs=[vmem] * len(out),
-        out_shape=out,
+        out_shape=[pltpu.VMEM(o.shape, o.dtype) for o in out],
         scratch_shapes=list(scratch),
         cost_estimate=pl.CostEstimate(flops=flops, bytes_accessed=1_000_000, transcendentals=0),
-    )(*operands)
+        compiler_params=pltpu.CompilerParams(vmem_limit_bytes=8 * 2**20),
+    )(*(in_vmem(a) for a in operands))
 
 
 def partial_kernel(own, r1, r2, r3, mq, mv, vq, vv, out):
@@ -179,33 +185,27 @@
 
 
 def weight_kernel(
-    s_own, s_other, u, pq, pv, g0, g1, g2, g3, wq, wv,
-    nq, nv, tq, tv, cq, cv,
-    pq_s, pv_s, w_s, cq_s, cv_s, p_sem, w_sem, c_sem,
+    s_own, s_other, u, pq, pv, g0, g1, g3, h_up, h_down, wq, wv,
+    nq, nv, tq, tv, cq, cv, cq_s, cv_s, c_sem,
 ):
-    loads = [pltpu.make_async_copy(pq, pq_s, p_sem.at[0]), pltpu.make_async_copy(pv, pv_s, p_sem.at[1])]
-    groups = [pltpu.make_async_copy(g, w_s.at[i], w_sem.at[i]) for i, g in enumerate((g0, g1, g2, g3))]
-    for copy in loads + groups:
-        copy.start()
     major, minor, per_major, per_minor = own_place()
     squares = jnp.sum(s_own[...] + s_other[...], axis=(0, 1), keepdims=True)
     scale = lax.rsqrt(squares / (RANK * (QK_W + V_W)) + norm_eps)
     uq, uv = u[:, :WQ], u[:, WQ:]
-    for copy in loads:
-        copy.wait()
+    keep = 1.0 - step_rate * decay_rate
     stores = []
-    for i in range(4):
-        groups[i].wait()
+    for i, pieces in ((0, (g0, g0)), (1, (g1, g1)), (3, (g3, g3)), (2, (h_up, h_down))):
         b_there = lax.rem(minor + 4 - i, 4)
         for j in range(4):
             a_there = lax.rem(major + 4 - j, 4)
             block = a_there * per_major + b_there * per_minor
             at = pl.ds(pl.multiple_of(block * ROWS, ROWS), ROWS)
-            back_q = scale * jnp.dot(pq_s[at, :], uq, preferred_element_type=F32)
-            back_v = scale * jnp.dot(pv_s[at, :], uv, preferred_element_type=F32)
-            held = w_s[i, j * ROWS : (j + 1) * ROWS, :].astype(F32)
+            back_q = scale * jnp.dot(pq[at, :], uq, preferred_element_type=F32)
+            back_v = scale * jnp.dot(pv[at, :], uv, preferred_element_type=F32)
+            piece = pieces[j // 2]
+            top = (j if piece.shape[0] == 4 * ROWS else j % 2) * ROWS
+            held = piece[top : top + ROWS, :].astype(F32)
             n = i * 4 + j
-            keep = 1.0 - step_rate * decay_rate
             cq_s[n] = (keep * held[:, :WQ] - step_rate * back_q).astype(BF16)
             cv_s[n] = (keep * held[:, WQ:] - step_rate * back_v).astype(BF16)
             for part, (source, target) in enumerate(((cq_s, cq), (cv_s, cv))):
@@ -233,38 +233,35 @@
         jax.ShapeDtypeStruct((16 * ROWS, WQ), BF16),
         jax.ShapeDtypeStruct((16 * ROWS, WV), BF16),
     ]
+    operands = (s_own, s_other, u, pq, pv, *groups, wq, wv)
     return pl.pallas_call(
         weight_kernel,
-        in_specs=[vmem] * 3 + [hbm] * 6 + [vmem] * 2,
+        in_specs=[vmem] * len(operands),
         out_specs=[vmem] * 4 + [hbm] * 2,
         out_shape=out,
         scratch_shapes=[
-            pltpu.VMEM((16 * ROWS, RANK), BF16),
-            pltpu.VMEM((16 * ROWS, RANK), BF16),
-            pltpu.VMEM((4, 4 * ROWS, W), BF16),
             pltpu.VMEM((16, ROWS, WQ), BF16),
             pltpu.VMEM((16, ROWS, WV), BF16),
-            pltpu.SemaphoreType.DMA((2,)),
-            pltpu.SemaphoreType.DMA((4,)),
             pltpu.SemaphoreType.DMA((16, 2)),
         ],
         cost_estimate=pl.CostEstimate(
             flops=2 * 16 * ROWS * RANK * W, bytes_accessed=12_000_000, transcendentals=0
         ),
+        compiler_params=pltpu.CompilerParams(vmem_limit_bytes=20 * 2**20),
         name="weights",
-    )(s_own, s_other, u, pq, pv, *groups, wq, wv)
+    )(*(in_vmem(a) for a in operands))
 
 
 def on_device(inputs, cq, cv, pq, pv, wq, wv, mq, mv, vq, vv):
     own, to_1, to_2, to_3, w16 = projected_gradient(inputs, cq, cv, pq, pv, wq, wv)
-    parts = [shifted(a, "major", n) for n, a in ((2, to_2), (1, to_1), (3, to_3))]
-    w_1, w_2, w_3 = (shifted(w16, "major", n) for n in (1, 2, 3))
+    r_2, r_1, r_3 = (shifted(a, "major", n) for n, a in ((2, to_2), (1, to_1), (3, to_3)))
+    w_1, w_3, w_2 = (shifted(w16, "major", n) for n in (1, 3, 2))
     message, = whole_call(
-        partial_kernel, [jax.ShapeDtypeStruct((96, W), BF16)], (own, *parts, mq, mv, vq, vv)
+        partial_kernel, [jax.ShapeDtypeStruct((96, W), BF16)], (own, r_1, r_2, r_3, mq, mv, vq, vv)
     )
     m_2, m_1, m_3 = (shifted(message, "minor", n) for n in (2, 1, 3))
     group = jnp.concatenate([w16, w_1, w_2, w_3], axis=0)
-    g_1, g_2, g_3 = (shifted(group, "minor", n) for n in (1, 2, 3))
+    g_1, g_3 = shifted(group, "minor", 1), shifted(group, "minor", 3)
     small = lambda n: jax.ShapeDtypeStruct((16, n), F32)
     u_own, first_q, first_v, second_q, second_v = whole_call(
         update_kernel,
@@ -279,10 +276,12 @@
         (u_own, u_1, u_2, u_3),
     )
     s_2, s_1, s_3 = (shifted(squares, "x", n) for n in (2, 1, 3))
+    h_up = shifted(g_1[: 2 * ROWS], "minor", 1)
+    h_down = shifted(g_3[2 * ROWS :], "minor", 3)
     chips = (squares + s_2) + (s_1 + s_3)
     other = shifted(chips, "core", 1)
     new_q, new_v, step_q, step_v, copy_q, copy_v = new_weights(
-        chips, other, u, pq, pv, (group, g_1, g_2, g_3), wq, wv
+        chips, other, u, pq, pv, (group, g_1, g_3, h_up, h_down), wq, wv
     )
     return (new_q, new_v, copy_q, copy_v, first_q, first_v, second_q, second_v, step_q, step_v)
 

time: 94.4 us -> 73.1 us (0.77)
  Pallas kernels: 26.3 us -> 15.8 us
  waiting for transfers between devices: 32.4 us -> 22.4 us
  starting transfers between devices: 30.2 us -> 31.4 us
  local copies, waits for them, and re-layouts: 3.66 us -> 2.59 us
    ppermute x19 -> x20, waiting for transfers between devices: 32.4 us -> 22.4 us  [shifted(): return lax.ppermute(array, AXES, shift_pairs(kind, offset))]
    pallas_call x3, Pallas kernels: 5.65 us -> 0.34 us  [whole_call(): pl.pallas_call(body, in_specs=[vmem] * len(operands), out_specs=[vmem] *...]
    pallas_call x1, Pallas kernels: 7.21 us -> 3.53 us  [new_weights(): pl.pallas_call(weight_kernel, in_specs=[vmem] * len(operands), out_specs=...]
    pallas_call x1, Pallas kernels: 13.4 us -> 11.9 us  [projected_gradient(): pl.pallas_call(gradient_kernel, grid=(tokens // TOKEN_BLOCK,), in_specs=[...]
    ppermute x19 -> x20, starting transfers between devices: 30.2 us -> 31.4 us  [shifted(): return lax.ppermute(array, AXES, shift_pairs(kind, offset))]
    unnamed x31 -> x23, local copies, waits for them, and re-layouts: 3.65 us -> 2.52 us
  transfers between devices with their start and end apart: 19 -> 20, of which waited for: 10 -> 13; matrix products, arithmetic and copies ran while one was open for 2% -> 3% of each run, Pallas kernels for 6% -> 0%
where the time goes in v2:
time: 73.1 us; the launch traced here: 73 us
  starting transfers between devices  31.4 us (43%)
  waiting for transfers between devices  22.4 us (31%)
  Pallas kernels  15.8 us (22%)
  local copies, waits for them, and re-layouts  2.59 us (4%)
  between operations  0.84 us (1%)
    ppermute x20, starting transfers between devices, shifted(): return lax.ppermute(array, AXES, shift_pairs(kind, offset))  31.4 us
    ppermute x20, waiting for transfers between devices, shifted(): return lax.ppermute(array, AXES, shift_pairs(kind, offset))  22.4 us
    pallas_call x1, Pallas kernels, projected_gradient(): pl.pallas_call(gradient_kernel, grid=(tokens // TOKEN_BLOCK,), in_specs=[...  11.9 us
    pallas_call x1, Pallas kernels, new_weights(): pl.pallas_call(weight_kernel, in_specs=[vmem] * len(operands), out_specs=...  3.53 us
    unnamed x23, local copies, waits for them, and re-layouts  2.52 us
  transfers between devices with their start and end apart: 20, of which 13 were waited for; matrix products, arithmetic and copies ran while one was open for 3% of the time, Pallas kernels for 0%

profile of v2, /device:TPU:1, one launch (start us, length us, event | category | flops | bytes accessed | tf_op | source)
XLA Modules:
  0.0 73.0 jit_solution(15554725906303519593)
XLA Ops:
  0.7 11.9 %gradient.1 = (f32[64,768]{1,0:T(8,128)S(1)}, bf16[64,768]{1,0:T(8,128)(2,1)S(1)}, bf16[64,768]{1,0:T(8,128)(2,1)S(1)}, bf16[64,768]{1,0:T(8,128)(2,1)S(1)}, bf16[128,768]{1,0:T(8,128)(2,1)S(1)}) custom-call(bf16[3072,2048]{1,0:T(8,128)(2,1)} %x.1, bf16[3072,256]{1,0:T(8,128)(2,1)} %cq.1, bf16[3072,512]{1,0:T(8,128)(2,1)} %cv.1, bf16[2048,256]{1,0:T(8,128)(2,1)} %pq.3, ...), custom_call_target="tpu_custom_call" | custom-call | flops 7650410496 | bytes 20000000 | tf_op jit(solution)/shard_map/gradient/pallas_call | solution.py:111
  12.6 2.2 %collective-permute-start.13 = (bf16[128,768]{1,0:T(8,128)(2,1)S(1)}, bf16[128,768]{1,0:T(8,128)(2,1)S(1)}, u32[]{:S(2)}, u32[]{:S(2)}) collective-permute-start(bf16[128,768]{1,0:T(8,128)(2,1)S(1)} %get-tuple-element.35), channel_id=1, source_target_pairs={{0,32},{1,9},{2,34},{3,11},{4,36},{5,13},{6,38},{7,15},{8,40},{9,1... | collective-permute-start | bytes 589832 | tf_op jit(solution)/shard_map/ppermute | solution.py:57
  14.8 1.5 %collective-permute-start.15 = (bf16[128,768]{1,0:T(8,128)(2,1)S(1)}, bf16[128,768]{1,0:T(8,128)(2,1)S(1)}, u32[]{:S(2)}, u32[]{:S(2)}) collective-permute-start(bf16[128,768]{1,0:T(8,128)(2,1)S(1)} %get-tuple-element.35), channel_id=1, source_target_pairs={{0,96},{1,25},{2,98},{3,27},{4,100},{5,29},{6,102},{7,31},{8,104},... | collective-permute-start | bytes 589832 | tf_op jit(solution)/shard_map/ppermute | solution.py:57
  16.3 1.6 %collective-permute-start.14 = (bf16[128,768]{1,0:T(8,128)(2,1)S(1)}, bf16[128,768]{1,0:T(8,128)(2,1)S(1)}, u32[]{:S(2)}, u32[]{:S(2)}) collective-permute-start(bf16[128,768]{1,0:T(8,128)(2,1)S(1)} %get-tuple-element.35), channel_id=1, source_target_pairs={{0,64},{1,17},{2,66},{3,19},{4,68},{5,21},{6,70},{7,23},{8,72},{9,... | collective-permute-start | bytes 589832 | tf_op jit(solution)/shard_map/ppermute | solution.py:57
  17.9 1.7 %collective-permute-done.13 = bf16[128,768]{1,0:T(8,128)(2,1)S(1)} collective-permute-done((bf16[128,768]{1,0:T(8,128)(2,1)S(1)}, bf16[128,768]{1,0:T(8,128)(2,1)S(1)}, u32[]{:S(2)}, u32[]{:S(2)}) %collective-permute-start.13) | collective-permute-done | bytes 196640 | tf_op jit(solution)/shard_map/ppermute | solution.py:57
  19.6 3.0 %collective-permute-done.14 = bf16[128,768]{1,0:T(8,128)(2,1)S(1)} collective-permute-done((bf16[128,768]{1,0:T(8,128)(2,1)S(1)}, bf16[128,768]{1,0:T(8,128)(2,1)S(1)}, u32[]{:S(2)}, u32[]{:S(2)}) %collective-permute-start.14) | collective-permute-done | bytes 196640 | tf_op jit(solution)/shard_map/ppermute | solution.py:57
  22.7 4.1 %collective-permute-start.17 = (bf16[512,768]{1,0:T(8,128)(2,1)S(1)}, bf16[512,768]{1,0:T(8,128)(2,1)S(1)}, u32[]{:S(2)}, u32[]{:S(2)}) collective-permute-start(bf16[512,768]{1,0:T(8,128)(2,1)S(1)} %constant_dynamic-update-slice_fusion.g0), channel_id=1, source_target_pairs={{0,24},{1,97},{2,26},{3,99},{4,28},{5,101},{6,30},{7,103},{8,0},{9... | collective-permute-start | bytes 2359304 | tf_op jit(solution)/shard_map/ppermute | solution.py:57
  26.8 0.9 %collective-permute-start = (bf16[64,768]{1,0:T(8,128)(2,1)S(1)}, bf16[64,768]{1,0:T(8,128)(2,1)S(1)}, u32[]{:S(2)}, u32[]{:S(2)}) collective-permute-start(bf16[64,768]{1,0:T(8,128)(2,1)S(1)} %get-tuple-element.29), channel_id=1, source_target_pairs={{0,32},{1,9},{2,34},{3,11},{4,36},{5,13},{6,38},{7,15},{8,40},{9,1... | collective-permute-start | bytes 294920 | tf_op jit(solution)/shard_map/ppermute | solution.py:57
  27.6 1.9 %collective-permute-start.1 = (bf16[64,768]{1,0:T(8,128)(2,1)S(1)}, bf16[64,768]{1,0:T(8,128)(2,1)S(1)}, u32[]{:S(2)}, u32[]{:S(2)}) collective-permute-start(bf16[64,768]{1,0:T(8,128)(2,1)S(1)} %get-tuple-element.30), channel_id=1, source_target_pairs={{0,64},{1,17},{2,66},{3,19},{4,68},{5,21},{6,70},{7,23},{8,72},{9,... | collective-permute-start | bytes 294920 | tf_op jit(solution)/shard_map/ppermute | solution.py:57
  29.5 0.7 collective-permute-start.2
  30.2 1.3 %collective-permute-done.r1 = bf16[64,768]{1,0:T(8,128)(2,1)S(1)} collective-permute-done((bf16[64,768]{1,0:T(8,128)(2,1)S(1)}, bf16[64,768]{1,0:T(8,128)(2,1)S(1)}, u32[]{:S(2)}, u32[]{:S(2)}) %collective-permute-start) | collective-permute-done | bytes 98336 | tf_op jit(solution)/shard_map/ppermute | solution.py:57
  31.5 2.1 %collective-permute-done.1.r2 = bf16[64,768]{1,0:T(8,128)(2,1)S(1)} collective-permute-done((bf16[64,768]{1,0:T(8,128)(2,1)S(1)}, bf16[64,768]{1,0:T(8,128)(2,1)S(1)}, u32[]{:S(2)}, u32[]{:S(2)}) %collective-permute-start.1) | collective-permute-done | bytes 98336 | tf_op jit(solution)/shard_map/ppermute | solution.py:57
  33.5 1.9 %collective-permute-done.2.r3 = bf16[64,768]{1,0:T(8,128)(2,1)S(1)} collective-permute-done((bf16[64,768]{1,0:T(8,128)(2,1)S(1)}, bf16[64,768]{1,0:T(8,128)(2,1)S(1)}, u32[]{:S(2)}, u32[]{:S(2)}) %collective-permute-start.2) | collective-permute-done | bytes 98336 | tf_op jit(solution)/shard_map/ppermute | solution.py:57
  35.6 2.7 %collective-permute-start.5 = (bf16[96,768]{1,0:T(8,128)(2,1)S(1)}, bf16[96,768]{1,0:T(8,128)(2,1)S(1)}, u32[]{:S(2)}, u32[]{:S(2)}) collective-permute-start(bf16[96,768]{1,0:T(8,128)(2,1)S(1)} %shard_map.186.own), channel_id=1, source_target_pairs={{0,24},{1,97},{2,26},{3,99},{4,28},{5,101},{6,30},{7,103},{8,0},{9... | collective-permute-start | bytes 442376 | tf_op jit(solution)/shard_map/ppermute | solution.py:57
  38.3 0.7 collective-permute-start.3
  39.0 2.3 %collective-permute-start.19 = (bf16[256,768]{1,0:T(8,128)(2,1)S(1)}, bf16[256,768]{1,0:T(8,128)(2,1)S(1)}, u32[]{:S(2)}, u32[]{:S(2)}) collective-permute-start(bf16[256,768]{1,0:T(8,128)(2,1)S(1)} %slice.9), channel_id=1, source_target_pairs={{0,24},{1,97},{2,26},{3,99},{4,28},{5,101},{6,30},{7,103},{8,0},{9... | collective-permute-start | bytes 1179656 | tf_op jit(solution)/shard_map/ppermute | solution.py:57
  42.0 1.9 %collective-permute-done.4.r2 = bf16[96,768]{1,0:T(8,128)(2,1)S(1)} collective-permute-done((bf16[96,768]{1,0:T(8,128)(2,1)S(1)}, bf16[96,768]{1,0:T(8,128)(2,1)S(1)}, u32[]{:S(2)}, u32[]{:S(2)}) %collective-permute-start.4) | collective-permute-done | bytes 147488 | tf_op jit(solution)/shard_map/ppermute | solution.py:57
  43.9 1.2 %collective-permute-done.3.r1 = bf16[96,768]{1,0:T(8,128)(2,1)S(1)} collective-permute-done((bf16[96,768]{1,0:T(8,128)(2,1)S(1)}, bf16[96,768]{1,0:T(8,128)(2,1)S(1)}, u32[]{:S(2)}, u32[]{:S(2)}) %collective-permute-start.3) | collective-permute-done | bytes 147488 | tf_op jit(solution)/shard_map/ppermute | solution.py:57
  45.3 1.9 %collective-permute-start.8 = (bf16[64,768]{1,0:T(8,128)(2,1)S(1)}, bf16[64,768]{1,0:T(8,128)(2,1)S(1)}, u32[]{:S(2)}, u32[]{:S(2)}) collective-permute-start(bf16[64,768]{1,0:T(8,128)(2,1)S(1)} %get-tuple-element.32.own), channel_id=1, source_target_pairs={{0,96},{1,25},{2,98},{3,27},{4,100},{5,29},{6,102},{7,31},{8,104},... | collective-permute-start | bytes 294920 | tf_op jit(solution)/shard_map/ppermute | solution.py:57
  47.3 0.6 collective-permute-start.6
  47.9 2.3 %collective-permute-done.8.r3 = bf16[64,768]{1,0:T(8,128)(2,1)S(1)} collective-permute-done((bf16[64,768]{1,0:T(8,128)(2,1)S(1)}, bf16[64,768]{1,0:T(8,128)(2,1)S(1)}, u32[]{:S(2)}, u32[]{:S(2)}) %collective-permute-start.8) | collective-permute-done | bytes 98336 | tf_op jit(solution)/shard_map/ppermute | solution.py:57
  50.2 3.1 %collective-permute-done.7.r2 = bf16[64,768]{1,0:T(8,128)(2,1)S(1)} collective-permute-done((bf16[64,768]{1,0:T(8,128)(2,1)S(1)}, bf16[64,768]{1,0:T(8,128)(2,1)S(1)}, u32[]{:S(2)}, u32[]{:S(2)}) %collective-permute-start.7) | collective-permute-done | bytes 98336 | tf_op jit(solution)/shard_map/ppermute | solution.py:57
  53.2 1.2 %collective-permute-done.6.r1 = bf16[64,768]{1,0:T(8,128)(2,1)S(1)} collective-permute-done((bf16[64,768]{1,0:T(8,128)(2,1)S(1)}, bf16[64,768]{1,0:T(8,128)(2,1)S(1)}, u32[]{:S(2)}, u32[]{:S(2)}) %collective-permute-start.6) | collective-permute-done | bytes 98336 | tf_op jit(solution)/shard_map/ppermute | solution.py:57
  54.5 2.5 %collective-permute-start.11 = (f32[8,128]{1,0:T(8,128)S(1)}, f32[8,128]{1,0:T(8,128)S(1)}, u32[]{:S(2)}, u32[]{:S(2)}) collective-permute-start(f32[8,128]{1,0:T(8,128)S(1)} %get-tuple-element.33), channel_id=1, source_target_pairs={{0,6},{1,7},{2,0},{3,1},{4,2},{5,3},{6,4},{7,5},{8,14},{9,15},{10,... | collective-permute-start | bytes 12296 | tf_op jit(solution)/shard_map/ppermute | solution.py:57
  57.1 1.7 %collective-permute-start.9 = (f32[8,128]{1,0:T(8,128)S(1)}, f32[8,128]{1,0:T(8,128)S(1)}, u32[]{:S(2)}, u32[]{:S(2)}) collective-permute-start(f32[8,128]{1,0:T(8,128)S(1)} %get-tuple-element.33), channel_id=1, source_target_pairs={{0,4},{1,5},{2,6},{3,7},{4,0},{5,1},{6,2},{7,3},{8,12},{9,13},{10,... | collective-permute-start | bytes 12296 | tf_op jit(solution)/shard_map/ppermute | solution.py:57
  58.8 1.9 %collective-permute-done.10 = f32[8,128]{1,0:T(8,128)S(1)} collective-permute-done((f32[8,128]{1,0:T(8,128)S(1)}, f32[8,128]{1,0:T(8,128)S(1)}, u32[]{:S(2)}, u32[]{:S(2)}) %collective-permute-start.10) | collective-permute-done | bytes 4128 | tf_op jit(solution)/shard_map/ppermute | solution.py:57
  61.0 6.0 %collective-permute-start.12 = (f32[8,128]{1,0:T(8,128)S(1)}, f32[8,128]{1,0:T(8,128)S(1)}, u32[]{:S(2)}, u32[]{:S(2)}) collective-permute-start(f32[8,128]{1,0:T(8,128)S(1)} %add_add_fusion.s_own), channel_id=1, source_target_pairs={{0,1},{1,0},{2,3},{3,2},{4,5},{5,4},{6,7},{7,6},{8,9},{9,8},{10,11... | collective-permute-start | bytes 12296 | tf_op jit(solution)/shard_map/ppermute | solution.py:57
  67.0 0.6 copy.24
  67.6 0.6 copy.26
  68.2 0.6 copy.25
  68.8 0.6 copy.27
  69.5 3.5 %weights.1 = (f32[128,256]{1,0:T(8,128)}, f32[128,512]{1,0:T(8,128)}, f32[128,256]{1,0:T(8,128)}, f32[128,512]{1,0:T(8,128)}, bf16[2048,256]{1,0:T(8,128)(2,1)}, /*index=5*/bf16[2048,512]{1,0:T(8,128)(2,1)}) custom-call(f32[8,128]{1,0:T(8,128)S(1)} %add_add_fusion.s_own, f32[8,128]{1,0:T(8,128)S(1)} %collective-permute-done.12.s_other, ...), custom_call_target="tpu_custom_call" | custom-call | flops 805306368 | bytes 12000000 | tf_op jit(solution)/shard_map/weights/pallas_call | solution.py:237
  (40 shorter events, 1.5 us)
Async XLA Ops:
  0.6 34.8 %copy-start.5 = (f32[16,512]{1,0:T(8,128)S(1)}, f32[16,512]{1,0:T(8,128)}, u32[]{:S(2)}) copy-start(f32[16,512]{1,0:T(8,128)} %vv.3) | copy-start | bytes 98308
  0.7 34.8 %copy-start.7 = (f32[16,256]{1,0:T(8,128)S(1)}, f32[16,256]{1,0:T(8,128)}, u32[]{:S(2)}) copy-start(f32[16,256]{1,0:T(8,128)} %vq.3) | copy-start | bytes 49156
  0.7 34.8 %copy-start.4 = (f32[16,512]{1,0:T(8,128)S(1)}, f32[16,512]{1,0:T(8,128)}, u32[]{:S(2)}) copy-start(f32[16,512]{1,0:T(8,128)} %mv.3) | copy-start | bytes 98308
  0.7 34.8 %copy-start.6 = (f32[16,256]{1,0:T(8,128)S(1)}, f32[16,256]{1,0:T(8,128)}, u32[]{:S(2)}) copy-start(f32[16,256]{1,0:T(8,128)} %mq.3) | copy-start | bytes 49156
  12.6 56.9 %copy-start = (bf16[2048,256]{1,0:T(8,128)(2,1)S(1)}, bf16[2048,256]{1,0:T(8,128)(2,1)}, u32[]{:S(2)}) copy-start(bf16[2048,256]{1,0:T(8,128)(2,1)} %pq.3) | copy-start | bytes 3145732
  12.6 56.9 %copy-start.1 = (bf16[2048,256]{1,0:T(8,128)(2,1)S(1)}, bf16[2048,256]{1,0:T(8,128)(2,1)}, u32[]{:S(2)}) copy-start(bf16[2048,256]{1,0:T(8,128)(2,1)} %pv.3) | copy-start | bytes 3145732
  12.6 56.9 %copy-start.2 = (f32[128,512]{1,0:T(8,128)S(1)}, f32[128,512]{1,0:T(8,128)}, u32[]{:S(2)}) copy-start(f32[128,512]{1,0:T(8,128)} %wv.3) | copy-start | bytes 786436
  12.6 56.9 %copy-start.3 = (f32[128,256]{1,0:T(8,128)S(1)}, f32[128,256]{1,0:T(8,128)}, u32[]{:S(2)}) copy-start(f32[128,256]{1,0:T(8,128)} %wq.3) | copy-start | bytes 393220
  12.6 7.0 %collective-permute-start.13 = (bf16[128,768]{1,0:T(8,128)(2,1)S(1)}, bf16[128,768]{1,0:T(8,128)(2,1)S(1)}, u32[]{:S(2)}, u32[]{:S(2)}) collective-permute-start(bf16[128,768]{1,0:T(8,128)(2,1)S(1)} %get-tuple-element.35), channel_id=1, source_target_pairs={{0,32},{1,9},{2,34},{3,11},{4,36},{5,13},{6,38},{7,15},{8,40},{9,1... | collective-permute-start | bytes 589832 | tf_op jit(solution)/shard_map/ppermute | solution.py:57
  14.8 7.8 %collective-permute-start.15 = (bf16[128,768]{1,0:T(8,128)(2,1)S(1)}, bf16[128,768]{1,0:T(8,128)(2,1)S(1)}, u32[]{:S(2)}, u32[]{:S(2)}) collective-permute-start(bf16[128,768]{1,0:T(8,128)(2,1)S(1)} %get-tuple-element.35), channel_id=1, source_target_pairs={{0,96},{1,25},{2,98},{3,27},{4,100},{5,29},{6,102},{7,31},{8,104},... | collective-permute-start | bytes 589832 | tf_op jit(solution)/shard_map/ppermute | solution.py:57
  16.3 6.3 %collective-permute-start.14 = (bf16[128,768]{1,0:T(8,128)(2,1)S(1)}, bf16[128,768]{1,0:T(8,128)(2,1)S(1)}, u32[]{:S(2)}, u32[]{:S(2)}) collective-permute-start(bf16[128,768]{1,0:T(8,128)(2,1)S(1)} %get-tuple-element.35), channel_id=1, source_target_pairs={{0,64},{1,17},{2,66},{3,19},{4,68},{5,21},{6,70},{7,23},{8,72},{9,... | collective-permute-start | bytes 589832 | tf_op jit(solution)/shard_map/ppermute | solution.py:57
  22.7 16.3 %collective-permute-start.17 = (bf16[512,768]{1,0:T(8,128)(2,1)S(1)}, bf16[512,768]{1,0:T(8,128)(2,1)S(1)}, u32[]{:S(2)}, u32[]{:S(2)}) collective-permute-start(bf16[512,768]{1,0:T(8,128)(2,1)S(1)} %constant_dynamic-update-slice_fusion.g0), channel_id=1, source_target_pairs={{0,24},{1,97},{2,26},{3,99},{4,28},{5,101},{6,30},{7,103},{8,0},{9... | collective-permute-start | bytes 2359304 | tf_op jit(solution)/shard_map/ppermute | solution.py:57
  26.8 14.6 %collective-permute-start.16 = (bf16[512,768]{1,0:T(8,128)(2,1)S(1)}, bf16[512,768]{1,0:T(8,128)(2,1)S(1)}, u32[]{:S(2)}, u32[]{:S(2)}) collective-permute-start(bf16[512,768]{1,0:T(8,128)(2,1)S(1)} %constant_dynamic-update-slice_fusion.g0), channel_id=1, source_target_pairs={{0,8},{1,33},{2,10},{3,35},{4,12},{5,37},{6,14},{7,39},{8,16},{9,4... | collective-permute-start | bytes 2359304 | tf_op jit(solution)/shard_map/ppermute | solution.py:57
  26.8 4.7 %collective-permute-start = (bf16[64,768]{1,0:T(8,128)(2,1)S(1)}, bf16[64,768]{1,0:T(8,128)(2,1)S(1)}, u32[]{:S(2)}, u32[]{:S(2)}) collective-permute-start(bf16[64,768]{1,0:T(8,128)(2,1)S(1)} %get-tuple-element.29), channel_id=1, source_target_pairs={{0,32},{1,9},{2,34},{3,11},{4,36},{5,13},{6,38},{7,15},{8,40},{9,1... | collective-permute-start | bytes 294920 | tf_op jit(solution)/shard_map/ppermute | solution.py:57
  27.6 5.9 %collective-permute-start.1 = (bf16[64,768]{1,0:T(8,128)(2,1)S(1)}, bf16[64,768]{1,0:T(8,128)(2,1)S(1)}, u32[]{:S(2)}, u32[]{:S(2)}) collective-permute-start(bf16[64,768]{1,0:T(8,128)(2,1)S(1)} %get-tuple-element.30), channel_id=1, source_target_pairs={{0,64},{1,17},{2,66},{3,19},{4,68},{5,21},{6,70},{7,23},{8,72},{9,... | collective-permute-start | bytes 294920 | tf_op jit(solution)/shard_map/ppermute | solution.py:57
  29.5 6.0 %collective-permute-start.2 = (bf16[64,768]{1,0:T(8,128)(2,1)S(1)}, bf16[64,768]{1,0:T(8,128)(2,1)S(1)}, u32[]{:S(2)}, u32[]{:S(2)}) collective-permute-start(bf16[64,768]{1,0:T(8,128)(2,1)S(1)} %get-tuple-element.31), channel_id=1, source_target_pairs={{0,96},{1,25},{2,98},{3,27},{4,100},{5,29},{6,102},{7,31},{8,104},... | collective-permute-start | bytes 294920 | tf_op jit(solution)/shard_map/ppermute | solution.py:57
  35.6 6.4 %collective-permute-start.5 = (bf16[96,768]{1,0:T(8,128)(2,1)S(1)}, bf16[96,768]{1,0:T(8,128)(2,1)S(1)}, u32[]{:S(2)}, u32[]{:S(2)}) collective-permute-start(bf16[96,768]{1,0:T(8,128)(2,1)S(1)} %shard_map.186.own), channel_id=1, source_target_pairs={{0,24},{1,97},{2,26},{3,99},{4,28},{5,101},{6,30},{7,103},{8,0},{9... | collective-permute-start | bytes 442376 | tf_op jit(solution)/shard_map/ppermute | solution.py:57
  38.3 5.6 %collective-permute-start.4 = (bf16[96,768]{1,0:T(8,128)(2,1)S(1)}, bf16[96,768]{1,0:T(8,128)(2,1)S(1)}, u32[]{:S(2)}, u32[]{:S(2)}) collective-permute-start(bf16[96,768]{1,0:T(8,128)(2,1)S(1)} %shard_map.186.own), channel_id=1, source_target_pairs={{0,16},{1,65},{2,18},{3,67},{4,20},{5,69},{6,22},{7,71},{8,24},{9,... | collective-permute-start | bytes 442376 | tf_op jit(solution)/shard_map/ppermute | solution.py:57
  38.3 6.8 %collective-permute-start.3 = (bf16[96,768]{1,0:T(8,128)(2,1)S(1)}, bf16[96,768]{1,0:T(8,128)(2,1)S(1)}, u32[]{:S(2)}, u32[]{:S(2)}) collective-permute-start(bf16[96,768]{1,0:T(8,128)(2,1)S(1)} %shard_map.186.own), channel_id=1, source_target_pairs={{0,8},{1,33},{2,10},{3,35},{4,12},{5,37},{6,14},{7,39},{8,16},{9,4... | collective-permute-start | bytes 442376 | tf_op jit(solution)/shard_map/ppermute | solution.py:57
  39.0 30.4 %collective-permute-start.19 = (bf16[256,768]{1,0:T(8,128)(2,1)S(1)}, bf16[256,768]{1,0:T(8,128)(2,1)S(1)}, u32[]{:S(2)}, u32[]{:S(2)}) collective-permute-start(bf16[256,768]{1,0:T(8,128)(2,1)S(1)} %slice.9), channel_id=1, source_target_pairs={{0,24},{1,97},{2,26},{3,99},{4,28},{5,101},{6,30},{7,103},{8,0},{9... | collective-permute-start | bytes 1179656 | tf_op jit(solution)/shard_map/ppermute | solution.py:57
  41.4 28.1 %collective-permute-start.18 = (bf16[256,768]{1,0:T(8,128)(2,1)S(1)}, bf16[256,768]{1,0:T(8,128)(2,1)S(1)}, u32[]{:S(2)}, u32[]{:S(2)}) collective-permute-start(bf16[256,768]{1,0:T(8,128)(2,1)S(1)} %slice.8), channel_id=1, source_target_pairs={{0,8},{1,33},{2,10},{3,35},{4,12},{5,37},{6,14},{7,39},{8,16},{9,4... | collective-permute-start | bytes 1179656 | tf_op jit(solution)/shard_map/ppermute | solution.py:57
  45.3 4.9 %collective-permute-start.8 = (bf16[64,768]{1,0:T(8,128)(2,1)S(1)}, bf16[64,768]{1,0:T(8,128)(2,1)S(1)}, u32[]{:S(2)}, u32[]{:S(2)}) collective-permute-start(bf16[64,768]{1,0:T(8,128)(2,1)S(1)} %get-tuple-element.32.own), channel_id=1, source_target_pairs={{0,96},{1,25},{2,98},{3,27},{4,100},{5,29},{6,102},{7,31},{8,104},... | collective-permute-start | bytes 294920 | tf_op jit(solution)/shard_map/ppermute | solution.py:57
  47.2 6.0 %collective-permute-start.7 = (bf16[64,768]{1,0:T(8,128)(2,1)S(1)}, bf16[64,768]{1,0:T(8,128)(2,1)S(1)}, u32[]{:S(2)}, u32[]{:S(2)}) collective-permute-start(bf16[64,768]{1,0:T(8,128)(2,1)S(1)} %get-tuple-element.32.own), channel_id=1, source_target_pairs={{0,64},{1,17},{2,66},{3,19},{4,68},{5,21},{6,70},{7,23},{8,72},{9,... | collective-permute-start | bytes 294920 | tf_op jit(solution)/shard_map/ppermute | solution.py:57
  47.3 7.1 %collective-permute-start.6 = (bf16[64,768]{1,0:T(8,128)(2,1)S(1)}, bf16[64,768]{1,0:T(8,128)(2,1)S(1)}, u32[]{:S(2)}, u32[]{:S(2)}) collective-permute-start(bf16[64,768]{1,0:T(8,128)(2,1)S(1)} %get-tuple-element.32.own), channel_id=1, source_target_pairs={{0,32},{1,9},{2,34},{3,11},{4,36},{5,13},{6,38},{7,15},{8,40},{9,1... | collective-permute-start | bytes 294920 | tf_op jit(solution)/shard_map/ppermute | solution.py:57
  54.5 4.3 %collective-permute-start.11 = (f32[8,128]{1,0:T(8,128)S(1)}, f32[8,128]{1,0:T(8,128)S(1)}, u32[]{:S(2)}, u32[]{:S(2)}) collective-permute-start(f32[8,128]{1,0:T(8,128)S(1)} %get-tuple-element.33), channel_id=1, source_target_pairs={{0,6},{1,7},{2,0},{3,1},{4,2},{5,3},{6,4},{7,5},{8,14},{9,15},{10,... | collective-permute-start | bytes 12296 | tf_op jit(solution)/shard_map/ppermute | solution.py:57
  57.1 3.7 %collective-permute-start.10 = (f32[8,128]{1,0:T(8,128)S(1)}, f32[8,128]{1,0:T(8,128)S(1)}, u32[]{:S(2)}, u32[]{:S(2)}) collective-permute-start(f32[8,128]{1,0:T(8,128)S(1)} %get-tuple-element.33), channel_id=1, source_target_pairs={{0,2},{1,3},{2,4},{3,5},{4,6},{5,7},{6,0},{7,1},{8,10},{9,11},{10,... | collective-permute-start | bytes 12296 | tf_op jit(solution)/shard_map/ppermute | solution.py:57
  57.1 4.0 %collective-permute-start.9 = (f32[8,128]{1,0:T(8,128)S(1)}, f32[8,128]{1,0:T(8,128)S(1)}, u32[]{:S(2)}, u32[]{:S(2)}) collective-permute-start(f32[8,128]{1,0:T(8,128)S(1)} %get-tuple-element.33), channel_id=1, source_target_pairs={{0,4},{1,5},{2,6},{3,7},{4,0},{5,1},{6,2},{7,3},{8,12},{9,13},{10,... | collective-permute-start | bytes 12296 | tf_op jit(solution)/shard_map/ppermute | solution.py:57
  61.0 8.4 %collective-permute-start.12 = (f32[8,128]{1,0:T(8,128)S(1)}, f32[8,128]{1,0:T(8,128)S(1)}, u32[]{:S(2)}, u32[]{:S(2)}) collective-permute-start(f32[8,128]{1,0:T(8,128)S(1)} %add_add_fusion.s_own), channel_id=1, source_target_pairs={{0,1},{1,0},{2,3},{3,2},{4,5},{5,4},{6,7},{7,6},{8,9},{9,8},{10,11... | collective-permute-start | bytes 12296 | tf_op jit(solution)/shard_map/ppermute | solution.py:57

commit v3 on v2

--- a/solution.py
+++ b/solution.py
@@ -25,7 +25,7 @@
 WV = 512
 W = WQ + WV
 ROWS = 128
-TOKEN_BLOCK = 768
+TOKEN_BLOCK = 1024
 
 F32 = jnp.float32
 BF16 = jnp.bfloat16
@@ -71,14 +71,51 @@
     return pltpu.with_memory_space_constraint(array, pltpu.VMEM)
 
 
-def gradient_kernel(x, cq, cv, pq, pv, wq, wv, own, to_1, to_2, to_3, w16, total):
+def in_hbm(array):
+    return pltpu.with_memory_space_constraint(array, pltpu.HBM)
+
+
+def prepare_kernel(wq, wv, pq, pv, w16, pq_out, pv_out, wq_s, wv_s, sem):
+    pairs = ((wq, wq_s), (wv, wv_s), (pq, pq_out), (pv, pv_out))
+    loads = [pltpu.make_async_copy(a, b, sem.at[n]) for n, (a, b) in enumerate(pairs)]
+    for copy in loads:
+        copy.start()
+    loads[0].wait()
+    w16[:, :WQ] = wq_s[...].astype(BF16)
+    loads[1].wait()
+    w16[:, WQ:] = wv_s[...].astype(BF16)
+    loads[2].wait()
+    loads[3].wait()
+
+
+def prepare(wq, wv, pq, pv):
+    vmem = pl.BlockSpec(memory_space=pltpu.VMEM)
+    return pl.pallas_call(
+        prepare_kernel,
+        in_specs=[pl.BlockSpec(memory_space=pl.ANY)] * 4,
+        out_specs=[vmem] * 3,
+        out_shape=[
+            pltpu.VMEM((ROWS, W), BF16),
+            pltpu.VMEM(pq.shape, BF16),
+            pltpu.VMEM(pv.shape, BF16),
+        ],
+        scratch_shapes=[
+            pltpu.VMEM(wq.shape, F32),
+            pltpu.VMEM(wv.shape, F32),
+            pltpu.SemaphoreType.DMA((4,)),
+        ],
+        cost_estimate=pl.CostEstimate(flops=1_000_000, bytes_accessed=3_000_000, transcendentals=0),
+        compiler_params=pltpu.CompilerParams(vmem_limit_bytes=8 * 2**20),
+        name="prepare",
+    )(*(in_hbm(a) for a in (wq, wv, pq, pv)))
+
+
+def gradient_kernel(x, cq, cv, pq, pv, own, to_1, to_2, to_3, total):
     step = pl.program_id(0)
 
     @pl.when(step == 0)
     def _():
         total[...] = jnp.zeros_like(total)
-        w16[:, :WQ] = wq[...].astype(BF16)
-        w16[:, WQ:] = wv[...].astype(BF16)
 
     rows = x[...]
     mixed_q = jnp.dot(rows, pq[...], preferred_element_type=F32).astype(BF16)
@@ -97,31 +134,23 @@
                 out[minor * 16 : (minor + 1) * 16, :] = total[pl.ds(start, 16), :].astype(out.dtype)
 
 
-def projected_gradient(inputs, cq, cv, pq, pv, wq, wv):
+def projected_gradient(inputs, cq, cv, pq, pv):
     tokens, width = inputs.shape
-    whole = lambda a: pl.BlockSpec(a.shape, lambda i: (0, 0))
+    vmem = pl.BlockSpec(memory_space=pltpu.VMEM)
     by_tokens = lambda a: pl.BlockSpec((TOKEN_BLOCK, a.shape[1]), lambda i: (i, 0))
-    out = [
-        jax.ShapeDtypeStruct((64, W), F32),
-        jax.ShapeDtypeStruct((64, W), BF16),
-        jax.ShapeDtypeStruct((64, W), BF16),
-        jax.ShapeDtypeStruct((64, W), BF16),
-        jax.ShapeDtypeStruct((ROWS, W), BF16),
-    ]
     return pl.pallas_call(
         gradient_kernel,
         grid=(tokens // TOKEN_BLOCK,),
-        in_specs=[by_tokens(inputs), by_tokens(cq), by_tokens(cv)]
-        + [whole(a) for a in (pq, pv, wq, wv)],
-        out_specs=[whole(a) for a in out],
-        out_shape=[pltpu.VMEM(o.shape, o.dtype) for o in out],
+        in_specs=[by_tokens(inputs), by_tokens(cq), by_tokens(cv), vmem, vmem],
+        out_specs=[vmem] * 4,
+        out_shape=[pltpu.VMEM((64, W), F32)] + [pltpu.VMEM((64, W), BF16)] * 3,
         scratch_shapes=[pltpu.VMEM((RANK, W), F32)],
         cost_estimate=pl.CostEstimate(
-            flops=2 * tokens * RANK * (2 * width + W), bytes_accessed=20_000_000, transcendentals=0
+            flops=2 * tokens * RANK * (2 * width + W), bytes_accessed=18_000_000, transcendentals=0
         ),
-        compiler_params=pltpu.CompilerParams(vmem_limit_bytes=28 * 2**20),
+        compiler_params=pltpu.CompilerParams(vmem_limit_bytes=32 * 2**20),
         name="gradient",
-    )(*(pltpu.with_memory_space_constraint(a, pltpu.HBM) for a in (inputs, cq, cv, pq, pv, wq, wv)))
+    )(in_hbm(inputs), in_hbm(cq), in_hbm(cv), in_vmem(pq), in_vmem(pv))
 
 
 def whole_call(body, out, operands, scratch=(), flops=1_000_000):
@@ -185,19 +214,28 @@
 
 
 def weight_kernel(
-    s_own, s_other, u, pq, pv, g0, g1, g3, h_up, h_down, wq, wv,
-    nq, nv, tq, tv, cq, cv, cq_s, cv_s, c_sem,
+    s_own, s_other, u, pq, pv, g0, g1, g3, h_up, h_down, wq, wv, fq, fv, sq, sv,
+    nq, nv, tq, tv, cq, cv, fq_out, fv_out, sq_out, sv_out,
+    nq_s, nv_s, tq_s, tv_s, cq_s, cv_s, c_sem, m_sem,
 ):
+    stores = []
+
+    def store(source, target, sem):
+        copy = pltpu.make_async_copy(source, target, sem)
+        copy.start()
+        stores.append(copy)
+
+    for n, (a, b) in enumerate(((fq, fq_out), (fv, fv_out), (sq, sq_out), (sv, sv_out))):
+        store(a, b, m_sem.at[n])
     major, minor, per_major, per_minor = own_place()
     squares = jnp.sum(s_own[...] + s_other[...], axis=(0, 1), keepdims=True)
     scale = lax.rsqrt(squares / (RANK * (QK_W + V_W)) + norm_eps)
     uq, uv = u[:, :WQ], u[:, WQ:]
     keep = 1.0 - step_rate * decay_rate
-    stores = []
     for i, pieces in ((0, (g0, g0)), (1, (g1, g1)), (3, (g3, g3)), (2, (h_up, h_down))):
-        b_there = lax.rem(minor + 4 - i, 4)
+        a_there = lax.rem(major + 4 - i, 4)
         for j in range(4):
-            a_there = lax.rem(major + 4 - j, 4)
+            b_there = lax.rem(minor + 4 - j, 4)
             block = a_there * per_major + b_there * per_minor
             at = pl.ds(pl.multiple_of(block * ROWS, ROWS), ROWS)
             back_q = scale * jnp.dot(pq[at, :], uq, preferred_element_type=F32)
@@ -209,20 +247,20 @@
             cq_s[n] = (keep * held[:, :WQ] - step_rate * back_q).astype(BF16)
             cv_s[n] = (keep * held[:, WQ:] - step_rate * back_v).astype(BF16)
             for part, (source, target) in enumerate(((cq_s, cq), (cv_s, cv))):
-                copy = pltpu.make_async_copy(source.at[n], target.at[at, :], c_sem.at[n, part])
-                copy.start()
-                stores.append(copy)
+                store(source.at[n], target.at[at, :], c_sem.at[n, part])
             if n == 0:
-                for back, w, t, new in ((back_q, wq, tq, nq), (back_v, wv, tv, nv)):
+                for back, w, t, new in ((back_q, wq, tq_s, nq_s), (back_v, wv, tv_s, nv_s)):
                     weight = w[...]
                     step = back + decay_rate * weight
                     t[...] = step
                     new[...] = weight - step_rate * step
+                for k, (a, b) in enumerate(((nq_s, nq), (nv_s, nv), (tq_s, tq), (tv_s, tv))):
+                    store(a, b, m_sem.at[4 + k])
     for copy in stores:
         copy.wait()
 
 
-def new_weights(s_own, s_other, u, pq, pv, groups, wq, wv):
+def new_weights(s_own, s_other, u, pq, pv, groups, wq, wv, kept):
     vmem = pl.BlockSpec(memory_space=pltpu.VMEM)
     hbm = pl.BlockSpec(memory_space=pl.ANY)
     out = [
@@ -232,17 +270,22 @@
         jax.ShapeDtypeStruct((ROWS, WV), F32),
         jax.ShapeDtypeStruct((16 * ROWS, WQ), BF16),
         jax.ShapeDtypeStruct((16 * ROWS, WV), BF16),
-    ]
-    operands = (s_own, s_other, u, pq, pv, *groups, wq, wv)
+    ] + [jax.ShapeDtypeStruct(a.shape, F32) for a in kept]
+    operands = (s_own, s_other, u, pq, pv, *groups, wq, wv, *kept)
     return pl.pallas_call(
         weight_kernel,
         in_specs=[vmem] * len(operands),
-        out_specs=[vmem] * 4 + [hbm] * 2,
+        out_specs=[hbm] * len(out),
         out_shape=out,
         scratch_shapes=[
+            pltpu.VMEM((ROWS, WQ), F32),
+            pltpu.VMEM((ROWS, WV), F32),
+            pltpu.VMEM((ROWS, WQ), F32),
+            pltpu.VMEM((ROWS, WV), F32),
             pltpu.VMEM((16, ROWS, WQ), BF16),
             pltpu.VMEM((16, ROWS, WV), BF16),
             pltpu.SemaphoreType.DMA((16, 2)),
+            pltpu.SemaphoreType.DMA((8,)),
         ],
         cost_estimate=pl.CostEstimate(
             flops=2 * 16 * ROWS * RANK * W, bytes_accessed=12_000_000, transcendentals=0
@@ -253,15 +296,16 @@
 
 
 def on_device(inputs, cq, cv, pq, pv, wq, wv, mq, mv, vq, vv):
-    own, to_1, to_2, to_3, w16 = projected_gradient(inputs, cq, cv, pq, pv, wq, wv)
+    w16, pq, pv = prepare(wq, wv, pq, pv)
+    w_1, w_3, w_2 = (shifted(w16, "minor", n) for n in (1, 3, 2))
+    own, to_1, to_2, to_3 = projected_gradient(inputs, cq, cv, pq, pv)
     r_2, r_1, r_3 = (shifted(a, "major", n) for n, a in ((2, to_2), (1, to_1), (3, to_3)))
-    w_1, w_3, w_2 = (shifted(w16, "major", n) for n in (1, 3, 2))
+    group = jnp.concatenate([w16, w_1, w_2, w_3], axis=0)
+    g_1, g_3 = shifted(group, "major", 1), shifted(group, "major", 3)
     message, = whole_call(
         partial_kernel, [jax.ShapeDtypeStruct((96, W), BF16)], (own, r_1, r_2, r_3, mq, mv, vq, vv)
     )
     m_2, m_1, m_3 = (shifted(message, "minor", n) for n in (2, 1, 3))
-    group = jnp.concatenate([w16, w_1, w_2, w_3], axis=0)
-    g_1, g_3 = shifted(group, "minor", 1), shifted(group, "minor", 3)
     small = lambda n: jax.ShapeDtypeStruct((16, n), F32)
     u_own, first_q, first_v, second_q, second_v = whole_call(
         update_kernel,
@@ -270,20 +314,21 @@
         [pltpu.VMEM((64, W), F32)],
     )
     u_2, u_1, u_3 = (shifted(u_own, "major", n) for n in (2, 1, 3))
+    h_up = shifted(g_1[: 2 * ROWS], "major", 1)
+    h_down = shifted(g_3[2 * ROWS :], "major", 3)
     u, squares = whole_call(
         assemble_kernel,
         [jax.ShapeDtypeStruct((RANK, W), BF16), jax.ShapeDtypeStruct((8, 128), F32)],
         (u_own, u_1, u_2, u_3),
     )
     s_2, s_1, s_3 = (shifted(squares, "x", n) for n in (2, 1, 3))
-    h_up = shifted(g_1[: 2 * ROWS], "minor", 1)
-    h_down = shifted(g_3[2 * ROWS :], "minor", 3)
     chips = (squares + s_2) + (s_1 + s_3)
     other = shifted(chips, "core", 1)
-    new_q, new_v, step_q, step_v, copy_q, copy_v = new_weights(
-        chips, other, u, pq, pv, (group, g_1, g_3, h_up, h_down), wq, wv
-    )
-    return (new_q, new_v, copy_q, copy_v, first_q, first_v, second_q, second_v, step_q, step_v)
+    kept = (first_q, first_v, second_q, second_v)
+    new_q, new_v, step_q, step_v, copy_q, copy_v, *kept = new_weights(
+        chips, other, u, pq, pv, (group, g_1, g_3, h_up, h_down), wq, wv, kept
+    )
+    return (new_q, new_v, copy_q, copy_v, *kept, step_q, step_v)
 
 
 def solution(mesh):

time: 73.1 us -> 72.7 us (level)
  local copies, waits for them, and re-layouts: 2.59 us -> 0.14 us
  starting transfers between devices: 31.4 us -> 32.9 us
    unnamed x23 -> x15, local copies, waits for them, and re-layouts: 2.52 us -> 0.07 us
    pallas_call x0 -> x1, Pallas kernels: none -> 1.74 us  [prepare(): pl.pallas_call(prepare_kernel, in_specs=[pl.BlockSpec(memory_space=pl.ANY...]
    ppermute x20, starting transfers between devices: 31.4 us -> 32.9 us  [shifted(): return lax.ppermute(array, AXES, shift_pairs(kind, offset))]
    pallas_call x1, Pallas kernels: 11.9 us -> 11.1 us  [projected_gradient(): pl.pallas_call(gradient_kernel, grid=(tokens // TOKEN_BLOCK,), in_specs=[...]
  transfers between devices with their start and end apart: 20 -> 20, of which waited for: 13 -> 14; matrix products, arithmetic and copies ran while one was open for 3% -> 0% of each run, Pallas kernels for 0% -> 16%
where the time goes in v3:
time: 72.7 us; the launch traced here: 72.6 us
  starting transfers between devices  32.9 us (45%)
  waiting for transfers between devices  22.7 us (31%)
  Pallas kernels  16 us (22%)
  between operations  0.79 us (1%)
    ppermute x20, starting transfers between devices, shifted(): return lax.ppermute(array, AXES, shift_pairs(kind, offset))  32.9 us
    ppermute x20, waiting for transfers between devices, shifted(): return lax.ppermute(array, AXES, shift_pairs(kind, offset))  22.7 us
    pallas_call x1, Pallas kernels, projected_gradient(): pl.pallas_call(gradient_kernel, grid=(tokens // TOKEN_BLOCK,), in_specs=[...  11.1 us
    pallas_call x1, Pallas kernels, new_weights(): pl.pallas_call(weight_kernel, in_specs=[vmem] * len(operands), out_specs=...  2.86 us
    pallas_call x1, Pallas kernels, prepare(): pl.pallas_call(prepare_kernel, in_specs=[pl.BlockSpec(memory_space=pl.ANY...  1.74 us
  transfers between devices with their start and end apart: 20, of which 14 were waited for; matrix products, arithmetic and copies ran while one was open for 0% of the time, Pallas kernels for 16%

profile of v3, /device:TPU:1, one launch (start us, length us, event | category | flops | bytes accessed | tf_op | source)
XLA Modules:
  0.0 72.6 jit_solution(1598787139337388098)
XLA Ops:
  0.6 1.7 %prepare.1 = (bf16[128,768]{1,0:T(8,128)(2,1)S(1)}, bf16[2048,256]{1,0:T(8,128)(2,1)S(1)}, bf16[2048,256]{1,0:T(8,128)(2,1)S(1)}) custom-call(f32[128,256]{1,0:T(8,128)} %wq.3, f32[128,512]{1,0:T(8,128)} %wv.3, bf16[2048,256]{1,0:T(8,128)(2,1)} %pq.1, bf16[2048,256]{1,0:T(8,128)(2,1)} %pv.1), custom_call_target="tpu_custom_call" | custom-call | flops 1000000 | bytes 3000000 | tf_op jit(solution)/shard_map/prepare/pallas_call | solution.py:93
  2.4 2.5 %collective-permute-start.13 = (bf16[128,768]{1,0:T(8,128)(2,1)S(1)}, bf16[128,768]{1,0:T(8,128)(2,1)S(1)}, u32[]{:S(2)}, u32[]{:S(2)}) collective-permute-start(bf16[128,768]{1,0:T(8,128)(2,1)S(1)} %get-tuple-element.43), channel_id=1, source_target_pairs={{0,8},{1,33},{2,10},{3,35},{4,12},{5,37},{6,14},{7,39},{8,16},{9,4... | collective-permute-start | bytes 589832 | tf_op jit(solution)/shard_map/ppermute | solution.py:57
  4.9 2.2 %collective-permute-start.15 = (bf16[128,768]{1,0:T(8,128)(2,1)S(1)}, bf16[128,768]{1,0:T(8,128)(2,1)S(1)}, u32[]{:S(2)}, u32[]{:S(2)}) collective-permute-start(bf16[128,768]{1,0:T(8,128)(2,1)S(1)} %get-tuple-element.43), channel_id=1, source_target_pairs={{0,24},{1,97},{2,26},{3,99},{4,28},{5,101},{6,30},{7,103},{8,0},{9... | collective-permute-start | bytes 589832 | tf_op jit(solution)/shard_map/ppermute | solution.py:57
  7.1 1.2 %collective-permute-start.14 = (bf16[128,768]{1,0:T(8,128)(2,1)S(1)}, bf16[128,768]{1,0:T(8,128)(2,1)S(1)}, u32[]{:S(2)}, u32[]{:S(2)}) collective-permute-start(bf16[128,768]{1,0:T(8,128)(2,1)S(1)} %get-tuple-element.43), channel_id=1, source_target_pairs={{0,16},{1,65},{2,18},{3,67},{4,20},{5,69},{6,22},{7,71},{8,24},{9,... | collective-permute-start | bytes 589832 | tf_op jit(solution)/shard_map/ppermute | solution.py:57
  8.4 2.0 %collective-permute-done.13 = bf16[128,768]{1,0:T(8,128)(2,1)S(1)} collective-permute-done((bf16[128,768]{1,0:T(8,128)(2,1)S(1)}, bf16[128,768]{1,0:T(8,128)(2,1)S(1)}, u32[]{:S(2)}, u32[]{:S(2)}) %collective-permute-start.13) | collective-permute-done | bytes 196640 | tf_op jit(solution)/shard_map/ppermute | solution.py:57
  10.3 3.3 %collective-permute-done.14 = bf16[128,768]{1,0:T(8,128)(2,1)S(1)} collective-permute-done((bf16[128,768]{1,0:T(8,128)(2,1)S(1)}, bf16[128,768]{1,0:T(8,128)(2,1)S(1)}, u32[]{:S(2)}, u32[]{:S(2)}) %collective-permute-start.14) | collective-permute-done | bytes 196640 | tf_op jit(solution)/shard_map/ppermute | solution.py:57
  13.7 2.5 %collective-permute-start.17 = (bf16[512,768]{1,0:T(8,128)(2,1)S(1)}, bf16[512,768]{1,0:T(8,128)(2,1)S(1)}, u32[]{:S(2)}, u32[]{:S(2)}) collective-permute-start(bf16[512,768]{1,0:T(8,128)(2,1)S(1)} %constant_dynamic-update-slice_fusion.g0), channel_id=1, source_target_pairs={{0,96},{1,25},{2,98},{3,27},{4,100},{5,29},{6,102},{7,31},{8,104},... | collective-permute-start | bytes 2359304 | tf_op jit(solution)/shard_map/ppermute | solution.py:57
  16.3 11.1 %gradient.1 = (f32[64,768]{1,0:T(8,128)S(1)}, bf16[64,768]{1,0:T(8,128)(2,1)S(1)}, bf16[64,768]{1,0:T(8,128)(2,1)S(1)}, bf16[64,768]{1,0:T(8,128)(2,1)S(1)}) custom-call(bf16[3072,2048]{1,0:T(8,128)(2,1)} %x.1, bf16[3072,256]{1,0:T(8,128)(2,1)} %cq.1, bf16[3072,512]{1,0:T(8,128)(2,1)} %cv.1, bf16[2048,256]{1,0:T(8,128)(2,1)S(1)} %get-tuple-element.34.pq, ...), custom_call_target="tpu_custom_call" | custom-call | flops 7650410496 | bytes 18000000 | tf_op jit(solution)/shard_map/gradient/pallas_call | solution.py:141
  27.5 3.8 %collective-permute-start.1 = (bf16[64,768]{1,0:T(8,128)(2,1)S(1)}, bf16[64,768]{1,0:T(8,128)(2,1)S(1)}, u32[]{:S(2)}, u32[]{:S(2)}) collective-permute-start(bf16[64,768]{1,0:T(8,128)(2,1)S(1)} %get-tuple-element.38), channel_id=1, source_target_pairs={{0,64},{1,17},{2,66},{3,19},{4,68},{5,21},{6,70},{7,23},{8,72},{9,... | collective-permute-start | bytes 294920 | tf_op jit(solution)/shard_map/ppermute | solution.py:57
  31.3 0.8 %collective-permute-done.r1 = bf16[64,768]{1,0:T(8,128)(2,1)S(1)} collective-permute-done((bf16[64,768]{1,0:T(8,128)(2,1)S(1)}, bf16[64,768]{1,0:T(8,128)(2,1)S(1)}, u32[]{:S(2)}, u32[]{:S(2)}) %collective-permute-start) | collective-permute-done | bytes 98336 | tf_op jit(solution)/shard_map/ppermute | solution.py:57
  32.1 2.2 %collective-permute-done.1.r2 = bf16[64,768]{1,0:T(8,128)(2,1)S(1)} collective-permute-done((bf16[64,768]{1,0:T(8,128)(2,1)S(1)}, bf16[64,768]{1,0:T(8,128)(2,1)S(1)}, u32[]{:S(2)}, u32[]{:S(2)}) %collective-permute-start.1) | collective-permute-done | bytes 98336 | tf_op jit(solution)/shard_map/ppermute | solution.py:57
  34.4 0.7 collective-permute-done.2.r3
  35.1 1.9 %collective-permute-start.5 = (bf16[96,768]{1,0:T(8,128)(2,1)S(1)}, bf16[96,768]{1,0:T(8,128)(2,1)S(1)}, u32[]{:S(2)}, u32[]{:S(2)}) collective-permute-start(bf16[96,768]{1,0:T(8,128)(2,1)S(1)} %shard_map.186.own), channel_id=1, source_target_pairs={{0,24},{1,97},{2,26},{3,99},{4,28},{5,101},{6,30},{7,103},{8,0},{9... | collective-permute-start | bytes 442376 | tf_op jit(solution)/shard_map/ppermute | solution.py:57
  37.1 1.0 %collective-permute-start.4 = (bf16[96,768]{1,0:T(8,128)(2,1)S(1)}, bf16[96,768]{1,0:T(8,128)(2,1)S(1)}, u32[]{:S(2)}, u32[]{:S(2)}) collective-permute-start(bf16[96,768]{1,0:T(8,128)(2,1)S(1)} %shard_map.186.own), channel_id=1, source_target_pairs={{0,16},{1,65},{2,18},{3,67},{4,20},{5,69},{6,22},{7,71},{8,24},{9,... | collective-permute-start | bytes 442376 | tf_op jit(solution)/shard_map/ppermute | solution.py:57
  38.1 1.2 %collective-permute-start.19 = (bf16[256,768]{1,0:T(8,128)(2,1)S(1)}, bf16[256,768]{1,0:T(8,128)(2,1)S(1)}, u32[]{:S(2)}, u32[]{:S(2)}) collective-permute-start(bf16[256,768]{1,0:T(8,128)(2,1)S(1)} %slice.9), channel_id=1, source_target_pairs={{0,96},{1,25},{2,98},{3,27},{4,100},{5,29},{6,102},{7,31},{8,104},... | collective-permute-start | bytes 1179656 | tf_op jit(solution)/shard_map/ppermute | solution.py:57
  39.3 0.4 collective-permute-start.18
  39.7 0.2 collective-permute-done.5.r3
  39.9 2.7 %collective-permute-done.4.r2 = bf16[96,768]{1,0:T(8,128)(2,1)S(1)} collective-permute-done((bf16[96,768]{1,0:T(8,128)(2,1)S(1)}, bf16[96,768]{1,0:T(8,128)(2,1)S(1)}, u32[]{:S(2)}, u32[]{:S(2)}) %collective-permute-start.4) | collective-permute-done | bytes 147488 | tf_op jit(solution)/shard_map/ppermute | solution.py:57
  42.6 1.5 %collective-permute-done.3.r1 = bf16[96,768]{1,0:T(8,128)(2,1)S(1)} collective-permute-done((bf16[96,768]{1,0:T(8,128)(2,1)S(1)}, bf16[96,768]{1,0:T(8,128)(2,1)S(1)}, u32[]{:S(2)}, u32[]{:S(2)}) %collective-permute-start.3) | collective-permute-done | bytes 147488 | tf_op jit(solution)/shard_map/ppermute | solution.py:57
  44.1 0.2 shard_map.187
  44.3 1.2 %collective-permute-start.8 = (bf16[64,768]{1,0:T(8,128)(2,1)S(1)}, bf16[64,768]{1,0:T(8,128)(2,1)S(1)}, u32[]{:S(2)}, u32[]{:S(2)}) collective-permute-start(bf16[64,768]{1,0:T(8,128)(2,1)S(1)} %get-tuple-element.40.own), channel_id=1, source_target_pairs={{0,96},{1,25},{2,98},{3,27},{4,100},{5,29},{6,102},{7,31},{8,104},... | collective-permute-start | bytes 294920 | tf_op jit(solution)/shard_map/ppermute | solution.py:57
  45.6 0.2 collective-permute-start.7
  45.8 0.7 collective-permute-start.6
  46.5 2.7 %collective-permute-done.8.r3 = bf16[64,768]{1,0:T(8,128)(2,1)S(1)} collective-permute-done((bf16[64,768]{1,0:T(8,128)(2,1)S(1)}, bf16[64,768]{1,0:T(8,128)(2,1)S(1)}, u32[]{:S(2)}, u32[]{:S(2)}) %collective-permute-start.8) | collective-permute-done | bytes 98336 | tf_op jit(solution)/shard_map/ppermute | solution.py:57
  49.2 1.4 %collective-permute-done.7.r2 = bf16[64,768]{1,0:T(8,128)(2,1)S(1)} collective-permute-done((bf16[64,768]{1,0:T(8,128)(2,1)S(1)}, bf16[64,768]{1,0:T(8,128)(2,1)S(1)}, u32[]{:S(2)}, u32[]{:S(2)}) %collective-permute-start.7) | collective-permute-done | bytes 98336 | tf_op jit(solution)/shard_map/ppermute | solution.py:57
  50.7 2.0 %collective-permute-done.6.r1 = bf16[64,768]{1,0:T(8,128)(2,1)S(1)} collective-permute-done((bf16[64,768]{1,0:T(8,128)(2,1)S(1)}, bf16[64,768]{1,0:T(8,128)(2,1)S(1)}, u32[]{:S(2)}, u32[]{:S(2)}) %collective-permute-start.6) | collective-permute-done | bytes 98336 | tf_op jit(solution)/shard_map/ppermute | solution.py:57
  52.7 2.6 %collective-permute-start.11 = (f32[8,128]{1,0:T(8,128)S(1)}, f32[8,128]{1,0:T(8,128)S(1)}, u32[]{:S(2)}, u32[]{:S(2)}) collective-permute-start(f32[8,128]{1,0:T(8,128)S(1)} %get-tuple-element.41), channel_id=1, source_target_pairs={{0,6},{1,7},{2,0},{3,1},{4,2},{5,3},{6,4},{7,5},{8,14},{9,15},{10,... | collective-permute-start | bytes 12296 | tf_op jit(solution)/shard_map/ppermute | solution.py:57
  55.3 1.7 %collective-permute-start.9 = (f32[8,128]{1,0:T(8,128)S(1)}, f32[8,128]{1,0:T(8,128)S(1)}, u32[]{:S(2)}, u32[]{:S(2)}) collective-permute-start(f32[8,128]{1,0:T(8,128)S(1)} %get-tuple-element.41), channel_id=1, source_target_pairs={{0,4},{1,5},{2,6},{3,7},{4,0},{5,1},{6,2},{7,3},{8,12},{9,13},{10,... | collective-permute-start | bytes 12296 | tf_op jit(solution)/shard_map/ppermute | solution.py:57
  57.0 2.1 %collective-permute-done.10 = f32[8,128]{1,0:T(8,128)S(1)} collective-permute-done((f32[8,128]{1,0:T(8,128)S(1)}, f32[8,128]{1,0:T(8,128)S(1)}, u32[]{:S(2)}, u32[]{:S(2)}) %collective-permute-start.10) | collective-permute-done | bytes 4128 | tf_op jit(solution)/shard_map/ppermute | solution.py:57
  59.2 9.7 %collective-permute-start.12 = (f32[8,128]{1,0:T(8,128)S(1)}, f32[8,128]{1,0:T(8,128)S(1)}, u32[]{:S(2)}, u32[]{:S(2)}) collective-permute-start(f32[8,128]{1,0:T(8,128)S(1)} %add_add_fusion.s_own), channel_id=1, source_target_pairs={{0,1},{1,0},{2,3},{3,2},{4,5},{5,4},{6,7},{7,6},{8,9},{9,8},{10,11... | collective-permute-start | bytes 12296 | tf_op jit(solution)/shard_map/ppermute | solution.py:57
  68.9 0.8 %collective-permute-done.12.s_other = f32[8,128]{1,0:T(8,128)S(1)} collective-permute-done((f32[8,128]{1,0:T(8,128)S(1)}, f32[8,128]{1,0:T(8,128)S(1)}, u32[]{:S(2)}, u32[]{:S(2)}) %collective-permute-start.12) | collective-permute-done | bytes 4128 | tf_op jit(solution)/shard_map/ppermute | solution.py:57
  69.7 2.9 %weights.1 = (f32[128,256]{1,0:T(8,128)}, f32[128,512]{1,0:T(8,128)}, f32[128,256]{1,0:T(8,128)}, f32[128,512]{1,0:T(8,128)}, bf16[2048,256]{1,0:T(8,128)(2,1)},...) custom-call(f32[8,128]{1,0:T(8,128)S(1)} %add_add_fusion.s_own, ...), custom_call_target="tpu_custom_call" | custom-call | flops 805306368 | bytes 12000000 | tf_op jit(solution)/shard_map/weights/pallas_call | solution.py:275
  (33 shorter events, 0.5 us)
Async XLA Ops:
  2.4 7.9 %collective-permute-start.13 = (bf16[128,768]{1,0:T(8,128)(2,1)S(1)}, bf16[128,768]{1,0:T(8,128)(2,1)S(1)}, u32[]{:S(2)}, u32[]{:S(2)}) collective-permute-start(bf16[128,768]{1,0:T(8,128)(2,1)S(1)} %get-tuple-element.43), channel_id=1, source_target_pairs={{0,8},{1,33},{2,10},{3,35},{4,12},{5,37},{6,14},{7,39},{8,16},{9,4... | collective-permute-start | bytes 589832 | tf_op jit(solution)/shard_map/ppermute | solution.py:57
  4.9 8.8 %collective-permute-start.15 = (bf16[128,768]{1,0:T(8,128)(2,1)S(1)}, bf16[128,768]{1,0:T(8,128)(2,1)S(1)}, u32[]{:S(2)}, u32[]{:S(2)}) collective-permute-start(bf16[128,768]{1,0:T(8,128)(2,1)S(1)} %get-tuple-element.43), channel_id=1, source_target_pairs={{0,24},{1,97},{2,26},{3,99},{4,28},{5,101},{6,30},{7,103},{8,0},{9... | collective-permute-start | bytes 589832 | tf_op jit(solution)/shard_map/ppermute | solution.py:57
  7.1 6.6 %collective-permute-start.14 = (bf16[128,768]{1,0:T(8,128)(2,1)S(1)}, bf16[128,768]{1,0:T(8,128)(2,1)S(1)}, u32[]{:S(2)}, u32[]{:S(2)}) collective-permute-start(bf16[128,768]{1,0:T(8,128)(2,1)S(1)} %get-tuple-element.43), channel_id=1, source_target_pairs={{0,16},{1,65},{2,18},{3,67},{4,20},{5,69},{6,22},{7,71},{8,24},{9,... | collective-permute-start | bytes 589832 | tf_op jit(solution)/shard_map/ppermute | solution.py:57
  13.7 24.3 %collective-permute-start.17 = (bf16[512,768]{1,0:T(8,128)(2,1)S(1)}, bf16[512,768]{1,0:T(8,128)(2,1)S(1)}, u32[]{:S(2)}, u32[]{:S(2)}) collective-permute-start(bf16[512,768]{1,0:T(8,128)(2,1)S(1)} %constant_dynamic-update-slice_fusion.g0), channel_id=1, source_target_pairs={{0,96},{1,25},{2,98},{3,27},{4,100},{5,29},{6,102},{7,31},{8,104},... | collective-permute-start | bytes 2359304 | tf_op jit(solution)/shard_map/ppermute | solution.py:57
  16.2 23.1 %collective-permute-start.16 = (bf16[512,768]{1,0:T(8,128)(2,1)S(1)}, bf16[512,768]{1,0:T(8,128)(2,1)S(1)}, u32[]{:S(2)}, u32[]{:S(2)}) collective-permute-start(bf16[512,768]{1,0:T(8,128)(2,1)S(1)} %constant_dynamic-update-slice_fusion.g0), channel_id=1, source_target_pairs={{0,32},{1,9},{2,34},{3,11},{4,36},{5,13},{6,38},{7,15},{8,40},{9,1... | collective-permute-start | bytes 2359304 | tf_op jit(solution)/shard_map/ppermute | solution.py:57
  16.2 18.8 %copy-start.2 = (f32[16,512]{1,0:T(8,128)S(1)}, f32[16,512]{1,0:T(8,128)}, u32[]{:S(2)}) copy-start(f32[16,512]{1,0:T(8,128)} %mv.3) | copy-start | bytes 98308
  16.2 18.8 %copy-start.3 = (f32[16,512]{1,0:T(8,128)S(1)}, f32[16,512]{1,0:T(8,128)}, u32[]{:S(2)}) copy-start(f32[16,512]{1,0:T(8,128)} %vv.3) | copy-start | bytes 98308
  16.2 18.8 %copy-start.4 = (f32[16,256]{1,0:T(8,128)S(1)}, f32[16,256]{1,0:T(8,128)}, u32[]{:S(2)}) copy-start(f32[16,256]{1,0:T(8,128)} %mq.3) | copy-start | bytes 49156
  16.2 18.8 %copy-start.5 = (f32[16,256]{1,0:T(8,128)S(1)}, f32[16,256]{1,0:T(8,128)}, u32[]{:S(2)}) copy-start(f32[16,256]{1,0:T(8,128)} %vq.3) | copy-start | bytes 49156
  27.4 42.4 %copy-start = (f32[128,512]{1,0:T(8,128)S(1)}, f32[128,512]{1,0:T(8,128)}, u32[]{:S(2)}) copy-start(f32[128,512]{1,0:T(8,128)} %wv.3) | copy-start | bytes 786436
  27.4 42.3 %copy-start.1 = (f32[128,256]{1,0:T(8,128)S(1)}, f32[128,256]{1,0:T(8,128)}, u32[]{:S(2)}) copy-start(f32[128,256]{1,0:T(8,128)} %wq.3) | copy-start | bytes 393220
  27.4 4.7 %collective-permute-start = (bf16[64,768]{1,0:T(8,128)(2,1)S(1)}, bf16[64,768]{1,0:T(8,128)(2,1)S(1)}, u32[]{:S(2)}, u32[]{:S(2)}) collective-permute-start(bf16[64,768]{1,0:T(8,128)(2,1)S(1)} %get-tuple-element.37), channel_id=1, source_target_pairs={{0,32},{1,9},{2,34},{3,11},{4,36},{5,13},{6,38},{7,15},{8,40},{9,1... | collective-permute-start | bytes 294920 | tf_op jit(solution)/shard_map/ppermute | solution.py:57
  27.5 6.9 %collective-permute-start.1 = (bf16[64,768]{1,0:T(8,128)(2,1)S(1)}, bf16[64,768]{1,0:T(8,128)(2,1)S(1)}, u32[]{:S(2)}, u32[]{:S(2)}) collective-permute-start(bf16[64,768]{1,0:T(8,128)(2,1)S(1)} %get-tuple-element.38), channel_id=1, source_target_pairs={{0,64},{1,17},{2,66},{3,19},{4,68},{5,21},{6,70},{7,23},{8,72},{9,... | collective-permute-start | bytes 294920 | tf_op jit(solution)/shard_map/ppermute | solution.py:57
  31.3 3.8 %collective-permute-start.2 = (bf16[64,768]{1,0:T(8,128)(2,1)S(1)}, bf16[64,768]{1,0:T(8,128)(2,1)S(1)}, u32[]{:S(2)}, u32[]{:S(2)}) collective-permute-start(bf16[64,768]{1,0:T(8,128)(2,1)S(1)} %get-tuple-element.39), channel_id=1, source_target_pairs={{0,96},{1,25},{2,98},{3,27},{4,100},{5,29},{6,102},{7,31},{8,104},... | collective-permute-start | bytes 294920 | tf_op jit(solution)/shard_map/ppermute | solution.py:57
  35.1 4.8 %collective-permute-start.5 = (bf16[96,768]{1,0:T(8,128)(2,1)S(1)}, bf16[96,768]{1,0:T(8,128)(2,1)S(1)}, u32[]{:S(2)}, u32[]{:S(2)}) collective-permute-start(bf16[96,768]{1,0:T(8,128)(2,1)S(1)} %shard_map.186.own), channel_id=1, source_target_pairs={{0,24},{1,97},{2,26},{3,99},{4,28},{5,101},{6,30},{7,103},{8,0},{9... | collective-permute-start | bytes 442376 | tf_op jit(solution)/shard_map/ppermute | solution.py:57
  37.1 5.6 %collective-permute-start.4 = (bf16[96,768]{1,0:T(8,128)(2,1)S(1)}, bf16[96,768]{1,0:T(8,128)(2,1)S(1)}, u32[]{:S(2)}, u32[]{:S(2)}) collective-permute-start(bf16[96,768]{1,0:T(8,128)(2,1)S(1)} %shard_map.186.own), channel_id=1, source_target_pairs={{0,16},{1,65},{2,18},{3,67},{4,20},{5,69},{6,22},{7,71},{8,24},{9,... | collective-permute-start | bytes 442376 | tf_op jit(solution)/shard_map/ppermute | solution.py:57
  38.0 6.1 %collective-permute-start.3 = (bf16[96,768]{1,0:T(8,128)(2,1)S(1)}, bf16[96,768]{1,0:T(8,128)(2,1)S(1)}, u32[]{:S(2)}, u32[]{:S(2)}) collective-permute-start(bf16[96,768]{1,0:T(8,128)(2,1)S(1)} %shard_map.186.own), channel_id=1, source_target_pairs={{0,8},{1,33},{2,10},{3,35},{4,12},{5,37},{6,14},{7,39},{8,16},{9,4... | collective-permute-start | bytes 442376 | tf_op jit(solution)/shard_map/ppermute | solution.py:57
  38.1 31.7 %collective-permute-start.19 = (bf16[256,768]{1,0:T(8,128)(2,1)S(1)}, bf16[256,768]{1,0:T(8,128)(2,1)S(1)}, u32[]{:S(2)}, u32[]{:S(2)}) collective-permute-start(bf16[256,768]{1,0:T(8,128)(2,1)S(1)} %slice.9), channel_id=1, source_target_pairs={{0,96},{1,25},{2,98},{3,27},{4,100},{5,29},{6,102},{7,31},{8,104},... | collective-permute-start | bytes 1179656 | tf_op jit(solution)/shard_map/ppermute | solution.py:57
  39.3 30.4 %collective-permute-start.18 = (bf16[256,768]{1,0:T(8,128)(2,1)S(1)}, bf16[256,768]{1,0:T(8,128)(2,1)S(1)}, u32[]{:S(2)}, u32[]{:S(2)}) collective-permute-start(bf16[256,768]{1,0:T(8,128)(2,1)S(1)} %slice.8), channel_id=1, source_target_pairs={{0,32},{1,9},{2,34},{3,11},{4,36},{5,13},{6,38},{7,15},{8,40},{9,1... | collective-permute-start | bytes 1179656 | tf_op jit(solution)/shard_map/ppermute | solution.py:57
  44.3 4.9 %collective-permute-start.8 = (bf16[64,768]{1,0:T(8,128)(2,1)S(1)}, bf16[64,768]{1,0:T(8,128)(2,1)S(1)}, u32[]{:S(2)}, u32[]{:S(2)}) collective-permute-start(bf16[64,768]{1,0:T(8,128)(2,1)S(1)} %get-tuple-element.40.own), channel_id=1, source_target_pairs={{0,96},{1,25},{2,98},{3,27},{4,100},{5,29},{6,102},{7,31},{8,104},... | collective-permute-start | bytes 294920 | tf_op jit(solution)/shard_map/ppermute | solution.py:57
  45.6 5.1 %collective-permute-start.7 = (bf16[64,768]{1,0:T(8,128)(2,1)S(1)}, bf16[64,768]{1,0:T(8,128)(2,1)S(1)}, u32[]{:S(2)}, u32[]{:S(2)}) collective-permute-start(bf16[64,768]{1,0:T(8,128)(2,1)S(1)} %get-tuple-element.40.own), channel_id=1, source_target_pairs={{0,64},{1,17},{2,66},{3,19},{4,68},{5,21},{6,70},{7,23},{8,72},{9,... | collective-permute-start | bytes 294920 | tf_op jit(solution)/shard_map/ppermute | solution.py:57
  45.8 6.8 %collective-permute-start.6 = (bf16[64,768]{1,0:T(8,128)(2,1)S(1)}, bf16[64,768]{1,0:T(8,128)(2,1)S(1)}, u32[]{:S(2)}, u32[]{:S(2)}) collective-permute-start(bf16[64,768]{1,0:T(8,128)(2,1)S(1)} %get-tuple-element.40.own), channel_id=1, source_target_pairs={{0,32},{1,9},{2,34},{3,11},{4,36},{5,13},{6,38},{7,15},{8,40},{9,1... | collective-permute-start | bytes 294920 | tf_op jit(solution)/shard_map/ppermute | solution.py:57
  52.7 4.3 %collective-permute-start.11 = (f32[8,128]{1,0:T(8,128)S(1)}, f32[8,128]{1,0:T(8,128)S(1)}, u32[]{:S(2)}, u32[]{:S(2)}) collective-permute-start(f32[8,128]{1,0:T(8,128)S(1)} %get-tuple-element.41), channel_id=1, source_target_pairs={{0,6},{1,7},{2,0},{3,1},{4,2},{5,3},{6,4},{7,5},{8,14},{9,15},{10,... | collective-permute-start | bytes 12296 | tf_op jit(solution)/shard_map/ppermute | solution.py:57
  55.3 3.8 %collective-permute-start.10 = (f32[8,128]{1,0:T(8,128)S(1)}, f32[8,128]{1,0:T(8,128)S(1)}, u32[]{:S(2)}, u32[]{:S(2)}) collective-permute-start(f32[8,128]{1,0:T(8,128)S(1)} %get-tuple-element.41), channel_id=1, source_target_pairs={{0,2},{1,3},{2,4},{3,5},{4,6},{5,7},{6,0},{7,1},{8,10},{9,11},{10,... | collective-permute-start | bytes 12296 | tf_op jit(solution)/shard_map/ppermute | solution.py:57
  55.3 4.0 %collective-permute-start.9 = (f32[8,128]{1,0:T(8,128)S(1)}, f32[8,128]{1,0:T(8,128)S(1)}, u32[]{:S(2)}, u32[]{:S(2)}) collective-permute-start(f32[8,128]{1,0:T(8,128)S(1)} %get-tuple-element.41), channel_id=1, source_target_pairs={{0,4},{1,5},{2,6},{3,7},{4,0},{5,1},{6,2},{7,3},{8,12},{9,13},{10,... | collective-permute-start | bytes 12296 | tf_op jit(solution)/shard_map/ppermute | solution.py:57
  59.2 10.5 %collective-permute-start.12 = (f32[8,128]{1,0:T(8,128)S(1)}, f32[8,128]{1,0:T(8,128)S(1)}, u32[]{:S(2)}, u32[]{:S(2)}) collective-permute-start(f32[8,128]{1,0:T(8,128)S(1)} %add_add_fusion.s_own), channel_id=1, source_target_pairs={{0,1},{1,0},{2,3},{3,2},{4,5},{5,4},{6,7},{7,6},{8,9},{9,8},{10,11... | collective-permute-start | bytes 12296 | tf_op jit(solution)/shard_map/ppermute | solution.py:57

commit v4 on v3

--- a/solution.py
+++ b/solution.py
@@ -25,7 +25,9 @@
 WV = 512
 W = WQ + WV
 ROWS = 128
-TOKEN_BLOCK = 1024
+MESSAGE = ROWS + 32
+FRONT = 1024
+AHEAD = 512
 
 F32 = jnp.float32
 BF16 = jnp.bfloat16
@@ -75,82 +77,157 @@
     return pltpu.with_memory_space_constraint(array, pltpu.HBM)
 
 
-def prepare_kernel(wq, wv, pq, pv, w16, pq_out, pv_out, wq_s, wv_s, sem):
-    pairs = ((wq, wq_s), (wv, wv_s), (pq, pq_out), (pv, pv_out))
+def prepare_kernel(wq, wv, pq, pv, mq, mv, vq, vv, w16, pq_out, pv_out, wq_s, wv_s, m_s, v_s, sem):
+    pairs = (
+        (wq, wq_s),
+        (wv, wv_s),
+        (mq, m_s.at[:, pl.ds(0, WQ)]),
+        (mv, m_s.at[:, pl.ds(WQ, WV)]),
+        (vq, v_s.at[:, pl.ds(0, WQ)]),
+        (vv, v_s.at[:, pl.ds(WQ, WV)]),
+        (pq, pq_out),
+        (pv, pv_out),
+    )
     loads = [pltpu.make_async_copy(a, b, sem.at[n]) for n, (a, b) in enumerate(pairs)]
     for copy in loads:
         copy.start()
-    loads[0].wait()
-    w16[:, :WQ] = wq_s[...].astype(BF16)
-    loads[1].wait()
-    w16[:, WQ:] = wv_s[...].astype(BF16)
-    loads[2].wait()
-    loads[3].wait()
-
-
-def prepare(wq, wv, pq, pv):
+    for copy in loads[:6]:
+        copy.wait()
+    w16[:ROWS, :WQ] = wq_s[...].astype(BF16)
+    w16[:ROWS, WQ:] = wv_s[...].astype(BF16)
+    w16[ROWS : ROWS + 16, :] = m_s[...].astype(BF16)
+    w16[ROWS + 16 :, :] = v_s[...].astype(BF16)
+    for copy in loads[6:]:
+        copy.wait()
+
+
+def prepare(wq, wv, pq, pv, mq, mv, vq, vv):
     vmem = pl.BlockSpec(memory_space=pltpu.VMEM)
     return pl.pallas_call(
         prepare_kernel,
-        in_specs=[pl.BlockSpec(memory_space=pl.ANY)] * 4,
+        in_specs=[pl.BlockSpec(memory_space=pl.ANY)] * 8,
         out_specs=[vmem] * 3,
         out_shape=[
-            pltpu.VMEM((ROWS, W), BF16),
+            pltpu.VMEM((MESSAGE, W), BF16),
             pltpu.VMEM(pq.shape, BF16),
             pltpu.VMEM(pv.shape, BF16),
         ],
         scratch_shapes=[
             pltpu.VMEM(wq.shape, F32),
             pltpu.VMEM(wv.shape, F32),
-            pltpu.SemaphoreType.DMA((4,)),
+            pltpu.VMEM((16, W), F32),
+            pltpu.VMEM((16, W), F32),
+            pltpu.SemaphoreType.DMA((8,)),
         ],
         cost_estimate=pl.CostEstimate(flops=1_000_000, bytes_accessed=3_000_000, transcendentals=0),
         compiler_params=pltpu.CompilerParams(vmem_limit_bytes=8 * 2**20),
         name="prepare",
-    )(*(in_hbm(a) for a in (wq, wv, pq, pv)))
-
-
-def gradient_kernel(x, cq, cv, pq, pv, own, to_1, to_2, to_3, total):
-    step = pl.program_id(0)
-
-    @pl.when(step == 0)
-    def _():
-        total[...] = jnp.zeros_like(total)
-
-    rows = x[...]
-    mixed_q = jnp.dot(rows, pq[...], preferred_element_type=F32).astype(BF16)
-    mixed_v = jnp.dot(rows, pv[...], preferred_element_type=F32).astype(BF16)
+    )(*(in_hbm(a) for a in (wq, wv, pq, pv, mq, mv, vq, vv)))
+
+
+def products(x, cq, cv, pq, pv):
     lead = (((0,), (0,)), ((), ()))
-    total[:, :WQ] += lax.dot_general(mixed_q, cq[...], lead, preferred_element_type=F32)
-    total[:, WQ:] += lax.dot_general(mixed_v, cv[...], lead, preferred_element_type=F32)
-
-    @pl.when(step == pl.num_programs(0) - 1)
-    def _():
-        major, _, per_major, per_minor = own_place()
-        for offset, out in enumerate((own, to_1, to_2, to_3)):
-            there = lax.rem(major + offset, 4)
-            for minor in range(4):
-                start = pl.multiple_of((there * per_major + minor * per_minor) * 16, 16)
-                out[minor * 16 : (minor + 1) * 16, :] = total[pl.ds(start, 16), :].astype(out.dtype)
-
-
-def projected_gradient(inputs, cq, cv, pq, pv):
-    tokens, width = inputs.shape
-    vmem = pl.BlockSpec(memory_space=pltpu.VMEM)
-    by_tokens = lambda a: pl.BlockSpec((TOKEN_BLOCK, a.shape[1]), lambda i: (i, 0))
+    mixed_q = jnp.dot(x, pq[...], preferred_element_type=F32).astype(BF16)
+    mixed_v = jnp.dot(x, pv[...], preferred_element_type=F32).astype(BF16)
+    return (
+        lax.dot_general(mixed_q, cq, lead, preferred_element_type=F32),
+        lax.dot_general(mixed_v, cv, lead, preferred_element_type=F32),
+    )
+
+
+def block_copies(sources, targets, start, size, at, sem):
+    return [
+        pltpu.make_async_copy(a.at[pl.ds(start, size), :], b.at[pl.ds(at, size), :], sem.at[n])
+        for n, (a, b) in enumerate(zip(sources, targets))
+    ]
+
+
+def front_kernel(x, cq, cv, pq, pv, total, xn, cqn, cvn, xs, cqs, cvs, sem):
+    sources, half = (x, cq, cv), FRONT // 2
+    blocks = [
+        block_copies(sources, (xs, cqs, cvs), n * half, half, n * half, sem.at[n]) for n in range(2)
+    ]
+    later = block_copies(sources, (xn, cqn, cvn), FRONT, AHEAD, 0, sem.at[2])
+    for copy in (*blocks[0], *blocks[1], *later):
+        copy.start()
+    for n in range(2):
+        for copy in blocks[n]:
+            copy.wait()
+        at = slice(n * half, (n + 1) * half)
+        part_q, part_v = products(xs[at, :], cqs[at, :], cvs[at, :], pq, pv)
+        if n == 0:
+            total[:, :WQ] = part_q
+            total[:, WQ:] = part_v
+        else:
+            total[:, :WQ] += part_q
+            total[:, WQ:] += part_v
+    for copy in later:
+        copy.wait()
+
+
+def rest_kernel(
+    x, cq, cv, pq, pv, so_far, xn, cqn, cvn, own, to_1, to_2, to_3, total, xs, cqs, cvs, sem
+):
+    sources, size = (x, cq, cv), xs.shape[0] // 2
+    first = FRONT + AHEAD
+    blocks = [
+        block_copies(sources, (xs, cqs, cvs), first + n * size, size, n * size, sem.at[n])
+        for n in range(2)
+    ]
+    for copy in (*blocks[0], *blocks[1]):
+        copy.start()
+    part_q, part_v = products(xn[...], cqn[...], cvn[...], pq, pv)
+    total[:, :WQ] = so_far[:, :WQ] + part_q
+    total[:, WQ:] = so_far[:, WQ:] + part_v
+    for n in range(2):
+        for copy in blocks[n]:
+            copy.wait()
+        at = slice(n * size, (n + 1) * size)
+        part_q, part_v = products(xs[at, :], cqs[at, :], cvs[at, :], pq, pv)
+        total[:, :WQ] += part_q
+        total[:, WQ:] += part_v
+    major, _, per_major, per_minor = own_place()
+    for offset, out in enumerate((own, to_1, to_2, to_3)):
+        there = lax.rem(major + offset, 4)
+        for minor in range(4):
+            start = pl.multiple_of((there * per_major + minor * per_minor) * 16, 16)
+            out[minor * 16 : (minor + 1) * 16, :] = total[pl.ds(start, 16), :].astype(out.dtype)
+
+
+def token_blocks(inputs, size):
+    return [pltpu.VMEM((size, n), BF16) for n in (inputs.shape[1], WQ, WV)]
+
+
+def product_call(body, arrays, held, out, scratch, tokens):
+    vmem, hbm = pl.BlockSpec(memory_space=pltpu.VMEM), pl.BlockSpec(memory_space=pl.ANY)
     return pl.pallas_call(
-        gradient_kernel,
-        grid=(tokens // TOKEN_BLOCK,),
-        in_specs=[by_tokens(inputs), by_tokens(cq), by_tokens(cv), vmem, vmem],
-        out_specs=[vmem] * 4,
-        out_shape=[pltpu.VMEM((64, W), F32)] + [pltpu.VMEM((64, W), BF16)] * 3,
-        scratch_shapes=[pltpu.VMEM((RANK, W), F32)],
+        body,
+        in_specs=[hbm] * 3 + [vmem] * len(held),
+        out_specs=[vmem] * len(out),
+        out_shape=out,
+        scratch_shapes=scratch + [pltpu.SemaphoreType.DMA((3, 3))],
         cost_estimate=pl.CostEstimate(
-            flops=2 * tokens * RANK * (2 * width + W), bytes_accessed=18_000_000, transcendentals=0
+            flops=2 * tokens * RANK * (2 * arrays[0].shape[1] + W),
+            bytes_accessed=6_000 * tokens,
+            transcendentals=0,
         ),
-        compiler_params=pltpu.CompilerParams(vmem_limit_bytes=32 * 2**20),
-        name="gradient",
-    )(in_hbm(inputs), in_hbm(cq), in_hbm(cv), in_vmem(pq), in_vmem(pv))
+        compiler_params=pltpu.CompilerParams(vmem_limit_bytes=28 * 2**20),
+    )(*(in_hbm(a) for a in arrays), *(in_vmem(a) for a in held))
+
+
+def front_products(inputs, cq, cv, pq, pv):
+    out = [pltpu.VMEM((RANK, W), F32)] + token_blocks(inputs, AHEAD)
+    return product_call(
+        front_kernel, (inputs, cq, cv), (pq, pv), out, token_blocks(inputs, FRONT), FRONT
+    )
+
+
+def rest_products(inputs, cq, cv, pq, pv, so_far, ahead):
+    left = inputs.shape[0] - FRONT - AHEAD
+    out = [pltpu.VMEM((64, W), F32)] + [pltpu.VMEM((64, W), BF16)] * 3
+    scratch = [pltpu.VMEM((RANK, W), F32)] + token_blocks(inputs, left)
+    held = (pq, pv, so_far, *ahead)
+    return product_call(rest_kernel, (inputs, cq, cv), held, out, scratch, left + AHEAD)
 
 
 def whole_call(body, out, operands, scratch=(), flops=1_000_000):
@@ -166,12 +243,13 @@
     )(*(in_vmem(a) for a in operands))
 
 
-def partial_kernel(own, r1, r2, r3, mq, mv, vq, vv, out):
-    out[:64, :] = (own[...] + r1[...].astype(F32) + (r2[...].astype(F32) + r3[...].astype(F32))).astype(BF16)
-    out[64:80, :WQ] = mq[...].astype(BF16)
-    out[64:80, WQ:] = mv[...].astype(BF16)
-    out[80:96, :WQ] = vq[...].astype(BF16)
-    out[80:96, WQ:] = vv[...].astype(BF16)
+def group_kernel(w0, w1, w2, w3, after, out):
+    for n, held in enumerate((w0, w1, w2, w3)):
+        out[n * ROWS : (n + 1) * ROWS, :] = held[:ROWS, :]
+
+
+def partial_kernel(own, r1, r2, r3, out):
+    out[...] = (own[...] + r1[...].astype(F32) + (r2[...].astype(F32) + r3[...].astype(F32))).astype(BF16)
 
 
 def moments(low, first, second):
@@ -180,15 +258,15 @@
     return first_new, second_new
 
 
-def update_kernel(own, r1, r2, r3, mq, mv, vq, vv, u, fq, fv, sq, sv, low):
-    low[...] = (own[:64, :].astype(F32) + r2[:64, :].astype(F32)) + (
-        r1[:64, :].astype(F32) + r3[:64, :].astype(F32)
-    )
+def update_kernel(own, r1, r2, r3, k0, k1, k2, k3, mq, mv, vq, vv, u, fq, fv, sq, sv, low):
+    low[...] = (own[...].astype(F32) + r2[...].astype(F32)) + (r1[...].astype(F32) + r3[...].astype(F32))
     _, minor, _, _ = own_place()
-    for offset, held in enumerate((own, r1, r2, r3)):
+    for offset, held in enumerate((k0, k1, k2, k3)):
         there = lax.rem(minor + 4 - offset, 4)
         at = pl.ds(pl.multiple_of(there * 16, 16), 16)
-        first, second = moments(low[at, :], held[64:80, :].astype(F32), held[80:96, :].astype(F32))
+        first = held[ROWS : ROWS + 16, :].astype(F32)
+        second = held[ROWS + 16 :, :].astype(F32)
+        first, second = moments(low[at, :], first, second)
         u[at, :] = (first / (jnp.sqrt(second) + adam_eps)).astype(BF16)
     mine = low[pl.ds(pl.multiple_of(minor * 16, 16), 16), :]
     fq[...], sq[...] = moments(mine[:, :WQ], mq[...], vq[...])
@@ -296,26 +374,29 @@
 
 
 def on_device(inputs, cq, cv, pq, pv, wq, wv, mq, mv, vq, vv):
-    w16, pq, pv = prepare(wq, wv, pq, pv)
-    w_1, w_3, w_2 = (shifted(w16, "minor", n) for n in (1, 3, 2))
-    own, to_1, to_2, to_3 = projected_gradient(inputs, cq, cv, pq, pv)
+    w16, pq, pv = prepare(wq, wv, pq, pv, mq, mv, vq, vv)
+    w_2, w_1, w_3 = (shifted(w16, "minor", n) for n in (2, 1, 3))
+    so_far, *ahead = front_products(inputs, cq, cv, pq, pv)
+    group, = whole_call(
+        group_kernel, [jax.ShapeDtypeStruct((4 * ROWS, W), BF16)], (w16, w_1, w_2, w_3, so_far)
+    )
+    g_1, g_3 = shifted(group, "major", 1), shifted(group, "major", 3)
+    own, to_1, to_2, to_3 = rest_products(inputs, cq, cv, pq, pv, so_far, ahead)
     r_2, r_1, r_3 = (shifted(a, "major", n) for n, a in ((2, to_2), (1, to_1), (3, to_3)))
-    group = jnp.concatenate([w16, w_1, w_2, w_3], axis=0)
-    g_1, g_3 = shifted(group, "major", 1), shifted(group, "major", 3)
     message, = whole_call(
-        partial_kernel, [jax.ShapeDtypeStruct((96, W), BF16)], (own, r_1, r_2, r_3, mq, mv, vq, vv)
+        partial_kernel, [jax.ShapeDtypeStruct((64, W), BF16)], (own, r_1, r_2, r_3)
     )
     m_2, m_1, m_3 = (shifted(message, "minor", n) for n in (2, 1, 3))
+    h_up = shifted(g_1[: 2 * ROWS], "major", 1)
+    h_down = shifted(g_3[2 * ROWS :], "major", 3)
     small = lambda n: jax.ShapeDtypeStruct((16, n), F32)
     u_own, first_q, first_v, second_q, second_v = whole_call(
         update_kernel,
         [jax.ShapeDtypeStruct((64, W), BF16), small(WQ), small(WV), small(WQ), small(WV)],
-        (message, m_1, m_2, m_3, mq, mv, vq, vv),
+        (message, m_1, m_2, m_3, w16, w_1, w_2, w_3, mq, mv, vq, vv),
         [pltpu.VMEM((64, W), F32)],
     )
     u_2, u_1, u_3 = (shifted(u_own, "major", n) for n in (2, 1, 3))
-    h_up = shifted(g_1[: 2 * ROWS], "major", 1)
-    h_down = shifted(g_3[2 * ROWS :], "major", 3)
     u, squares = whole_call(
         assemble_kernel,
         [jax.ShapeDtypeStruct((RANK, W), BF16), jax.ShapeDtypeStruct((8, 128), F32)],

time: 72.7 us -> 69.7 us (0.959)
  waiting for transfers between devices: 22.7 us -> 19.8 us
  starting transfers between devices: 32.9 us -> 30.5 us
  Pallas kernels: 16 us -> 18.1 us
    ppermute x20, waiting for transfers between devices: 22.7 us -> 19.8 us  [shifted(): return lax.ppermute(array, AXES, shift_pairs(kind, offset))]
    ppermute x20, starting transfers between devices: 32.9 us -> 30.5 us  [shifted(): return lax.ppermute(array, AXES, shift_pairs(kind, offset))]
    pallas_call x1 -> x2, Pallas kernels: 11.1 us -> 13 us  [product_call(): pl.pallas_call(body, in_specs=[hbm] * 3 + [vmem] * len(held), out_specs=[...]
  transfers between devices with their start and end apart: 20 -> 20, of which waited for: 14 -> 14; matrix products, arithmetic and copies ran while one was open for 0% -> 0% of each run, Pallas kernels for 16% -> 19%
where the time goes in v4:
time: 69.7 us; the launch traced here: 69.5 us
  starting transfers between devices  30.5 us (44%)
  waiting for transfers between devices  19.8 us (28%)
  Pallas kernels  18.1 us (26%)
  between operations  0.95 us (1%)
    ppermute x20, starting transfers between devices, shifted(): return lax.ppermute(array, AXES, shift_pairs(kind, offset))  30.5 us
    ppermute x20, waiting for transfers between devices, shifted(): return lax.ppermute(array, AXES, shift_pairs(kind, offset))  19.8 us
    pallas_call x2, Pallas kernels, product_call(): pl.pallas_call(body, in_specs=[hbm] * 3 + [vmem] * len(held), out_specs=[...  13 us
    pallas_call x1, Pallas kernels, new_weights(): pl.pallas_call(weight_kernel, in_specs=[vmem] * len(operands), out_specs=...  2.86 us
    pallas_call x1, Pallas kernels, prepare(): pl.pallas_call(prepare_kernel, in_specs=[pl.BlockSpec(memory_space=pl.ANY...  1.84 us
  transfers between devices with their start and end apart: 20, of which 14 were waited for; matrix products, arithmetic and copies ran while one was open for 0% of the time, Pallas kernels for 19%

profile of v4, /device:TPU:1, one launch (start us, length us, event | category | flops | bytes accessed | tf_op | source)
XLA Modules:
  0.0 69.5 jit_solution(14899907659758390750)
XLA Ops:
  0.6 1.8 %prepare.1 = (bf16[160,768]{1,0:T(8,128)(2,1)S(1)}, bf16[2048,256]{1,0:T(8,128)(2,1)S(1)}, bf16[2048,256]{1,0:T(8,128)(2,1)S(1)}) custom-call(f32[128,256]{1,0:T(8,128)} %wq.3, f32[128,512]{1,0:T(8,128)} %wv.3, bf16[2048,256]{1,0:T(8,128)(2,1)} %pq.1, bf16[2048,256]{1,0:T(8,128)(2,1)} %pv.1, f32[16,256]{1,0:T(8,128)} %mq.3, f32[16,512]{1,0:T(8,128)} %mv.3, ...), custom_call_target="tpu_custom_call" | custom-call | flops 1000000 | bytes 3000000 | tf_op jit(solution)/shard_map/prepare/pallas_call | solution.py:106
  2.5 4.6 %collective-permute-start.8 = (bf16[160,768]{1,0:T(8,128)(2,1)S(1)}, bf16[160,768]{1,0:T(8,128)(2,1)S(1)}, u32[]{:S(2)}, u32[]{:S(2)}) collective-permute-start(bf16[160,768]{1,0:T(8,128)(2,1)S(1)} %get-tuple-element.48.k0.w0), channel_id=1, source_target_pairs={{0,24},{1,97},{2,26},{3,99},{4,28},{5,101},{6,30},{7,103},{8,0},{9... | collective-permute-start | bytes 737288 | tf_op jit(solution)/shard_map/ppermute | solution.py:59
  7.1 0.7 %collective-permute-start.6 = (bf16[160,768]{1,0:T(8,128)(2,1)S(1)}, bf16[160,768]{1,0:T(8,128)(2,1)S(1)}, u32[]{:S(2)}, u32[]{:S(2)}) collective-permute-start(bf16[160,768]{1,0:T(8,128)(2,1)S(1)} %get-tuple-element.48.k0.w0), channel_id=1, source_target_pairs={{0,8},{1,33},{2,10},{3,35},{4,12},{5,37},{6,14},{7,39},{8,16},{9,4... | collective-permute-start | bytes 737288 | tf_op jit(solution)/shard_map/ppermute | solution.py:59
  7.8 5.0 %shard_map.186 = (f32[256,768]{1,0:T(8,128)S(1)}, bf16[512,2048]{1,0:T(8,128)(2,1)S(1)}, bf16[512,256]{1,0:T(8,128)(2,1)S(1)}, bf16[512,512]{1,0:T(8,128)(2,1)S(1)}) custom-call(bf16[3072,2048]{1,0:T(8,128)(2,1)} %x.3, bf16[3072,256]{1,0:T(8,128)(2,1)} %cq.3, bf16[3072,512]{1,0:T(8,128)(2,1)} %cv.3, bf16[2048,256]{1,0:T(8,128)(2,1)S(1)} %get-tuple-element.38.pq, ...), custom_call_target="tpu_custom_call" | custom-call | flops 2550136832 | bytes 6144000 | tf_op jit(solution)/shard_map/pallas_call | solution.py:203
  12.9 1.1 %collective-permute-done.7.k2.w2 = bf16[160,768]{1,0:T(8,128)(2,1)S(1)} collective-permute-done((bf16[160,768]{1,0:T(8,128)(2,1)S(1)}, bf16[160,768]{1,0:T(8,128)(2,1)S(1)}, u32[]{:S(2)}, u32[]{:S(2)}) %collective-permute-start.7) | collective-permute-done | bytes 245792 | tf_op jit(solution)/shard_map/ppermute | solution.py:59
  14.0 2.3 %collective-permute-done.6.k1.w1 = bf16[160,768]{1,0:T(8,128)(2,1)S(1)} collective-permute-done((bf16[160,768]{1,0:T(8,128)(2,1)S(1)}, bf16[160,768]{1,0:T(8,128)(2,1)S(1)}, u32[]{:S(2)}, u32[]{:S(2)}) %collective-permute-start.6) | collective-permute-done | bytes 245792 | tf_op jit(solution)/shard_map/ppermute | solution.py:59
  16.4 2.5 %collective-permute-start.17 = (bf16[512,768]{1,0:T(8,128)(2,1)S(1)}, bf16[512,768]{1,0:T(8,128)(2,1)S(1)}, u32[]{:S(2)}, u32[]{:S(2)}) collective-permute-start(bf16[512,768]{1,0:T(8,128)(2,1)S(1)} %shard_map.191.g0), channel_id=1, source_target_pairs={{0,96},{1,25},{2,98},{3,27},{4,100},{5,29},{6,102},{7,31},{8,104},... | collective-permute-start | bytes 2359304 | tf_op jit(solution)/shard_map/ppermute | solution.py:59
  18.9 8.1 %shard_map.187 = (f32[64,768]{1,0:T(8,128)S(1)}, bf16[64,768]{1,0:T(8,128)(2,1)S(1)}, bf16[64,768]{1,0:T(8,128)(2,1)S(1)}, bf16[64,768]{1,0:T(8,128)(2,1)S(1)}) custom-call(bf16[3072,2048]{1,0:T(8,128)(2,1)} %x.3, bf16[3072,256]{1,0:T(8,128)(2,1)} %cq.3, bf16[3072,512]{1,0:T(8,128)(2,1)} %cv.3, bf16[2048,256]{1,0:T(8,128)(2,1)S(1)} %get-tuple-element.38.pq, ...), custom_call_target="tpu_custom_call" | custom-call | flops 5100273664 | bytes 12288000 | tf_op jit(solution)/shard_map/pallas_call | solution.py:203
  27.1 3.8 %collective-permute-start.1 = (bf16[64,768]{1,0:T(8,128)(2,1)S(1)}, bf16[64,768]{1,0:T(8,128)(2,1)S(1)}, u32[]{:S(2)}, u32[]{:S(2)}) collective-permute-start(bf16[64,768]{1,0:T(8,128)(2,1)S(1)} %get-tuple-element.46), channel_id=1, source_target_pairs={{0,64},{1,17},{2,66},{3,19},{4,68},{5,21},{6,70},{7,23},{8,72},{9,... | collective-permute-start | bytes 294920 | tf_op jit(solution)/shard_map/ppermute | solution.py:59
  31.0 1.3 %collective-permute-done.r1 = bf16[64,768]{1,0:T(8,128)(2,1)S(1)} collective-permute-done((bf16[64,768]{1,0:T(8,128)(2,1)S(1)}, bf16[64,768]{1,0:T(8,128)(2,1)S(1)}, u32[]{:S(2)}, u32[]{:S(2)}) %collective-permute-start) | collective-permute-done | bytes 98336 | tf_op jit(solution)/shard_map/ppermute | solution.py:59
  32.3 1.7 %collective-permute-done.1.r2 = bf16[64,768]{1,0:T(8,128)(2,1)S(1)} collective-permute-done((bf16[64,768]{1,0:T(8,128)(2,1)S(1)}, bf16[64,768]{1,0:T(8,128)(2,1)S(1)}, u32[]{:S(2)}, u32[]{:S(2)}) %collective-permute-start.1) | collective-permute-done | bytes 98336 | tf_op jit(solution)/shard_map/ppermute | solution.py:59
  34.0 0.7 %collective-permute-done.2.r3 = bf16[64,768]{1,0:T(8,128)(2,1)S(1)} collective-permute-done((bf16[64,768]{1,0:T(8,128)(2,1)S(1)}, bf16[64,768]{1,0:T(8,128)(2,1)S(1)}, u32[]{:S(2)}, u32[]{:S(2)}) %collective-permute-start.2) | collective-permute-done | bytes 98336 | tf_op jit(solution)/shard_map/ppermute | solution.py:59
  34.8 0.7 collective-permute-start.5
  35.5 0.3 collective-permute-start.4
  35.7 0.6 collective-permute-start.3
  36.4 1.4 %collective-permute-start.19 = (bf16[256,768]{1,0:T(8,128)(2,1)S(1)}, bf16[256,768]{1,0:T(8,128)(2,1)S(1)}, u32[]{:S(2)}, u32[]{:S(2)}) collective-permute-start(bf16[256,768]{1,0:T(8,128)(2,1)S(1)} %slice.9), channel_id=1, source_target_pairs={{0,96},{1,25},{2,98},{3,27},{4,100},{5,29},{6,102},{7,31},{8,104},... | collective-permute-start | bytes 1179656 | tf_op jit(solution)/shard_map/ppermute | solution.py:59
  37.7 0.3 collective-permute-start.18
  38.0 1.6 %collective-permute-done.5.r3 = bf16[64,768]{1,0:T(8,128)(2,1)S(1)} collective-permute-done((bf16[64,768]{1,0:T(8,128)(2,1)S(1)}, bf16[64,768]{1,0:T(8,128)(2,1)S(1)}, u32[]{:S(2)}, u32[]{:S(2)}) %collective-permute-start.5) | collective-permute-done | bytes 98336 | tf_op jit(solution)/shard_map/ppermute | solution.py:59
  39.6 1.0 %collective-permute-done.4.r2 = bf16[64,768]{1,0:T(8,128)(2,1)S(1)} collective-permute-done((bf16[64,768]{1,0:T(8,128)(2,1)S(1)}, bf16[64,768]{1,0:T(8,128)(2,1)S(1)}, u32[]{:S(2)}, u32[]{:S(2)}) %collective-permute-start.4) | collective-permute-done | bytes 98336 | tf_op jit(solution)/shard_map/ppermute | solution.py:59
  40.5 1.0 %collective-permute-done.3.r1 = bf16[64,768]{1,0:T(8,128)(2,1)S(1)} collective-permute-done((bf16[64,768]{1,0:T(8,128)(2,1)S(1)}, bf16[64,768]{1,0:T(8,128)(2,1)S(1)}, u32[]{:S(2)}, u32[]{:S(2)}) %collective-permute-start.3) | collective-permute-done | bytes 98336 | tf_op jit(solution)/shard_map/ppermute | solution.py:59
  41.7 1.5 %collective-permute-start.11 = (bf16[64,768]{1,0:T(8,128)(2,1)S(1)}, bf16[64,768]{1,0:T(8,128)(2,1)S(1)}, u32[]{:S(2)}, u32[]{:S(2)}) collective-permute-start(bf16[64,768]{1,0:T(8,128)(2,1)S(1)} %get-tuple-element.49.own), channel_id=1, source_target_pairs={{0,96},{1,25},{2,98},{3,27},{4,100},{5,29},{6,102},{7,31},{8,104},... | collective-permute-start | bytes 294920 | tf_op jit(solution)/shard_map/ppermute | solution.py:59
  43.2 0.4 collective-permute-start.10
  43.6 0.5 collective-permute-start.9
  44.1 2.5 %collective-permute-done.11.r3 = bf16[64,768]{1,0:T(8,128)(2,1)S(1)} collective-permute-done((bf16[64,768]{1,0:T(8,128)(2,1)S(1)}, bf16[64,768]{1,0:T(8,128)(2,1)S(1)}, u32[]{:S(2)}, u32[]{:S(2)}) %collective-permute-start.11) | collective-permute-done | bytes 98336 | tf_op jit(solution)/shard_map/ppermute | solution.py:59
  46.6 2.5 %collective-permute-done.10.r2 = bf16[64,768]{1,0:T(8,128)(2,1)S(1)} collective-permute-done((bf16[64,768]{1,0:T(8,128)(2,1)S(1)}, bf16[64,768]{1,0:T(8,128)(2,1)S(1)}, u32[]{:S(2)}, u32[]{:S(2)}) %collective-permute-start.10) | collective-permute-done | bytes 98336 | tf_op jit(solution)/shard_map/ppermute | solution.py:59
  49.1 1.0 %collective-permute-done.9.r1 = bf16[64,768]{1,0:T(8,128)(2,1)S(1)} collective-permute-done((bf16[64,768]{1,0:T(8,128)(2,1)S(1)}, bf16[64,768]{1,0:T(8,128)(2,1)S(1)}, u32[]{:S(2)}, u32[]{:S(2)}) %collective-permute-start.9) | collective-permute-done | bytes 98336 | tf_op jit(solution)/shard_map/ppermute | solution.py:59
  50.2 2.6 %collective-permute-start.14 = (f32[8,128]{1,0:T(8,128)S(1)}, f32[8,128]{1,0:T(8,128)S(1)}, u32[]{:S(2)}, u32[]{:S(2)}) collective-permute-start(f32[8,128]{1,0:T(8,128)S(1)} %get-tuple-element.50), channel_id=1, source_target_pairs={{0,6},{1,7},{2,0},{3,1},{4,2},{5,3},{6,4},{7,5},{8,14},{9,15},{10,... | collective-permute-start | bytes 12296 | tf_op jit(solution)/shard_map/ppermute | solution.py:59
  52.8 1.7 %collective-permute-start.12 = (f32[8,128]{1,0:T(8,128)S(1)}, f32[8,128]{1,0:T(8,128)S(1)}, u32[]{:S(2)}, u32[]{:S(2)}) collective-permute-start(f32[8,128]{1,0:T(8,128)S(1)} %get-tuple-element.50), channel_id=1, source_target_pairs={{0,4},{1,5},{2,6},{3,7},{4,0},{5,1},{6,2},{7,3},{8,12},{9,13},{10,... | collective-permute-start | bytes 12296 | tf_op jit(solution)/shard_map/ppermute | solution.py:59
  54.5 2.2 %collective-permute-done.13 = f32[8,128]{1,0:T(8,128)S(1)} collective-permute-done((f32[8,128]{1,0:T(8,128)S(1)}, f32[8,128]{1,0:T(8,128)S(1)}, u32[]{:S(2)}, u32[]{:S(2)}) %collective-permute-start.13) | collective-permute-done | bytes 4128 | tf_op jit(solution)/shard_map/ppermute | solution.py:59
  56.8 8.9 %collective-permute-start.15 = (f32[8,128]{1,0:T(8,128)S(1)}, f32[8,128]{1,0:T(8,128)S(1)}, u32[]{:S(2)}, u32[]{:S(2)}) collective-permute-start(f32[8,128]{1,0:T(8,128)S(1)} %add_add_fusion.s_own), channel_id=1, source_target_pairs={{0,1},{1,0},{2,3},{3,2},{4,5},{5,4},{6,7},{7,6},{8,9},{9,8},{10,11... | collective-permute-start | bytes 12296 | tf_op jit(solution)/shard_map/ppermute | solution.py:59
  65.7 0.8 %collective-permute-done.15.s_other = f32[8,128]{1,0:T(8,128)S(1)} collective-permute-done((f32[8,128]{1,0:T(8,128)S(1)}, f32[8,128]{1,0:T(8,128)S(1)}, u32[]{:S(2)}, u32[]{:S(2)}) %collective-permute-start.15) | collective-permute-done | bytes 4128 | tf_op jit(solution)/shard_map/ppermute | solution.py:59
  66.5 2.9 %weights.1 = (f32[128,256]{1,0:T(8,128)}, f32[128,512]{1,0:T(8,128)}, f32[128,256]{1,0:T(8,128)}, f32[128,512]{1,0:T(8,128)}, bf16[2048,256]{1,0:T(8,128)(2,1)},...) custom-call(f32[8,128]{1,0:T(8,128)S(1)} %add_add_fusion.s_own, ...), custom_call_target="tpu_custom_call" | custom-call | flops 805306368 | bytes 12000000 | tf_op jit(solution)/shard_map/weights/pallas_call | solution.py:353
  (31 shorter events, 0.7 us)
Async XLA Ops:
  2.5 10.4 %collective-permute-start.8 = (bf16[160,768]{1,0:T(8,128)(2,1)S(1)}, bf16[160,768]{1,0:T(8,128)(2,1)S(1)}, u32[]{:S(2)}, u32[]{:S(2)}) collective-permute-start(bf16[160,768]{1,0:T(8,128)(2,1)S(1)} %get-tuple-element.48.k0.w0), channel_id=1, source_target_pairs={{0,24},{1,97},{2,26},{3,99},{4,28},{5,101},{6,30},{7,103},{8,0},{9... | collective-permute-start | bytes 737288 | tf_op jit(solution)/shard_map/ppermute | solution.py:59
  7.1 6.9 %collective-permute-start.7 = (bf16[160,768]{1,0:T(8,128)(2,1)S(1)}, bf16[160,768]{1,0:T(8,128)(2,1)S(1)}, u32[]{:S(2)}, u32[]{:S(2)}) collective-permute-start(bf16[160,768]{1,0:T(8,128)(2,1)S(1)} %get-tuple-element.48.k0.w0), channel_id=1, source_target_pairs={{0,16},{1,65},{2,18},{3,67},{4,20},{5,69},{6,22},{7,71},{8,24},{9,... | collective-permute-start | bytes 737288 | tf_op jit(solution)/shard_map/ppermute | solution.py:59
  7.1 9.2 %collective-permute-start.6 = (bf16[160,768]{1,0:T(8,128)(2,1)S(1)}, bf16[160,768]{1,0:T(8,128)(2,1)S(1)}, u32[]{:S(2)}, u32[]{:S(2)}) collective-permute-start(bf16[160,768]{1,0:T(8,128)(2,1)S(1)} %get-tuple-element.48.k0.w0), channel_id=1, source_target_pairs={{0,8},{1,33},{2,10},{3,35},{4,12},{5,37},{6,14},{7,39},{8,16},{9,4... | collective-permute-start | bytes 737288 | tf_op jit(solution)/shard_map/ppermute | solution.py:59
  16.4 19.9 %collective-permute-start.17 = (bf16[512,768]{1,0:T(8,128)(2,1)S(1)}, bf16[512,768]{1,0:T(8,128)(2,1)S(1)}, u32[]{:S(2)}, u32[]{:S(2)}) collective-permute-start(bf16[512,768]{1,0:T(8,128)(2,1)S(1)} %shard_map.191.g0), channel_id=1, source_target_pairs={{0,96},{1,25},{2,98},{3,27},{4,100},{5,29},{6,102},{7,31},{8,104},... | collective-permute-start | bytes 2359304 | tf_op jit(solution)/shard_map/ppermute | solution.py:59
  18.9 18.8 %collective-permute-start.16 = (bf16[512,768]{1,0:T(8,128)(2,1)S(1)}, bf16[512,768]{1,0:T(8,128)(2,1)S(1)}, u32[]{:S(2)}, u32[]{:S(2)}) collective-permute-start(bf16[512,768]{1,0:T(8,128)(2,1)S(1)} %shard_map.191.g0), channel_id=1, source_target_pairs={{0,32},{1,9},{2,34},{3,11},{4,36},{5,13},{6,38},{7,15},{8,40},{9,1... | collective-permute-start | bytes 2359304 | tf_op jit(solution)/shard_map/ppermute | solution.py:59
  27.0 14.5 %copy-start.2 = (f32[16,512]{1,0:T(8,128)S(1)}, f32[16,512]{1,0:T(8,128)}, u32[]{:S(2)}) copy-start(f32[16,512]{1,0:T(8,128)} %mv.3) | copy-start | bytes 98308
  27.0 14.5 %copy-start.3 = (f32[16,512]{1,0:T(8,128)S(1)}, f32[16,512]{1,0:T(8,128)}, u32[]{:S(2)}) copy-start(f32[16,512]{1,0:T(8,128)} %vv.3) | copy-start | bytes 98308
  27.0 14.5 %copy-start.4 = (f32[16,256]{1,0:T(8,128)S(1)}, f32[16,256]{1,0:T(8,128)}, u32[]{:S(2)}) copy-start(f32[16,256]{1,0:T(8,128)} %mq.3) | copy-start | bytes 49156
  27.0 14.5 %copy-start.5 = (f32[16,256]{1,0:T(8,128)S(1)}, f32[16,256]{1,0:T(8,128)}, u32[]{:S(2)}) copy-start(f32[16,256]{1,0:T(8,128)} %vq.3) | copy-start | bytes 49156
  27.0 39.5 %copy-start = (f32[128,512]{1,0:T(8,128)S(1)}, f32[128,512]{1,0:T(8,128)}, u32[]{:S(2)}) copy-start(f32[128,512]{1,0:T(8,128)} %wv.3) | copy-start | bytes 786436
  27.0 39.5 %copy-start.1 = (f32[128,256]{1,0:T(8,128)S(1)}, f32[128,256]{1,0:T(8,128)}, u32[]{:S(2)}) copy-start(f32[128,256]{1,0:T(8,128)} %wq.3) | copy-start | bytes 393220
  27.0 5.2 %collective-permute-start = (bf16[64,768]{1,0:T(8,128)(2,1)S(1)}, bf16[64,768]{1,0:T(8,128)(2,1)S(1)}, u32[]{:S(2)}, u32[]{:S(2)}) collective-permute-start(bf16[64,768]{1,0:T(8,128)(2,1)S(1)} %get-tuple-element.45), channel_id=1, source_target_pairs={{0,32},{1,9},{2,34},{3,11},{4,36},{5,13},{6,38},{7,15},{8,40},{9,1... | collective-permute-start | bytes 294920 | tf_op jit(solution)/shard_map/ppermute | solution.py:59
  27.1 6.9 %collective-permute-start.1 = (bf16[64,768]{1,0:T(8,128)(2,1)S(1)}, bf16[64,768]{1,0:T(8,128)(2,1)S(1)}, u32[]{:S(2)}, u32[]{:S(2)}) collective-permute-start(bf16[64,768]{1,0:T(8,128)(2,1)S(1)} %get-tuple-element.46), channel_id=1, source_target_pairs={{0,64},{1,17},{2,66},{3,19},{4,68},{5,21},{6,70},{7,23},{8,72},{9,... | collective-permute-start | bytes 294920 | tf_op jit(solution)/shard_map/ppermute | solution.py:59
  31.0 3.8 %collective-permute-start.2 = (bf16[64,768]{1,0:T(8,128)(2,1)S(1)}, bf16[64,768]{1,0:T(8,128)(2,1)S(1)}, u32[]{:S(2)}, u32[]{:S(2)}) collective-permute-start(bf16[64,768]{1,0:T(8,128)(2,1)S(1)} %get-tuple-element.47), channel_id=1, source_target_pairs={{0,96},{1,25},{2,98},{3,27},{4,100},{5,29},{6,102},{7,31},{8,104},... | collective-permute-start | bytes 294920 | tf_op jit(solution)/shard_map/ppermute | solution.py:59
  34.8 4.8 %collective-permute-start.5 = (bf16[64,768]{1,0:T(8,128)(2,1)S(1)}, bf16[64,768]{1,0:T(8,128)(2,1)S(1)}, u32[]{:S(2)}, u32[]{:S(2)}) collective-permute-start(bf16[64,768]{1,0:T(8,128)(2,1)S(1)} %shard_map.188.own), channel_id=1, source_target_pairs={{0,24},{1,97},{2,26},{3,99},{4,28},{5,101},{6,30},{7,103},{8,0},{9... | collective-permute-start | bytes 294920 | tf_op jit(solution)/shard_map/ppermute | solution.py:59
  35.5 5.1 %collective-permute-start.4 = (bf16[64,768]{1,0:T(8,128)(2,1)S(1)}, bf16[64,768]{1,0:T(8,128)(2,1)S(1)}, u32[]{:S(2)}, u32[]{:S(2)}) collective-permute-start(bf16[64,768]{1,0:T(8,128)(2,1)S(1)} %shard_map.188.own), channel_id=1, source_target_pairs={{0,16},{1,65},{2,18},{3,67},{4,20},{5,69},{6,22},{7,71},{8,24},{9,... | collective-permute-start | bytes 294920 | tf_op jit(solution)/shard_map/ppermute | solution.py:59
  35.7 5.8 %collective-permute-start.3 = (bf16[64,768]{1,0:T(8,128)(2,1)S(1)}, bf16[64,768]{1,0:T(8,128)(2,1)S(1)}, u32[]{:S(2)}, u32[]{:S(2)}) collective-permute-start(bf16[64,768]{1,0:T(8,128)(2,1)S(1)} %shard_map.188.own), channel_id=1, source_target_pairs={{0,8},{1,33},{2,10},{3,35},{4,12},{5,37},{6,14},{7,39},{8,16},{9,4... | collective-permute-start | bytes 294920 | tf_op jit(solution)/shard_map/ppermute | solution.py:59
  36.4 30.2 %collective-permute-start.19 = (bf16[256,768]{1,0:T(8,128)(2,1)S(1)}, bf16[256,768]{1,0:T(8,128)(2,1)S(1)}, u32[]{:S(2)}, u32[]{:S(2)}) collective-permute-start(bf16[256,768]{1,0:T(8,128)(2,1)S(1)} %slice.9), channel_id=1, source_target_pairs={{0,96},{1,25},{2,98},{3,27},{4,100},{5,29},{6,102},{7,31},{8,104},... | collective-permute-start | bytes 1179656 | tf_op jit(solution)/shard_map/ppermute | solution.py:59
  37.7 28.8 %collective-permute-start.18 = (bf16[256,768]{1,0:T(8,128)(2,1)S(1)}, bf16[256,768]{1,0:T(8,128)(2,1)S(1)}, u32[]{:S(2)}, u32[]{:S(2)}) collective-permute-start(bf16[256,768]{1,0:T(8,128)(2,1)S(1)} %slice.8), channel_id=1, source_target_pairs={{0,32},{1,9},{2,34},{3,11},{4,36},{5,13},{6,38},{7,15},{8,40},{9,1... | collective-permute-start | bytes 1179656 | tf_op jit(solution)/shard_map/ppermute | solution.py:59
  41.7 4.9 %collective-permute-start.11 = (bf16[64,768]{1,0:T(8,128)(2,1)S(1)}, bf16[64,768]{1,0:T(8,128)(2,1)S(1)}, u32[]{:S(2)}, u32[]{:S(2)}) collective-permute-start(bf16[64,768]{1,0:T(8,128)(2,1)S(1)} %get-tuple-element.49.own), channel_id=1, source_target_pairs={{0,96},{1,25},{2,98},{3,27},{4,100},{5,29},{6,102},{7,31},{8,104},... | collective-permute-start | bytes 294920 | tf_op jit(solution)/shard_map/ppermute | solution.py:59
  43.2 5.9 %collective-permute-start.10 = (bf16[64,768]{1,0:T(8,128)(2,1)S(1)}, bf16[64,768]{1,0:T(8,128)(2,1)S(1)}, u32[]{:S(2)}, u32[]{:S(2)}) collective-permute-start(bf16[64,768]{1,0:T(8,128)(2,1)S(1)} %get-tuple-element.49.own), channel_id=1, source_target_pairs={{0,64},{1,17},{2,66},{3,19},{4,68},{5,21},{6,70},{7,23},{8,72},{9,... | collective-permute-start | bytes 294920 | tf_op jit(solution)/shard_map/ppermute | solution.py:59
  43.6 6.5 %collective-permute-start.9 = (bf16[64,768]{1,0:T(8,128)(2,1)S(1)}, bf16[64,768]{1,0:T(8,128)(2,1)S(1)}, u32[]{:S(2)}, u32[]{:S(2)}) collective-permute-start(bf16[64,768]{1,0:T(8,128)(2,1)S(1)} %get-tuple-element.49.own), channel_id=1, source_target_pairs={{0,32},{1,9},{2,34},{3,11},{4,36},{5,13},{6,38},{7,15},{8,40},{9,1... | collective-permute-start | bytes 294920 | tf_op jit(solution)/shard_map/ppermute | solution.py:59
  50.2 4.3 %collective-permute-start.14 = (f32[8,128]{1,0:T(8,128)S(1)}, f32[8,128]{1,0:T(8,128)S(1)}, u32[]{:S(2)}, u32[]{:S(2)}) collective-permute-start(f32[8,128]{1,0:T(8,128)S(1)} %get-tuple-element.50), channel_id=1, source_target_pairs={{0,6},{1,7},{2,0},{3,1},{4,2},{5,3},{6,4},{7,5},{8,14},{9,15},{10,... | collective-permute-start | bytes 12296 | tf_op jit(solution)/shard_map/ppermute | solution.py:59
  52.8 4.0 %collective-permute-start.13 = (f32[8,128]{1,0:T(8,128)S(1)}, f32[8,128]{1,0:T(8,128)S(1)}, u32[]{:S(2)}, u32[]{:S(2)}) collective-permute-start(f32[8,128]{1,0:T(8,128)S(1)} %get-tuple-element.50), channel_id=1, source_target_pairs={{0,2},{1,3},{2,4},{3,5},{4,6},{5,7},{6,0},{7,1},{8,10},{9,11},{10,... | collective-permute-start | bytes 12296 | tf_op jit(solution)/shard_map/ppermute | solution.py:59
  52.8 4.0 %collective-permute-start.12 = (f32[8,128]{1,0:T(8,128)S(1)}, f32[8,128]{1,0:T(8,128)S(1)}, u32[]{:S(2)}, u32[]{:S(2)}) collective-permute-start(f32[8,128]{1,0:T(8,128)S(1)} %get-tuple-element.50), channel_id=1, source_target_pairs={{0,4},{1,5},{2,6},{3,7},{4,0},{5,1},{6,2},{7,3},{8,12},{9,13},{10,... | collective-permute-start | bytes 12296 | tf_op jit(solution)/shard_map/ppermute | solution.py:59
  56.8 9.7 %collective-permute-start.15 = (f32[8,128]{1,0:T(8,128)S(1)}, f32[8,128]{1,0:T(8,128)S(1)}, u32[]{:S(2)}, u32[]{:S(2)}) collective-permute-start(f32[8,128]{1,0:T(8,128)S(1)} %add_add_fusion.s_own), channel_id=1, source_target_pairs={{0,1},{1,0},{2,3},{3,2},{4,5},{5,4},{6,7},{7,6},{8,9},{9,8},{10,11... | collective-permute-start | bytes 12296 | tf_op jit(solution)/shard_map/ppermute | solution.py:59

commit v5 on v3

--- a/solution.py
+++ b/solution.py
@@ -25,6 +25,7 @@
 WV = 512
 W = WQ + WV
 ROWS = 128
+MESSAGE = ROWS + 32
 TOKEN_BLOCK = 1024
 
 F32 = jnp.float32
@@ -57,6 +58,11 @@
     return lax.ppermute(array, AXES, shift_pairs(kind, offset))
 
 
+def to_all(kind, arrays):
+    two = shifted(arrays[1], kind, 2)
+    return shifted(arrays[0], kind, 1), two, shifted(arrays[2], kind, 3)
+
+
 def own_place():
     z, y, c = lax.axis_index("z"), lax.axis_index("y"), lax.axis_index("c")
     first = c == 0
@@ -75,39 +81,52 @@
     return pltpu.with_memory_space_constraint(array, pltpu.HBM)
 
 
-def prepare_kernel(wq, wv, pq, pv, w16, pq_out, pv_out, wq_s, wv_s, sem):
-    pairs = ((wq, wq_s), (wv, wv_s), (pq, pq_out), (pv, pv_out))
+def prepare_kernel(wq, wv, pq, pv, mq, mv, vq, vv, w16, pq_out, pv_out, wq_s, wv_s, m_s, v_s, sem):
+    pairs = (
+        (wq, wq_s),
+        (wv, wv_s),
+        (mq, m_s.at[:, pl.ds(0, WQ)]),
+        (mv, m_s.at[:, pl.ds(WQ, WV)]),
+        (vq, v_s.at[:, pl.ds(0, WQ)]),
+        (vv, v_s.at[:, pl.ds(WQ, WV)]),
+        (pq, pq_out),
+        (pv, pv_out),
+    )
     loads = [pltpu.make_async_copy(a, b, sem.at[n]) for n, (a, b) in enumerate(pairs)]
     for copy in loads:
         copy.start()
-    loads[0].wait()
-    w16[:, :WQ] = wq_s[...].astype(BF16)
-    loads[1].wait()
-    w16[:, WQ:] = wv_s[...].astype(BF16)
-    loads[2].wait()
-    loads[3].wait()
-
-
-def prepare(wq, wv, pq, pv):
+    for copy in loads[:6]:
+        copy.wait()
+    w16[:ROWS, :WQ] = wq_s[...].astype(BF16)
+    w16[:ROWS, WQ:] = wv_s[...].astype(BF16)
+    w16[ROWS : ROWS + 16, :] = m_s[...].astype(BF16)
+    w16[ROWS + 16 :, :] = v_s[...].astype(BF16)
+    for copy in loads[6:]:
+        copy.wait()
+
+
+def prepare(wq, wv, pq, pv, mq, mv, vq, vv):
     vmem = pl.BlockSpec(memory_space=pltpu.VMEM)
     return pl.pallas_call(
         prepare_kernel,
-        in_specs=[pl.BlockSpec(memory_space=pl.ANY)] * 4,
+        in_specs=[pl.BlockSpec(memory_space=pl.ANY)] * 8,
         out_specs=[vmem] * 3,
         out_shape=[
-            pltpu.VMEM((ROWS, W), BF16),
+            pltpu.VMEM((MESSAGE, W), BF16),
             pltpu.VMEM(pq.shape, BF16),
             pltpu.VMEM(pv.shape, BF16),
         ],
         scratch_shapes=[
             pltpu.VMEM(wq.shape, F32),
             pltpu.VMEM(wv.shape, F32),
-            pltpu.SemaphoreType.DMA((4,)),
+            pltpu.VMEM((16, W), F32),
+            pltpu.VMEM((16, W), F32),
+            pltpu.SemaphoreType.DMA((8,)),
         ],
         cost_estimate=pl.CostEstimate(flops=1_000_000, bytes_accessed=3_000_000, transcendentals=0),
         compiler_params=pltpu.CompilerParams(vmem_limit_bytes=8 * 2**20),
         name="prepare",
-    )(*(in_hbm(a) for a in (wq, wv, pq, pv)))
+    )(*(in_hbm(a) for a in (wq, wv, pq, pv, mq, mv, vq, vv)))
 
 
 def gradient_kernel(x, cq, cv, pq, pv, own, to_1, to_2, to_3, total):
@@ -166,12 +185,13 @@
     )(*(in_vmem(a) for a in operands))
 
 
-def partial_kernel(own, r1, r2, r3, mq, mv, vq, vv, out):
-    out[:64, :] = (own[...] + r1[...].astype(F32) + (r2[...].astype(F32) + r3[...].astype(F32))).astype(BF16)
-    out[64:80, :WQ] = mq[...].astype(BF16)
-    out[64:80, WQ:] = mv[...].astype(BF16)
-    out[80:96, :WQ] = vq[...].astype(BF16)
-    out[80:96, WQ:] = vv[...].astype(BF16)
+def group_kernel(w0, w1, w2, w3, out):
+    for n, held in enumerate((w0, w1, w2, w3)):
+        out[n * ROWS : (n + 1) * ROWS, :] = held[:ROWS, :]
+
+
+def partial_kernel(own, r1, r2, r3, out):
+    out[...] = (own[...] + r1[...].astype(F32) + (r2[...].astype(F32) + r3[...].astype(F32))).astype(BF16)
 
 
 def moments(low, first, second):
@@ -180,15 +200,15 @@
     return first_new, second_new
 
 
-def update_kernel(own, r1, r2, r3, mq, mv, vq, vv, u, fq, fv, sq, sv, low):
-    low[...] = (own[:64, :].astype(F32) + r2[:64, :].astype(F32)) + (
-        r1[:64, :].astype(F32) + r3[:64, :].astype(F32)
-    )
+def update_kernel(own, r1, r2, r3, k0, k1, k2, k3, mq, mv, vq, vv, u, fq, fv, sq, sv, low):
+    low[...] = (own[...].astype(F32) + r2[...].astype(F32)) + (r1[...].astype(F32) + r3[...].astype(F32))
     _, minor, _, _ = own_place()
-    for offset, held in enumerate((own, r1, r2, r3)):
+    for offset, held in enumerate((k0, k1, k2, k3)):
         there = lax.rem(minor + 4 - offset, 4)
         at = pl.ds(pl.multiple_of(there * 16, 16), 16)
-        first, second = moments(low[at, :], held[64:80, :].astype(F32), held[80:96, :].astype(F32))
+        first = held[ROWS : ROWS + 16, :].astype(F32)
+        second = held[ROWS + 16 :, :].astype(F32)
+        first, second = moments(low[at, :], first, second)
         u[at, :] = (first / (jnp.sqrt(second) + adam_eps)).astype(BF16)
     mine = low[pl.ds(pl.multiple_of(minor * 16, 16), 16), :]
     fq[...], sq[...] = moments(mine[:, :WQ], mq[...], vq[...])
@@ -296,24 +316,26 @@
 
 
 def on_device(inputs, cq, cv, pq, pv, wq, wv, mq, mv, vq, vv):
-    w16, pq, pv = prepare(wq, wv, pq, pv)
-    w_1, w_3, w_2 = (shifted(w16, "minor", n) for n in (1, 3, 2))
-    own, to_1, to_2, to_3 = projected_gradient(inputs, cq, cv, pq, pv)
-    r_2, r_1, r_3 = (shifted(a, "major", n) for n, a in ((2, to_2), (1, to_1), (3, to_3)))
-    group = jnp.concatenate([w16, w_1, w_2, w_3], axis=0)
+    w16, pq, pv = prepare(wq, wv, pq, pv, mq, mv, vq, vv)
+    w_1, w_2, w_3 = to_all("minor", (w16,) * 3)
+    own, *parts = projected_gradient(inputs, cq, cv, pq, pv)
+    r_1, r_2, r_3 = to_all("major", parts)
+    group, = whole_call(
+        group_kernel, [jax.ShapeDtypeStruct((4 * ROWS, W), BF16)], (w16, w_1, w_2, w_3)
+    )
     g_1, g_3 = shifted(group, "major", 1), shifted(group, "major", 3)
     message, = whole_call(
-        partial_kernel, [jax.ShapeDtypeStruct((96, W), BF16)], (own, r_1, r_2, r_3, mq, mv, vq, vv)
-    )
-    m_2, m_1, m_3 = (shifted(message, "minor", n) for n in (2, 1, 3))
+        partial_kernel, [jax.ShapeDtypeStruct((64, W), BF16)], (own, r_1, r_2, r_3)
+    )
+    m_1, m_2, m_3 = to_all("minor", (message,) * 3)
     small = lambda n: jax.ShapeDtypeStruct((16, n), F32)
     u_own, first_q, first_v, second_q, second_v = whole_call(
         update_kernel,
         [jax.ShapeDtypeStruct((64, W), BF16), small(WQ), small(WV), small(WQ), small(WV)],
-        (message, m_1, m_2, m_3, mq, mv, vq, vv),
+        (message, m_1, m_2, m_3, w16, w_1, w_2, w_3, mq, mv, vq, vv),
         [pltpu.VMEM((64, W), F32)],
     )
-    u_2, u_1, u_3 = (shifted(u_own, "major", n) for n in (2, 1, 3))
+    u_1, u_2, u_3 = to_all("major", (u_own,) * 3)
     h_up = shifted(g_1[: 2 * ROWS], "major", 1)
     h_down = shifted(g_3[2 * ROWS :], "major", 3)
     u, squares = whole_call(
@@ -321,7 +343,7 @@
         [jax.ShapeDtypeStruct((RANK, W), BF16), jax.ShapeDtypeStruct((8, 128), F32)],
         (u_own, u_1, u_2, u_3),
     )
-    s_2, s_1, s_3 = (shifted(squares, "x", n) for n in (2, 1, 3))
+    s_1, s_2, s_3 = to_all("x", (squares,) * 3)
     chips = (squares + s_2) + (s_1 + s_3)
     other = shifted(chips, "core", 1)
     kept = (first_q, first_v, second_q, second_v)

time: 72.7 us -> 72.6 us (level)
  starting transfers between devices: 32.9 us -> 30.6 us
  waiting for transfers between devices: 22.7 us -> 24.8 us
    ppermute x20, starting transfers between devices: 32.9 us -> 30.6 us  [shifted(): return lax.ppermute(array, AXES, shift_pairs(kind, offset))]
    ppermute x20, waiting for transfers between devices: 22.7 us -> 24.8 us  [shifted(): return lax.ppermute(array, AXES, shift_pairs(kind, offset))]
where the time goes in v5:
time: 72.6 us; the launch traced here: 72.5 us
  starting transfers between devices  30.6 us (42%)
  waiting for transfers between devices  24.8 us (34%)
  Pallas kernels  16.2 us (22%)
  between operations  0.76 us (1%)
    ppermute x20, starting transfers between devices, shifted(): return lax.ppermute(array, AXES, shift_pairs(kind, offset))  30.6 us
    ppermute x20, waiting for transfers between devices, shifted(): return lax.ppermute(array, AXES, shift_pairs(kind, offset))  24.8 us
    pallas_call x1, Pallas kernels, projected_gradient(): pl.pallas_call(gradient_kernel, grid=(tokens // TOKEN_BLOCK,), in_specs=[...  11.1 us
    pallas_call x1, Pallas kernels, new_weights(): pl.pallas_call(weight_kernel, in_specs=[vmem] * len(operands), out_specs=...  2.86 us
    pallas_call x1, Pallas kernels, prepare(): pl.pallas_call(prepare_kernel, in_specs=[pl.BlockSpec(memory_space=pl.ANY...  1.84 us
  transfers between devices with their start and end apart: 20, of which 14 were waited for; matrix products, arithmetic and copies ran while one was open for 0% of the time, Pallas kernels for 16%

profile of v5, /device:TPU:1, one launch (start us, length us, event | category | flops | bytes accessed | tf_op | source)
XLA Modules:
  0.0 72.5 jit_solution(6911881425610068195)
XLA Ops:
  0.6 1.8 %prepare.1 = (bf16[160,768]{1,0:T(8,128)(2,1)S(1)}, bf16[2048,256]{1,0:T(8,128)(2,1)S(1)}, bf16[2048,256]{1,0:T(8,128)(2,1)S(1)}) custom-call(f32[128,256]{1,0:T(8,128)} %wq.3, f32[128,512]{1,0:T(8,128)} %wv.3, bf16[2048,256]{1,0:T(8,128)(2,1)} %pq.1, bf16[2048,256]{1,0:T(8,128)(2,1)} %pv.1, f32[16,256]{1,0:T(8,128)} %mq.3, f32[16,512]{1,0:T(8,128)} %mv.3, ...), custom_call_target="tpu_custom_call" | custom-call | flops 1000000 | bytes 3000000 | tf_op jit(solution)/shard_map/prepare/pallas_call | solution.py:110
  2.5 4.6 %collective-permute-start.8 = (bf16[160,768]{1,0:T(8,128)(2,1)S(1)}, bf16[160,768]{1,0:T(8,128)(2,1)S(1)}, u32[]{:S(2)}, u32[]{:S(2)}) collective-permute-start(bf16[160,768]{1,0:T(8,128)(2,1)S(1)} %get-tuple-element.40.k0.w0), channel_id=1, source_target_pairs={{0,24},{1,97},{2,26},{3,99},{4,28},{5,101},{6,30},{7,103},{8,0},{9... | collective-permute-start | bytes 737288 | tf_op jit(solution)/shard_map/ppermute | solution.py:58
  7.1 0.7 collective-permute-start.6
  7.8 5.1 %collective-permute-done.8.k3.w3 = bf16[160,768]{1,0:T(8,128)(2,1)S(1)} collective-permute-done((bf16[160,768]{1,0:T(8,128)(2,1)S(1)}, bf16[160,768]{1,0:T(8,128)(2,1)S(1)}, u32[]{:S(2)}, u32[]{:S(2)}) %collective-permute-start.8) | collective-permute-done | bytes 245792 | tf_op jit(solution)/shard_map/ppermute | solution.py:58
  12.9 1.1 %collective-permute-done.7.k2.w2 = bf16[160,768]{1,0:T(8,128)(2,1)S(1)} collective-permute-done((bf16[160,768]{1,0:T(8,128)(2,1)S(1)}, bf16[160,768]{1,0:T(8,128)(2,1)S(1)}, u32[]{:S(2)}, u32[]{:S(2)}) %collective-permute-start.7) | collective-permute-done | bytes 245792 | tf_op jit(solution)/shard_map/ppermute | solution.py:58
  14.0 2.3 %collective-permute-done.6.k1.w1 = bf16[160,768]{1,0:T(8,128)(2,1)S(1)} collective-permute-done((bf16[160,768]{1,0:T(8,128)(2,1)S(1)}, bf16[160,768]{1,0:T(8,128)(2,1)S(1)}, u32[]{:S(2)}, u32[]{:S(2)}) %collective-permute-start.6) | collective-permute-done | bytes 245792 | tf_op jit(solution)/shard_map/ppermute | solution.py:58
  16.4 2.5 %collective-permute-start.17 = (bf16[512,768]{1,0:T(8,128)(2,1)S(1)}, bf16[512,768]{1,0:T(8,128)(2,1)S(1)}, u32[]{:S(2)}, u32[]{:S(2)}) collective-permute-start(bf16[512,768]{1,0:T(8,128)(2,1)S(1)} %shard_map.189.g0), channel_id=1, source_target_pairs={{0,96},{1,25},{2,98},{3,27},{4,100},{5,29},{6,102},{7,31},{8,104},... | collective-permute-start | bytes 2359304 | tf_op jit(solution)/shard_map/ppermute | solution.py:58
  18.9 11.1 %gradient.1 = (f32[64,768]{1,0:T(8,128)S(1)}, bf16[64,768]{1,0:T(8,128)(2,1)S(1)}, bf16[64,768]{1,0:T(8,128)(2,1)S(1)}, bf16[64,768]{1,0:T(8,128)(2,1)S(1)}) custom-call(bf16[3072,2048]{1,0:T(8,128)(2,1)} %x.1, bf16[3072,256]{1,0:T(8,128)(2,1)} %cq.1, bf16[3072,512]{1,0:T(8,128)(2,1)} %cv.1, bf16[2048,256]{1,0:T(8,128)(2,1)S(1)} %get-tuple-element.34.pq, ...), custom_call_target="tpu_custom_call" | custom-call | flops 7650410496 | bytes 18000000 | tf_op jit(solution)/shard_map/gradient/pallas_call | solution.py:160
  30.1 3.8 %collective-permute-start.1 = (bf16[64,768]{1,0:T(8,128)(2,1)S(1)}, bf16[64,768]{1,0:T(8,128)(2,1)S(1)}, u32[]{:S(2)}, u32[]{:S(2)}) collective-permute-start(bf16[64,768]{1,0:T(8,128)(2,1)S(1)} %get-tuple-element.38), channel_id=1, source_target_pairs={{0,64},{1,17},{2,66},{3,19},{4,68},{5,21},{6,70},{7,23},{8,72},{9,... | collective-permute-start | bytes 294920 | tf_op jit(solution)/shard_map/ppermute | solution.py:58
  34.0 0.8 %collective-permute-done.r1 = bf16[64,768]{1,0:T(8,128)(2,1)S(1)} collective-permute-done((bf16[64,768]{1,0:T(8,128)(2,1)S(1)}, bf16[64,768]{1,0:T(8,128)(2,1)S(1)}, u32[]{:S(2)}, u32[]{:S(2)}) %collective-permute-start) | collective-permute-done | bytes 98336 | tf_op jit(solution)/shard_map/ppermute | solution.py:58
  34.8 2.2 %collective-permute-done.1.r2 = bf16[64,768]{1,0:T(8,128)(2,1)S(1)} collective-permute-done((bf16[64,768]{1,0:T(8,128)(2,1)S(1)}, bf16[64,768]{1,0:T(8,128)(2,1)S(1)}, u32[]{:S(2)}, u32[]{:S(2)}) %collective-permute-start.1) | collective-permute-done | bytes 98336 | tf_op jit(solution)/shard_map/ppermute | solution.py:58
  37.0 0.7 collective-permute-done.2.r3
  37.8 0.7 collective-permute-start.5
  38.6 0.7 collective-permute-start.3
  39.4 1.4 %collective-permute-start.19 = (bf16[256,768]{1,0:T(8,128)(2,1)S(1)}, bf16[256,768]{1,0:T(8,128)(2,1)S(1)}, u32[]{:S(2)}, u32[]{:S(2)}) collective-permute-start(bf16[256,768]{1,0:T(8,128)(2,1)S(1)} %slice.9), channel_id=1, source_target_pairs={{0,96},{1,25},{2,98},{3,27},{4,100},{5,29},{6,102},{7,31},{8,104},... | collective-permute-start | bytes 1179656 | tf_op jit(solution)/shard_map/ppermute | solution.py:58
  40.7 0.2 collective-permute-start.18
  41.0 1.6 %collective-permute-done.5.r3 = bf16[64,768]{1,0:T(8,128)(2,1)S(1)} collective-permute-done((bf16[64,768]{1,0:T(8,128)(2,1)S(1)}, bf16[64,768]{1,0:T(8,128)(2,1)S(1)}, u32[]{:S(2)}, u32[]{:S(2)}) %collective-permute-start.5) | collective-permute-done | bytes 98336 | tf_op jit(solution)/shard_map/ppermute | solution.py:58
  42.6 1.0 %collective-permute-done.4.r2 = bf16[64,768]{1,0:T(8,128)(2,1)S(1)} collective-permute-done((bf16[64,768]{1,0:T(8,128)(2,1)S(1)}, bf16[64,768]{1,0:T(8,128)(2,1)S(1)}, u32[]{:S(2)}, u32[]{:S(2)}) %collective-permute-start.4) | collective-permute-done | bytes 98336 | tf_op jit(solution)/shard_map/ppermute | solution.py:58
  43.5 1.0 %collective-permute-done.3.r1 = bf16[64,768]{1,0:T(8,128)(2,1)S(1)} collective-permute-done((bf16[64,768]{1,0:T(8,128)(2,1)S(1)}, bf16[64,768]{1,0:T(8,128)(2,1)S(1)}, u32[]{:S(2)}, u32[]{:S(2)}) %collective-permute-start.3) | collective-permute-done | bytes 98336 | tf_op jit(solution)/shard_map/ppermute | solution.py:58
  44.5 0.2 shard_map.187
  44.7 1.5 %collective-permute-start.11 = (bf16[64,768]{1,0:T(8,128)(2,1)S(1)}, bf16[64,768]{1,0:T(8,128)(2,1)S(1)}, u32[]{:S(2)}, u32[]{:S(2)}) collective-permute-start(bf16[64,768]{1,0:T(8,128)(2,1)S(1)} %get-tuple-element.41.own), channel_id=1, source_target_pairs={{0,96},{1,25},{2,98},{3,27},{4,100},{5,29},{6,102},{7,31},{8,104},... | collective-permute-start | bytes 294920 | tf_op jit(solution)/shard_map/ppermute | solution.py:58
  46.2 0.4 collective-permute-start.10
  46.6 0.5 collective-permute-start.9
  47.1 2.5 %collective-permute-done.11.r3 = bf16[64,768]{1,0:T(8,128)(2,1)S(1)} collective-permute-done((bf16[64,768]{1,0:T(8,128)(2,1)S(1)}, bf16[64,768]{1,0:T(8,128)(2,1)S(1)}, u32[]{:S(2)}, u32[]{:S(2)}) %collective-permute-start.11) | collective-permute-done | bytes 98336 | tf_op jit(solution)/shard_map/ppermute | solution.py:58
  49.6 2.5 %collective-permute-done.10.r2 = bf16[64,768]{1,0:T(8,128)(2,1)S(1)} collective-permute-done((bf16[64,768]{1,0:T(8,128)(2,1)S(1)}, bf16[64,768]{1,0:T(8,128)(2,1)S(1)}, u32[]{:S(2)}, u32[]{:S(2)}) %collective-permute-start.10) | collective-permute-done | bytes 98336 | tf_op jit(solution)/shard_map/ppermute | solution.py:58
  52.1 1.0 %collective-permute-done.9.r1 = bf16[64,768]{1,0:T(8,128)(2,1)S(1)} collective-permute-done((bf16[64,768]{1,0:T(8,128)(2,1)S(1)}, bf16[64,768]{1,0:T(8,128)(2,1)S(1)}, u32[]{:S(2)}, u32[]{:S(2)}) %collective-permute-start.9) | collective-permute-done | bytes 98336 | tf_op jit(solution)/shard_map/ppermute | solution.py:58
  53.3 2.5 %collective-permute-start.14 = (f32[8,128]{1,0:T(8,128)S(1)}, f32[8,128]{1,0:T(8,128)S(1)}, u32[]{:S(2)}, u32[]{:S(2)}) collective-permute-start(f32[8,128]{1,0:T(8,128)S(1)} %get-tuple-element.42), channel_id=1, source_target_pairs={{0,6},{1,7},{2,0},{3,1},{4,2},{5,3},{6,4},{7,5},{8,14},{9,15},{10,... | collective-permute-start | bytes 12296 | tf_op jit(solution)/shard_map/ppermute | solution.py:58
  55.8 1.7 %collective-permute-start.12 = (f32[8,128]{1,0:T(8,128)S(1)}, f32[8,128]{1,0:T(8,128)S(1)}, u32[]{:S(2)}, u32[]{:S(2)}) collective-permute-start(f32[8,128]{1,0:T(8,128)S(1)} %get-tuple-element.42), channel_id=1, source_target_pairs={{0,4},{1,5},{2,6},{3,7},{4,0},{5,1},{6,2},{7,3},{8,12},{9,13},{10,... | collective-permute-start | bytes 12296 | tf_op jit(solution)/shard_map/ppermute | solution.py:58
  57.5 2.2 %collective-permute-done.13 = f32[8,128]{1,0:T(8,128)S(1)} collective-permute-done((f32[8,128]{1,0:T(8,128)S(1)}, f32[8,128]{1,0:T(8,128)S(1)}, u32[]{:S(2)}, u32[]{:S(2)}) %collective-permute-start.13) | collective-permute-done | bytes 4128 | tf_op jit(solution)/shard_map/ppermute | solution.py:58
  59.8 9.0 %collective-permute-start.15 = (f32[8,128]{1,0:T(8,128)S(1)}, f32[8,128]{1,0:T(8,128)S(1)}, u32[]{:S(2)}, u32[]{:S(2)}) collective-permute-start(f32[8,128]{1,0:T(8,128)S(1)} %add_add_fusion.s_own), channel_id=1, source_target_pairs={{0,1},{1,0},{2,3},{3,2},{4,5},{5,4},{6,7},{7,6},{8,9},{9,8},{10,11... | collective-permute-start | bytes 12296 | tf_op jit(solution)/shard_map/ppermute | solution.py:58
  68.8 0.8 %collective-permute-done.15.s_other = f32[8,128]{1,0:T(8,128)S(1)} collective-permute-done((f32[8,128]{1,0:T(8,128)S(1)}, f32[8,128]{1,0:T(8,128)S(1)}, u32[]{:S(2)}, u32[]{:S(2)}) %collective-permute-start.15) | collective-permute-done | bytes 4128 | tf_op jit(solution)/shard_map/ppermute | solution.py:58
  69.6 2.9 %weights.1 = (f32[128,256]{1,0:T(8,128)}, f32[128,512]{1,0:T(8,128)}, f32[128,256]{1,0:T(8,128)}, f32[128,512]{1,0:T(8,128)}, bf16[2048,256]{1,0:T(8,128)(2,1)},...) custom-call(f32[8,128]{1,0:T(8,128)S(1)} %add_add_fusion.s_own, ...), custom_call_target="tpu_custom_call" | custom-call | flops 805306368 | bytes 12000000 | tf_op jit(solution)/shard_map/weights/pallas_call | solution.py:295
  (30 shorter events, 0.6 us)
Async XLA Ops:
  2.5 10.4 %collective-permute-start.8 = (bf16[160,768]{1,0:T(8,128)(2,1)S(1)}, bf16[160,768]{1,0:T(8,128)(2,1)S(1)}, u32[]{:S(2)}, u32[]{:S(2)}) collective-permute-start(bf16[160,768]{1,0:T(8,128)(2,1)S(1)} %get-tuple-element.40.k0.w0), channel_id=1, source_target_pairs={{0,24},{1,97},{2,26},{3,99},{4,28},{5,101},{6,30},{7,103},{8,0},{9... | collective-permute-start | bytes 737288 | tf_op jit(solution)/shard_map/ppermute | solution.py:58
  7.1 6.9 %collective-permute-start.7 = (bf16[160,768]{1,0:T(8,128)(2,1)S(1)}, bf16[160,768]{1,0:T(8,128)(2,1)S(1)}, u32[]{:S(2)}, u32[]{:S(2)}) collective-permute-start(bf16[160,768]{1,0:T(8,128)(2,1)S(1)} %get-tuple-element.40.k0.w0), channel_id=1, source_target_pairs={{0,16},{1,65},{2,18},{3,67},{4,20},{5,69},{6,22},{7,71},{8,24},{9,... | collective-permute-start | bytes 737288 | tf_op jit(solution)/shard_map/ppermute | solution.py:58
  7.1 9.2 %collective-permute-start.6 = (bf16[160,768]{1,0:T(8,128)(2,1)S(1)}, bf16[160,768]{1,0:T(8,128)(2,1)S(1)}, u32[]{:S(2)}, u32[]{:S(2)}) collective-permute-start(bf16[160,768]{1,0:T(8,128)(2,1)S(1)} %get-tuple-element.40.k0.w0), channel_id=1, source_target_pairs={{0,8},{1,33},{2,10},{3,35},{4,12},{5,37},{6,14},{7,39},{8,16},{9,4... | collective-permute-start | bytes 737288 | tf_op jit(solution)/shard_map/ppermute | solution.py:58
  16.4 22.9 %collective-permute-start.17 = (bf16[512,768]{1,0:T(8,128)(2,1)S(1)}, bf16[512,768]{1,0:T(8,128)(2,1)S(1)}, u32[]{:S(2)}, u32[]{:S(2)}) collective-permute-start(bf16[512,768]{1,0:T(8,128)(2,1)S(1)} %shard_map.189.g0), channel_id=1, source_target_pairs={{0,96},{1,25},{2,98},{3,27},{4,100},{5,29},{6,102},{7,31},{8,104},... | collective-permute-start | bytes 2359304 | tf_op jit(solution)/shard_map/ppermute | solution.py:58
  18.9 21.8 %collective-permute-start.16 = (bf16[512,768]{1,0:T(8,128)(2,1)S(1)}, bf16[512,768]{1,0:T(8,128)(2,1)S(1)}, u32[]{:S(2)}, u32[]{:S(2)}) collective-permute-start(bf16[512,768]{1,0:T(8,128)(2,1)S(1)} %shard_map.189.g0), channel_id=1, source_target_pairs={{0,32},{1,9},{2,34},{3,11},{4,36},{5,13},{6,38},{7,15},{8,40},{9,1... | collective-permute-start | bytes 2359304 | tf_op jit(solution)/shard_map/ppermute | solution.py:58
  18.9 25.6 %copy-start.2 = (f32[16,512]{1,0:T(8,128)S(1)}, f32[16,512]{1,0:T(8,128)}, u32[]{:S(2)}) copy-start(f32[16,512]{1,0:T(8,128)} %mv.3) | copy-start | bytes 98308
  18.9 25.6 %copy-start.3 = (f32[16,512]{1,0:T(8,128)S(1)}, f32[16,512]{1,0:T(8,128)}, u32[]{:S(2)}) copy-start(f32[16,512]{1,0:T(8,128)} %vv.3) | copy-start | bytes 98308
  18.9 25.6 %copy-start.4 = (f32[16,256]{1,0:T(8,128)S(1)}, f32[16,256]{1,0:T(8,128)}, u32[]{:S(2)}) copy-start(f32[16,256]{1,0:T(8,128)} %mq.3) | copy-start | bytes 49156
  18.9 25.6 %copy-start.5 = (f32[16,256]{1,0:T(8,128)S(1)}, f32[16,256]{1,0:T(8,128)}, u32[]{:S(2)}) copy-start(f32[16,256]{1,0:T(8,128)} %vq.3) | copy-start | bytes 49156
  30.0 39.6 %copy-start = (f32[128,512]{1,0:T(8,128)S(1)}, f32[128,512]{1,0:T(8,128)}, u32[]{:S(2)}) copy-start(f32[128,512]{1,0:T(8,128)} %wv.3) | copy-start | bytes 786436
  30.0 39.6 %copy-start.1 = (f32[128,256]{1,0:T(8,128)S(1)}, f32[128,256]{1,0:T(8,128)}, u32[]{:S(2)}) copy-start(f32[128,256]{1,0:T(8,128)} %wq.3) | copy-start | bytes 393220
  30.0 4.7 %collective-permute-start = (bf16[64,768]{1,0:T(8,128)(2,1)S(1)}, bf16[64,768]{1,0:T(8,128)(2,1)S(1)}, u32[]{:S(2)}, u32[]{:S(2)}) collective-permute-start(bf16[64,768]{1,0:T(8,128)(2,1)S(1)} %get-tuple-element.37), channel_id=1, source_target_pairs={{0,32},{1,9},{2,34},{3,11},{4,36},{5,13},{6,38},{7,15},{8,40},{9,1... | collective-permute-start | bytes 294920 | tf_op jit(solution)/shard_map/ppermute | solution.py:58
  30.1 6.9 %collective-permute-start.1 = (bf16[64,768]{1,0:T(8,128)(2,1)S(1)}, bf16[64,768]{1,0:T(8,128)(2,1)S(1)}, u32[]{:S(2)}, u32[]{:S(2)}) collective-permute-start(bf16[64,768]{1,0:T(8,128)(2,1)S(1)} %get-tuple-element.38), channel_id=1, source_target_pairs={{0,64},{1,17},{2,66},{3,19},{4,68},{5,21},{6,70},{7,23},{8,72},{9,... | collective-permute-start | bytes 294920 | tf_op jit(solution)/shard_map/ppermute | solution.py:58
  34.0 3.8 %collective-permute-start.2 = (bf16[64,768]{1,0:T(8,128)(2,1)S(1)}, bf16[64,768]{1,0:T(8,128)(2,1)S(1)}, u32[]{:S(2)}, u32[]{:S(2)}) collective-permute-start(bf16[64,768]{1,0:T(8,128)(2,1)S(1)} %get-tuple-element.39), channel_id=1, source_target_pairs={{0,96},{1,25},{2,98},{3,27},{4,100},{5,29},{6,102},{7,31},{8,104},... | collective-permute-start | bytes 294920 | tf_op jit(solution)/shard_map/ppermute | solution.py:58
  37.8 4.8 %collective-permute-start.5 = (bf16[64,768]{1,0:T(8,128)(2,1)S(1)}, bf16[64,768]{1,0:T(8,128)(2,1)S(1)}, u32[]{:S(2)}, u32[]{:S(2)}) collective-permute-start(bf16[64,768]{1,0:T(8,128)(2,1)S(1)} %shard_map.186.own), channel_id=1, source_target_pairs={{0,24},{1,97},{2,26},{3,99},{4,28},{5,101},{6,30},{7,103},{8,0},{9... | collective-permute-start | bytes 294920 | tf_op jit(solution)/shard_map/ppermute | solution.py:58
  38.5 5.1 %collective-permute-start.4 = (bf16[64,768]{1,0:T(8,128)(2,1)S(1)}, bf16[64,768]{1,0:T(8,128)(2,1)S(1)}, u32[]{:S(2)}, u32[]{:S(2)}) collective-permute-start(bf16[64,768]{1,0:T(8,128)(2,1)S(1)} %shard_map.186.own), channel_id=1, source_target_pairs={{0,16},{1,65},{2,18},{3,67},{4,20},{5,69},{6,22},{7,71},{8,24},{9,... | collective-permute-start | bytes 294920 | tf_op jit(solution)/shard_map/ppermute | solution.py:58
  38.6 5.9 %collective-permute-start.3 = (bf16[64,768]{1,0:T(8,128)(2,1)S(1)}, bf16[64,768]{1,0:T(8,128)(2,1)S(1)}, u32[]{:S(2)}, u32[]{:S(2)}) collective-permute-start(bf16[64,768]{1,0:T(8,128)(2,1)S(1)} %shard_map.186.own), channel_id=1, source_target_pairs={{0,8},{1,33},{2,10},{3,35},{4,12},{5,37},{6,14},{7,39},{8,16},{9,4... | collective-permute-start | bytes 294920 | tf_op jit(solution)/shard_map/ppermute | solution.py:58
  39.4 30.2 %collective-permute-start.19 = (bf16[256,768]{1,0:T(8,128)(2,1)S(1)}, bf16[256,768]{1,0:T(8,128)(2,1)S(1)}, u32[]{:S(2)}, u32[]{:S(2)}) collective-permute-start(bf16[256,768]{1,0:T(8,128)(2,1)S(1)} %slice.9), channel_id=1, source_target_pairs={{0,96},{1,25},{2,98},{3,27},{4,100},{5,29},{6,102},{7,31},{8,104},... | collective-permute-start | bytes 1179656 | tf_op jit(solution)/shard_map/ppermute | solution.py:58
  40.7 28.8 %collective-permute-start.18 = (bf16[256,768]{1,0:T(8,128)(2,1)S(1)}, bf16[256,768]{1,0:T(8,128)(2,1)S(1)}, u32[]{:S(2)}, u32[]{:S(2)}) collective-permute-start(bf16[256,768]{1,0:T(8,128)(2,1)S(1)} %slice.8), channel_id=1, source_target_pairs={{0,32},{1,9},{2,34},{3,11},{4,36},{5,13},{6,38},{7,15},{8,40},{9,1... | collective-permute-start | bytes 1179656 | tf_op jit(solution)/shard_map/ppermute | solution.py:58
  44.7 4.9 %collective-permute-start.11 = (bf16[64,768]{1,0:T(8,128)(2,1)S(1)}, bf16[64,768]{1,0:T(8,128)(2,1)S(1)}, u32[]{:S(2)}, u32[]{:S(2)}) collective-permute-start(bf16[64,768]{1,0:T(8,128)(2,1)S(1)} %get-tuple-element.41.own), channel_id=1, source_target_pairs={{0,96},{1,25},{2,98},{3,27},{4,100},{5,29},{6,102},{7,31},{8,104},... | collective-permute-start | bytes 294920 | tf_op jit(solution)/shard_map/ppermute | solution.py:58
  46.2 5.9 %collective-permute-start.10 = (bf16[64,768]{1,0:T(8,128)(2,1)S(1)}, bf16[64,768]{1,0:T(8,128)(2,1)S(1)}, u32[]{:S(2)}, u32[]{:S(2)}) collective-permute-start(bf16[64,768]{1,0:T(8,128)(2,1)S(1)} %get-tuple-element.41.own), channel_id=1, source_target_pairs={{0,64},{1,17},{2,66},{3,19},{4,68},{5,21},{6,70},{7,23},{8,72},{9,... | collective-permute-start | bytes 294920 | tf_op jit(solution)/shard_map/ppermute | solution.py:58
  46.6 6.6 %collective-permute-start.9 = (bf16[64,768]{1,0:T(8,128)(2,1)S(1)}, bf16[64,768]{1,0:T(8,128)(2,1)S(1)}, u32[]{:S(2)}, u32[]{:S(2)}) collective-permute-start(bf16[64,768]{1,0:T(8,128)(2,1)S(1)} %get-tuple-element.41.own), channel_id=1, source_target_pairs={{0,32},{1,9},{2,34},{3,11},{4,36},{5,13},{6,38},{7,15},{8,40},{9,1... | collective-permute-start | bytes 294920 | tf_op jit(solution)/shard_map/ppermute | solution.py:58
  53.3 4.3 %collective-permute-start.14 = (f32[8,128]{1,0:T(8,128)S(1)}, f32[8,128]{1,0:T(8,128)S(1)}, u32[]{:S(2)}, u32[]{:S(2)}) collective-permute-start(f32[8,128]{1,0:T(8,128)S(1)} %get-tuple-element.42), channel_id=1, source_target_pairs={{0,6},{1,7},{2,0},{3,1},{4,2},{5,3},{6,4},{7,5},{8,14},{9,15},{10,... | collective-permute-start | bytes 12296 | tf_op jit(solution)/shard_map/ppermute | solution.py:58
  55.8 4.0 %collective-permute-start.13 = (f32[8,128]{1,0:T(8,128)S(1)}, f32[8,128]{1,0:T(8,128)S(1)}, u32[]{:S(2)}, u32[]{:S(2)}) collective-permute-start(f32[8,128]{1,0:T(8,128)S(1)} %get-tuple-element.42), channel_id=1, source_target_pairs={{0,2},{1,3},{2,4},{3,5},{4,6},{5,7},{6,0},{7,1},{8,10},{9,11},{10,... | collective-permute-start | bytes 12296 | tf_op jit(solution)/shard_map/ppermute | solution.py:58
  55.8 4.0 %collective-permute-start.12 = (f32[8,128]{1,0:T(8,128)S(1)}, f32[8,128]{1,0:T(8,128)S(1)}, u32[]{:S(2)}, u32[]{:S(2)}) collective-permute-start(f32[8,128]{1,0:T(8,128)S(1)} %get-tuple-element.42), channel_id=1, source_target_pairs={{0,4},{1,5},{2,6},{3,7},{4,0},{5,1},{6,2},{7,3},{8,12},{9,13},{10,... | collective-permute-start | bytes 12296 | tf_op jit(solution)/shard_map/ppermute | solution.py:58
  59.8 9.8 %collective-permute-start.15 = (f32[8,128]{1,0:T(8,128)S(1)}, f32[8,128]{1,0:T(8,128)S(1)}, u32[]{:S(2)}, u32[]{:S(2)}) collective-permute-start(f32[8,128]{1,0:T(8,128)S(1)} %add_add_fusion.s_own), channel_id=1, source_target_pairs={{0,1},{1,0},{2,3},{3,2},{4,5},{5,4},{6,7},{7,6},{8,9},{9,8},{10,11... | collective-permute-start | bytes 12296 | tf_op jit(solution)/shard_map/ppermute | solution.py:58

commit v6 on v5

--- a/solution.py
+++ b/solution.py
@@ -26,7 +26,7 @@
 W = WQ + WV
 ROWS = 128
 MESSAGE = ROWS + 32
-TOKEN_BLOCK = 1024
+X_BLOCKS = 3
 
 F32 = jnp.float32
 BF16 = jnp.bfloat16
@@ -81,7 +81,24 @@
     return pltpu.with_memory_space_constraint(array, pltpu.HBM)
 
 
-def prepare_kernel(wq, wv, pq, pv, mq, mv, vq, vv, w16, pq_out, pv_out, wq_s, wv_s, m_s, v_s, sem):
+def mix_kernel(
+    x, cq, cv, pq, pv, wq, wv, mq, mv, vq, vv,
+    mixed, w16, pq_out, pv_out, cq_out, cv_out,
+    xs, wq_s, wv_s, m_s, v_s, sem, p_sem, x_sem, c_sem,
+):
+    half, block = mixed.shape[0], xs.shape[0] // X_BLOCKS
+    core = lax.axis_index("c")
+    mine = pl.multiple_of(core * half, half)
+    other = pl.multiple_of((1 - core) * half, half)
+    factors = [
+        pltpu.make_async_copy(a, b, p_sem.at[n]) for n, (a, b) in enumerate(((pq, pq_out), (pv, pv_out)))
+    ]
+    blocks = [
+        pltpu.make_async_copy(
+            x.at[pl.ds(mine + n * block, block), :], xs.at[pl.ds(n * block, block), :], x_sem.at[n]
+        )
+        for n in range(X_BLOCKS)
+    ]
     pairs = (
         (wq, wq_s),
         (wv, wv_s),
@@ -89,87 +106,90 @@
         (mv, m_s.at[:, pl.ds(WQ, WV)]),
         (vq, v_s.at[:, pl.ds(0, WQ)]),
         (vv, v_s.at[:, pl.ds(WQ, WV)]),
-        (pq, pq_out),
-        (pv, pv_out),
-    )
-    loads = [pltpu.make_async_copy(a, b, sem.at[n]) for n, (a, b) in enumerate(pairs)]
-    for copy in loads:
+    )
+    small = [pltpu.make_async_copy(a, b, sem.at[n]) for n, (a, b) in enumerate(pairs)]
+    cotangents = [
+        pltpu.make_async_copy(
+            a.at[pl.ds(start, half), :], b.at[pl.ds(at * half, half), :], c_sem.at[n, at]
+        )
+        for n, (a, b) in enumerate(((cq, cq_out), (cv, cv_out)))
+        for at, start in enumerate((mine, other))
+    ]
+    for copy in (*factors, *blocks, *small, *cotangents):
         copy.start()
-    for copy in loads[:6]:
+    for copy in factors:
+        copy.wait()
+    for n in range(X_BLOCKS):
+        blocks[n].wait()
+        at = slice(n * block, (n + 1) * block)
+        rows = xs[at, :]
+        mixed[at, :RANK] = jnp.dot(rows, pq_out[...], preferred_element_type=F32).astype(BF16)
+        mixed[at, RANK:] = jnp.dot(rows, pv_out[...], preferred_element_type=F32).astype(BF16)
+    for copy in small:
         copy.wait()
     w16[:ROWS, :WQ] = wq_s[...].astype(BF16)
     w16[:ROWS, WQ:] = wv_s[...].astype(BF16)
     w16[ROWS : ROWS + 16, :] = m_s[...].astype(BF16)
     w16[ROWS + 16 :, :] = v_s[...].astype(BF16)
-    for copy in loads[6:]:
+    for copy in cotangents:
         copy.wait()
 
 
-def prepare(wq, wv, pq, pv, mq, mv, vq, vv):
-    vmem = pl.BlockSpec(memory_space=pltpu.VMEM)
+def mix(inputs, cq, cv, pq, pv, *state):
+    vmem, hbm = pl.BlockSpec(memory_space=pltpu.VMEM), pl.BlockSpec(memory_space=pl.ANY)
+    tokens, width = inputs.shape
+    half = tokens // 2
+    operands = (inputs, cq, cv, pq, pv, *state)
     return pl.pallas_call(
-        prepare_kernel,
-        in_specs=[pl.BlockSpec(memory_space=pl.ANY)] * 8,
-        out_specs=[vmem] * 3,
+        mix_kernel,
+        in_specs=[hbm] * len(operands),
+        out_specs=[vmem] * 6,
         out_shape=[
+            pltpu.VMEM((half, 2 * RANK), BF16),
             pltpu.VMEM((MESSAGE, W), BF16),
             pltpu.VMEM(pq.shape, BF16),
             pltpu.VMEM(pv.shape, BF16),
+            pltpu.VMEM(cq.shape, BF16),
+            pltpu.VMEM(cv.shape, BF16),
         ],
         scratch_shapes=[
-            pltpu.VMEM(wq.shape, F32),
-            pltpu.VMEM(wv.shape, F32),
+            pltpu.VMEM((half, width), BF16),
+            pltpu.VMEM((ROWS, WQ), F32),
+            pltpu.VMEM((ROWS, WV), F32),
             pltpu.VMEM((16, W), F32),
             pltpu.VMEM((16, W), F32),
-            pltpu.SemaphoreType.DMA((8,)),
+            pltpu.SemaphoreType.DMA((6,)),
+            pltpu.SemaphoreType.DMA((2,)),
+            pltpu.SemaphoreType.DMA((X_BLOCKS,)),
+            pltpu.SemaphoreType.DMA((2, 2)),
         ],
-        cost_estimate=pl.CostEstimate(flops=1_000_000, bytes_accessed=3_000_000, transcendentals=0),
-        compiler_params=pltpu.CompilerParams(vmem_limit_bytes=8 * 2**20),
-        name="prepare",
-    )(*(in_hbm(a) for a in (wq, wv, pq, pv, mq, mv, vq, vv)))
-
-
-def gradient_kernel(x, cq, cv, pq, pv, own, to_1, to_2, to_3, total):
-    step = pl.program_id(0)
-
-    @pl.when(step == 0)
-    def _():
-        total[...] = jnp.zeros_like(total)
-
-    rows = x[...]
-    mixed_q = jnp.dot(rows, pq[...], preferred_element_type=F32).astype(BF16)
-    mixed_v = jnp.dot(rows, pv[...], preferred_element_type=F32).astype(BF16)
+        cost_estimate=pl.CostEstimate(
+            flops=4 * half * RANK * width, bytes_accessed=14_000_000, transcendentals=0
+        ),
+        compiler_params=pltpu.CompilerParams(vmem_limit_bytes=24 * 2**20),
+        name="mix",
+    )(*(in_hbm(a) for a in operands))
+
+
+def lead_kernel(mixed, swapped, cq, cv, own, to_1, to_2, to_3, total):
     lead = (((0,), (0,)), ((), ()))
-    total[:, :WQ] += lax.dot_general(mixed_q, cq[...], lead, preferred_element_type=F32)
-    total[:, WQ:] += lax.dot_general(mixed_v, cv[...], lead, preferred_element_type=F32)
-
-    @pl.when(step == pl.num_programs(0) - 1)
-    def _():
-        major, _, per_major, per_minor = own_place()
-        for offset, out in enumerate((own, to_1, to_2, to_3)):
-            there = lax.rem(major + offset, 4)
-            for minor in range(4):
-                start = pl.multiple_of((there * per_major + minor * per_minor) * 16, 16)
-                out[minor * 16 : (minor + 1) * 16, :] = total[pl.ds(start, 16), :].astype(out.dtype)
-
-
-def projected_gradient(inputs, cq, cv, pq, pv):
-    tokens, width = inputs.shape
-    vmem = pl.BlockSpec(memory_space=pltpu.VMEM)
-    by_tokens = lambda a: pl.BlockSpec((TOKEN_BLOCK, a.shape[1]), lambda i: (i, 0))
-    return pl.pallas_call(
-        gradient_kernel,
-        grid=(tokens // TOKEN_BLOCK,),
-        in_specs=[by_tokens(inputs), by_tokens(cq), by_tokens(cv), vmem, vmem],
-        out_specs=[vmem] * 4,
-        out_shape=[pltpu.VMEM((64, W), F32)] + [pltpu.VMEM((64, W), BF16)] * 3,
-        scratch_shapes=[pltpu.VMEM((RANK, W), F32)],
-        cost_estimate=pl.CostEstimate(
-            flops=2 * tokens * RANK * (2 * width + W), bytes_accessed=18_000_000, transcendentals=0
-        ),
-        compiler_params=pltpu.CompilerParams(vmem_limit_bytes=32 * 2**20),
-        name="gradient",
-    )(in_hbm(inputs), in_hbm(cq), in_hbm(cv), in_vmem(pq), in_vmem(pv))
+    half = mixed.shape[0]
+    for n, held in enumerate((mixed, swapped)):
+        at = slice(n * half, (n + 1) * half)
+        part_q = lax.dot_general(held[:, :RANK], cq[at, :], lead, preferred_element_type=F32)
+        part_v = lax.dot_general(held[:, RANK:], cv[at, :], lead, preferred_element_type=F32)
+        if n == 0:
+            total[:, :WQ] = part_q
+            total[:, WQ:] = part_v
+        else:
+            total[:, :WQ] += part_q
+            total[:, WQ:] += part_v
+    major, _, per_major, per_minor = own_place()
+    for offset, out in enumerate((own, to_1, to_2, to_3)):
+        there = lax.rem(major + offset, 4)
+        for minor in range(4):
+            start = pl.multiple_of((there * per_major + minor * per_minor) * 16, 16)
+            out[minor * 16 : (minor + 1) * 16, :] = total[pl.ds(start, 16), :].astype(out.dtype)
 
 
 def whole_call(body, out, operands, scratch=(), flops=1_000_000):
@@ -181,11 +201,11 @@
         out_shape=[pltpu.VMEM(o.shape, o.dtype) for o in out],
         scratch_shapes=list(scratch),
         cost_estimate=pl.CostEstimate(flops=flops, bytes_accessed=1_000_000, transcendentals=0),
-        compiler_params=pltpu.CompilerParams(vmem_limit_bytes=8 * 2**20),
+        compiler_params=pltpu.CompilerParams(vmem_limit_bytes=12 * 2**20),
     )(*(in_vmem(a) for a in operands))
 
 
-def group_kernel(w0, w1, w2, w3, out):
+def group_kernel(w0, w1, w2, w3, after, out):
     for n, held in enumerate((w0, w1, w2, w3)):
         out[n * ROWS : (n + 1) * ROWS, :] = held[:ROWS, :]
 
@@ -316,12 +336,20 @@
 
 
 def on_device(inputs, cq, cv, pq, pv, wq, wv, mq, mv, vq, vv):
-    w16, pq, pv = prepare(wq, wv, pq, pv, mq, mv, vq, vv)
+    mixed, w16, pq, pv, cq, cv = mix(inputs, cq, cv, pq, pv, wq, wv, mq, mv, vq, vv)
+    swapped = shifted(mixed, "core", 1)
     w_1, w_2, w_3 = to_all("minor", (w16,) * 3)
-    own, *parts = projected_gradient(inputs, cq, cv, pq, pv)
+    chunk = lambda t: jax.ShapeDtypeStruct((64, W), t)
+    own, *parts = whole_call(
+        lead_kernel,
+        [chunk(F32), chunk(BF16), chunk(BF16), chunk(BF16)],
+        (mixed, swapped, cq, cv),
+        [pltpu.VMEM((RANK, W), F32)],
+        flops=2 * inputs.shape[0] * RANK * W,
+    )
     r_1, r_2, r_3 = to_all("major", parts)
     group, = whole_call(
-        group_kernel, [jax.ShapeDtypeStruct((4 * ROWS, W), BF16)], (w16, w_1, w_2, w_3)
+        group_kernel, [jax.ShapeDtypeStruct((4 * ROWS, W), BF16)], (w16, w_1, w_2, w_3, own)
     )
     g_1, g_3 = shifted(group, "major", 1), shifted(group, "major", 3)
     message, = whole_call(

time: 72.6 us -> 70 us (0.964)
  starting transfers between devices: 30.6 us -> 36 us
  waiting for transfers between devices: 24.8 us -> 19.7 us
  Pallas kernels: 16.2 us -> 13.2 us
    ppermute x20 -> x21, starting transfers between devices: 30.6 us -> 36 us  [shifted(): return lax.ppermute(array, AXES, shift_pairs(kind, offset))]
    ppermute x20 -> x21, waiting for transfers between devices: 24.8 us -> 19.7 us  [shifted(): return lax.ppermute(array, AXES, shift_pairs(kind, offset))]
    pallas_call x2 -> x1, Pallas kernels: 12.9 us -> 8.41 us  [mix(): pl.pallas_call(mix_kernel, in_specs=[hbm] * len(operands), out_specs=[vme...]
    pallas_call x4 -> x5, Pallas kernels: 0.39 us -> 1.87 us  [whole_call(): pl.pallas_call(body, in_specs=[vmem] * len(operands), out_specs=[vmem] *...]
  transfers between devices with their start and end apart: 20 -> 21, of which waited for: 14 -> 9; matrix products, arithmetic and copies ran while one was open for 0% -> 0% of each run, Pallas kernels for 16% -> 3%
where the time goes in v6:
time: 70 us; the launch traced here: 69.8 us
  starting transfers between devices  36 us (51%)
  waiting for transfers between devices  19.7 us (28%)
  Pallas kernels  13.2 us (19%)
  between operations  0.81 us (1%)
    ppermute x21, starting transfers between devices, shifted(): return lax.ppermute(array, AXES, shift_pairs(kind, offset))  36 us
    ppermute x21, waiting for transfers between devices, shifted(): return lax.ppermute(array, AXES, shift_pairs(kind, offset))  19.7 us
    pallas_call x1, Pallas kernels, mix(): pl.pallas_call(mix_kernel, in_specs=[hbm] * len(operands), out_specs=[vme...  8.41 us
    pallas_call x1, Pallas kernels, new_weights(): pl.pallas_call(weight_kernel, in_specs=[vmem] * len(operands), out_specs=...  2.96 us
    pallas_call x5, Pallas kernels, whole_call(): pl.pallas_call(body, in_specs=[vmem] * len(operands), out_specs=[vmem] *...  1.87 us
  transfers between devices with their start and end apart: 21, of which 9 were waited for; matrix products, arithmetic and copies ran while one was open for 0% of the time, Pallas kernels for 3%

profile of v6, /device:TPU:1, one launch (start us, length us, event | category | flops | bytes accessed | tf_op | source)
XLA Modules:
  0.0 69.8 jit_solution(12762350961526650798)
XLA Ops:
  0.6 8.4 %mix.1 = (bf16[1536,512]{1,0:T(8,128)(2,1)S(1)}, bf16[160,768]{1,0:T(8,128)(2,1)S(1)}, bf16[2048,256]{1,0:T(8,128)(2,1)S(1)}, bf16[2048,256]{1,0:T(8,128)(2,1)S(...) custom-call(bf16[3072,2048]{1,0:T(8,128)(2,1)} %x.1, bf16[3072,256]{1,0:T(8,128)(2,1)} %cq.1, ...), custom_call_target="tpu_custom_call" | custom-call | flops 3221225472 | bytes 14000000 | tf_op jit(solution)/shard_map/mix/pallas_call | solution.py:143
  9.1 1.5 %collective-permute-start = (bf16[1536,512]{1,0:T(8,128)(2,1)S(1)}, bf16[1536,512]{1,0:T(8,128)(2,1)S(1)}, u32[]{:S(2)}, u32[]{:S(2)}) collective-permute-start(bf16[1536,512]{1,0:T(8,128)(2,1)S(1)} %get-tuple-element.37.mixed), channel_id=1, source_target_pairs={{0,1},{1,0},{2,3},{3,2},{4,5},{5,4},{6,7},{7,6},{8,9},{9,8},{10,11... | collective-permute-start | bytes 4718600 | tf_op jit(solution)/shard_map/ppermute | solution.py:58
  10.5 1.8 %collective-permute-start.7 = (bf16[160,768]{1,0:T(8,128)(2,1)S(1)}, bf16[160,768]{1,0:T(8,128)(2,1)S(1)}, u32[]{:S(2)}, u32[]{:S(2)}) collective-permute-start(bf16[160,768]{1,0:T(8,128)(2,1)S(1)} %get-tuple-element.44.k0.w0), channel_id=1, source_target_pairs={{0,8},{1,33},{2,10},{3,35},{4,12},{5,37},{6,14},{7,39},{8,16},{9,4... | collective-permute-start | bytes 737288 | tf_op jit(solution)/shard_map/ppermute | solution.py:58
  12.3 3.3 %collective-permute-start.8 = (bf16[160,768]{1,0:T(8,128)(2,1)S(1)}, bf16[160,768]{1,0:T(8,128)(2,1)S(1)}, u32[]{:S(2)}, u32[]{:S(2)}) collective-permute-start(bf16[160,768]{1,0:T(8,128)(2,1)S(1)} %get-tuple-element.44.k0.w0), channel_id=1, source_target_pairs={{0,16},{1,65},{2,18},{3,67},{4,20},{5,69},{6,22},{7,71},{8,24},{9,... | collective-permute-start | bytes 737288 | tf_op jit(solution)/shard_map/ppermute | solution.py:58
  15.6 0.7 %collective-permute-start.9 = (bf16[160,768]{1,0:T(8,128)(2,1)S(1)}, bf16[160,768]{1,0:T(8,128)(2,1)S(1)}, u32[]{:S(2)}, u32[]{:S(2)}) collective-permute-start(bf16[160,768]{1,0:T(8,128)(2,1)S(1)} %get-tuple-element.44.k0.w0), channel_id=1, source_target_pairs={{0,24},{1,97},{2,26},{3,99},{4,28},{5,101},{6,30},{7,103},{8,0},{9... | collective-permute-start | bytes 737288 | tf_op jit(solution)/shard_map/ppermute | solution.py:58
  16.3 1.5 %shard_map.186 = (f32[64,768]{1,0:T(8,128)S(1)}, bf16[64,768]{1,0:T(8,128)(2,1)S(1)}, bf16[64,768]{1,0:T(8,128)(2,1)S(1)}, bf16[64,768]{1,0:T(8,128)(2,1)S(1)}) custom-call(bf16[1536,512]{1,0:T(8,128)(2,1)S(1)} %get-tuple-element.37.mixed, bf16[1536,512]{1,0:T(8,128)(2,1)S(1)} %collective-permute-done.swapped, bf16[3072,256]{1,0:T(8,128)(2,1)S(1)} %get-tuple-element.38.cq, ...), custom_call_target="tpu_custom_call" | custom-call | flops 1207959552 | bytes 1000000 | tf_op jit(solution)/shard_map/pallas_call | solution.py:197
  17.8 0.1 collective-permute-done.7.k1.w1
  18.0 3.8 %collective-permute-done.8.k2.w2 = bf16[160,768]{1,0:T(8,128)(2,1)S(1)} collective-permute-done((bf16[160,768]{1,0:T(8,128)(2,1)S(1)}, bf16[160,768]{1,0:T(8,128)(2,1)S(1)}, u32[]{:S(2)}, u32[]{:S(2)}) %collective-permute-start.8) | collective-permute-done | bytes 245792 | tf_op jit(solution)/shard_map/ppermute | solution.py:58
  21.9 1.4 %collective-permute-start.17 = (bf16[512,768]{1,0:T(8,128)(2,1)S(1)}, bf16[512,768]{1,0:T(8,128)(2,1)S(1)}, u32[]{:S(2)}, u32[]{:S(2)}) collective-permute-start(bf16[512,768]{1,0:T(8,128)(2,1)S(1)} %shard_map.190.g0), channel_id=1, source_target_pairs={{0,32},{1,9},{2,34},{3,11},{4,36},{5,13},{6,38},{7,15},{8,40},{9,1... | collective-permute-start | bytes 2359304 | tf_op jit(solution)/shard_map/ppermute | solution.py:58
  23.2 1.5 %collective-permute-start.18 = (bf16[512,768]{1,0:T(8,128)(2,1)S(1)}, bf16[512,768]{1,0:T(8,128)(2,1)S(1)}, u32[]{:S(2)}, u32[]{:S(2)}) collective-permute-start(bf16[512,768]{1,0:T(8,128)(2,1)S(1)} %shard_map.190.g0), channel_id=1, source_target_pairs={{0,96},{1,25},{2,98},{3,27},{4,100},{5,29},{6,102},{7,31},{8,104},... | collective-permute-start | bytes 2359304 | tf_op jit(solution)/shard_map/ppermute | solution.py:58
  24.8 2.6 %collective-permute-start.2 = (bf16[64,768]{1,0:T(8,128)(2,1)S(1)}, bf16[64,768]{1,0:T(8,128)(2,1)S(1)}, u32[]{:S(2)}, u32[]{:S(2)}) collective-permute-start(bf16[64,768]{1,0:T(8,128)(2,1)S(1)} %get-tuple-element.42), channel_id=1, source_target_pairs={{0,64},{1,17},{2,66},{3,19},{4,68},{5,21},{6,70},{7,23},{8,72},{9,... | collective-permute-start | bytes 294920 | tf_op jit(solution)/shard_map/ppermute | solution.py:58
  27.3 1.1 %collective-permute-start.3 = (bf16[64,768]{1,0:T(8,128)(2,1)S(1)}, bf16[64,768]{1,0:T(8,128)(2,1)S(1)}, u32[]{:S(2)}, u32[]{:S(2)}) collective-permute-start(bf16[64,768]{1,0:T(8,128)(2,1)S(1)} %get-tuple-element.43), channel_id=1, source_target_pairs={{0,96},{1,25},{2,98},{3,27},{4,100},{5,29},{6,102},{7,31},{8,104},... | collective-permute-start | bytes 294920 | tf_op jit(solution)/shard_map/ppermute | solution.py:58
  28.4 7.0 %collective-permute-done.1.r1 = bf16[64,768]{1,0:T(8,128)(2,1)S(1)} collective-permute-done((bf16[64,768]{1,0:T(8,128)(2,1)S(1)}, bf16[64,768]{1,0:T(8,128)(2,1)S(1)}, u32[]{:S(2)}, u32[]{:S(2)}) %collective-permute-start.1) | collective-permute-done | bytes 98336 | tf_op jit(solution)/shard_map/ppermute | solution.py:58
  35.4 1.9 %collective-permute-done.2.r2 = bf16[64,768]{1,0:T(8,128)(2,1)S(1)} collective-permute-done((bf16[64,768]{1,0:T(8,128)(2,1)S(1)}, bf16[64,768]{1,0:T(8,128)(2,1)S(1)}, u32[]{:S(2)}, u32[]{:S(2)}) %collective-permute-start.2) | collective-permute-done | bytes 98336 | tf_op jit(solution)/shard_map/ppermute | solution.py:58
  37.4 0.9 %collective-permute-start.4 = (bf16[64,768]{1,0:T(8,128)(2,1)S(1)}, bf16[64,768]{1,0:T(8,128)(2,1)S(1)}, u32[]{:S(2)}, u32[]{:S(2)}) collective-permute-start(bf16[64,768]{1,0:T(8,128)(2,1)S(1)} %shard_map.187.own), channel_id=1, source_target_pairs={{0,8},{1,33},{2,10},{3,35},{4,12},{5,37},{6,14},{7,39},{8,16},{9,4... | collective-permute-start | bytes 294920 | tf_op jit(solution)/shard_map/ppermute | solution.py:58
  38.3 2.4 %collective-permute-start.5 = (bf16[64,768]{1,0:T(8,128)(2,1)S(1)}, bf16[64,768]{1,0:T(8,128)(2,1)S(1)}, u32[]{:S(2)}, u32[]{:S(2)}) collective-permute-start(bf16[64,768]{1,0:T(8,128)(2,1)S(1)} %shard_map.187.own), channel_id=1, source_target_pairs={{0,16},{1,65},{2,18},{3,67},{4,20},{5,69},{6,22},{7,71},{8,24},{9,... | collective-permute-start | bytes 294920 | tf_op jit(solution)/shard_map/ppermute | solution.py:58
  40.7 1.1 %collective-permute-start.6 = (bf16[64,768]{1,0:T(8,128)(2,1)S(1)}, bf16[64,768]{1,0:T(8,128)(2,1)S(1)}, u32[]{:S(2)}, u32[]{:S(2)}) collective-permute-start(bf16[64,768]{1,0:T(8,128)(2,1)S(1)} %shard_map.187.own), channel_id=1, source_target_pairs={{0,24},{1,97},{2,26},{3,99},{4,28},{5,101},{6,30},{7,103},{8,0},{9... | collective-permute-start | bytes 294920 | tf_op jit(solution)/shard_map/ppermute | solution.py:58
  41.8 0.5 collective-permute-start.19
  42.4 2.3 %collective-permute-start.20 = (bf16[256,768]{1,0:T(8,128)(2,1)S(1)}, bf16[256,768]{1,0:T(8,128)(2,1)S(1)}, u32[]{:S(2)}, u32[]{:S(2)}) collective-permute-start(bf16[256,768]{1,0:T(8,128)(2,1)S(1)} %slice.9), channel_id=1, source_target_pairs={{0,96},{1,25},{2,98},{3,27},{4,100},{5,29},{6,102},{7,31},{8,104},... | collective-permute-start | bytes 1179656 | tf_op jit(solution)/shard_map/ppermute | solution.py:58
  44.7 0.2 shard_map.188
  45.0 2.5 %collective-permute-start.11 = (bf16[64,768]{1,0:T(8,128)(2,1)S(1)}, bf16[64,768]{1,0:T(8,128)(2,1)S(1)}, u32[]{:S(2)}, u32[]{:S(2)}) collective-permute-start(bf16[64,768]{1,0:T(8,128)(2,1)S(1)} %get-tuple-element.45.own), channel_id=1, source_target_pairs={{0,64},{1,17},{2,66},{3,19},{4,68},{5,21},{6,70},{7,23},{8,72},{9,... | collective-permute-start | bytes 294920 | tf_op jit(solution)/shard_map/ppermute | solution.py:58
  47.6 1.1 %collective-permute-start.12 = (bf16[64,768]{1,0:T(8,128)(2,1)S(1)}, bf16[64,768]{1,0:T(8,128)(2,1)S(1)}, u32[]{:S(2)}, u32[]{:S(2)}) collective-permute-start(bf16[64,768]{1,0:T(8,128)(2,1)S(1)} %get-tuple-element.45.own), channel_id=1, source_target_pairs={{0,96},{1,25},{2,98},{3,27},{4,100},{5,29},{6,102},{7,31},{8,104},... | collective-permute-start | bytes 294920 | tf_op jit(solution)/shard_map/ppermute | solution.py:58
  48.6 3.5 %collective-permute-done.10.r1 = bf16[64,768]{1,0:T(8,128)(2,1)S(1)} collective-permute-done((bf16[64,768]{1,0:T(8,128)(2,1)S(1)}, bf16[64,768]{1,0:T(8,128)(2,1)S(1)}, u32[]{:S(2)}, u32[]{:S(2)}) %collective-permute-start.10) | collective-permute-done | bytes 98336 | tf_op jit(solution)/shard_map/ppermute | solution.py:58
  52.1 0.8 %collective-permute-done.11.r2 = bf16[64,768]{1,0:T(8,128)(2,1)S(1)} collective-permute-done((bf16[64,768]{1,0:T(8,128)(2,1)S(1)}, bf16[64,768]{1,0:T(8,128)(2,1)S(1)}, u32[]{:S(2)}, u32[]{:S(2)}) %collective-permute-start.11) | collective-permute-done | bytes 98336 | tf_op jit(solution)/shard_map/ppermute | solution.py:58
  53.0 0.6 collective-permute-done.12.r3
  53.7 2.8 %collective-permute-start.13 = (f32[8,128]{1,0:T(8,128)S(1)}, f32[8,128]{1,0:T(8,128)S(1)}, u32[]{:S(2)}, u32[]{:S(2)}) collective-permute-start(f32[8,128]{1,0:T(8,128)S(1)} %get-tuple-element.46), channel_id=1, source_target_pairs={{0,4},{1,5},{2,6},{3,7},{4,0},{5,1},{6,2},{7,3},{8,12},{9,13},{10,... | collective-permute-start | bytes 12296 | tf_op jit(solution)/shard_map/ppermute | solution.py:58
  56.5 0.3 collective-permute-start.14
  56.8 2.4 %collective-permute-start.15 = (f32[8,128]{1,0:T(8,128)S(1)}, f32[8,128]{1,0:T(8,128)S(1)}, u32[]{:S(2)}, u32[]{:S(2)}) collective-permute-start(f32[8,128]{1,0:T(8,128)S(1)} %get-tuple-element.46), channel_id=1, source_target_pairs={{0,6},{1,7},{2,0},{3,1},{4,2},{5,3},{6,4},{7,5},{8,14},{9,15},{10,... | collective-permute-start | bytes 12296 | tf_op jit(solution)/shard_map/ppermute | solution.py:58
  59.2 1.0 %collective-permute-done.14 = f32[8,128]{1,0:T(8,128)S(1)} collective-permute-done((f32[8,128]{1,0:T(8,128)S(1)}, f32[8,128]{1,0:T(8,128)S(1)}, u32[]{:S(2)}, u32[]{:S(2)}) %collective-permute-start.14) | collective-permute-done | bytes 4128 | tf_op jit(solution)/shard_map/ppermute | solution.py:58
  60.2 5.9 %collective-permute-start.16 = (f32[8,128]{1,0:T(8,128)S(1)}, f32[8,128]{1,0:T(8,128)S(1)}, u32[]{:S(2)}, u32[]{:S(2)}) collective-permute-start(f32[8,128]{1,0:T(8,128)S(1)} %add_add_fusion.s_own), channel_id=1, source_target_pairs={{0,1},{1,0},{2,3},{3,2},{4,5},{5,4},{6,7},{7,6},{8,9},{9,8},{10,11... | collective-permute-start | bytes 12296 | tf_op jit(solution)/shard_map/ppermute | solution.py:58
  66.0 0.8 %collective-permute-done.16.s_other = f32[8,128]{1,0:T(8,128)S(1)} collective-permute-done((f32[8,128]{1,0:T(8,128)S(1)}, f32[8,128]{1,0:T(8,128)S(1)}, u32[]{:S(2)}, u32[]{:S(2)}) %collective-permute-start.16) | collective-permute-done | bytes 4128 | tf_op jit(solution)/shard_map/ppermute | solution.py:58
  66.9 3.0 %weights.1 = (f32[128,256]{1,0:T(8,128)}, f32[128,512]{1,0:T(8,128)}, f32[128,256]{1,0:T(8,128)}, f32[128,512]{1,0:T(8,128)}, bf16[2048,256]{1,0:T(8,128)(2,1)},...) custom-call(f32[8,128]{1,0:T(8,128)S(1)} %add_add_fusion.s_own, ...), custom_call_target="tpu_custom_call" | custom-call | flops 805306368 | bytes 12000000 | tf_op jit(solution)/shard_map/weights/pallas_call | solution.py:315
  (32 shorter events, 0.4 us)
Async XLA Ops:
  9.1 7.2 %collective-permute-start = (bf16[1536,512]{1,0:T(8,128)(2,1)S(1)}, bf16[1536,512]{1,0:T(8,128)(2,1)S(1)}, u32[]{:S(2)}, u32[]{:S(2)}) collective-permute-start(bf16[1536,512]{1,0:T(8,128)(2,1)S(1)} %get-tuple-element.37.mixed), channel_id=1, source_target_pairs={{0,1},{1,0},{2,3},{3,2},{4,5},{5,4},{6,7},{7,6},{8,9},{9,8},{10,11... | collective-permute-start | bytes 4718600 | tf_op jit(solution)/shard_map/ppermute | solution.py:58
  10.5 7.5 %collective-permute-start.7 = (bf16[160,768]{1,0:T(8,128)(2,1)S(1)}, bf16[160,768]{1,0:T(8,128)(2,1)S(1)}, u32[]{:S(2)}, u32[]{:S(2)}) collective-permute-start(bf16[160,768]{1,0:T(8,128)(2,1)S(1)} %get-tuple-element.44.k0.w0), channel_id=1, source_target_pairs={{0,8},{1,33},{2,10},{3,35},{4,12},{5,37},{6,14},{7,39},{8,16},{9,4... | collective-permute-start | bytes 737288 | tf_op jit(solution)/shard_map/ppermute | solution.py:58
  12.3 9.5 %collective-permute-start.8 = (bf16[160,768]{1,0:T(8,128)(2,1)S(1)}, bf16[160,768]{1,0:T(8,128)(2,1)S(1)}, u32[]{:S(2)}, u32[]{:S(2)}) collective-permute-start(bf16[160,768]{1,0:T(8,128)(2,1)S(1)} %get-tuple-element.44.k0.w0), channel_id=1, source_target_pairs={{0,16},{1,65},{2,18},{3,67},{4,20},{5,69},{6,22},{7,71},{8,24},{9,... | collective-permute-start | bytes 737288 | tf_op jit(solution)/shard_map/ppermute | solution.py:58
  15.6 6.2 %collective-permute-start.9 = (bf16[160,768]{1,0:T(8,128)(2,1)S(1)}, bf16[160,768]{1,0:T(8,128)(2,1)S(1)}, u32[]{:S(2)}, u32[]{:S(2)}) collective-permute-start(bf16[160,768]{1,0:T(8,128)(2,1)S(1)} %get-tuple-element.44.k0.w0), channel_id=1, source_target_pairs={{0,24},{1,97},{2,26},{3,99},{4,28},{5,101},{6,30},{7,103},{8,0},{9... | collective-permute-start | bytes 737288 | tf_op jit(solution)/shard_map/ppermute | solution.py:58
  17.8 26.9 %copy-start.2 = (f32[16,512]{1,0:T(8,128)S(1)}, f32[16,512]{1,0:T(8,128)}, u32[]{:S(2)}) copy-start(f32[16,512]{1,0:T(8,128)} %mv.3) | copy-start | bytes 98308
  17.8 26.9 %copy-start.3 = (f32[16,512]{1,0:T(8,128)S(1)}, f32[16,512]{1,0:T(8,128)}, u32[]{:S(2)}) copy-start(f32[16,512]{1,0:T(8,128)} %vv.3) | copy-start | bytes 98308
  17.8 26.9 %copy-start.4 = (f32[16,256]{1,0:T(8,128)S(1)}, f32[16,256]{1,0:T(8,128)}, u32[]{:S(2)}) copy-start(f32[16,256]{1,0:T(8,128)} %mq.3) | copy-start | bytes 49156
  17.8 26.9 %copy-start.5 = (f32[16,256]{1,0:T(8,128)S(1)}, f32[16,256]{1,0:T(8,128)}, u32[]{:S(2)}) copy-start(f32[16,256]{1,0:T(8,128)} %vq.3) | copy-start | bytes 49156
  21.9 45.0 %copy-start = (f32[128,512]{1,0:T(8,128)S(1)}, f32[128,512]{1,0:T(8,128)}, u32[]{:S(2)}) copy-start(f32[128,512]{1,0:T(8,128)} %wv.3) | copy-start | bytes 786436
  21.9 45.0 %copy-start.1 = (f32[128,256]{1,0:T(8,128)S(1)}, f32[128,256]{1,0:T(8,128)}, u32[]{:S(2)}) copy-start(f32[128,256]{1,0:T(8,128)} %wq.3) | copy-start | bytes 393220
  21.9 19.9 %collective-permute-start.17 = (bf16[512,768]{1,0:T(8,128)(2,1)S(1)}, bf16[512,768]{1,0:T(8,128)(2,1)S(1)}, u32[]{:S(2)}, u32[]{:S(2)}) collective-permute-start(bf16[512,768]{1,0:T(8,128)(2,1)S(1)} %shard_map.190.g0), channel_id=1, source_target_pairs={{0,32},{1,9},{2,34},{3,11},{4,36},{5,13},{6,38},{7,15},{8,40},{9,1... | collective-permute-start | bytes 2359304 | tf_op jit(solution)/shard_map/ppermute | solution.py:58
  23.2 19.1 %collective-permute-start.18 = (bf16[512,768]{1,0:T(8,128)(2,1)S(1)}, bf16[512,768]{1,0:T(8,128)(2,1)S(1)}, u32[]{:S(2)}, u32[]{:S(2)}) collective-permute-start(bf16[512,768]{1,0:T(8,128)(2,1)S(1)} %shard_map.190.g0), channel_id=1, source_target_pairs={{0,96},{1,25},{2,98},{3,27},{4,100},{5,29},{6,102},{7,31},{8,104},... | collective-permute-start | bytes 2359304 | tf_op jit(solution)/shard_map/ppermute | solution.py:58
  24.8 10.6 %collective-permute-start.1 = (bf16[64,768]{1,0:T(8,128)(2,1)S(1)}, bf16[64,768]{1,0:T(8,128)(2,1)S(1)}, u32[]{:S(2)}, u32[]{:S(2)}) collective-permute-start(bf16[64,768]{1,0:T(8,128)(2,1)S(1)} %get-tuple-element.41), channel_id=1, source_target_pairs={{0,32},{1,9},{2,34},{3,11},{4,36},{5,13},{6,38},{7,15},{8,40},{9,1... | collective-permute-start | bytes 294920 | tf_op jit(solution)/shard_map/ppermute | solution.py:58
  24.8 12.6 %collective-permute-start.2 = (bf16[64,768]{1,0:T(8,128)(2,1)S(1)}, bf16[64,768]{1,0:T(8,128)(2,1)S(1)}, u32[]{:S(2)}, u32[]{:S(2)}) collective-permute-start(bf16[64,768]{1,0:T(8,128)(2,1)S(1)} %get-tuple-element.42), channel_id=1, source_target_pairs={{0,64},{1,17},{2,66},{3,19},{4,68},{5,21},{6,70},{7,23},{8,72},{9,... | collective-permute-start | bytes 294920 | tf_op jit(solution)/shard_map/ppermute | solution.py:58
  27.3 10.0 %collective-permute-start.3 = (bf16[64,768]{1,0:T(8,128)(2,1)S(1)}, bf16[64,768]{1,0:T(8,128)(2,1)S(1)}, u32[]{:S(2)}, u32[]{:S(2)}) collective-permute-start(bf16[64,768]{1,0:T(8,128)(2,1)S(1)} %get-tuple-element.43), channel_id=1, source_target_pairs={{0,96},{1,25},{2,98},{3,27},{4,100},{5,29},{6,102},{7,31},{8,104},... | collective-permute-start | bytes 294920 | tf_op jit(solution)/shard_map/ppermute | solution.py:58
  37.4 7.3 %collective-permute-start.4 = (bf16[64,768]{1,0:T(8,128)(2,1)S(1)}, bf16[64,768]{1,0:T(8,128)(2,1)S(1)}, u32[]{:S(2)}, u32[]{:S(2)}) collective-permute-start(bf16[64,768]{1,0:T(8,128)(2,1)S(1)} %shard_map.187.own), channel_id=1, source_target_pairs={{0,8},{1,33},{2,10},{3,35},{4,12},{5,37},{6,14},{7,39},{8,16},{9,4... | collective-permute-start | bytes 294920 | tf_op jit(solution)/shard_map/ppermute | solution.py:58
  38.3 6.3 %collective-permute-start.5 = (bf16[64,768]{1,0:T(8,128)(2,1)S(1)}, bf16[64,768]{1,0:T(8,128)(2,1)S(1)}, u32[]{:S(2)}, u32[]{:S(2)}) collective-permute-start(bf16[64,768]{1,0:T(8,128)(2,1)S(1)} %shard_map.187.own), channel_id=1, source_target_pairs={{0,16},{1,65},{2,18},{3,67},{4,20},{5,69},{6,22},{7,71},{8,24},{9,... | collective-permute-start | bytes 294920 | tf_op jit(solution)/shard_map/ppermute | solution.py:58
  40.7 3.9 %collective-permute-start.6 = (bf16[64,768]{1,0:T(8,128)(2,1)S(1)}, bf16[64,768]{1,0:T(8,128)(2,1)S(1)}, u32[]{:S(2)}, u32[]{:S(2)}) collective-permute-start(bf16[64,768]{1,0:T(8,128)(2,1)S(1)} %shard_map.187.own), channel_id=1, source_target_pairs={{0,24},{1,97},{2,26},{3,99},{4,28},{5,101},{6,30},{7,103},{8,0},{9... | collective-permute-start | bytes 294920 | tf_op jit(solution)/shard_map/ppermute | solution.py:58
  41.8 25.0 %collective-permute-start.19 = (bf16[256,768]{1,0:T(8,128)(2,1)S(1)}, bf16[256,768]{1,0:T(8,128)(2,1)S(1)}, u32[]{:S(2)}, u32[]{:S(2)}) collective-permute-start(bf16[256,768]{1,0:T(8,128)(2,1)S(1)} %slice.8), channel_id=1, source_target_pairs={{0,32},{1,9},{2,34},{3,11},{4,36},{5,13},{6,38},{7,15},{8,40},{9,1... | collective-permute-start | bytes 1179656 | tf_op jit(solution)/shard_map/ppermute | solution.py:58
  42.4 24.5 %collective-permute-start.20 = (bf16[256,768]{1,0:T(8,128)(2,1)S(1)}, bf16[256,768]{1,0:T(8,128)(2,1)S(1)}, u32[]{:S(2)}, u32[]{:S(2)}) collective-permute-start(bf16[256,768]{1,0:T(8,128)(2,1)S(1)} %slice.9), channel_id=1, source_target_pairs={{0,96},{1,25},{2,98},{3,27},{4,100},{5,29},{6,102},{7,31},{8,104},... | collective-permute-start | bytes 1179656 | tf_op jit(solution)/shard_map/ppermute | solution.py:58
  44.9 7.2 %collective-permute-start.10 = (bf16[64,768]{1,0:T(8,128)(2,1)S(1)}, bf16[64,768]{1,0:T(8,128)(2,1)S(1)}, u32[]{:S(2)}, u32[]{:S(2)}) collective-permute-start(bf16[64,768]{1,0:T(8,128)(2,1)S(1)} %get-tuple-element.45.own), channel_id=1, source_target_pairs={{0,32},{1,9},{2,34},{3,11},{4,36},{5,13},{6,38},{7,15},{8,40},{9,1... | collective-permute-start | bytes 294920 | tf_op jit(solution)/shard_map/ppermute | solution.py:58
  45.0 7.9 %collective-permute-start.11 = (bf16[64,768]{1,0:T(8,128)(2,1)S(1)}, bf16[64,768]{1,0:T(8,128)(2,1)S(1)}, u32[]{:S(2)}, u32[]{:S(2)}) collective-permute-start(bf16[64,768]{1,0:T(8,128)(2,1)S(1)} %get-tuple-element.45.own), channel_id=1, source_target_pairs={{0,64},{1,17},{2,66},{3,19},{4,68},{5,21},{6,70},{7,23},{8,72},{9,... | collective-permute-start | bytes 294920 | tf_op jit(solution)/shard_map/ppermute | solution.py:58
  47.6 6.0 %collective-permute-start.12 = (bf16[64,768]{1,0:T(8,128)(2,1)S(1)}, bf16[64,768]{1,0:T(8,128)(2,1)S(1)}, u32[]{:S(2)}, u32[]{:S(2)}) collective-permute-start(bf16[64,768]{1,0:T(8,128)(2,1)S(1)} %get-tuple-element.45.own), channel_id=1, source_target_pairs={{0,96},{1,25},{2,98},{3,27},{4,100},{5,29},{6,102},{7,31},{8,104},... | collective-permute-start | bytes 294920 | tf_op jit(solution)/shard_map/ppermute | solution.py:58
  53.7 5.5 %collective-permute-start.13 = (f32[8,128]{1,0:T(8,128)S(1)}, f32[8,128]{1,0:T(8,128)S(1)}, u32[]{:S(2)}, u32[]{:S(2)}) collective-permute-start(f32[8,128]{1,0:T(8,128)S(1)} %get-tuple-element.46), channel_id=1, source_target_pairs={{0,4},{1,5},{2,6},{3,7},{4,0},{5,1},{6,2},{7,3},{8,12},{9,13},{10,... | collective-permute-start | bytes 12296 | tf_op jit(solution)/shard_map/ppermute | solution.py:58
  56.5 3.7 %collective-permute-start.14 = (f32[8,128]{1,0:T(8,128)S(1)}, f32[8,128]{1,0:T(8,128)S(1)}, u32[]{:S(2)}, u32[]{:S(2)}) collective-permute-start(f32[8,128]{1,0:T(8,128)S(1)} %get-tuple-element.46), channel_id=1, source_target_pairs={{0,2},{1,3},{2,4},{3,5},{4,6},{5,7},{6,0},{7,1},{8,10},{9,11},{10,... | collective-permute-start | bytes 12296 | tf_op jit(solution)/shard_map/ppermute | solution.py:58
  56.8 3.4 %collective-permute-start.15 = (f32[8,128]{1,0:T(8,128)S(1)}, f32[8,128]{1,0:T(8,128)S(1)}, u32[]{:S(2)}, u32[]{:S(2)}) collective-permute-start(f32[8,128]{1,0:T(8,128)S(1)} %get-tuple-element.46), channel_id=1, source_target_pairs={{0,6},{1,7},{2,0},{3,1},{4,2},{5,3},{6,4},{7,5},{8,14},{9,15},{10,... | collective-permute-start | bytes 12296 | tf_op jit(solution)/shard_map/ppermute | solution.py:58
  60.2 6.7 %collective-permute-start.16 = (f32[8,128]{1,0:T(8,128)S(1)}, f32[8,128]{1,0:T(8,128)S(1)}, u32[]{:S(2)}, u32[]{:S(2)}) collective-permute-start(f32[8,128]{1,0:T(8,128)S(1)} %add_add_fusion.s_own), channel_id=1, source_target_pairs={{0,1},{1,0},{2,3},{3,2},{4,5},{5,4},{6,7},{7,6},{8,9},{9,8},{10,11... | collective-permute-start | bytes 12296 | tf_op jit(solution)/shard_map/ppermute | solution.py:58

commit v7 on v6

--- a/solution.py
+++ b/solution.py
@@ -27,6 +27,7 @@
 ROWS = 128
 MESSAGE = ROWS + 32
 X_BLOCKS = 3
+DEPTHS = 4
 
 F32 = jnp.float32
 BF16 = jnp.bfloat16
@@ -90,14 +91,21 @@
     core = lax.axis_index("c")
     mine = pl.multiple_of(core * half, half)
     other = pl.multiple_of((1 - core) * half, half)
-    factors = [
-        pltpu.make_async_copy(a, b, p_sem.at[n]) for n, (a, b) in enumerate(((pq, pq_out), (pv, pv_out)))
+    depth = pq.shape[0] // DEPTHS
+    parts = [pl.ds(k * depth, depth) for k in range(DEPTHS)]
+    first = [
+        [
+            pltpu.make_async_copy(pq.at[k, :], pq_out.at[k, :], p_sem.at[n, 0]),
+            pltpu.make_async_copy(pv.at[k, :], pv_out.at[k, :], p_sem.at[n, 1]),
+            pltpu.make_async_copy(x.at[pl.ds(mine, block), k], xs.at[pl.ds(0, block), k], p_sem.at[n, 2]),
+        ]
+        for n, k in enumerate(parts)
     ]
     blocks = [
         pltpu.make_async_copy(
-            x.at[pl.ds(mine + n * block, block), :], xs.at[pl.ds(n * block, block), :], x_sem.at[n]
+            x.at[pl.ds(mine + n * block, block), :], xs.at[pl.ds(n * block, block), :], x_sem.at[n - 1]
         )
-        for n in range(X_BLOCKS)
+        for n in range(1, X_BLOCKS)
     ]
     pairs = (
         (wq, wq_s),
@@ -115,12 +123,23 @@
         for n, (a, b) in enumerate(((cq, cq_out), (cv, cv_out)))
         for at, start in enumerate((mine, other))
     ]
-    for copy in (*factors, *blocks, *small, *cotangents):
+    for copy in (*(c for piece in first for c in piece), *blocks):
         copy.start()
-    for copy in factors:
-        copy.wait()
-    for n in range(X_BLOCKS):
-        blocks[n].wait()
+    part_q = part_v = None
+    for piece, k in zip(first, parts):
+        for copy in piece:
+            copy.wait()
+        rows = xs[:block, k]
+        piece_q = jnp.dot(rows, pq_out[k, :], preferred_element_type=F32)
+        piece_v = jnp.dot(rows, pv_out[k, :], preferred_element_type=F32)
+        part_q = piece_q if part_q is None else part_q + piece_q
+        part_v = piece_v if part_v is None else part_v + piece_v
+    for copy in (*small, *cotangents):
+        copy.start()
+    mixed[:block, :RANK] = part_q.astype(BF16)
+    mixed[:block, RANK:] = part_v.astype(BF16)
+    for n in range(1, X_BLOCKS):
+        blocks[n - 1].wait()
         at = slice(n * block, (n + 1) * block)
         rows = xs[at, :]
         mixed[at, :RANK] = jnp.dot(rows, pq_out[...], preferred_element_type=F32).astype(BF16)
@@ -159,8 +178,8 @@
             pltpu.VMEM((16, W), F32),
             pltpu.VMEM((16, W), F32),
             pltpu.SemaphoreType.DMA((6,)),
-            pltpu.SemaphoreType.DMA((2,)),
-            pltpu.SemaphoreType.DMA((X_BLOCKS,)),
+            pltpu.SemaphoreType.DMA((DEPTHS, 3)),
+            pltpu.SemaphoreType.DMA((X_BLOCKS - 1,)),
             pltpu.SemaphoreType.DMA((2, 2)),
         ],
         cost_estimate=pl.CostEstimate(

time: 70 us -> 67.2 us (0.960)
  Pallas kernels: 13.2 us -> 10.5 us
    pallas_call x1, Pallas kernels: 8.41 us -> 5.66 us  [mix(): pl.pallas_call(mix_kernel, in_specs=[hbm] * len(operands), out_specs=[vme...]
where the time goes in v7:
time: 67.2 us; the launch traced here: 67.1 us
  starting transfers between devices  36 us (54%)
  waiting for transfers between devices  19.7 us (29%)
  Pallas kernels  10.5 us (16%)
  between operations  0.81 us (1%)
    ppermute x21, starting transfers between devices, shifted(): return lax.ppermute(array, AXES, shift_pairs(kind, offset))  36 us
    ppermute x21, waiting for transfers between devices, shifted(): return lax.ppermute(array, AXES, shift_pairs(kind, offset))  19.7 us
    pallas_call x1, Pallas kernels, mix(): pl.pallas_call(mix_kernel, in_specs=[hbm] * len(operands), out_specs=[vme...  5.66 us
    pallas_call x1, Pallas kernels, new_weights(): pl.pallas_call(weight_kernel, in_specs=[vmem] * len(operands), out_specs=...  2.96 us
    pallas_call x5, Pallas kernels, whole_call(): pl.pallas_call(body, in_specs=[vmem] * len(operands), out_specs=[vmem] *...  1.87 us
  transfers between devices with their start and end apart: 21, of which 9 were waited for; matrix products, arithmetic and copies ran while one was open for 0% of the time, Pallas kernels for 3%

profile of v7, /device:TPU:1, one launch (start us, length us, event | category | flops | bytes accessed | tf_op | source)
XLA Modules:
  0.0 67.1 jit_solution(8554050943309703379)
XLA Ops:
  0.6 5.7 %mix.1 = (bf16[1536,512]{1,0:T(8,128)(2,1)S(1)}, bf16[160,768]{1,0:T(8,128)(2,1)S(1)}, bf16[2048,256]{1,0:T(8,128)(2,1)S(1)}, bf16[2048,256]{1,0:T(8,128)(2,1)S(...) custom-call(bf16[3072,2048]{1,0:T(8,128)(2,1)} %x.1, bf16[3072,256]{1,0:T(8,128)(2,1)} %cq.1, ...), custom_call_target="tpu_custom_call" | custom-call | flops 3221225472 | bytes 14000000 | tf_op jit(solution)/shard_map/mix/pallas_call | solution.py:162
  6.3 1.5 %collective-permute-start = (bf16[1536,512]{1,0:T(8,128)(2,1)S(1)}, bf16[1536,512]{1,0:T(8,128)(2,1)S(1)}, u32[]{:S(2)}, u32[]{:S(2)}) collective-permute-start(bf16[1536,512]{1,0:T(8,128)(2,1)S(1)} %get-tuple-element.37.mixed), channel_id=1, source_target_pairs={{0,1},{1,0},{2,3},{3,2},{4,5},{5,4},{6,7},{7,6},{8,9},{9,8},{10,11... | collective-permute-start | bytes 4718600 | tf_op jit(solution)/shard_map/ppermute | solution.py:59
  7.8 1.7 %collective-permute-start.7 = (bf16[160,768]{1,0:T(8,128)(2,1)S(1)}, bf16[160,768]{1,0:T(8,128)(2,1)S(1)}, u32[]{:S(2)}, u32[]{:S(2)}) collective-permute-start(bf16[160,768]{1,0:T(8,128)(2,1)S(1)} %get-tuple-element.44.k0.w0), channel_id=1, source_target_pairs={{0,8},{1,33},{2,10},{3,35},{4,12},{5,37},{6,14},{7,39},{8,16},{9,4... | collective-permute-start | bytes 737288 | tf_op jit(solution)/shard_map/ppermute | solution.py:59
  9.5 3.3 %collective-permute-start.8 = (bf16[160,768]{1,0:T(8,128)(2,1)S(1)}, bf16[160,768]{1,0:T(8,128)(2,1)S(1)}, u32[]{:S(2)}, u32[]{:S(2)}) collective-permute-start(bf16[160,768]{1,0:T(8,128)(2,1)S(1)} %get-tuple-element.44.k0.w0), channel_id=1, source_target_pairs={{0,16},{1,65},{2,18},{3,67},{4,20},{5,69},{6,22},{7,71},{8,24},{9,... | collective-permute-start | bytes 737288 | tf_op jit(solution)/shard_map/ppermute | solution.py:59
  12.8 0.7 %collective-permute-start.9 = (bf16[160,768]{1,0:T(8,128)(2,1)S(1)}, bf16[160,768]{1,0:T(8,128)(2,1)S(1)}, u32[]{:S(2)}, u32[]{:S(2)}) collective-permute-start(bf16[160,768]{1,0:T(8,128)(2,1)S(1)} %get-tuple-element.44.k0.w0), channel_id=1, source_target_pairs={{0,24},{1,97},{2,26},{3,99},{4,28},{5,101},{6,30},{7,103},{8,0},{9... | collective-permute-start | bytes 737288 | tf_op jit(solution)/shard_map/ppermute | solution.py:59
  13.6 1.5 %shard_map.186 = (f32[64,768]{1,0:T(8,128)S(1)}, bf16[64,768]{1,0:T(8,128)(2,1)S(1)}, bf16[64,768]{1,0:T(8,128)(2,1)S(1)}, bf16[64,768]{1,0:T(8,128)(2,1)S(1)}) custom-call(bf16[1536,512]{1,0:T(8,128)(2,1)S(1)} %get-tuple-element.37.mixed, bf16[1536,512]{1,0:T(8,128)(2,1)S(1)} %collective-permute-done.swapped, bf16[3072,256]{1,0:T(8,128)(2,1)S(1)} %get-tuple-element.38.cq, ...), custom_call_target="tpu_custom_call" | custom-call | flops 1207959552 | bytes 1000000 | tf_op jit(solution)/shard_map/pallas_call | solution.py:216
  15.1 0.1 collective-permute-done.7.k1.w1
  15.2 3.8 %collective-permute-done.8.k2.w2 = bf16[160,768]{1,0:T(8,128)(2,1)S(1)} collective-permute-done((bf16[160,768]{1,0:T(8,128)(2,1)S(1)}, bf16[160,768]{1,0:T(8,128)(2,1)S(1)}, u32[]{:S(2)}, u32[]{:S(2)}) %collective-permute-start.8) | collective-permute-done | bytes 245792 | tf_op jit(solution)/shard_map/ppermute | solution.py:59
  19.1 1.4 %collective-permute-start.17 = (bf16[512,768]{1,0:T(8,128)(2,1)S(1)}, bf16[512,768]{1,0:T(8,128)(2,1)S(1)}, u32[]{:S(2)}, u32[]{:S(2)}) collective-permute-start(bf16[512,768]{1,0:T(8,128)(2,1)S(1)} %shard_map.190.g0), channel_id=1, source_target_pairs={{0,32},{1,9},{2,34},{3,11},{4,36},{5,13},{6,38},{7,15},{8,40},{9,1... | collective-permute-start | bytes 2359304 | tf_op jit(solution)/shard_map/ppermute | solution.py:59
  20.5 1.5 %collective-permute-start.18 = (bf16[512,768]{1,0:T(8,128)(2,1)S(1)}, bf16[512,768]{1,0:T(8,128)(2,1)S(1)}, u32[]{:S(2)}, u32[]{:S(2)}) collective-permute-start(bf16[512,768]{1,0:T(8,128)(2,1)S(1)} %shard_map.190.g0), channel_id=1, source_target_pairs={{0,96},{1,25},{2,98},{3,27},{4,100},{5,29},{6,102},{7,31},{8,104},... | collective-permute-start | bytes 2359304 | tf_op jit(solution)/shard_map/ppermute | solution.py:59
  22.0 2.6 %collective-permute-start.2 = (bf16[64,768]{1,0:T(8,128)(2,1)S(1)}, bf16[64,768]{1,0:T(8,128)(2,1)S(1)}, u32[]{:S(2)}, u32[]{:S(2)}) collective-permute-start(bf16[64,768]{1,0:T(8,128)(2,1)S(1)} %get-tuple-element.42), channel_id=1, source_target_pairs={{0,64},{1,17},{2,66},{3,19},{4,68},{5,21},{6,70},{7,23},{8,72},{9,... | collective-permute-start | bytes 294920 | tf_op jit(solution)/shard_map/ppermute | solution.py:59
  24.6 1.1 %collective-permute-start.3 = (bf16[64,768]{1,0:T(8,128)(2,1)S(1)}, bf16[64,768]{1,0:T(8,128)(2,1)S(1)}, u32[]{:S(2)}, u32[]{:S(2)}) collective-permute-start(bf16[64,768]{1,0:T(8,128)(2,1)S(1)} %get-tuple-element.43), channel_id=1, source_target_pairs={{0,96},{1,25},{2,98},{3,27},{4,100},{5,29},{6,102},{7,31},{8,104},... | collective-permute-start | bytes 294920 | tf_op jit(solution)/shard_map/ppermute | solution.py:59
  25.6 7.0 %collective-permute-done.1.r1 = bf16[64,768]{1,0:T(8,128)(2,1)S(1)} collective-permute-done((bf16[64,768]{1,0:T(8,128)(2,1)S(1)}, bf16[64,768]{1,0:T(8,128)(2,1)S(1)}, u32[]{:S(2)}, u32[]{:S(2)}) %collective-permute-start.1) | collective-permute-done | bytes 98336 | tf_op jit(solution)/shard_map/ppermute | solution.py:59
  32.7 1.9 %collective-permute-done.2.r2 = bf16[64,768]{1,0:T(8,128)(2,1)S(1)} collective-permute-done((bf16[64,768]{1,0:T(8,128)(2,1)S(1)}, bf16[64,768]{1,0:T(8,128)(2,1)S(1)}, u32[]{:S(2)}, u32[]{:S(2)}) %collective-permute-start.2) | collective-permute-done | bytes 98336 | tf_op jit(solution)/shard_map/ppermute | solution.py:59
  34.7 0.9 %collective-permute-start.4 = (bf16[64,768]{1,0:T(8,128)(2,1)S(1)}, bf16[64,768]{1,0:T(8,128)(2,1)S(1)}, u32[]{:S(2)}, u32[]{:S(2)}) collective-permute-start(bf16[64,768]{1,0:T(8,128)(2,1)S(1)} %shard_map.187.own), channel_id=1, source_target_pairs={{0,8},{1,33},{2,10},{3,35},{4,12},{5,37},{6,14},{7,39},{8,16},{9,4... | collective-permute-start | bytes 294920 | tf_op jit(solution)/shard_map/ppermute | solution.py:59
  35.6 2.4 %collective-permute-start.5 = (bf16[64,768]{1,0:T(8,128)(2,1)S(1)}, bf16[64,768]{1,0:T(8,128)(2,1)S(1)}, u32[]{:S(2)}, u32[]{:S(2)}) collective-permute-start(bf16[64,768]{1,0:T(8,128)(2,1)S(1)} %shard_map.187.own), channel_id=1, source_target_pairs={{0,16},{1,65},{2,18},{3,67},{4,20},{5,69},{6,22},{7,71},{8,24},{9,... | collective-permute-start | bytes 294920 | tf_op jit(solution)/shard_map/ppermute | solution.py:59
  38.0 1.1 %collective-permute-start.6 = (bf16[64,768]{1,0:T(8,128)(2,1)S(1)}, bf16[64,768]{1,0:T(8,128)(2,1)S(1)}, u32[]{:S(2)}, u32[]{:S(2)}) collective-permute-start(bf16[64,768]{1,0:T(8,128)(2,1)S(1)} %shard_map.187.own), channel_id=1, source_target_pairs={{0,24},{1,97},{2,26},{3,99},{4,28},{5,101},{6,30},{7,103},{8,0},{9... | collective-permute-start | bytes 294920 | tf_op jit(solution)/shard_map/ppermute | solution.py:59
  39.1 0.5 collective-permute-start.19
  39.6 2.3 %collective-permute-start.20 = (bf16[256,768]{1,0:T(8,128)(2,1)S(1)}, bf16[256,768]{1,0:T(8,128)(2,1)S(1)}, u32[]{:S(2)}, u32[]{:S(2)}) collective-permute-start(bf16[256,768]{1,0:T(8,128)(2,1)S(1)} %slice.9), channel_id=1, source_target_pairs={{0,96},{1,25},{2,98},{3,27},{4,100},{5,29},{6,102},{7,31},{8,104},... | collective-permute-start | bytes 1179656 | tf_op jit(solution)/shard_map/ppermute | solution.py:59
  42.0 0.2 shard_map.188
  42.3 2.5 %collective-permute-start.11 = (bf16[64,768]{1,0:T(8,128)(2,1)S(1)}, bf16[64,768]{1,0:T(8,128)(2,1)S(1)}, u32[]{:S(2)}, u32[]{:S(2)}) collective-permute-start(bf16[64,768]{1,0:T(8,128)(2,1)S(1)} %get-tuple-element.45.own), channel_id=1, source_target_pairs={{0,64},{1,17},{2,66},{3,19},{4,68},{5,21},{6,70},{7,23},{8,72},{9,... | collective-permute-start | bytes 294920 | tf_op jit(solution)/shard_map/ppermute | solution.py:59
  44.8 1.1 %collective-permute-start.12 = (bf16[64,768]{1,0:T(8,128)(2,1)S(1)}, bf16[64,768]{1,0:T(8,128)(2,1)S(1)}, u32[]{:S(2)}, u32[]{:S(2)}) collective-permute-start(bf16[64,768]{1,0:T(8,128)(2,1)S(1)} %get-tuple-element.45.own), channel_id=1, source_target_pairs={{0,96},{1,25},{2,98},{3,27},{4,100},{5,29},{6,102},{7,31},{8,104},... | collective-permute-start | bytes 294920 | tf_op jit(solution)/shard_map/ppermute | solution.py:59
  45.9 3.5 %collective-permute-done.10.r1 = bf16[64,768]{1,0:T(8,128)(2,1)S(1)} collective-permute-done((bf16[64,768]{1,0:T(8,128)(2,1)S(1)}, bf16[64,768]{1,0:T(8,128)(2,1)S(1)}, u32[]{:S(2)}, u32[]{:S(2)}) %collective-permute-start.10) | collective-permute-done | bytes 98336 | tf_op jit(solution)/shard_map/ppermute | solution.py:59
  49.4 0.8 %collective-permute-done.11.r2 = bf16[64,768]{1,0:T(8,128)(2,1)S(1)} collective-permute-done((bf16[64,768]{1,0:T(8,128)(2,1)S(1)}, bf16[64,768]{1,0:T(8,128)(2,1)S(1)}, u32[]{:S(2)}, u32[]{:S(2)}) %collective-permute-start.11) | collective-permute-done | bytes 98336 | tf_op jit(solution)/shard_map/ppermute | solution.py:59
  50.2 0.6 collective-permute-done.12.r3
  50.9 2.8 %collective-permute-start.13 = (f32[8,128]{1,0:T(8,128)S(1)}, f32[8,128]{1,0:T(8,128)S(1)}, u32[]{:S(2)}, u32[]{:S(2)}) collective-permute-start(f32[8,128]{1,0:T(8,128)S(1)} %get-tuple-element.46), channel_id=1, source_target_pairs={{0,4},{1,5},{2,6},{3,7},{4,0},{5,1},{6,2},{7,3},{8,12},{9,13},{10,... | collective-permute-start | bytes 12296 | tf_op jit(solution)/shard_map/ppermute | solution.py:59
  53.7 0.3 collective-permute-start.14
  54.0 2.4 %collective-permute-start.15 = (f32[8,128]{1,0:T(8,128)S(1)}, f32[8,128]{1,0:T(8,128)S(1)}, u32[]{:S(2)}, u32[]{:S(2)}) collective-permute-start(f32[8,128]{1,0:T(8,128)S(1)} %get-tuple-element.46), channel_id=1, source_target_pairs={{0,6},{1,7},{2,0},{3,1},{4,2},{5,3},{6,4},{7,5},{8,14},{9,15},{10,... | collective-permute-start | bytes 12296 | tf_op jit(solution)/shard_map/ppermute | solution.py:59
  56.4 1.0 %collective-permute-done.14 = f32[8,128]{1,0:T(8,128)S(1)} collective-permute-done((f32[8,128]{1,0:T(8,128)S(1)}, f32[8,128]{1,0:T(8,128)S(1)}, u32[]{:S(2)}, u32[]{:S(2)}) %collective-permute-start.14) | collective-permute-done | bytes 4128 | tf_op jit(solution)/shard_map/ppermute | solution.py:59
  57.4 5.9 %collective-permute-start.16 = (f32[8,128]{1,0:T(8,128)S(1)}, f32[8,128]{1,0:T(8,128)S(1)}, u32[]{:S(2)}, u32[]{:S(2)}) collective-permute-start(f32[8,128]{1,0:T(8,128)S(1)} %add_add_fusion.s_own), channel_id=1, source_target_pairs={{0,1},{1,0},{2,3},{3,2},{4,5},{5,4},{6,7},{7,6},{8,9},{9,8},{10,11... | collective-permute-start | bytes 12296 | tf_op jit(solution)/shard_map/ppermute | solution.py:59
  63.3 0.8 %collective-permute-done.16.s_other = f32[8,128]{1,0:T(8,128)S(1)} collective-permute-done((f32[8,128]{1,0:T(8,128)S(1)}, f32[8,128]{1,0:T(8,128)S(1)}, u32[]{:S(2)}, u32[]{:S(2)}) %collective-permute-start.16) | collective-permute-done | bytes 4128 | tf_op jit(solution)/shard_map/ppermute | solution.py:59
  64.1 3.0 %weights.1 = (f32[128,256]{1,0:T(8,128)}, f32[128,512]{1,0:T(8,128)}, f32[128,256]{1,0:T(8,128)}, f32[128,512]{1,0:T(8,128)}, bf16[2048,256]{1,0:T(8,128)(2,1)},...) custom-call(f32[8,128]{1,0:T(8,128)S(1)} %add_add_fusion.s_own, ...), custom_call_target="tpu_custom_call" | custom-call | flops 805306368 | bytes 12000000 | tf_op jit(solution)/shard_map/weights/pallas_call | solution.py:334
  (32 shorter events, 0.4 us)
Async XLA Ops:
  6.3 7.2 %collective-permute-start = (bf16[1536,512]{1,0:T(8,128)(2,1)S(1)}, bf16[1536,512]{1,0:T(8,128)(2,1)S(1)}, u32[]{:S(2)}, u32[]{:S(2)}) collective-permute-start(bf16[1536,512]{1,0:T(8,128)(2,1)S(1)} %get-tuple-element.37.mixed), channel_id=1, source_target_pairs={{0,1},{1,0},{2,3},{3,2},{4,5},{5,4},{6,7},{7,6},{8,9},{9,8},{10,11... | collective-permute-start | bytes 4718600 | tf_op jit(solution)/shard_map/ppermute | solution.py:59
  7.8 7.5 %collective-permute-start.7 = (bf16[160,768]{1,0:T(8,128)(2,1)S(1)}, bf16[160,768]{1,0:T(8,128)(2,1)S(1)}, u32[]{:S(2)}, u32[]{:S(2)}) collective-permute-start(bf16[160,768]{1,0:T(8,128)(2,1)S(1)} %get-tuple-element.44.k0.w0), channel_id=1, source_target_pairs={{0,8},{1,33},{2,10},{3,35},{4,12},{5,37},{6,14},{7,39},{8,16},{9,4... | collective-permute-start | bytes 737288 | tf_op jit(solution)/shard_map/ppermute | solution.py:59
  9.5 9.5 %collective-permute-start.8 = (bf16[160,768]{1,0:T(8,128)(2,1)S(1)}, bf16[160,768]{1,0:T(8,128)(2,1)S(1)}, u32[]{:S(2)}, u32[]{:S(2)}) collective-permute-start(bf16[160,768]{1,0:T(8,128)(2,1)S(1)} %get-tuple-element.44.k0.w0), channel_id=1, source_target_pairs={{0,16},{1,65},{2,18},{3,67},{4,20},{5,69},{6,22},{7,71},{8,24},{9,... | collective-permute-start | bytes 737288 | tf_op jit(solution)/shard_map/ppermute | solution.py:59
  12.8 6.2 %collective-permute-start.9 = (bf16[160,768]{1,0:T(8,128)(2,1)S(1)}, bf16[160,768]{1,0:T(8,128)(2,1)S(1)}, u32[]{:S(2)}, u32[]{:S(2)}) collective-permute-start(bf16[160,768]{1,0:T(8,128)(2,1)S(1)} %get-tuple-element.44.k0.w0), channel_id=1, source_target_pairs={{0,24},{1,97},{2,26},{3,99},{4,28},{5,101},{6,30},{7,103},{8,0},{9... | collective-permute-start | bytes 737288 | tf_op jit(solution)/shard_map/ppermute | solution.py:59
  15.0 26.9 %copy-start.2 = (f32[16,512]{1,0:T(8,128)S(1)}, f32[16,512]{1,0:T(8,128)}, u32[]{:S(2)}) copy-start(f32[16,512]{1,0:T(8,128)} %mv.3) | copy-start | bytes 98308
  15.1 26.9 %copy-start.3 = (f32[16,512]{1,0:T(8,128)S(1)}, f32[16,512]{1,0:T(8,128)}, u32[]{:S(2)}) copy-start(f32[16,512]{1,0:T(8,128)} %vv.3) | copy-start | bytes 98308
  15.1 26.9 %copy-start.4 = (f32[16,256]{1,0:T(8,128)S(1)}, f32[16,256]{1,0:T(8,128)}, u32[]{:S(2)}) copy-start(f32[16,256]{1,0:T(8,128)} %mq.3) | copy-start | bytes 49156
  15.1 26.9 %copy-start.5 = (f32[16,256]{1,0:T(8,128)S(1)}, f32[16,256]{1,0:T(8,128)}, u32[]{:S(2)}) copy-start(f32[16,256]{1,0:T(8,128)} %vq.3) | copy-start | bytes 49156
  19.1 45.0 %copy-start = (f32[128,512]{1,0:T(8,128)S(1)}, f32[128,512]{1,0:T(8,128)}, u32[]{:S(2)}) copy-start(f32[128,512]{1,0:T(8,128)} %wv.3) | copy-start | bytes 786436
  19.1 45.0 %copy-start.1 = (f32[128,256]{1,0:T(8,128)S(1)}, f32[128,256]{1,0:T(8,128)}, u32[]{:S(2)}) copy-start(f32[128,256]{1,0:T(8,128)} %wq.3) | copy-start | bytes 393220
  19.1 19.9 %collective-permute-start.17 = (bf16[512,768]{1,0:T(8,128)(2,1)S(1)}, bf16[512,768]{1,0:T(8,128)(2,1)S(1)}, u32[]{:S(2)}, u32[]{:S(2)}) collective-permute-start(bf16[512,768]{1,0:T(8,128)(2,1)S(1)} %shard_map.190.g0), channel_id=1, source_target_pairs={{0,32},{1,9},{2,34},{3,11},{4,36},{5,13},{6,38},{7,15},{8,40},{9,1... | collective-permute-start | bytes 2359304 | tf_op jit(solution)/shard_map/ppermute | solution.py:59
  20.5 19.1 %collective-permute-start.18 = (bf16[512,768]{1,0:T(8,128)(2,1)S(1)}, bf16[512,768]{1,0:T(8,128)(2,1)S(1)}, u32[]{:S(2)}, u32[]{:S(2)}) collective-permute-start(bf16[512,768]{1,0:T(8,128)(2,1)S(1)} %shard_map.190.g0), channel_id=1, source_target_pairs={{0,96},{1,25},{2,98},{3,27},{4,100},{5,29},{6,102},{7,31},{8,104},... | collective-permute-start | bytes 2359304 | tf_op jit(solution)/shard_map/ppermute | solution.py:59
  22.0 10.6 %collective-permute-start.1 = (bf16[64,768]{1,0:T(8,128)(2,1)S(1)}, bf16[64,768]{1,0:T(8,128)(2,1)S(1)}, u32[]{:S(2)}, u32[]{:S(2)}) collective-permute-start(bf16[64,768]{1,0:T(8,128)(2,1)S(1)} %get-tuple-element.41), channel_id=1, source_target_pairs={{0,32},{1,9},{2,34},{3,11},{4,36},{5,13},{6,38},{7,15},{8,40},{9,1... | collective-permute-start | bytes 294920 | tf_op jit(solution)/shard_map/ppermute | solution.py:59
  22.0 12.6 %collective-permute-start.2 = (bf16[64,768]{1,0:T(8,128)(2,1)S(1)}, bf16[64,768]{1,0:T(8,128)(2,1)S(1)}, u32[]{:S(2)}, u32[]{:S(2)}) collective-permute-start(bf16[64,768]{1,0:T(8,128)(2,1)S(1)} %get-tuple-element.42), channel_id=1, source_target_pairs={{0,64},{1,17},{2,66},{3,19},{4,68},{5,21},{6,70},{7,23},{8,72},{9,... | collective-permute-start | bytes 294920 | tf_op jit(solution)/shard_map/ppermute | solution.py:59
  24.6 10.0 %collective-permute-start.3 = (bf16[64,768]{1,0:T(8,128)(2,1)S(1)}, bf16[64,768]{1,0:T(8,128)(2,1)S(1)}, u32[]{:S(2)}, u32[]{:S(2)}) collective-permute-start(bf16[64,768]{1,0:T(8,128)(2,1)S(1)} %get-tuple-element.43), channel_id=1, source_target_pairs={{0,96},{1,25},{2,98},{3,27},{4,100},{5,29},{6,102},{7,31},{8,104},... | collective-permute-start | bytes 294920 | tf_op jit(solution)/shard_map/ppermute | solution.py:59
  34.7 7.3 %collective-permute-start.4 = (bf16[64,768]{1,0:T(8,128)(2,1)S(1)}, bf16[64,768]{1,0:T(8,128)(2,1)S(1)}, u32[]{:S(2)}, u32[]{:S(2)}) collective-permute-start(bf16[64,768]{1,0:T(8,128)(2,1)S(1)} %shard_map.187.own), channel_id=1, source_target_pairs={{0,8},{1,33},{2,10},{3,35},{4,12},{5,37},{6,14},{7,39},{8,16},{9,4... | collective-permute-start | bytes 294920 | tf_op jit(solution)/shard_map/ppermute | solution.py:59
  35.6 6.3 %collective-permute-start.5 = (bf16[64,768]{1,0:T(8,128)(2,1)S(1)}, bf16[64,768]{1,0:T(8,128)(2,1)S(1)}, u32[]{:S(2)}, u32[]{:S(2)}) collective-permute-start(bf16[64,768]{1,0:T(8,128)(2,1)S(1)} %shard_map.187.own), channel_id=1, source_target_pairs={{0,16},{1,65},{2,18},{3,67},{4,20},{5,69},{6,22},{7,71},{8,24},{9,... | collective-permute-start | bytes 294920 | tf_op jit(solution)/shard_map/ppermute | solution.py:59
  38.0 3.9 %collective-permute-start.6 = (bf16[64,768]{1,0:T(8,128)(2,1)S(1)}, bf16[64,768]{1,0:T(8,128)(2,1)S(1)}, u32[]{:S(2)}, u32[]{:S(2)}) collective-permute-start(bf16[64,768]{1,0:T(8,128)(2,1)S(1)} %shard_map.187.own), channel_id=1, source_target_pairs={{0,24},{1,97},{2,26},{3,99},{4,28},{5,101},{6,30},{7,103},{8,0},{9... | collective-permute-start | bytes 294920 | tf_op jit(solution)/shard_map/ppermute | solution.py:59
  39.1 25.0 %collective-permute-start.19 = (bf16[256,768]{1,0:T(8,128)(2,1)S(1)}, bf16[256,768]{1,0:T(8,128)(2,1)S(1)}, u32[]{:S(2)}, u32[]{:S(2)}) collective-permute-start(bf16[256,768]{1,0:T(8,128)(2,1)S(1)} %slice.8), channel_id=1, source_target_pairs={{0,32},{1,9},{2,34},{3,11},{4,36},{5,13},{6,38},{7,15},{8,40},{9,1... | collective-permute-start | bytes 1179656 | tf_op jit(solution)/shard_map/ppermute | solution.py:59
  39.6 24.5 %collective-permute-start.20 = (bf16[256,768]{1,0:T(8,128)(2,1)S(1)}, bf16[256,768]{1,0:T(8,128)(2,1)S(1)}, u32[]{:S(2)}, u32[]{:S(2)}) collective-permute-start(bf16[256,768]{1,0:T(8,128)(2,1)S(1)} %slice.9), channel_id=1, source_target_pairs={{0,96},{1,25},{2,98},{3,27},{4,100},{5,29},{6,102},{7,31},{8,104},... | collective-permute-start | bytes 1179656 | tf_op jit(solution)/shard_map/ppermute | solution.py:59
  42.2 7.2 %collective-permute-start.10 = (bf16[64,768]{1,0:T(8,128)(2,1)S(1)}, bf16[64,768]{1,0:T(8,128)(2,1)S(1)}, u32[]{:S(2)}, u32[]{:S(2)}) collective-permute-start(bf16[64,768]{1,0:T(8,128)(2,1)S(1)} %get-tuple-element.45.own), channel_id=1, source_target_pairs={{0,32},{1,9},{2,34},{3,11},{4,36},{5,13},{6,38},{7,15},{8,40},{9,1... | collective-permute-start | bytes 294920 | tf_op jit(solution)/shard_map/ppermute | solution.py:59
  42.3 7.9 %collective-permute-start.11 = (bf16[64,768]{1,0:T(8,128)(2,1)S(1)}, bf16[64,768]{1,0:T(8,128)(2,1)S(1)}, u32[]{:S(2)}, u32[]{:S(2)}) collective-permute-start(bf16[64,768]{1,0:T(8,128)(2,1)S(1)} %get-tuple-element.45.own), channel_id=1, source_target_pairs={{0,64},{1,17},{2,66},{3,19},{4,68},{5,21},{6,70},{7,23},{8,72},{9,... | collective-permute-start | bytes 294920 | tf_op jit(solution)/shard_map/ppermute | solution.py:59
  44.8 6.0 %collective-permute-start.12 = (bf16[64,768]{1,0:T(8,128)(2,1)S(1)}, bf16[64,768]{1,0:T(8,128)(2,1)S(1)}, u32[]{:S(2)}, u32[]{:S(2)}) collective-permute-start(bf16[64,768]{1,0:T(8,128)(2,1)S(1)} %get-tuple-element.45.own), channel_id=1, source_target_pairs={{0,96},{1,25},{2,98},{3,27},{4,100},{5,29},{6,102},{7,31},{8,104},... | collective-permute-start | bytes 294920 | tf_op jit(solution)/shard_map/ppermute | solution.py:59
  50.9 5.5 %collective-permute-start.13 = (f32[8,128]{1,0:T(8,128)S(1)}, f32[8,128]{1,0:T(8,128)S(1)}, u32[]{:S(2)}, u32[]{:S(2)}) collective-permute-start(f32[8,128]{1,0:T(8,128)S(1)} %get-tuple-element.46), channel_id=1, source_target_pairs={{0,4},{1,5},{2,6},{3,7},{4,0},{5,1},{6,2},{7,3},{8,12},{9,13},{10,... | collective-permute-start | bytes 12296 | tf_op jit(solution)/shard_map/ppermute | solution.py:59
  53.7 3.7 %collective-permute-start.14 = (f32[8,128]{1,0:T(8,128)S(1)}, f32[8,128]{1,0:T(8,128)S(1)}, u32[]{:S(2)}, u32[]{:S(2)}) collective-permute-start(f32[8,128]{1,0:T(8,128)S(1)} %get-tuple-element.46), channel_id=1, source_target_pairs={{0,2},{1,3},{2,4},{3,5},{4,6},{5,7},{6,0},{7,1},{8,10},{9,11},{10,... | collective-permute-start | bytes 12296 | tf_op jit(solution)/shard_map/ppermute | solution.py:59
  54.0 3.4 %collective-permute-start.15 = (f32[8,128]{1,0:T(8,128)S(1)}, f32[8,128]{1,0:T(8,128)S(1)}, u32[]{:S(2)}, u32[]{:S(2)}) collective-permute-start(f32[8,128]{1,0:T(8,128)S(1)} %get-tuple-element.46), channel_id=1, source_target_pairs={{0,6},{1,7},{2,0},{3,1},{4,2},{5,3},{6,4},{7,5},{8,14},{9,15},{10,... | collective-permute-start | bytes 12296 | tf_op jit(solution)/shard_map/ppermute | solution.py:59
  57.4 6.7 %collective-permute-start.16 = (f32[8,128]{1,0:T(8,128)S(1)}, f32[8,128]{1,0:T(8,128)S(1)}, u32[]{:S(2)}, u32[]{:S(2)}) collective-permute-start(f32[8,128]{1,0:T(8,128)S(1)} %add_add_fusion.s_own), channel_id=1, source_target_pairs={{0,1},{1,0},{2,3},{3,2},{4,5},{5,4},{6,7},{7,6},{8,9},{9,8},{10,11... | collective-permute-start | bytes 12296 | tf_op jit(solution)/shard_map/ppermute | solution.py:59

commit v8 on v7

--- a/solution.py
+++ b/solution.py
@@ -273,7 +273,7 @@
 
 
 def weight_kernel(
-    s_own, s_other, u, pq, pv, g0, g1, g3, h_up, h_down, wq, wv, fq, fv, sq, sv,
+    s_own, s_other, u, pq, pv, g0, g1, g2, g3, wq, wv, fq, fv, sq, sv,
     nq, nv, tq, tv, cq, cv, fq_out, fv_out, sq_out, sv_out,
     nq_s, nv_s, tq_s, tv_s, cq_s, cv_s, c_sem, m_sem,
 ):
@@ -291,7 +291,7 @@
     scale = lax.rsqrt(squares / (RANK * (QK_W + V_W)) + norm_eps)
     uq, uv = u[:, :WQ], u[:, WQ:]
     keep = 1.0 - step_rate * decay_rate
-    for i, pieces in ((0, (g0, g0)), (1, (g1, g1)), (3, (g3, g3)), (2, (h_up, h_down))):
+    for i, piece in ((0, g0), (1, g1), (3, g3), (2, g2)):
         a_there = lax.rem(major + 4 - i, 4)
         for j in range(4):
             b_there = lax.rem(minor + 4 - j, 4)
@@ -299,9 +299,7 @@
             at = pl.ds(pl.multiple_of(block * ROWS, ROWS), ROWS)
             back_q = scale * jnp.dot(pq[at, :], uq, preferred_element_type=F32)
             back_v = scale * jnp.dot(pv[at, :], uv, preferred_element_type=F32)
-            piece = pieces[j // 2]
-            top = (j if piece.shape[0] == 4 * ROWS else j % 2) * ROWS
-            held = piece[top : top + ROWS, :].astype(F32)
+            held = piece[j * ROWS : (j + 1) * ROWS, :].astype(F32)
             n = i * 4 + j
             cq_s[n] = (keep * held[:, :WQ] - step_rate * back_q).astype(BF16)
             cv_s[n] = (keep * held[:, WQ:] - step_rate * back_v).astype(BF16)
@@ -383,8 +381,7 @@
         [pltpu.VMEM((64, W), F32)],
     )
     u_1, u_2, u_3 = to_all("major", (u_own,) * 3)
-    h_up = shifted(g_1[: 2 * ROWS], "major", 1)
-    h_down = shifted(g_3[2 * ROWS :], "major", 3)
+    g_2 = shifted(g_3, "major", 3)
     u, squares = whole_call(
         assemble_kernel,
         [jax.ShapeDtypeStruct((RANK, W), BF16), jax.ShapeDtypeStruct((8, 128), F32)],
@@ -395,7 +392,7 @@
     other = shifted(chips, "core", 1)
     kept = (first_q, first_v, second_q, second_v)
     new_q, new_v, step_q, step_v, copy_q, copy_v, *kept = new_weights(
-        chips, other, u, pq, pv, (group, g_1, g_3, h_up, h_down), wq, wv, kept
+        chips, other, u, pq, pv, (group, g_1, g_2, g_3), wq, wv, kept
     )
     return (new_q, new_v, copy_q, copy_v, *kept, step_q, step_v)
 

time: 67.2 us -> 80.2 us (1.19)
  waiting for transfers between devices: 19.7 us -> 29.2 us
  starting transfers between devices: 36 us -> 39.3 us
    ppermute x21 -> x20, waiting for transfers between devices: 19.7 us -> 29.2 us  [shifted(): return lax.ppermute(array, AXES, shift_pairs(kind, offset))]
    ppermute x21 -> x20, starting transfers between devices: 36 us -> 39.3 us  [shifted(): return lax.ppermute(array, AXES, shift_pairs(kind, offset))]
  transfers between devices with their start and end apart: 21 -> 20, of which waited for: 9 -> 13; matrix products, arithmetic and copies ran while one was open for 0% -> 0% of each run, Pallas kernels for 3% -> 2%
where the time goes in v8:
time: 80.2 us; the launch traced here: 79.8 us
  starting transfers between devices  39.3 us (49%)
  waiting for transfers between devices  29.2 us (36%)
  Pallas kernels  10.5 us (13%)
    ppermute x20, starting transfers between devices, shifted(): return lax.ppermute(array, AXES, shift_pairs(kind, offset))  39.3 us
    ppermute x20, waiting for transfers between devices, shifted(): return lax.ppermute(array, AXES, shift_pairs(kind, offset))  29.2 us
    pallas_call x1, Pallas kernels, mix(): pl.pallas_call(mix_kernel, in_specs=[hbm] * len(operands), out_specs=[vme...  5.66 us
    pallas_call x1, Pallas kernels, new_weights(): pl.pallas_call(weight_kernel, in_specs=[vmem] * len(operands), out_specs=...  2.95 us
    pallas_call x5, Pallas kernels, whole_call(): pl.pallas_call(body, in_specs=[vmem] * len(operands), out_specs=[vmem] *...  1.86 us
  transfers between devices with their start and end apart: 20, of which 13 were waited for; matrix products, arithmetic and copies ran while one was open for 0% of the time, Pallas kernels for 2%

profile of v8, /device:TPU:1, one launch (start us, length us, event | category | flops | bytes accessed | tf_op | source)
XLA Modules:
  0.0 79.8 jit_solution(12629326263314127729)
XLA Ops:
  0.6 5.7 %mix.1 = (bf16[1536,512]{1,0:T(8,128)(2,1)S(1)}, bf16[160,768]{1,0:T(8,128)(2,1)S(1)}, bf16[2048,256]{1,0:T(8,128)(2,1)S(1)}, bf16[2048,256]{1,0:T(8,128)(2,1)S(...) custom-call(bf16[3072,2048]{1,0:T(8,128)(2,1)} %x.1, bf16[3072,256]{1,0:T(8,128)(2,1)} %cq.1, ...), custom_call_target="tpu_custom_call" | custom-call | flops 3221225472 | bytes 14000000 | tf_op jit(solution)/shard_map/mix/pallas_call | solution.py:162
  6.3 1.5 %collective-permute-start = (bf16[1536,512]{1,0:T(8,128)(2,1)S(1)}, bf16[1536,512]{1,0:T(8,128)(2,1)S(1)}, u32[]{:S(2)}, u32[]{:S(2)}) collective-permute-start(bf16[1536,512]{1,0:T(8,128)(2,1)S(1)} %get-tuple-element.37.mixed), channel_id=1, source_target_pairs={{0,1},{1,0},{2,3},{3,2},{4,5},{5,4},{6,7},{7,6},{8,9},{9,8},{10,11... | collective-permute-start | bytes 4718600 | tf_op jit(solution)/shard_map/ppermute | solution.py:59
  7.8 1.7 %collective-permute-start.7 = (bf16[160,768]{1,0:T(8,128)(2,1)S(1)}, bf16[160,768]{1,0:T(8,128)(2,1)S(1)}, u32[]{:S(2)}, u32[]{:S(2)}) collective-permute-start(bf16[160,768]{1,0:T(8,128)(2,1)S(1)} %get-tuple-element.44.k0.w0), channel_id=1, source_target_pairs={{0,8},{1,33},{2,10},{3,35},{4,12},{5,37},{6,14},{7,39},{8,16},{9,4... | collective-permute-start | bytes 737288 | tf_op jit(solution)/shard_map/ppermute | solution.py:59
  9.5 3.3 %collective-permute-start.8 = (bf16[160,768]{1,0:T(8,128)(2,1)S(1)}, bf16[160,768]{1,0:T(8,128)(2,1)S(1)}, u32[]{:S(2)}, u32[]{:S(2)}) collective-permute-start(bf16[160,768]{1,0:T(8,128)(2,1)S(1)} %get-tuple-element.44.k0.w0), channel_id=1, source_target_pairs={{0,16},{1,65},{2,18},{3,67},{4,20},{5,69},{6,22},{7,71},{8,24},{9,... | collective-permute-start | bytes 737288 | tf_op jit(solution)/shard_map/ppermute | solution.py:59
  12.8 0.7 collective-permute-start.9
  13.6 1.5 %shard_map.186 = (f32[64,768]{1,0:T(8,128)S(1)}, bf16[64,768]{1,0:T(8,128)(2,1)S(1)}, bf16[64,768]{1,0:T(8,128)(2,1)S(1)}, bf16[64,768]{1,0:T(8,128)(2,1)S(1)}) custom-call(bf16[1536,512]{1,0:T(8,128)(2,1)S(1)} %get-tuple-element.37.mixed, bf16[1536,512]{1,0:T(8,128)(2,1)S(1)} %collective-permute-done.swapped, bf16[3072,256]{1,0:T(8,128)(2,1)S(1)} %get-tuple-element.38.cq, ...), custom_call_target="tpu_custom_call" | custom-call | flops 1207959552 | bytes 1000000 | tf_op jit(solution)/shard_map/pallas_call | solution.py:216
  15.2 3.8 %collective-permute-done.8.k2.w2 = bf16[160,768]{1,0:T(8,128)(2,1)S(1)} collective-permute-done((bf16[160,768]{1,0:T(8,128)(2,1)S(1)}, bf16[160,768]{1,0:T(8,128)(2,1)S(1)}, u32[]{:S(2)}, u32[]{:S(2)}) %collective-permute-start.8) | collective-permute-done | bytes 245792 | tf_op jit(solution)/shard_map/ppermute | solution.py:59
  19.1 2.8 %collective-permute-start.18 = (bf16[512,768]{1,0:T(8,128)(2,1)S(1)}, bf16[512,768]{1,0:T(8,128)(2,1)S(1)}, u32[]{:S(2)}, u32[]{:S(2)}) collective-permute-start(bf16[512,768]{1,0:T(8,128)(2,1)S(1)} %shard_map.190.g0), channel_id=1, source_target_pairs={{0,96},{1,25},{2,98},{3,27},{4,100},{5,29},{6,102},{7,31},{8,104},... | collective-permute-start | bytes 2359304 | tf_op jit(solution)/shard_map/ppermute | solution.py:59
  21.9 8.9 %collective-permute-done.18.g3 = bf16[512,768]{1,0:T(8,128)(2,1)S(1)} collective-permute-done((bf16[512,768]{1,0:T(8,128)(2,1)S(1)}, bf16[512,768]{1,0:T(8,128)(2,1)S(1)}, u32[]{:S(2)}, u32[]{:S(2)}) %collective-permute-start.18) | collective-permute-done | bytes 786464 | tf_op jit(solution)/shard_map/ppermute | solution.py:59
  30.8 3.4 %collective-permute-start.19 = (bf16[512,768]{1,0:T(8,128)(2,1)S(1)}, bf16[512,768]{1,0:T(8,128)(2,1)S(1)}, u32[]{:S(2)}, u32[]{:S(2)}) collective-permute-start(bf16[512,768]{1,0:T(8,128)(2,1)S(1)} %collective-permute-done.18.g3), channel_id=1, source_target_pairs={{0,96},{1,25},{2,98},{3,27},{4,100},{5,29},{6,102},{7,31},{8,104},... | collective-permute-start | bytes 2359304 | tf_op jit(solution)/shard_map/ppermute | solution.py:59
  34.3 1.2 %collective-permute-start.2 = (bf16[64,768]{1,0:T(8,128)(2,1)S(1)}, bf16[64,768]{1,0:T(8,128)(2,1)S(1)}, u32[]{:S(2)}, u32[]{:S(2)}) collective-permute-start(bf16[64,768]{1,0:T(8,128)(2,1)S(1)} %get-tuple-element.42), channel_id=1, source_target_pairs={{0,64},{1,17},{2,66},{3,19},{4,68},{5,21},{6,70},{7,23},{8,72},{9,... | collective-permute-start | bytes 294920 | tf_op jit(solution)/shard_map/ppermute | solution.py:59
  35.4 1.5 %collective-permute-start.3 = (bf16[64,768]{1,0:T(8,128)(2,1)S(1)}, bf16[64,768]{1,0:T(8,128)(2,1)S(1)}, u32[]{:S(2)}, u32[]{:S(2)}) collective-permute-start(bf16[64,768]{1,0:T(8,128)(2,1)S(1)} %get-tuple-element.43), channel_id=1, source_target_pairs={{0,96},{1,25},{2,98},{3,27},{4,100},{5,29},{6,102},{7,31},{8,104},... | collective-permute-start | bytes 294920 | tf_op jit(solution)/shard_map/ppermute | solution.py:59
  36.9 3.1 %collective-permute-done.1.r1 = bf16[64,768]{1,0:T(8,128)(2,1)S(1)} collective-permute-done((bf16[64,768]{1,0:T(8,128)(2,1)S(1)}, bf16[64,768]{1,0:T(8,128)(2,1)S(1)}, u32[]{:S(2)}, u32[]{:S(2)}) %collective-permute-start.1) | collective-permute-done | bytes 98336 | tf_op jit(solution)/shard_map/ppermute | solution.py:59
  40.0 5.3 %collective-permute-done.3.r3 = bf16[64,768]{1,0:T(8,128)(2,1)S(1)} collective-permute-done((bf16[64,768]{1,0:T(8,128)(2,1)S(1)}, bf16[64,768]{1,0:T(8,128)(2,1)S(1)}, u32[]{:S(2)}, u32[]{:S(2)}) %collective-permute-start.3) | collective-permute-done | bytes 98336 | tf_op jit(solution)/shard_map/ppermute | solution.py:59
  45.3 0.6 collective-permute-start.4
  46.0 2.7 %collective-permute-start.5 = (bf16[64,768]{1,0:T(8,128)(2,1)S(1)}, bf16[64,768]{1,0:T(8,128)(2,1)S(1)}, u32[]{:S(2)}, u32[]{:S(2)}) collective-permute-start(bf16[64,768]{1,0:T(8,128)(2,1)S(1)} %shard_map.187.own), channel_id=1, source_target_pairs={{0,16},{1,65},{2,18},{3,67},{4,20},{5,69},{6,22},{7,71},{8,24},{9,... | collective-permute-start | bytes 294920 | tf_op jit(solution)/shard_map/ppermute | solution.py:59
  48.7 0.8 collective-permute-start.6
  49.4 0.7 collective-permute-done.4.r1
  50.1 1.6 %collective-permute-done.5.r2 = bf16[64,768]{1,0:T(8,128)(2,1)S(1)} collective-permute-done((bf16[64,768]{1,0:T(8,128)(2,1)S(1)}, bf16[64,768]{1,0:T(8,128)(2,1)S(1)}, u32[]{:S(2)}, u32[]{:S(2)}) %collective-permute-start.5) | collective-permute-done | bytes 98336 | tf_op jit(solution)/shard_map/ppermute | solution.py:59
  51.7 0.4 collective-permute-done.6.r3
  52.4 0.3 collective-permute-start.10
  52.7 4.3 %collective-permute-start.11 = (bf16[64,768]{1,0:T(8,128)(2,1)S(1)}, bf16[64,768]{1,0:T(8,128)(2,1)S(1)}, u32[]{:S(2)}, u32[]{:S(2)}) collective-permute-start(bf16[64,768]{1,0:T(8,128)(2,1)S(1)} %get-tuple-element.45.own), channel_id=1, source_target_pairs={{0,64},{1,17},{2,66},{3,19},{4,68},{5,21},{6,70},{7,23},{8,72},{9,... | collective-permute-start | bytes 294920 | tf_op jit(solution)/shard_map/ppermute | solution.py:59
  57.0 0.8 %collective-permute-done.10.r1 = bf16[64,768]{1,0:T(8,128)(2,1)S(1)} collective-permute-done((bf16[64,768]{1,0:T(8,128)(2,1)S(1)}, bf16[64,768]{1,0:T(8,128)(2,1)S(1)}, u32[]{:S(2)}, u32[]{:S(2)}) %collective-permute-start.10) | collective-permute-done | bytes 98336 | tf_op jit(solution)/shard_map/ppermute | solution.py:59
  57.9 2.2 %collective-permute-done.11.r2 = bf16[64,768]{1,0:T(8,128)(2,1)S(1)} collective-permute-done((bf16[64,768]{1,0:T(8,128)(2,1)S(1)}, bf16[64,768]{1,0:T(8,128)(2,1)S(1)}, u32[]{:S(2)}, u32[]{:S(2)}) %collective-permute-start.11) | collective-permute-done | bytes 98336 | tf_op jit(solution)/shard_map/ppermute | solution.py:59
  60.1 0.4 collective-permute-done.12.r3
  60.6 2.8 %collective-permute-start.13 = (f32[8,128]{1,0:T(8,128)S(1)}, f32[8,128]{1,0:T(8,128)S(1)}, u32[]{:S(2)}, u32[]{:S(2)}) collective-permute-start(f32[8,128]{1,0:T(8,128)S(1)} %get-tuple-element.46), channel_id=1, source_target_pairs={{0,4},{1,5},{2,6},{3,7},{4,0},{5,1},{6,2},{7,3},{8,12},{9,13},{10,... | collective-permute-start | bytes 12296 | tf_op jit(solution)/shard_map/ppermute | solution.py:59
  63.4 0.3 collective-permute-start.14
  63.7 2.4 %collective-permute-start.15 = (f32[8,128]{1,0:T(8,128)S(1)}, f32[8,128]{1,0:T(8,128)S(1)}, u32[]{:S(2)}, u32[]{:S(2)}) collective-permute-start(f32[8,128]{1,0:T(8,128)S(1)} %get-tuple-element.46), channel_id=1, source_target_pairs={{0,6},{1,7},{2,0},{3,1},{4,2},{5,3},{6,4},{7,5},{8,14},{9,15},{10,... | collective-permute-start | bytes 12296 | tf_op jit(solution)/shard_map/ppermute | solution.py:59
  66.1 1.0 %collective-permute-done.14 = f32[8,128]{1,0:T(8,128)S(1)} collective-permute-done((f32[8,128]{1,0:T(8,128)S(1)}, f32[8,128]{1,0:T(8,128)S(1)}, u32[]{:S(2)}, u32[]{:S(2)}) %collective-permute-start.14) | collective-permute-done | bytes 4128 | tf_op jit(solution)/shard_map/ppermute | solution.py:59
  67.1 8.9 %collective-permute-start.16 = (f32[8,128]{1,0:T(8,128)S(1)}, f32[8,128]{1,0:T(8,128)S(1)}, u32[]{:S(2)}, u32[]{:S(2)}) collective-permute-start(f32[8,128]{1,0:T(8,128)S(1)} %add_add_fusion.s_own), channel_id=1, source_target_pairs={{0,1},{1,0},{2,3},{3,2},{4,5},{5,4},{6,7},{7,6},{8,9},{9,8},{10,11... | collective-permute-start | bytes 12296 | tf_op jit(solution)/shard_map/ppermute | solution.py:59
  76.0 0.8 %collective-permute-done.16.s_other = f32[8,128]{1,0:T(8,128)S(1)} collective-permute-done((f32[8,128]{1,0:T(8,128)S(1)}, f32[8,128]{1,0:T(8,128)S(1)}, u32[]{:S(2)}, u32[]{:S(2)}) %collective-permute-start.16) | collective-permute-done | bytes 4128 | tf_op jit(solution)/shard_map/ppermute | solution.py:59
  76.9 3.0 %weights.1 = (f32[128,256]{1,0:T(8,128)}, f32[128,512]{1,0:T(8,128)}, f32[128,256]{1,0:T(8,128)}, f32[128,512]{1,0:T(8,128)}, bf16[2048,256]{1,0:T(8,128)(2,1)},...) custom-call(f32[8,128]{1,0:T(8,128)S(1)} %add_add_fusion.s_own, ...), custom_call_target="tpu_custom_call" | custom-call | flops 805306368 | bytes 12000000 | tf_op jit(solution)/shard_map/weights/pallas_call | solution.py:332
  (28 shorter events, 0.6 us)
Async XLA Ops:
  6.3 7.2 %collective-permute-start = (bf16[1536,512]{1,0:T(8,128)(2,1)S(1)}, bf16[1536,512]{1,0:T(8,128)(2,1)S(1)}, u32[]{:S(2)}, u32[]{:S(2)}) collective-permute-start(bf16[1536,512]{1,0:T(8,128)(2,1)S(1)} %get-tuple-element.37.mixed), channel_id=1, source_target_pairs={{0,1},{1,0},{2,3},{3,2},{4,5},{5,4},{6,7},{7,6},{8,9},{9,8},{10,11... | collective-permute-start | bytes 4718600 | tf_op jit(solution)/shard_map/ppermute | solution.py:59
  7.8 7.5 %collective-permute-start.7 = (bf16[160,768]{1,0:T(8,128)(2,1)S(1)}, bf16[160,768]{1,0:T(8,128)(2,1)S(1)}, u32[]{:S(2)}, u32[]{:S(2)}) collective-permute-start(bf16[160,768]{1,0:T(8,128)(2,1)S(1)} %get-tuple-element.44.k0.w0), channel_id=1, source_target_pairs={{0,8},{1,33},{2,10},{3,35},{4,12},{5,37},{6,14},{7,39},{8,16},{9,4... | collective-permute-start | bytes 737288 | tf_op jit(solution)/shard_map/ppermute | solution.py:59
  9.5 9.5 %collective-permute-start.8 = (bf16[160,768]{1,0:T(8,128)(2,1)S(1)}, bf16[160,768]{1,0:T(8,128)(2,1)S(1)}, u32[]{:S(2)}, u32[]{:S(2)}) collective-permute-start(bf16[160,768]{1,0:T(8,128)(2,1)S(1)} %get-tuple-element.44.k0.w0), channel_id=1, source_target_pairs={{0,16},{1,65},{2,18},{3,67},{4,20},{5,69},{6,22},{7,71},{8,24},{9,... | collective-permute-start | bytes 737288 | tf_op jit(solution)/shard_map/ppermute | solution.py:59
  12.8 6.2 %collective-permute-start.9 = (bf16[160,768]{1,0:T(8,128)(2,1)S(1)}, bf16[160,768]{1,0:T(8,128)(2,1)S(1)}, u32[]{:S(2)}, u32[]{:S(2)}) collective-permute-start(bf16[160,768]{1,0:T(8,128)(2,1)S(1)} %get-tuple-element.44.k0.w0), channel_id=1, source_target_pairs={{0,24},{1,97},{2,26},{3,99},{4,28},{5,101},{6,30},{7,103},{8,0},{9... | collective-permute-start | bytes 737288 | tf_op jit(solution)/shard_map/ppermute | solution.py:59
  15.0 37.1 %copy-start.2 = (f32[16,512]{1,0:T(8,128)S(1)}, f32[16,512]{1,0:T(8,128)}, u32[]{:S(2)}) copy-start(f32[16,512]{1,0:T(8,128)} %mv.3) | copy-start | bytes 98308
  15.1 37.1 %copy-start.3 = (f32[16,512]{1,0:T(8,128)S(1)}, f32[16,512]{1,0:T(8,128)}, u32[]{:S(2)}) copy-start(f32[16,512]{1,0:T(8,128)} %vv.3) | copy-start | bytes 98308
  15.1 37.1 %copy-start.4 = (f32[16,256]{1,0:T(8,128)S(1)}, f32[16,256]{1,0:T(8,128)}, u32[]{:S(2)}) copy-start(f32[16,256]{1,0:T(8,128)} %mq.3) | copy-start | bytes 49156
  15.1 37.1 %copy-start.5 = (f32[16,256]{1,0:T(8,128)S(1)}, f32[16,256]{1,0:T(8,128)}, u32[]{:S(2)}) copy-start(f32[16,256]{1,0:T(8,128)} %vq.3) | copy-start | bytes 49156
  19.0 57.8 %copy-start = (f32[128,512]{1,0:T(8,128)S(1)}, f32[128,512]{1,0:T(8,128)}, u32[]{:S(2)}) copy-start(f32[128,512]{1,0:T(8,128)} %wv.3) | copy-start | bytes 786436
  19.0 57.8 %copy-start.1 = (f32[128,256]{1,0:T(8,128)S(1)}, f32[128,256]{1,0:T(8,128)}, u32[]{:S(2)}) copy-start(f32[128,256]{1,0:T(8,128)} %wq.3) | copy-start | bytes 393220
  19.1 11.7 %collective-permute-start.18 = (bf16[512,768]{1,0:T(8,128)(2,1)S(1)}, bf16[512,768]{1,0:T(8,128)(2,1)S(1)}, u32[]{:S(2)}, u32[]{:S(2)}) collective-permute-start(bf16[512,768]{1,0:T(8,128)(2,1)S(1)} %shard_map.190.g0), channel_id=1, source_target_pairs={{0,96},{1,25},{2,98},{3,27},{4,100},{5,29},{6,102},{7,31},{8,104},... | collective-permute-start | bytes 2359304 | tf_op jit(solution)/shard_map/ppermute | solution.py:59
  21.9 55.0 %collective-permute-start.17 = (bf16[512,768]{1,0:T(8,128)(2,1)S(1)}, bf16[512,768]{1,0:T(8,128)(2,1)S(1)}, u32[]{:S(2)}, u32[]{:S(2)}) collective-permute-start(bf16[512,768]{1,0:T(8,128)(2,1)S(1)} %shard_map.190.g0), channel_id=1, source_target_pairs={{0,32},{1,9},{2,34},{3,11},{4,36},{5,13},{6,38},{7,15},{8,40},{9,1... | collective-permute-start | bytes 2359304 | tf_op jit(solution)/shard_map/ppermute | solution.py:59
  30.8 46.0 %collective-permute-start.19 = (bf16[512,768]{1,0:T(8,128)(2,1)S(1)}, bf16[512,768]{1,0:T(8,128)(2,1)S(1)}, u32[]{:S(2)}, u32[]{:S(2)}) collective-permute-start(bf16[512,768]{1,0:T(8,128)(2,1)S(1)} %collective-permute-done.18.g3), channel_id=1, source_target_pairs={{0,96},{1,25},{2,98},{3,27},{4,100},{5,29},{6,102},{7,31},{8,104},... | collective-permute-start | bytes 2359304 | tf_op jit(solution)/shard_map/ppermute | solution.py:59
  34.3 5.7 %collective-permute-start.1 = (bf16[64,768]{1,0:T(8,128)(2,1)S(1)}, bf16[64,768]{1,0:T(8,128)(2,1)S(1)}, u32[]{:S(2)}, u32[]{:S(2)}) collective-permute-start(bf16[64,768]{1,0:T(8,128)(2,1)S(1)} %get-tuple-element.41), channel_id=1, source_target_pairs={{0,32},{1,9},{2,34},{3,11},{4,36},{5,13},{6,38},{7,15},{8,40},{9,1... | collective-permute-start | bytes 294920 | tf_op jit(solution)/shard_map/ppermute | solution.py:59
  34.3 5.7 %collective-permute-start.2 = (bf16[64,768]{1,0:T(8,128)(2,1)S(1)}, bf16[64,768]{1,0:T(8,128)(2,1)S(1)}, u32[]{:S(2)}, u32[]{:S(2)}) collective-permute-start(bf16[64,768]{1,0:T(8,128)(2,1)S(1)} %get-tuple-element.42), channel_id=1, source_target_pairs={{0,64},{1,17},{2,66},{3,19},{4,68},{5,21},{6,70},{7,23},{8,72},{9,... | collective-permute-start | bytes 294920 | tf_op jit(solution)/shard_map/ppermute | solution.py:59
  35.4 9.9 %collective-permute-start.3 = (bf16[64,768]{1,0:T(8,128)(2,1)S(1)}, bf16[64,768]{1,0:T(8,128)(2,1)S(1)}, u32[]{:S(2)}, u32[]{:S(2)}) collective-permute-start(bf16[64,768]{1,0:T(8,128)(2,1)S(1)} %get-tuple-element.43), channel_id=1, source_target_pairs={{0,96},{1,25},{2,98},{3,27},{4,100},{5,29},{6,102},{7,31},{8,104},... | collective-permute-start | bytes 294920 | tf_op jit(solution)/shard_map/ppermute | solution.py:59
  45.3 4.7 %collective-permute-start.4 = (bf16[64,768]{1,0:T(8,128)(2,1)S(1)}, bf16[64,768]{1,0:T(8,128)(2,1)S(1)}, u32[]{:S(2)}, u32[]{:S(2)}) collective-permute-start(bf16[64,768]{1,0:T(8,128)(2,1)S(1)} %shard_map.187.own), channel_id=1, source_target_pairs={{0,8},{1,33},{2,10},{3,35},{4,12},{5,37},{6,14},{7,39},{8,16},{9,4... | collective-permute-start | bytes 294920 | tf_op jit(solution)/shard_map/ppermute | solution.py:59
  46.0 5.8 %collective-permute-start.5 = (bf16[64,768]{1,0:T(8,128)(2,1)S(1)}, bf16[64,768]{1,0:T(8,128)(2,1)S(1)}, u32[]{:S(2)}, u32[]{:S(2)}) collective-permute-start(bf16[64,768]{1,0:T(8,128)(2,1)S(1)} %shard_map.187.own), channel_id=1, source_target_pairs={{0,16},{1,65},{2,18},{3,67},{4,20},{5,69},{6,22},{7,71},{8,24},{9,... | collective-permute-start | bytes 294920 | tf_op jit(solution)/shard_map/ppermute | solution.py:59
  48.7 3.5 %collective-permute-start.6 = (bf16[64,768]{1,0:T(8,128)(2,1)S(1)}, bf16[64,768]{1,0:T(8,128)(2,1)S(1)}, u32[]{:S(2)}, u32[]{:S(2)}) collective-permute-start(bf16[64,768]{1,0:T(8,128)(2,1)S(1)} %shard_map.187.own), channel_id=1, source_target_pairs={{0,24},{1,97},{2,26},{3,99},{4,28},{5,101},{6,30},{7,103},{8,0},{9... | collective-permute-start | bytes 294920 | tf_op jit(solution)/shard_map/ppermute | solution.py:59
  52.4 5.5 %collective-permute-start.10 = (bf16[64,768]{1,0:T(8,128)(2,1)S(1)}, bf16[64,768]{1,0:T(8,128)(2,1)S(1)}, u32[]{:S(2)}, u32[]{:S(2)}) collective-permute-start(bf16[64,768]{1,0:T(8,128)(2,1)S(1)} %get-tuple-element.45.own), channel_id=1, source_target_pairs={{0,32},{1,9},{2,34},{3,11},{4,36},{5,13},{6,38},{7,15},{8,40},{9,1... | collective-permute-start | bytes 294920 | tf_op jit(solution)/shard_map/ppermute | solution.py:59
  52.7 7.4 %collective-permute-start.11 = (bf16[64,768]{1,0:T(8,128)(2,1)S(1)}, bf16[64,768]{1,0:T(8,128)(2,1)S(1)}, u32[]{:S(2)}, u32[]{:S(2)}) collective-permute-start(bf16[64,768]{1,0:T(8,128)(2,1)S(1)} %get-tuple-element.45.own), channel_id=1, source_target_pairs={{0,64},{1,17},{2,66},{3,19},{4,68},{5,21},{6,70},{7,23},{8,72},{9,... | collective-permute-start | bytes 294920 | tf_op jit(solution)/shard_map/ppermute | solution.py:59
  57.0 3.5 %collective-permute-start.12 = (bf16[64,768]{1,0:T(8,128)(2,1)S(1)}, bf16[64,768]{1,0:T(8,128)(2,1)S(1)}, u32[]{:S(2)}, u32[]{:S(2)}) collective-permute-start(bf16[64,768]{1,0:T(8,128)(2,1)S(1)} %get-tuple-element.45.own), channel_id=1, source_target_pairs={{0,96},{1,25},{2,98},{3,27},{4,100},{5,29},{6,102},{7,31},{8,104},... | collective-permute-start | bytes 294920 | tf_op jit(solution)/shard_map/ppermute | solution.py:59
  60.6 5.5 %collective-permute-start.13 = (f32[8,128]{1,0:T(8,128)S(1)}, f32[8,128]{1,0:T(8,128)S(1)}, u32[]{:S(2)}, u32[]{:S(2)}) collective-permute-start(f32[8,128]{1,0:T(8,128)S(1)} %get-tuple-element.46), channel_id=1, source_target_pairs={{0,4},{1,5},{2,6},{3,7},{4,0},{5,1},{6,2},{7,3},{8,12},{9,13},{10,... | collective-permute-start | bytes 12296 | tf_op jit(solution)/shard_map/ppermute | solution.py:59
  63.4 3.7 %collective-permute-start.14 = (f32[8,128]{1,0:T(8,128)S(1)}, f32[8,128]{1,0:T(8,128)S(1)}, u32[]{:S(2)}, u32[]{:S(2)}) collective-permute-start(f32[8,128]{1,0:T(8,128)S(1)} %get-tuple-element.46), channel_id=1, source_target_pairs={{0,2},{1,3},{2,4},{3,5},{4,6},{5,7},{6,0},{7,1},{8,10},{9,11},{10,... | collective-permute-start | bytes 12296 | tf_op jit(solution)/shard_map/ppermute | solution.py:59
  63.7 3.4 %collective-permute-start.15 = (f32[8,128]{1,0:T(8,128)S(1)}, f32[8,128]{1,0:T(8,128)S(1)}, u32[]{:S(2)}, u32[]{:S(2)}) collective-permute-start(f32[8,128]{1,0:T(8,128)S(1)} %get-tuple-element.46), channel_id=1, source_target_pairs={{0,6},{1,7},{2,0},{3,1},{4,2},{5,3},{6,4},{7,5},{8,14},{9,15},{10,... | collective-permute-start | bytes 12296 | tf_op jit(solution)/shard_map/ppermute | solution.py:59
  67.1 9.8 %collective-permute-start.16 = (f32[8,128]{1,0:T(8,128)S(1)}, f32[8,128]{1,0:T(8,128)S(1)}, u32[]{:S(2)}, u32[]{:S(2)}) collective-permute-start(f32[8,128]{1,0:T(8,128)S(1)} %add_add_fusion.s_own), channel_id=1, source_target_pairs={{0,1},{1,0},{2,3},{3,2},{4,5},{5,4},{6,7},{7,6},{8,9},{9,8},{10,11... | collective-permute-start | bytes 12296 | tf_op jit(solution)/shard_map/ppermute | solution.py:59

commit v9 on v8

--- a/solution.py
+++ b/solution.py
@@ -365,14 +365,14 @@
         flops=2 * inputs.shape[0] * RANK * W,
     )
     r_1, r_2, r_3 = to_all("major", parts)
-    group, = whole_call(
-        group_kernel, [jax.ShapeDtypeStruct((4 * ROWS, W), BF16)], (w16, w_1, w_2, w_3, own)
-    )
-    g_1, g_3 = shifted(group, "major", 1), shifted(group, "major", 3)
     message, = whole_call(
         partial_kernel, [jax.ShapeDtypeStruct((64, W), BF16)], (own, r_1, r_2, r_3)
     )
     m_1, m_2, m_3 = to_all("minor", (message,) * 3)
+    group, = whole_call(
+        group_kernel, [jax.ShapeDtypeStruct((4 * ROWS, W), BF16)], (w16, w_1, w_2, w_3, message)
+    )
+    g_3 = shifted(group, "major", 3)
     small = lambda n: jax.ShapeDtypeStruct((16, n), F32)
     u_own, first_q, first_v, second_q, second_v = whole_call(
         update_kernel,
@@ -382,6 +382,7 @@
     )
     u_1, u_2, u_3 = to_all("major", (u_own,) * 3)
     g_2 = shifted(g_3, "major", 3)
+    g_1 = shifted(group, "major", 1)
     u, squares = whole_call(
         assemble_kernel,
         [jax.ShapeDtypeStruct((RANK, W), BF16), jax.ShapeDtypeStruct((8, 128), F32)],

time: 80.2 us -> 71.2 us (0.89)
  waiting for transfers between devices: 29.2 us -> 22.2 us
  starting transfers between devices: 39.3 us -> 37.6 us
    ppermute x20, waiting for transfers between devices: 29.2 us -> 22.2 us  [shifted(): return lax.ppermute(array, AXES, shift_pairs(kind, offset))]
    ppermute x20, starting transfers between devices: 39.3 us -> 37.6 us  [shifted(): return lax.ppermute(array, AXES, shift_pairs(kind, offset))]
  transfers between devices with their start and end apart: 20 -> 20, of which waited for: 13 -> 11; matrix products, arithmetic and copies ran while one was open for 0% -> 0% of each run, Pallas kernels for 2% -> 3%
where the time goes in v9:
time: 71.2 us; the launch traced here: 71.1 us
  starting transfers between devices  37.6 us (53%)
  waiting for transfers between devices  22.2 us (31%)
  Pallas kernels  10.5 us (15%)
  between operations  0.79 us (1%)
    ppermute x20, starting transfers between devices, shifted(): return lax.ppermute(array, AXES, shift_pairs(kind, offset))  37.6 us
    ppermute x20, waiting for transfers between devices, shifted(): return lax.ppermute(array, AXES, shift_pairs(kind, offset))  22.2 us
    pallas_call x1, Pallas kernels, mix(): pl.pallas_call(mix_kernel, in_specs=[hbm] * len(operands), out_specs=[vme...  5.66 us
    pallas_call x1, Pallas kernels, new_weights(): pl.pallas_call(weight_kernel, in_specs=[vmem] * len(operands), out_specs=...  2.96 us
    pallas_call x5, Pallas kernels, whole_call(): pl.pallas_call(body, in_specs=[vmem] * len(operands), out_specs=[vmem] *...  1.87 us
  transfers between devices with their start and end apart: 20, of which 11 were waited for; matrix products, arithmetic and copies ran while one was open for 0% of the time, Pallas kernels for 3%

profile of v9, /device:TPU:1, one launch (start us, length us, event | category | flops | bytes accessed | tf_op | source)
XLA Modules:
  0.0 71.1 jit_solution(8897092145112703113)
XLA Ops:
  0.6 5.7 %mix.1 = (bf16[1536,512]{1,0:T(8,128)(2,1)S(1)}, bf16[160,768]{1,0:T(8,128)(2,1)S(1)}, bf16[2048,256]{1,0:T(8,128)(2,1)S(1)}, bf16[2048,256]{1,0:T(8,128)(2,1)S(...) custom-call(bf16[3072,2048]{1,0:T(8,128)(2,1)} %x.1, bf16[3072,256]{1,0:T(8,128)(2,1)} %cq.1, ...), custom_call_target="tpu_custom_call" | custom-call | flops 3221225472 | bytes 14000000 | tf_op jit(solution)/shard_map/mix/pallas_call | solution.py:162
  6.3 1.5 %collective-permute-start = (bf16[1536,512]{1,0:T(8,128)(2,1)S(1)}, bf16[1536,512]{1,0:T(8,128)(2,1)S(1)}, u32[]{:S(2)}, u32[]{:S(2)}) collective-permute-start(bf16[1536,512]{1,0:T(8,128)(2,1)S(1)} %get-tuple-element.37.mixed), channel_id=1, source_target_pairs={{0,1},{1,0},{2,3},{3,2},{4,5},{5,4},{6,7},{7,6},{8,9},{9,8},{10,11... | collective-permute-start | bytes 4718600 | tf_op jit(solution)/shard_map/ppermute | solution.py:59
  7.8 1.7 %collective-permute-start.7 = (bf16[160,768]{1,0:T(8,128)(2,1)S(1)}, bf16[160,768]{1,0:T(8,128)(2,1)S(1)}, u32[]{:S(2)}, u32[]{:S(2)}) collective-permute-start(bf16[160,768]{1,0:T(8,128)(2,1)S(1)} %get-tuple-element.44.k0.w0), channel_id=1, source_target_pairs={{0,8},{1,33},{2,10},{3,35},{4,12},{5,37},{6,14},{7,39},{8,16},{9,4... | collective-permute-start | bytes 737288 | tf_op jit(solution)/shard_map/ppermute | solution.py:59
  9.5 3.3 %collective-permute-start.8 = (bf16[160,768]{1,0:T(8,128)(2,1)S(1)}, bf16[160,768]{1,0:T(8,128)(2,1)S(1)}, u32[]{:S(2)}, u32[]{:S(2)}) collective-permute-start(bf16[160,768]{1,0:T(8,128)(2,1)S(1)} %get-tuple-element.44.k0.w0), channel_id=1, source_target_pairs={{0,16},{1,65},{2,18},{3,67},{4,20},{5,69},{6,22},{7,71},{8,24},{9,... | collective-permute-start | bytes 737288 | tf_op jit(solution)/shard_map/ppermute | solution.py:59
  12.8 0.7 %collective-permute-start.9 = (bf16[160,768]{1,0:T(8,128)(2,1)S(1)}, bf16[160,768]{1,0:T(8,128)(2,1)S(1)}, u32[]{:S(2)}, u32[]{:S(2)}) collective-permute-start(bf16[160,768]{1,0:T(8,128)(2,1)S(1)} %get-tuple-element.44.k0.w0), channel_id=1, source_target_pairs={{0,24},{1,97},{2,26},{3,99},{4,28},{5,101},{6,30},{7,103},{8,0},{9... | collective-permute-start | bytes 737288 | tf_op jit(solution)/shard_map/ppermute | solution.py:59
  13.6 1.5 %shard_map.186 = (f32[64,768]{1,0:T(8,128)S(1)}, bf16[64,768]{1,0:T(8,128)(2,1)S(1)}, bf16[64,768]{1,0:T(8,128)(2,1)S(1)}, bf16[64,768]{1,0:T(8,128)(2,1)S(1)}) custom-call(bf16[1536,512]{1,0:T(8,128)(2,1)S(1)} %get-tuple-element.37.mixed, bf16[1536,512]{1,0:T(8,128)(2,1)S(1)} %collective-permute-done.swapped, bf16[3072,256]{1,0:T(8,128)(2,1)S(1)} %get-tuple-element.38.cq, ...), custom_call_target="tpu_custom_call" | custom-call | flops 1207959552 | bytes 1000000 | tf_op jit(solution)/shard_map/pallas_call | solution.py:216
  15.1 1.4 %collective-permute-start.1 = (bf16[64,768]{1,0:T(8,128)(2,1)S(1)}, bf16[64,768]{1,0:T(8,128)(2,1)S(1)}, u32[]{:S(2)}, u32[]{:S(2)}) collective-permute-start(bf16[64,768]{1,0:T(8,128)(2,1)S(1)} %get-tuple-element.41), channel_id=1, source_target_pairs={{0,32},{1,9},{2,34},{3,11},{4,36},{5,13},{6,38},{7,15},{8,40},{9,1... | collective-permute-start | bytes 294920 | tf_op jit(solution)/shard_map/ppermute | solution.py:59
  16.5 2.6 %collective-permute-start.2 = (bf16[64,768]{1,0:T(8,128)(2,1)S(1)}, bf16[64,768]{1,0:T(8,128)(2,1)S(1)}, u32[]{:S(2)}, u32[]{:S(2)}) collective-permute-start(bf16[64,768]{1,0:T(8,128)(2,1)S(1)} %get-tuple-element.42), channel_id=1, source_target_pairs={{0,64},{1,17},{2,66},{3,19},{4,68},{5,21},{6,70},{7,23},{8,72},{9,... | collective-permute-start | bytes 294920 | tf_op jit(solution)/shard_map/ppermute | solution.py:59
  19.1 0.8 %collective-permute-done.1.r1 = bf16[64,768]{1,0:T(8,128)(2,1)S(1)} collective-permute-done((bf16[64,768]{1,0:T(8,128)(2,1)S(1)}, bf16[64,768]{1,0:T(8,128)(2,1)S(1)}, u32[]{:S(2)}, u32[]{:S(2)}) %collective-permute-start.1) | collective-permute-done | bytes 98336 | tf_op jit(solution)/shard_map/ppermute | solution.py:59
  19.9 1.8 %collective-permute-start.3 = (bf16[64,768]{1,0:T(8,128)(2,1)S(1)}, bf16[64,768]{1,0:T(8,128)(2,1)S(1)}, u32[]{:S(2)}, u32[]{:S(2)}) collective-permute-start(bf16[64,768]{1,0:T(8,128)(2,1)S(1)} %get-tuple-element.43), channel_id=1, source_target_pairs={{0,96},{1,25},{2,98},{3,27},{4,100},{5,29},{6,102},{7,31},{8,104},... | collective-permute-start | bytes 294920 | tf_op jit(solution)/shard_map/ppermute | solution.py:59
  21.7 0.5 collective-permute-done.2.r2
  22.1 1.5 %collective-permute-done.3.r3 = bf16[64,768]{1,0:T(8,128)(2,1)S(1)} collective-permute-done((bf16[64,768]{1,0:T(8,128)(2,1)S(1)}, bf16[64,768]{1,0:T(8,128)(2,1)S(1)}, u32[]{:S(2)}, u32[]{:S(2)}) %collective-permute-start.3) | collective-permute-done | bytes 98336 | tf_op jit(solution)/shard_map/ppermute | solution.py:59
  23.8 2.7 %collective-permute-start.18 = (bf16[512,768]{1,0:T(8,128)(2,1)S(1)}, bf16[512,768]{1,0:T(8,128)(2,1)S(1)}, u32[]{:S(2)}, u32[]{:S(2)}) collective-permute-start(bf16[512,768]{1,0:T(8,128)(2,1)S(1)} %shard_map.190.g0), channel_id=1, source_target_pairs={{0,96},{1,25},{2,98},{3,27},{4,100},{5,29},{6,102},{7,31},{8,104},... | collective-permute-start | bytes 2359304 | tf_op jit(solution)/shard_map/ppermute | solution.py:59
  26.6 8.9 %collective-permute-done.18.g3 = bf16[512,768]{1,0:T(8,128)(2,1)S(1)} collective-permute-done((bf16[512,768]{1,0:T(8,128)(2,1)S(1)}, bf16[512,768]{1,0:T(8,128)(2,1)S(1)}, u32[]{:S(2)}, u32[]{:S(2)}) %collective-permute-start.18) | collective-permute-done | bytes 786464 | tf_op jit(solution)/shard_map/ppermute | solution.py:59
  35.5 3.4 %collective-permute-start.19 = (bf16[512,768]{1,0:T(8,128)(2,1)S(1)}, bf16[512,768]{1,0:T(8,128)(2,1)S(1)}, u32[]{:S(2)}, u32[]{:S(2)}) collective-permute-start(bf16[512,768]{1,0:T(8,128)(2,1)S(1)} %collective-permute-done.18.g3), channel_id=1, source_target_pairs={{0,96},{1,25},{2,98},{3,27},{4,100},{5,29},{6,102},{7,31},{8,104},... | collective-permute-start | bytes 2359304 | tf_op jit(solution)/shard_map/ppermute | solution.py:59
  38.9 0.4 collective-permute-start.4
  39.3 3.2 %collective-permute-start.5 = (bf16[64,768]{1,0:T(8,128)(2,1)S(1)}, bf16[64,768]{1,0:T(8,128)(2,1)S(1)}, u32[]{:S(2)}, u32[]{:S(2)}) collective-permute-start(bf16[64,768]{1,0:T(8,128)(2,1)S(1)} %shard_map.187.own.after), channel_id=1, source_target_pairs={{0,16},{1,65},{2,18},{3,67},{4,20},{5,69},{6,22},{7,71},{8,24},{9,... | collective-permute-start | bytes 294920 | tf_op jit(solution)/shard_map/ppermute | solution.py:59
  42.7 1.0 %collective-permute-done.4.r1 = bf16[64,768]{1,0:T(8,128)(2,1)S(1)} collective-permute-done((bf16[64,768]{1,0:T(8,128)(2,1)S(1)}, bf16[64,768]{1,0:T(8,128)(2,1)S(1)}, u32[]{:S(2)}, u32[]{:S(2)}) %collective-permute-start.4) | collective-permute-done | bytes 98336 | tf_op jit(solution)/shard_map/ppermute | solution.py:59
  43.7 1.9 %collective-permute-done.5.r2 = bf16[64,768]{1,0:T(8,128)(2,1)S(1)} collective-permute-done((bf16[64,768]{1,0:T(8,128)(2,1)S(1)}, bf16[64,768]{1,0:T(8,128)(2,1)S(1)}, u32[]{:S(2)}, u32[]{:S(2)}) %collective-permute-start.5) | collective-permute-done | bytes 98336 | tf_op jit(solution)/shard_map/ppermute | solution.py:59
  45.6 2.0 %collective-permute-done.6.r3 = bf16[64,768]{1,0:T(8,128)(2,1)S(1)} collective-permute-done((bf16[64,768]{1,0:T(8,128)(2,1)S(1)}, bf16[64,768]{1,0:T(8,128)(2,1)S(1)}, u32[]{:S(2)}, u32[]{:S(2)}) %collective-permute-start.6) | collective-permute-done | bytes 98336 | tf_op jit(solution)/shard_map/ppermute | solution.py:59
  47.6 0.2 shard_map.188
  47.9 1.1 %collective-permute-start.11 = (bf16[64,768]{1,0:T(8,128)(2,1)S(1)}, bf16[64,768]{1,0:T(8,128)(2,1)S(1)}, u32[]{:S(2)}, u32[]{:S(2)}) collective-permute-start(bf16[64,768]{1,0:T(8,128)(2,1)S(1)} %get-tuple-element.45.own), channel_id=1, source_target_pairs={{0,64},{1,17},{2,66},{3,19},{4,68},{5,21},{6,70},{7,23},{8,72},{9,... | collective-permute-start | bytes 294920 | tf_op jit(solution)/shard_map/ppermute | solution.py:59
  49.0 1.6 %collective-permute-start.12 = (bf16[64,768]{1,0:T(8,128)(2,1)S(1)}, bf16[64,768]{1,0:T(8,128)(2,1)S(1)}, u32[]{:S(2)}, u32[]{:S(2)}) collective-permute-start(bf16[64,768]{1,0:T(8,128)(2,1)S(1)} %get-tuple-element.45.own), channel_id=1, source_target_pairs={{0,96},{1,25},{2,98},{3,27},{4,100},{5,29},{6,102},{7,31},{8,104},... | collective-permute-start | bytes 294920 | tf_op jit(solution)/shard_map/ppermute | solution.py:59
  50.6 3.1 %collective-permute-done.10.r1 = bf16[64,768]{1,0:T(8,128)(2,1)S(1)} collective-permute-done((bf16[64,768]{1,0:T(8,128)(2,1)S(1)}, bf16[64,768]{1,0:T(8,128)(2,1)S(1)}, u32[]{:S(2)}, u32[]{:S(2)}) %collective-permute-start.10) | collective-permute-done | bytes 98336 | tf_op jit(solution)/shard_map/ppermute | solution.py:59
  53.6 0.6 collective-permute-done.12.r3
  54.4 2.8 %collective-permute-start.13 = (f32[8,128]{1,0:T(8,128)S(1)}, f32[8,128]{1,0:T(8,128)S(1)}, u32[]{:S(2)}, u32[]{:S(2)}) collective-permute-start(f32[8,128]{1,0:T(8,128)S(1)} %get-tuple-element.46), channel_id=1, source_target_pairs={{0,4},{1,5},{2,6},{3,7},{4,0},{5,1},{6,2},{7,3},{8,12},{9,13},{10,... | collective-permute-start | bytes 12296 | tf_op jit(solution)/shard_map/ppermute | solution.py:59
  57.2 0.3 collective-permute-start.14
  57.5 2.4 %collective-permute-start.15 = (f32[8,128]{1,0:T(8,128)S(1)}, f32[8,128]{1,0:T(8,128)S(1)}, u32[]{:S(2)}, u32[]{:S(2)}) collective-permute-start(f32[8,128]{1,0:T(8,128)S(1)} %get-tuple-element.46), channel_id=1, source_target_pairs={{0,6},{1,7},{2,0},{3,1},{4,2},{5,3},{6,4},{7,5},{8,14},{9,15},{10,... | collective-permute-start | bytes 12296 | tf_op jit(solution)/shard_map/ppermute | solution.py:59
  59.9 1.0 %collective-permute-done.14 = f32[8,128]{1,0:T(8,128)S(1)} collective-permute-done((f32[8,128]{1,0:T(8,128)S(1)}, f32[8,128]{1,0:T(8,128)S(1)}, u32[]{:S(2)}, u32[]{:S(2)}) %collective-permute-start.14) | collective-permute-done | bytes 4128 | tf_op jit(solution)/shard_map/ppermute | solution.py:59
  60.9 6.4 %collective-permute-start.16 = (f32[8,128]{1,0:T(8,128)S(1)}, f32[8,128]{1,0:T(8,128)S(1)}, u32[]{:S(2)}, u32[]{:S(2)}) collective-permute-start(f32[8,128]{1,0:T(8,128)S(1)} %add_add_fusion.s_own), channel_id=1, source_target_pairs={{0,1},{1,0},{2,3},{3,2},{4,5},{5,4},{6,7},{7,6},{8,9},{9,8},{10,11... | collective-permute-start | bytes 12296 | tf_op jit(solution)/shard_map/ppermute | solution.py:59
  67.3 0.8 %collective-permute-done.16.s_other = f32[8,128]{1,0:T(8,128)S(1)} collective-permute-done((f32[8,128]{1,0:T(8,128)S(1)}, f32[8,128]{1,0:T(8,128)S(1)}, u32[]{:S(2)}, u32[]{:S(2)}) %collective-permute-start.16) | collective-permute-done | bytes 4128 | tf_op jit(solution)/shard_map/ppermute | solution.py:59
  68.1 3.0 %weights.1 = (f32[128,256]{1,0:T(8,128)}, f32[128,512]{1,0:T(8,128)}, f32[128,256]{1,0:T(8,128)}, f32[128,512]{1,0:T(8,128)}, bf16[2048,256]{1,0:T(8,128)(2,1)},...) custom-call(f32[8,128]{1,0:T(8,128)S(1)} %add_add_fusion.s_own, ...), custom_call_target="tpu_custom_call" | custom-call | flops 805306368 | bytes 12000000 | tf_op jit(solution)/shard_map/weights/pallas_call | solution.py:332
  (28 shorter events, 0.5 us)
Async XLA Ops:
  6.3 7.2 %collective-permute-start = (bf16[1536,512]{1,0:T(8,128)(2,1)S(1)}, bf16[1536,512]{1,0:T(8,128)(2,1)S(1)}, u32[]{:S(2)}, u32[]{:S(2)}) collective-permute-start(bf16[1536,512]{1,0:T(8,128)(2,1)S(1)} %get-tuple-element.37.mixed), channel_id=1, source_target_pairs={{0,1},{1,0},{2,3},{3,2},{4,5},{5,4},{6,7},{7,6},{8,9},{9,8},{10,11... | collective-permute-start | bytes 4718600 | tf_op jit(solution)/shard_map/ppermute | solution.py:59
  7.8 15.9 %collective-permute-start.7 = (bf16[160,768]{1,0:T(8,128)(2,1)S(1)}, bf16[160,768]{1,0:T(8,128)(2,1)S(1)}, u32[]{:S(2)}, u32[]{:S(2)}) collective-permute-start(bf16[160,768]{1,0:T(8,128)(2,1)S(1)} %get-tuple-element.44.k0.w0), channel_id=1, source_target_pairs={{0,8},{1,33},{2,10},{3,35},{4,12},{5,37},{6,14},{7,39},{8,16},{9,4... | collective-permute-start | bytes 737288 | tf_op jit(solution)/shard_map/ppermute | solution.py:59
  9.5 14.2 %collective-permute-start.8 = (bf16[160,768]{1,0:T(8,128)(2,1)S(1)}, bf16[160,768]{1,0:T(8,128)(2,1)S(1)}, u32[]{:S(2)}, u32[]{:S(2)}) collective-permute-start(bf16[160,768]{1,0:T(8,128)(2,1)S(1)} %get-tuple-element.44.k0.w0), channel_id=1, source_target_pairs={{0,16},{1,65},{2,18},{3,67},{4,20},{5,69},{6,22},{7,71},{8,24},{9,... | collective-permute-start | bytes 737288 | tf_op jit(solution)/shard_map/ppermute | solution.py:59
  12.8 10.9 %collective-permute-start.9 = (bf16[160,768]{1,0:T(8,128)(2,1)S(1)}, bf16[160,768]{1,0:T(8,128)(2,1)S(1)}, u32[]{:S(2)}, u32[]{:S(2)}) collective-permute-start(bf16[160,768]{1,0:T(8,128)(2,1)S(1)} %get-tuple-element.44.k0.w0), channel_id=1, source_target_pairs={{0,24},{1,97},{2,26},{3,99},{4,28},{5,101},{6,30},{7,103},{8,0},{9... | collective-permute-start | bytes 737288 | tf_op jit(solution)/shard_map/ppermute | solution.py:59
  15.0 32.6 %copy-start.2 = (f32[16,512]{1,0:T(8,128)S(1)}, f32[16,512]{1,0:T(8,128)}, u32[]{:S(2)}) copy-start(f32[16,512]{1,0:T(8,128)} %mv.3) | copy-start | bytes 98308
  15.1 32.6 %copy-start.3 = (f32[16,512]{1,0:T(8,128)S(1)}, f32[16,512]{1,0:T(8,128)}, u32[]{:S(2)}) copy-start(f32[16,512]{1,0:T(8,128)} %vv.3) | copy-start | bytes 98308
  15.1 32.6 %copy-start.4 = (f32[16,256]{1,0:T(8,128)S(1)}, f32[16,256]{1,0:T(8,128)}, u32[]{:S(2)}) copy-start(f32[16,256]{1,0:T(8,128)} %mq.3) | copy-start | bytes 49156
  15.1 32.5 %copy-start.5 = (f32[16,256]{1,0:T(8,128)S(1)}, f32[16,256]{1,0:T(8,128)}, u32[]{:S(2)}) copy-start(f32[16,256]{1,0:T(8,128)} %vq.3) | copy-start | bytes 49156
  15.1 4.8 %collective-permute-start.1 = (bf16[64,768]{1,0:T(8,128)(2,1)S(1)}, bf16[64,768]{1,0:T(8,128)(2,1)S(1)}, u32[]{:S(2)}, u32[]{:S(2)}) collective-permute-start(bf16[64,768]{1,0:T(8,128)(2,1)S(1)} %get-tuple-element.41), channel_id=1, source_target_pairs={{0,32},{1,9},{2,34},{3,11},{4,36},{5,13},{6,38},{7,15},{8,40},{9,1... | collective-permute-start | bytes 294920 | tf_op jit(solution)/shard_map/ppermute | solution.py:59
  16.5 5.7 %collective-permute-start.2 = (bf16[64,768]{1,0:T(8,128)(2,1)S(1)}, bf16[64,768]{1,0:T(8,128)(2,1)S(1)}, u32[]{:S(2)}, u32[]{:S(2)}) collective-permute-start(bf16[64,768]{1,0:T(8,128)(2,1)S(1)} %get-tuple-element.42), channel_id=1, source_target_pairs={{0,64},{1,17},{2,66},{3,19},{4,68},{5,21},{6,70},{7,23},{8,72},{9,... | collective-permute-start | bytes 294920 | tf_op jit(solution)/shard_map/ppermute | solution.py:59
  19.9 3.8 %collective-permute-start.3 = (bf16[64,768]{1,0:T(8,128)(2,1)S(1)}, bf16[64,768]{1,0:T(8,128)(2,1)S(1)}, u32[]{:S(2)}, u32[]{:S(2)}) collective-permute-start(bf16[64,768]{1,0:T(8,128)(2,1)S(1)} %get-tuple-element.43), channel_id=1, source_target_pairs={{0,96},{1,25},{2,98},{3,27},{4,100},{5,29},{6,102},{7,31},{8,104},... | collective-permute-start | bytes 294920 | tf_op jit(solution)/shard_map/ppermute | solution.py:59
  23.7 44.4 %copy-start = (f32[128,512]{1,0:T(8,128)S(1)}, f32[128,512]{1,0:T(8,128)}, u32[]{:S(2)}) copy-start(f32[128,512]{1,0:T(8,128)} %wv.3) | copy-start | bytes 786436
  23.7 44.4 %copy-start.1 = (f32[128,256]{1,0:T(8,128)S(1)}, f32[128,256]{1,0:T(8,128)}, u32[]{:S(2)}) copy-start(f32[128,256]{1,0:T(8,128)} %wq.3) | copy-start | bytes 393220
  23.8 11.7 %collective-permute-start.18 = (bf16[512,768]{1,0:T(8,128)(2,1)S(1)}, bf16[512,768]{1,0:T(8,128)(2,1)S(1)}, u32[]{:S(2)}, u32[]{:S(2)}) collective-permute-start(bf16[512,768]{1,0:T(8,128)(2,1)S(1)} %shard_map.190.g0), channel_id=1, source_target_pairs={{0,96},{1,25},{2,98},{3,27},{4,100},{5,29},{6,102},{7,31},{8,104},... | collective-permute-start | bytes 2359304 | tf_op jit(solution)/shard_map/ppermute | solution.py:59
  26.6 41.5 %collective-permute-start.17 = (bf16[512,768]{1,0:T(8,128)(2,1)S(1)}, bf16[512,768]{1,0:T(8,128)(2,1)S(1)}, u32[]{:S(2)}, u32[]{:S(2)}) collective-permute-start(bf16[512,768]{1,0:T(8,128)(2,1)S(1)} %shard_map.190.g0), channel_id=1, source_target_pairs={{0,32},{1,9},{2,34},{3,11},{4,36},{5,13},{6,38},{7,15},{8,40},{9,1... | collective-permute-start | bytes 2359304 | tf_op jit(solution)/shard_map/ppermute | solution.py:59
  35.5 32.6 %collective-permute-start.19 = (bf16[512,768]{1,0:T(8,128)(2,1)S(1)}, bf16[512,768]{1,0:T(8,128)(2,1)S(1)}, u32[]{:S(2)}, u32[]{:S(2)}) collective-permute-start(bf16[512,768]{1,0:T(8,128)(2,1)S(1)} %collective-permute-done.18.g3), channel_id=1, source_target_pairs={{0,96},{1,25},{2,98},{3,27},{4,100},{5,29},{6,102},{7,31},{8,104},... | collective-permute-start | bytes 2359304 | tf_op jit(solution)/shard_map/ppermute | solution.py:59
  38.9 4.8 %collective-permute-start.4 = (bf16[64,768]{1,0:T(8,128)(2,1)S(1)}, bf16[64,768]{1,0:T(8,128)(2,1)S(1)}, u32[]{:S(2)}, u32[]{:S(2)}) collective-permute-start(bf16[64,768]{1,0:T(8,128)(2,1)S(1)} %shard_map.187.own.after), channel_id=1, source_target_pairs={{0,8},{1,33},{2,10},{3,35},{4,12},{5,37},{6,14},{7,39},{8,16},{9,4... | collective-permute-start | bytes 294920 | tf_op jit(solution)/shard_map/ppermute | solution.py:59
  39.3 6.3 %collective-permute-start.5 = (bf16[64,768]{1,0:T(8,128)(2,1)S(1)}, bf16[64,768]{1,0:T(8,128)(2,1)S(1)}, u32[]{:S(2)}, u32[]{:S(2)}) collective-permute-start(bf16[64,768]{1,0:T(8,128)(2,1)S(1)} %shard_map.187.own.after), channel_id=1, source_target_pairs={{0,16},{1,65},{2,18},{3,67},{4,20},{5,69},{6,22},{7,71},{8,24},{9,... | collective-permute-start | bytes 294920 | tf_op jit(solution)/shard_map/ppermute | solution.py:59
  42.5 5.1 %collective-permute-start.6 = (bf16[64,768]{1,0:T(8,128)(2,1)S(1)}, bf16[64,768]{1,0:T(8,128)(2,1)S(1)}, u32[]{:S(2)}, u32[]{:S(2)}) collective-permute-start(bf16[64,768]{1,0:T(8,128)(2,1)S(1)} %shard_map.187.own.after), channel_id=1, source_target_pairs={{0,24},{1,97},{2,26},{3,99},{4,28},{5,101},{6,30},{7,103},{8,0},{9... | collective-permute-start | bytes 294920 | tf_op jit(solution)/shard_map/ppermute | solution.py:59
  47.8 5.8 %collective-permute-start.10 = (bf16[64,768]{1,0:T(8,128)(2,1)S(1)}, bf16[64,768]{1,0:T(8,128)(2,1)S(1)}, u32[]{:S(2)}, u32[]{:S(2)}) collective-permute-start(bf16[64,768]{1,0:T(8,128)(2,1)S(1)} %get-tuple-element.45.own), channel_id=1, source_target_pairs={{0,32},{1,9},{2,34},{3,11},{4,36},{5,13},{6,38},{7,15},{8,40},{9,1... | collective-permute-start | bytes 294920 | tf_op jit(solution)/shard_map/ppermute | solution.py:59
  47.9 5.7 %collective-permute-start.11 = (bf16[64,768]{1,0:T(8,128)(2,1)S(1)}, bf16[64,768]{1,0:T(8,128)(2,1)S(1)}, u32[]{:S(2)}, u32[]{:S(2)}) collective-permute-start(bf16[64,768]{1,0:T(8,128)(2,1)S(1)} %get-tuple-element.45.own), channel_id=1, source_target_pairs={{0,64},{1,17},{2,66},{3,19},{4,68},{5,21},{6,70},{7,23},{8,72},{9,... | collective-permute-start | bytes 294920 | tf_op jit(solution)/shard_map/ppermute | solution.py:59
  49.0 5.3 %collective-permute-start.12 = (bf16[64,768]{1,0:T(8,128)(2,1)S(1)}, bf16[64,768]{1,0:T(8,128)(2,1)S(1)}, u32[]{:S(2)}, u32[]{:S(2)}) collective-permute-start(bf16[64,768]{1,0:T(8,128)(2,1)S(1)} %get-tuple-element.45.own), channel_id=1, source_target_pairs={{0,96},{1,25},{2,98},{3,27},{4,100},{5,29},{6,102},{7,31},{8,104},... | collective-permute-start | bytes 294920 | tf_op jit(solution)/shard_map/ppermute | solution.py:59
  54.4 5.5 %collective-permute-start.13 = (f32[8,128]{1,0:T(8,128)S(1)}, f32[8,128]{1,0:T(8,128)S(1)}, u32[]{:S(2)}, u32[]{:S(2)}) collective-permute-start(f32[8,128]{1,0:T(8,128)S(1)} %get-tuple-element.46), channel_id=1, source_target_pairs={{0,4},{1,5},{2,6},{3,7},{4,0},{5,1},{6,2},{7,3},{8,12},{9,13},{10,... | collective-permute-start | bytes 12296 | tf_op jit(solution)/shard_map/ppermute | solution.py:59
  57.2 3.7 %collective-permute-start.14 = (f32[8,128]{1,0:T(8,128)S(1)}, f32[8,128]{1,0:T(8,128)S(1)}, u32[]{:S(2)}, u32[]{:S(2)}) collective-permute-start(f32[8,128]{1,0:T(8,128)S(1)} %get-tuple-element.46), channel_id=1, source_target_pairs={{0,2},{1,3},{2,4},{3,5},{4,6},{5,7},{6,0},{7,1},{8,10},{9,11},{10,... | collective-permute-start | bytes 12296 | tf_op jit(solution)/shard_map/ppermute | solution.py:59
  57.5 3.4 %collective-permute-start.15 = (f32[8,128]{1,0:T(8,128)S(1)}, f32[8,128]{1,0:T(8,128)S(1)}, u32[]{:S(2)}, u32[]{:S(2)}) collective-permute-start(f32[8,128]{1,0:T(8,128)S(1)} %get-tuple-element.46), channel_id=1, source_target_pairs={{0,6},{1,7},{2,0},{3,1},{4,2},{5,3},{6,4},{7,5},{8,14},{9,15},{10,... | collective-permute-start | bytes 12296 | tf_op jit(solution)/shard_map/ppermute | solution.py:59
  60.9 7.2 %collective-permute-start.16 = (f32[8,128]{1,0:T(8,128)S(1)}, f32[8,128]{1,0:T(8,128)S(1)}, u32[]{:S(2)}, u32[]{:S(2)}) collective-permute-start(f32[8,128]{1,0:T(8,128)S(1)} %add_add_fusion.s_own), channel_id=1, source_target_pairs={{0,1},{1,0},{2,3},{3,2},{4,5},{5,4},{6,7},{7,6},{8,9},{9,8},{10,11... | collective-permute-start | bytes 12296 | tf_op jit(solution)/shard_map/ppermute | solution.py:59

commit v10 on v8

--- a/solution.py
+++ b/solution.py
@@ -272,8 +272,15 @@
     squares[...] = folded
 
 
+def back_kernel(u, pq, pv, back):
+    for n in range(4):
+        at = slice(n * 4 * ROWS, (n + 1) * 4 * ROWS)
+        back[at, :WQ] = jnp.dot(pq[at, :], u[:, :WQ], preferred_element_type=F32)
+        back[at, WQ:] = jnp.dot(pv[at, :], u[:, WQ:], preferred_element_type=F32)
+
+
 def weight_kernel(
-    s_own, s_other, u, pq, pv, g0, g1, g2, g3, wq, wv, fq, fv, sq, sv,
+    s_own, s_other, back, g0, g1, g2, g3, wq, wv, fq, fv, sq, sv,
     nq, nv, tq, tv, cq, cv, fq_out, fv_out, sq_out, sv_out,
     nq_s, nv_s, tq_s, tv_s, cq_s, cv_s, c_sem, m_sem,
 ):
@@ -289,7 +296,6 @@
     major, minor, per_major, per_minor = own_place()
     squares = jnp.sum(s_own[...] + s_other[...], axis=(0, 1), keepdims=True)
     scale = lax.rsqrt(squares / (RANK * (QK_W + V_W)) + norm_eps)
-    uq, uv = u[:, :WQ], u[:, WQ:]
     keep = 1.0 - step_rate * decay_rate
     for i, piece in ((0, g0), (1, g1), (3, g3), (2, g2)):
         a_there = lax.rem(major + 4 - i, 4)
@@ -297,8 +303,8 @@
             b_there = lax.rem(minor + 4 - j, 4)
             block = a_there * per_major + b_there * per_minor
             at = pl.ds(pl.multiple_of(block * ROWS, ROWS), ROWS)
-            back_q = scale * jnp.dot(pq[at, :], uq, preferred_element_type=F32)
-            back_v = scale * jnp.dot(pv[at, :], uv, preferred_element_type=F32)
+            back_q = scale * back[at, :WQ]
+            back_v = scale * back[at, WQ:]
             held = piece[j * ROWS : (j + 1) * ROWS, :].astype(F32)
             n = i * 4 + j
             cq_s[n] = (keep * held[:, :WQ] - step_rate * back_q).astype(BF16)
@@ -306,9 +312,9 @@
             for part, (source, target) in enumerate(((cq_s, cq), (cv_s, cv))):
                 store(source.at[n], target.at[at, :], c_sem.at[n, part])
             if n == 0:
-                for back, w, t, new in ((back_q, wq, tq_s, nq_s), (back_v, wv, tv_s, nv_s)):
+                for scaled, w, t, new in ((back_q, wq, tq_s, nq_s), (back_v, wv, tv_s, nv_s)):
                     weight = w[...]
-                    step = back + decay_rate * weight
+                    step = scaled + decay_rate * weight
                     t[...] = step
                     new[...] = weight - step_rate * step
                 for k, (a, b) in enumerate(((nq_s, nq), (nv_s, nv), (tq_s, tq), (tv_s, tv))):
@@ -317,7 +323,7 @@
         copy.wait()
 
 
-def new_weights(s_own, s_other, u, pq, pv, groups, wq, wv, kept):
+def new_weights(s_own, s_other, back, groups, wq, wv, kept):
     vmem = pl.BlockSpec(memory_space=pltpu.VMEM)
     hbm = pl.BlockSpec(memory_space=pl.ANY)
     out = [
@@ -328,7 +334,7 @@
         jax.ShapeDtypeStruct((16 * ROWS, WQ), BF16),
         jax.ShapeDtypeStruct((16 * ROWS, WV), BF16),
     ] + [jax.ShapeDtypeStruct(a.shape, F32) for a in kept]
-    operands = (s_own, s_other, u, pq, pv, *groups, wq, wv, *kept)
+    operands = (s_own, s_other, back, *groups, wq, wv, *kept)
     return pl.pallas_call(
         weight_kernel,
         in_specs=[vmem] * len(operands),
@@ -345,7 +351,7 @@
             pltpu.SemaphoreType.DMA((8,)),
         ],
         cost_estimate=pl.CostEstimate(
-            flops=2 * 16 * ROWS * RANK * W, bytes_accessed=12_000_000, transcendentals=0
+            flops=16 * ROWS * W * 4, bytes_accessed=12_000_000, transcendentals=0
         ),
         compiler_params=pltpu.CompilerParams(vmem_limit_bytes=20 * 2**20),
         name="weights",
@@ -368,7 +374,7 @@
     group, = whole_call(
         group_kernel, [jax.ShapeDtypeStruct((4 * ROWS, W), BF16)], (w16, w_1, w_2, w_3, own)
     )
-    g_1, g_3 = shifted(group, "major", 1), shifted(group, "major", 3)
+    g_3 = shifted(group, "major", 3)
     message, = whole_call(
         partial_kernel, [jax.ShapeDtypeStruct((64, W), BF16)], (own, r_1, r_2, r_3)
     )
@@ -382,17 +388,24 @@
     )
     u_1, u_2, u_3 = to_all("major", (u_own,) * 3)
     g_2 = shifted(g_3, "major", 3)
+    g_1 = shifted(group, "major", 1)
     u, squares = whole_call(
         assemble_kernel,
         [jax.ShapeDtypeStruct((RANK, W), BF16), jax.ShapeDtypeStruct((8, 128), F32)],
         (u_own, u_1, u_2, u_3),
     )
     s_1, s_2, s_3 = to_all("x", (squares,) * 3)
+    back, = whole_call(
+        back_kernel,
+        [jax.ShapeDtypeStruct((16 * ROWS, W), F32)],
+        (u, pq, pv),
+        flops=2 * 16 * ROWS * RANK * W,
+    )
     chips = (squares + s_2) + (s_1 + s_3)
     other = shifted(chips, "core", 1)
     kept = (first_q, first_v, second_q, second_v)
     new_q, new_v, step_q, step_v, copy_q, copy_v, *kept = new_weights(
-        chips, other, u, pq, pv, (group, g_1, g_2, g_3), wq, wv, kept
+        chips, other, back, (group, g_1, g_2, g_3), wq, wv, kept
     )
     return (new_q, new_v, copy_q, copy_v, *kept, step_q, step_v)
 

time: 80.2 us -> 85.1 us (1.061)
  waiting for transfers between devices: 29.2 us -> 36.9 us
  starting transfers between devices: 39.3 us -> 35.6 us
  Pallas kernels: 10.5 us -> 11.5 us
    ppermute x20, waiting for transfers between devices: 29.2 us -> 36.9 us  [shifted(): return lax.ppermute(array, AXES, shift_pairs(kind, offset))]
    ppermute x20, starting transfers between devices: 39.3 us -> 35.6 us  [shifted(): return lax.ppermute(array, AXES, shift_pairs(kind, offset))]
    pallas_call x5 -> x6, Pallas kernels: 1.86 us -> 2.85 us  [whole_call(): pl.pallas_call(body, in_specs=[vmem] * len(operands), out_specs=[vmem] *...]
  transfers between devices with their start and end apart: 20 -> 20, of which waited for: 13 -> 14; matrix products, arithmetic and copies ran while one was open for 0% -> 0% of each run, Pallas kernels for 2% -> 3%
where the time goes in v10:
time: 85.1 us; the launch traced here: 85 us
  waiting for transfers between devices  36.9 us (43%)
  starting transfers between devices  35.6 us (42%)
  Pallas kernels  11.5 us (14%)
  between operations  0.95 us (1%)
    ppermute x20, waiting for transfers between devices, shifted(): return lax.ppermute(array, AXES, shift_pairs(kind, offset))  36.9 us
    ppermute x20, starting transfers between devices, shifted(): return lax.ppermute(array, AXES, shift_pairs(kind, offset))  35.6 us
    pallas_call x1, Pallas kernels, mix(): pl.pallas_call(mix_kernel, in_specs=[hbm] * len(operands), out_specs=[vme...  5.66 us
    pallas_call x1, Pallas kernels, new_weights(): pl.pallas_call(weight_kernel, in_specs=[vmem] * len(operands), out_specs=...  2.95 us
    pallas_call x6, Pallas kernels, whole_call(): pl.pallas_call(body, in_specs=[vmem] * len(operands), out_specs=[vmem] *...  2.85 us
  transfers between devices with their start and end apart: 20, of which 14 were waited for; matrix products, arithmetic and copies ran while one was open for 0% of the time, Pallas kernels for 3%

profile of v10, /device:TPU:1, one launch (start us, length us, event | category | flops | bytes accessed | tf_op | source)
XLA Modules:
  0.0 85.0 jit_solution(8184592603848646696)
XLA Ops:
  0.6 5.7 %mix.1 = (bf16[1536,512]{1,0:T(8,128)(2,1)S(1)}, bf16[160,768]{1,0:T(8,128)(2,1)S(1)}, bf16[2048,256]{1,0:T(8,128)(2,1)S(1)}, bf16[2048,256]{1,0:T(8,128)(2,1)S(...) custom-call(bf16[3072,2048]{1,0:T(8,128)(2,1)} %x.1, bf16[3072,256]{1,0:T(8,128)(2,1)} %cq.1, ...), custom_call_target="tpu_custom_call" | custom-call | flops 3221225472 | bytes 14000000 | tf_op jit(solution)/shard_map/mix/pallas_call | solution.py:162
  6.3 1.5 %collective-permute-start = (bf16[1536,512]{1,0:T(8,128)(2,1)S(1)}, bf16[1536,512]{1,0:T(8,128)(2,1)S(1)}, u32[]{:S(2)}, u32[]{:S(2)}) collective-permute-start(bf16[1536,512]{1,0:T(8,128)(2,1)S(1)} %get-tuple-element.37.mixed), channel_id=1, source_target_pairs={{0,1},{1,0},{2,3},{3,2},{4,5},{5,4},{6,7},{7,6},{8,9},{9,8},{10,11... | collective-permute-start | bytes 4718600 | tf_op jit(solution)/shard_map/ppermute | solution.py:59
  7.8 3.9 %collective-permute-start.9 = (bf16[160,768]{1,0:T(8,128)(2,1)S(1)}, bf16[160,768]{1,0:T(8,128)(2,1)S(1)}, u32[]{:S(2)}, u32[]{:S(2)}) collective-permute-start(bf16[160,768]{1,0:T(8,128)(2,1)S(1)} %get-tuple-element.44.k0.w0), channel_id=1, source_target_pairs={{0,24},{1,97},{2,26},{3,99},{4,28},{5,101},{6,30},{7,103},{8,0},{9... | collective-permute-start | bytes 737288 | tf_op jit(solution)/shard_map/ppermute | solution.py:59
  11.6 0.7 collective-permute-start.7
  12.3 1.5 %shard_map.186 = (f32[64,768]{1,0:T(8,128)S(1)}, bf16[64,768]{1,0:T(8,128)(2,1)S(1)}, bf16[64,768]{1,0:T(8,128)(2,1)S(1)}, bf16[64,768]{1,0:T(8,128)(2,1)S(1)}) custom-call(bf16[1536,512]{1,0:T(8,128)(2,1)S(1)} %get-tuple-element.37.mixed, bf16[1536,512]{1,0:T(8,128)(2,1)S(1)} %collective-permute-done.swapped, bf16[3072,256]{1,0:T(8,128)(2,1)S(1)} %get-tuple-element.38.cq, ...), custom_call_target="tpu_custom_call" | custom-call | flops 1207959552 | bytes 1000000 | tf_op jit(solution)/shard_map/pallas_call | solution.py:216
  13.9 3.5 %collective-permute-done.9.k3.w3 = bf16[160,768]{1,0:T(8,128)(2,1)S(1)} collective-permute-done((bf16[160,768]{1,0:T(8,128)(2,1)S(1)}, bf16[160,768]{1,0:T(8,128)(2,1)S(1)}, u32[]{:S(2)}, u32[]{:S(2)}) %collective-permute-start.9) | collective-permute-done | bytes 245792 | tf_op jit(solution)/shard_map/ppermute | solution.py:59
  17.4 0.9 %collective-permute-done.8.k2.w2 = bf16[160,768]{1,0:T(8,128)(2,1)S(1)} collective-permute-done((bf16[160,768]{1,0:T(8,128)(2,1)S(1)}, bf16[160,768]{1,0:T(8,128)(2,1)S(1)}, u32[]{:S(2)}, u32[]{:S(2)}) %collective-permute-start.8) | collective-permute-done | bytes 245792 | tf_op jit(solution)/shard_map/ppermute | solution.py:59
  18.3 2.5 %collective-permute-done.7.k1.w1 = bf16[160,768]{1,0:T(8,128)(2,1)S(1)} collective-permute-done((bf16[160,768]{1,0:T(8,128)(2,1)S(1)}, bf16[160,768]{1,0:T(8,128)(2,1)S(1)}, u32[]{:S(2)}, u32[]{:S(2)}) %collective-permute-start.7) | collective-permute-done | bytes 245792 | tf_op jit(solution)/shard_map/ppermute | solution.py:59
  20.9 2.5 %collective-permute-start.18 = (bf16[512,768]{1,0:T(8,128)(2,1)S(1)}, bf16[512,768]{1,0:T(8,128)(2,1)S(1)}, u32[]{:S(2)}, u32[]{:S(2)}) collective-permute-start(bf16[512,768]{1,0:T(8,128)(2,1)S(1)} %shard_map.191.g0), channel_id=1, source_target_pairs={{0,96},{1,25},{2,98},{3,27},{4,100},{5,29},{6,102},{7,31},{8,104},... | collective-permute-start | bytes 2359304 | tf_op jit(solution)/shard_map/ppermute | solution.py:59
  23.4 8.9 %collective-permute-done.18.g3 = bf16[512,768]{1,0:T(8,128)(2,1)S(1)} collective-permute-done((bf16[512,768]{1,0:T(8,128)(2,1)S(1)}, bf16[512,768]{1,0:T(8,128)(2,1)S(1)}, u32[]{:S(2)}, u32[]{:S(2)}) %collective-permute-start.18) | collective-permute-done | bytes 786464 | tf_op jit(solution)/shard_map/ppermute | solution.py:59
  32.3 3.4 %collective-permute-start.19 = (bf16[512,768]{1,0:T(8,128)(2,1)S(1)}, bf16[512,768]{1,0:T(8,128)(2,1)S(1)}, u32[]{:S(2)}, u32[]{:S(2)}) collective-permute-start(bf16[512,768]{1,0:T(8,128)(2,1)S(1)} %collective-permute-done.18.g3), channel_id=1, source_target_pairs={{0,96},{1,25},{2,98},{3,27},{4,100},{5,29},{6,102},{7,31},{8,104},... | collective-permute-start | bytes 2359304 | tf_op jit(solution)/shard_map/ppermute | solution.py:59
  35.7 1.2 %collective-permute-start.2 = (bf16[64,768]{1,0:T(8,128)(2,1)S(1)}, bf16[64,768]{1,0:T(8,128)(2,1)S(1)}, u32[]{:S(2)}, u32[]{:S(2)}) collective-permute-start(bf16[64,768]{1,0:T(8,128)(2,1)S(1)} %get-tuple-element.42), channel_id=1, source_target_pairs={{0,64},{1,17},{2,66},{3,19},{4,68},{5,21},{6,70},{7,23},{8,72},{9,... | collective-permute-start | bytes 294920 | tf_op jit(solution)/shard_map/ppermute | solution.py:59
  36.9 1.5 %collective-permute-start.3 = (bf16[64,768]{1,0:T(8,128)(2,1)S(1)}, bf16[64,768]{1,0:T(8,128)(2,1)S(1)}, u32[]{:S(2)}, u32[]{:S(2)}) collective-permute-start(bf16[64,768]{1,0:T(8,128)(2,1)S(1)} %get-tuple-element.43), channel_id=1, source_target_pairs={{0,96},{1,25},{2,98},{3,27},{4,100},{5,29},{6,102},{7,31},{8,104},... | collective-permute-start | bytes 294920 | tf_op jit(solution)/shard_map/ppermute | solution.py:59
  38.4 3.1 %collective-permute-done.1.r1 = bf16[64,768]{1,0:T(8,128)(2,1)S(1)} collective-permute-done((bf16[64,768]{1,0:T(8,128)(2,1)S(1)}, bf16[64,768]{1,0:T(8,128)(2,1)S(1)}, u32[]{:S(2)}, u32[]{:S(2)}) %collective-permute-start.1) | collective-permute-done | bytes 98336 | tf_op jit(solution)/shard_map/ppermute | solution.py:59
  41.5 5.3 %collective-permute-done.3.r3 = bf16[64,768]{1,0:T(8,128)(2,1)S(1)} collective-permute-done((bf16[64,768]{1,0:T(8,128)(2,1)S(1)}, bf16[64,768]{1,0:T(8,128)(2,1)S(1)}, u32[]{:S(2)}, u32[]{:S(2)}) %collective-permute-start.3) | collective-permute-done | bytes 98336 | tf_op jit(solution)/shard_map/ppermute | solution.py:59
  46.8 1.0 %collective-permute-start.6 = (bf16[64,768]{1,0:T(8,128)(2,1)S(1)}, bf16[64,768]{1,0:T(8,128)(2,1)S(1)}, u32[]{:S(2)}, u32[]{:S(2)}) collective-permute-start(bf16[64,768]{1,0:T(8,128)(2,1)S(1)} %shard_map.187.own), channel_id=1, source_target_pairs={{0,24},{1,97},{2,26},{3,99},{4,28},{5,101},{6,30},{7,103},{8,0},{9... | collective-permute-start | bytes 294920 | tf_op jit(solution)/shard_map/ppermute | solution.py:59
  47.8 0.7 collective-permute-start.4
  48.5 2.9 %collective-permute-done.6.r3 = bf16[64,768]{1,0:T(8,128)(2,1)S(1)} collective-permute-done((bf16[64,768]{1,0:T(8,128)(2,1)S(1)}, bf16[64,768]{1,0:T(8,128)(2,1)S(1)}, u32[]{:S(2)}, u32[]{:S(2)}) %collective-permute-start.6) | collective-permute-done | bytes 98336 | tf_op jit(solution)/shard_map/ppermute | solution.py:59
  51.3 1.5 %collective-permute-done.5.r2 = bf16[64,768]{1,0:T(8,128)(2,1)S(1)} collective-permute-done((bf16[64,768]{1,0:T(8,128)(2,1)S(1)}, bf16[64,768]{1,0:T(8,128)(2,1)S(1)}, u32[]{:S(2)}, u32[]{:S(2)}) %collective-permute-start.5) | collective-permute-done | bytes 98336 | tf_op jit(solution)/shard_map/ppermute | solution.py:59
  52.9 0.9 %collective-permute-done.4.r1 = bf16[64,768]{1,0:T(8,128)(2,1)S(1)} collective-permute-done((bf16[64,768]{1,0:T(8,128)(2,1)S(1)}, bf16[64,768]{1,0:T(8,128)(2,1)S(1)}, u32[]{:S(2)}, u32[]{:S(2)}) %collective-permute-start.4) | collective-permute-done | bytes 98336 | tf_op jit(solution)/shard_map/ppermute | solution.py:59
  54.1 3.5 %collective-permute-start.12 = (bf16[64,768]{1,0:T(8,128)(2,1)S(1)}, bf16[64,768]{1,0:T(8,128)(2,1)S(1)}, u32[]{:S(2)}, u32[]{:S(2)}) collective-permute-start(bf16[64,768]{1,0:T(8,128)(2,1)S(1)} %get-tuple-element.45.own), channel_id=1, source_target_pairs={{0,96},{1,25},{2,98},{3,27},{4,100},{5,29},{6,102},{7,31},{8,104},... | collective-permute-start | bytes 294920 | tf_op jit(solution)/shard_map/ppermute | solution.py:59
  57.6 0.7 collective-permute-start.10
  58.2 1.9 %collective-permute-done.12.r3 = bf16[64,768]{1,0:T(8,128)(2,1)S(1)} collective-permute-done((bf16[64,768]{1,0:T(8,128)(2,1)S(1)}, bf16[64,768]{1,0:T(8,128)(2,1)S(1)}, u32[]{:S(2)}, u32[]{:S(2)}) %collective-permute-start.12) | collective-permute-done | bytes 98336 | tf_op jit(solution)/shard_map/ppermute | solution.py:59
  60.2 2.5 %collective-permute-done.11.r2 = bf16[64,768]{1,0:T(8,128)(2,1)S(1)} collective-permute-done((bf16[64,768]{1,0:T(8,128)(2,1)S(1)}, bf16[64,768]{1,0:T(8,128)(2,1)S(1)}, u32[]{:S(2)}, u32[]{:S(2)}) %collective-permute-start.11) | collective-permute-done | bytes 98336 | tf_op jit(solution)/shard_map/ppermute | solution.py:59
  62.6 0.7 collective-permute-done.10.r1
  63.4 2.5 %collective-permute-start.15 = (f32[8,128]{1,0:T(8,128)S(1)}, f32[8,128]{1,0:T(8,128)S(1)}, u32[]{:S(2)}, u32[]{:S(2)}) collective-permute-start(f32[8,128]{1,0:T(8,128)S(1)} %get-tuple-element.46), channel_id=1, source_target_pairs={{0,6},{1,7},{2,0},{3,1},{4,2},{5,3},{6,4},{7,5},{8,14},{9,15},{10,... | collective-permute-start | bytes 12296 | tf_op jit(solution)/shard_map/ppermute | solution.py:59
  65.9 1.7 %collective-permute-start.13 = (f32[8,128]{1,0:T(8,128)S(1)}, f32[8,128]{1,0:T(8,128)S(1)}, u32[]{:S(2)}, u32[]{:S(2)}) collective-permute-start(f32[8,128]{1,0:T(8,128)S(1)} %get-tuple-element.46), channel_id=1, source_target_pairs={{0,4},{1,5},{2,6},{3,7},{4,0},{5,1},{6,2},{7,3},{8,12},{9,13},{10,... | collective-permute-start | bytes 12296 | tf_op jit(solution)/shard_map/ppermute | solution.py:59
  67.7 1.9 %collective-permute-done.14 = f32[8,128]{1,0:T(8,128)S(1)} collective-permute-done((f32[8,128]{1,0:T(8,128)S(1)}, f32[8,128]{1,0:T(8,128)S(1)}, u32[]{:S(2)}, u32[]{:S(2)}) %collective-permute-start.14) | collective-permute-done | bytes 4128 | tf_op jit(solution)/shard_map/ppermute | solution.py:59
  69.6 0.3 collective-permute-done.13
  69.9 10.9 %collective-permute-start.16 = (f32[8,128]{1,0:T(8,128)S(1)}, f32[8,128]{1,0:T(8,128)S(1)}, u32[]{:S(2)}, u32[]{:S(2)}) collective-permute-start(f32[8,128]{1,0:T(8,128)S(1)} %add_add_fusion.s_own), channel_id=1, source_target_pairs={{0,1},{1,0},{2,3},{3,2},{4,5},{5,4},{6,7},{7,6},{8,9},{9,8},{10,11... | collective-permute-start | bytes 12296 | tf_op jit(solution)/shard_map/ppermute | solution.py:59
  80.8 1.0 %shard_map.190.back = f32[2048,768]{1,0:T(8,128)S(1)} custom-call(bf16[256,768]{1,0:T(8,128)(2,1)S(1)} %get-tuple-element.47.u, bf16[2048,256]{1,0:T(8,128)(2,1)S(1)} %get-tuple-element.48.pq, bf16[2048,256]{1,0:T(8,128)(2,1)S(1)} %get-tuple-element.49.pv), custom_call_target="tpu_custom_call" | custom-call | flops 805306368 | bytes 1000000 | tf_op jit(solution)/shard_map/pallas_call | solution.py:216
  81.9 2.9 %weights.1 = (f32[128,256]{1,0:T(8,128)}, f32[128,512]{1,0:T(8,128)}, f32[128,256]{1,0:T(8,128)}, f32[128,512]{1,0:T(8,128)}, bf16[2048,256]{1,0:T(8,128)(2,1)},...) custom-call(f32[8,128]{1,0:T(8,128)S(1)} %add_add_fusion.s_own, ...), custom_call_target="tpu_custom_call" | custom-call | flops 6291456 | bytes 12000000 | tf_op jit(solution)/shard_map/weights/pallas_call | solution.py:338
  (29 shorter events, 0.5 us)
Async XLA Ops:
  6.3 6.0 %collective-permute-start = (bf16[1536,512]{1,0:T(8,128)(2,1)S(1)}, bf16[1536,512]{1,0:T(8,128)(2,1)S(1)}, u32[]{:S(2)}, u32[]{:S(2)}) collective-permute-start(bf16[1536,512]{1,0:T(8,128)(2,1)S(1)} %get-tuple-element.37.mixed), channel_id=1, source_target_pairs={{0,1},{1,0},{2,3},{3,2},{4,5},{5,4},{6,7},{7,6},{8,9},{9,8},{10,11... | collective-permute-start | bytes 4718600 | tf_op jit(solution)/shard_map/ppermute | solution.py:59
  7.8 9.6 %collective-permute-start.9 = (bf16[160,768]{1,0:T(8,128)(2,1)S(1)}, bf16[160,768]{1,0:T(8,128)(2,1)S(1)}, u32[]{:S(2)}, u32[]{:S(2)}) collective-permute-start(bf16[160,768]{1,0:T(8,128)(2,1)S(1)} %get-tuple-element.44.k0.w0), channel_id=1, source_target_pairs={{0,24},{1,97},{2,26},{3,99},{4,28},{5,101},{6,30},{7,103},{8,0},{9... | collective-permute-start | bytes 737288 | tf_op jit(solution)/shard_map/ppermute | solution.py:59
  11.6 6.7 %collective-permute-start.8 = (bf16[160,768]{1,0:T(8,128)(2,1)S(1)}, bf16[160,768]{1,0:T(8,128)(2,1)S(1)}, u32[]{:S(2)}, u32[]{:S(2)}) collective-permute-start(bf16[160,768]{1,0:T(8,128)(2,1)S(1)} %get-tuple-element.44.k0.w0), channel_id=1, source_target_pairs={{0,16},{1,65},{2,18},{3,67},{4,20},{5,69},{6,22},{7,71},{8,24},{9,... | collective-permute-start | bytes 737288 | tf_op jit(solution)/shard_map/ppermute | solution.py:59
  11.6 9.2 %collective-permute-start.7 = (bf16[160,768]{1,0:T(8,128)(2,1)S(1)}, bf16[160,768]{1,0:T(8,128)(2,1)S(1)}, u32[]{:S(2)}, u32[]{:S(2)}) collective-permute-start(bf16[160,768]{1,0:T(8,128)(2,1)S(1)} %get-tuple-element.44.k0.w0), channel_id=1, source_target_pairs={{0,8},{1,33},{2,10},{3,35},{4,12},{5,37},{6,14},{7,39},{8,16},{9,4... | collective-permute-start | bytes 737288 | tf_op jit(solution)/shard_map/ppermute | solution.py:59
  13.8 40.0 %copy-start.2 = (f32[16,512]{1,0:T(8,128)S(1)}, f32[16,512]{1,0:T(8,128)}, u32[]{:S(2)}) copy-start(f32[16,512]{1,0:T(8,128)} %mv.3) | copy-start | bytes 98308
  13.8 40.0 %copy-start.3 = (f32[16,512]{1,0:T(8,128)S(1)}, f32[16,512]{1,0:T(8,128)}, u32[]{:S(2)}) copy-start(f32[16,512]{1,0:T(8,128)} %vv.3) | copy-start | bytes 98308
  13.9 40.0 %copy-start.4 = (f32[16,256]{1,0:T(8,128)S(1)}, f32[16,256]{1,0:T(8,128)}, u32[]{:S(2)}) copy-start(f32[16,256]{1,0:T(8,128)} %mq.3) | copy-start | bytes 49156
  13.9 40.0 %copy-start.5 = (f32[16,256]{1,0:T(8,128)S(1)}, f32[16,256]{1,0:T(8,128)}, u32[]{:S(2)}) copy-start(f32[16,256]{1,0:T(8,128)} %vq.3) | copy-start | bytes 49156
  20.9 11.4 %collective-permute-start.18 = (bf16[512,768]{1,0:T(8,128)(2,1)S(1)}, bf16[512,768]{1,0:T(8,128)(2,1)S(1)}, u32[]{:S(2)}, u32[]{:S(2)}) collective-permute-start(bf16[512,768]{1,0:T(8,128)(2,1)S(1)} %shard_map.191.g0), channel_id=1, source_target_pairs={{0,96},{1,25},{2,98},{3,27},{4,100},{5,29},{6,102},{7,31},{8,104},... | collective-permute-start | bytes 2359304 | tf_op jit(solution)/shard_map/ppermute | solution.py:59
  23.4 58.4 %collective-permute-start.17 = (bf16[512,768]{1,0:T(8,128)(2,1)S(1)}, bf16[512,768]{1,0:T(8,128)(2,1)S(1)}, u32[]{:S(2)}, u32[]{:S(2)}) collective-permute-start(bf16[512,768]{1,0:T(8,128)(2,1)S(1)} %shard_map.191.g0), channel_id=1, source_target_pairs={{0,32},{1,9},{2,34},{3,11},{4,36},{5,13},{6,38},{7,15},{8,40},{9,1... | collective-permute-start | bytes 2359304 | tf_op jit(solution)/shard_map/ppermute | solution.py:59
  32.3 49.5 %collective-permute-start.19 = (bf16[512,768]{1,0:T(8,128)(2,1)S(1)}, bf16[512,768]{1,0:T(8,128)(2,1)S(1)}, u32[]{:S(2)}, u32[]{:S(2)}) collective-permute-start(bf16[512,768]{1,0:T(8,128)(2,1)S(1)} %collective-permute-done.18.g3), channel_id=1, source_target_pairs={{0,96},{1,25},{2,98},{3,27},{4,100},{5,29},{6,102},{7,31},{8,104},... | collective-permute-start | bytes 2359304 | tf_op jit(solution)/shard_map/ppermute | solution.py:59
  35.7 5.7 %collective-permute-start.1 = (bf16[64,768]{1,0:T(8,128)(2,1)S(1)}, bf16[64,768]{1,0:T(8,128)(2,1)S(1)}, u32[]{:S(2)}, u32[]{:S(2)}) collective-permute-start(bf16[64,768]{1,0:T(8,128)(2,1)S(1)} %get-tuple-element.41), channel_id=1, source_target_pairs={{0,32},{1,9},{2,34},{3,11},{4,36},{5,13},{6,38},{7,15},{8,40},{9,1... | collective-permute-start | bytes 294920 | tf_op jit(solution)/shard_map/ppermute | solution.py:59
  35.7 5.7 %collective-permute-start.2 = (bf16[64,768]{1,0:T(8,128)(2,1)S(1)}, bf16[64,768]{1,0:T(8,128)(2,1)S(1)}, u32[]{:S(2)}, u32[]{:S(2)}) collective-permute-start(bf16[64,768]{1,0:T(8,128)(2,1)S(1)} %get-tuple-element.42), channel_id=1, source_target_pairs={{0,64},{1,17},{2,66},{3,19},{4,68},{5,21},{6,70},{7,23},{8,72},{9,... | collective-permute-start | bytes 294920 | tf_op jit(solution)/shard_map/ppermute | solution.py:59
  36.9 9.9 %collective-permute-start.3 = (bf16[64,768]{1,0:T(8,128)(2,1)S(1)}, bf16[64,768]{1,0:T(8,128)(2,1)S(1)}, u32[]{:S(2)}, u32[]{:S(2)}) collective-permute-start(bf16[64,768]{1,0:T(8,128)(2,1)S(1)} %get-tuple-element.43), channel_id=1, source_target_pairs={{0,96},{1,25},{2,98},{3,27},{4,100},{5,29},{6,102},{7,31},{8,104},... | collective-permute-start | bytes 294920 | tf_op jit(solution)/shard_map/ppermute | solution.py:59
  46.8 4.5 %collective-permute-start.6 = (bf16[64,768]{1,0:T(8,128)(2,1)S(1)}, bf16[64,768]{1,0:T(8,128)(2,1)S(1)}, u32[]{:S(2)}, u32[]{:S(2)}) collective-permute-start(bf16[64,768]{1,0:T(8,128)(2,1)S(1)} %shard_map.187.own), channel_id=1, source_target_pairs={{0,24},{1,97},{2,26},{3,99},{4,28},{5,101},{6,30},{7,103},{8,0},{9... | collective-permute-start | bytes 294920 | tf_op jit(solution)/shard_map/ppermute | solution.py:59
  47.8 5.1 %collective-permute-start.5 = (bf16[64,768]{1,0:T(8,128)(2,1)S(1)}, bf16[64,768]{1,0:T(8,128)(2,1)S(1)}, u32[]{:S(2)}, u32[]{:S(2)}) collective-permute-start(bf16[64,768]{1,0:T(8,128)(2,1)S(1)} %shard_map.187.own), channel_id=1, source_target_pairs={{0,16},{1,65},{2,18},{3,67},{4,20},{5,69},{6,22},{7,71},{8,24},{9,... | collective-permute-start | bytes 294920 | tf_op jit(solution)/shard_map/ppermute | solution.py:59
  47.8 6.0 %collective-permute-start.4 = (bf16[64,768]{1,0:T(8,128)(2,1)S(1)}, bf16[64,768]{1,0:T(8,128)(2,1)S(1)}, u32[]{:S(2)}, u32[]{:S(2)}) collective-permute-start(bf16[64,768]{1,0:T(8,128)(2,1)S(1)} %shard_map.187.own), channel_id=1, source_target_pairs={{0,8},{1,33},{2,10},{3,35},{4,12},{5,37},{6,14},{7,39},{8,16},{9,4... | collective-permute-start | bytes 294920 | tf_op jit(solution)/shard_map/ppermute | solution.py:59
  54.1 6.1 %collective-permute-start.12 = (bf16[64,768]{1,0:T(8,128)(2,1)S(1)}, bf16[64,768]{1,0:T(8,128)(2,1)S(1)}, u32[]{:S(2)}, u32[]{:S(2)}) collective-permute-start(bf16[64,768]{1,0:T(8,128)(2,1)S(1)} %get-tuple-element.45.own), channel_id=1, source_target_pairs={{0,96},{1,25},{2,98},{3,27},{4,100},{5,29},{6,102},{7,31},{8,104},... | collective-permute-start | bytes 294920 | tf_op jit(solution)/shard_map/ppermute | solution.py:59
  57.6 5.1 %collective-permute-start.11 = (bf16[64,768]{1,0:T(8,128)(2,1)S(1)}, bf16[64,768]{1,0:T(8,128)(2,1)S(1)}, u32[]{:S(2)}, u32[]{:S(2)}) collective-permute-start(bf16[64,768]{1,0:T(8,128)(2,1)S(1)} %get-tuple-element.45.own), channel_id=1, source_target_pairs={{0,64},{1,17},{2,66},{3,19},{4,68},{5,21},{6,70},{7,23},{8,72},{9,... | collective-permute-start | bytes 294920 | tf_op jit(solution)/shard_map/ppermute | solution.py:59
  57.6 5.7 %collective-permute-start.10 = (bf16[64,768]{1,0:T(8,128)(2,1)S(1)}, bf16[64,768]{1,0:T(8,128)(2,1)S(1)}, u32[]{:S(2)}, u32[]{:S(2)}) collective-permute-start(bf16[64,768]{1,0:T(8,128)(2,1)S(1)} %get-tuple-element.45.own), channel_id=1, source_target_pairs={{0,32},{1,9},{2,34},{3,11},{4,36},{5,13},{6,38},{7,15},{8,40},{9,1... | collective-permute-start | bytes 294920 | tf_op jit(solution)/shard_map/ppermute | solution.py:59
  63.4 4.3 %collective-permute-start.15 = (f32[8,128]{1,0:T(8,128)S(1)}, f32[8,128]{1,0:T(8,128)S(1)}, u32[]{:S(2)}, u32[]{:S(2)}) collective-permute-start(f32[8,128]{1,0:T(8,128)S(1)} %get-tuple-element.46), channel_id=1, source_target_pairs={{0,6},{1,7},{2,0},{3,1},{4,2},{5,3},{6,4},{7,5},{8,14},{9,15},{10,... | collective-permute-start | bytes 12296 | tf_op jit(solution)/shard_map/ppermute | solution.py:59
  65.9 3.7 %collective-permute-start.14 = (f32[8,128]{1,0:T(8,128)S(1)}, f32[8,128]{1,0:T(8,128)S(1)}, u32[]{:S(2)}, u32[]{:S(2)}) collective-permute-start(f32[8,128]{1,0:T(8,128)S(1)} %get-tuple-element.46), channel_id=1, source_target_pairs={{0,2},{1,3},{2,4},{3,5},{4,6},{5,7},{6,0},{7,1},{8,10},{9,11},{10,... | collective-permute-start | bytes 12296 | tf_op jit(solution)/shard_map/ppermute | solution.py:59
  65.9 4.0 %collective-permute-start.13 = (f32[8,128]{1,0:T(8,128)S(1)}, f32[8,128]{1,0:T(8,128)S(1)}, u32[]{:S(2)}, u32[]{:S(2)}) collective-permute-start(f32[8,128]{1,0:T(8,128)S(1)} %get-tuple-element.46), channel_id=1, source_target_pairs={{0,4},{1,5},{2,6},{3,7},{4,0},{5,1},{6,2},{7,3},{8,12},{9,13},{10,... | collective-permute-start | bytes 12296 | tf_op jit(solution)/shard_map/ppermute | solution.py:59
  69.9 11.9 %collective-permute-start.16 = (f32[8,128]{1,0:T(8,128)S(1)}, f32[8,128]{1,0:T(8,128)S(1)}, u32[]{:S(2)}, u32[]{:S(2)}) collective-permute-start(f32[8,128]{1,0:T(8,128)S(1)} %add_add_fusion.s_own), channel_id=1, source_target_pairs={{0,1},{1,0},{2,3},{3,2},{4,5},{5,4},{6,7},{7,6},{8,9},{9,8},{10,11... | collective-permute-start | bytes 12296 | tf_op jit(solution)/shard_map/ppermute | solution.py:59
  80.8 1.0 %copy-start = (f32[128,512]{1,0:T(8,128)S(1)}, f32[128,512]{1,0:T(8,128)}, u32[]{:S(2)}) copy-start(f32[128,512]{1,0:T(8,128)} %wv.3) | copy-start | bytes 786436
  80.8 1.0 %copy-start.1 = (f32[128,256]{1,0:T(8,128)S(1)}, f32[128,256]{1,0:T(8,128)}, u32[]{:S(2)}) copy-start(f32[128,256]{1,0:T(8,128)} %wq.3) | copy-start | bytes 393220

commit v11 on v8

--- a/solution.py
+++ b/solution.py
@@ -355,7 +355,8 @@
 def on_device(inputs, cq, cv, pq, pv, wq, wv, mq, mv, vq, vv):
     mixed, w16, pq, pv, cq, cv = mix(inputs, cq, cv, pq, pv, wq, wv, mq, mv, vq, vv)
     swapped = shifted(mixed, "core", 1)
-    w_1, w_2, w_3 = to_all("minor", (w16,) * 3)
+    w_1, w_3 = shifted(w16, "minor", 1), shifted(w16, "minor", 3)
+    w_2 = shifted(w_3, "minor", 3)
     chunk = lambda t: jax.ShapeDtypeStruct((64, W), t)
     own, *parts = whole_call(
         lead_kernel,
@@ -368,7 +369,7 @@
     group, = whole_call(
         group_kernel, [jax.ShapeDtypeStruct((4 * ROWS, W), BF16)], (w16, w_1, w_2, w_3, own)
     )
-    g_1, g_3 = shifted(group, "major", 1), shifted(group, "major", 3)
+    g_3 = shifted(group, "major", 3)
     message, = whole_call(
         partial_kernel, [jax.ShapeDtypeStruct((64, W), BF16)], (own, r_1, r_2, r_3)
     )
@@ -382,6 +383,7 @@
     )
     u_1, u_2, u_3 = to_all("major", (u_own,) * 3)
     g_2 = shifted(g_3, "major", 3)
+    g_1 = shifted(group, "major", 1)
     u, squares = whole_call(
         assemble_kernel,
         [jax.ShapeDtypeStruct((RANK, W), BF16), jax.ShapeDtypeStruct((8, 128), F32)],

time: 80.2 us -> 84.1 us (1.049)
  starting transfers between devices: 39.3 us -> 41.6 us
  waiting for transfers between devices: 29.2 us -> 31.1 us
    ppermute x20, starting transfers between devices: 39.3 us -> 41.6 us  [shifted(): return lax.ppermute(array, AXES, shift_pairs(kind, offset))]
    ppermute x20, waiting for transfers between devices: 29.2 us -> 31.1 us  [shifted(): return lax.ppermute(array, AXES, shift_pairs(kind, offset))]
where the time goes in v11:
time: 84.1 us; the launch traced here: 84 us
  starting transfers between devices  41.6 us (49%)
  waiting for transfers between devices  31.1 us (37%)
  Pallas kernels  10.5 us (12%)
    ppermute x20, starting transfers between devices, shifted(): return lax.ppermute(array, AXES, shift_pairs(kind, offset))  41.6 us
    ppermute x20, waiting for transfers between devices, shifted(): return lax.ppermute(array, AXES, shift_pairs(kind, offset))  31.1 us
    pallas_call x1, Pallas kernels, mix(): pl.pallas_call(mix_kernel, in_specs=[hbm] * len(operands), out_specs=[vme...  5.66 us
    pallas_call x1, Pallas kernels, new_weights(): pl.pallas_call(weight_kernel, in_specs=[vmem] * len(operands), out_specs=...  2.95 us
    pallas_call x5, Pallas kernels, whole_call(): pl.pallas_call(body, in_specs=[vmem] * len(operands), out_specs=[vmem] *...  1.86 us
  transfers between devices with their start and end apart: 20, of which 13 were waited for; matrix products, arithmetic and copies ran while one was open for 0% of the time, Pallas kernels for 2%

profile of v11, /device:TPU:1, one launch (start us, length us, event | category | flops | bytes accessed | tf_op | source)
XLA Modules:
  0.0 84.0 jit_solution(9591992539985747615)
XLA Ops:
  0.6 5.7 %mix.1 = (bf16[1536,512]{1,0:T(8,128)(2,1)S(1)}, bf16[160,768]{1,0:T(8,128)(2,1)S(1)}, bf16[2048,256]{1,0:T(8,128)(2,1)S(1)}, bf16[2048,256]{1,0:T(8,128)(2,1)S(...) custom-call(bf16[3072,2048]{1,0:T(8,128)(2,1)} %x.1, bf16[3072,256]{1,0:T(8,128)(2,1)} %cq.1, ...), custom_call_target="tpu_custom_call" | custom-call | flops 3221225472 | bytes 14000000 | tf_op jit(solution)/shard_map/mix/pallas_call | solution.py:162
  6.3 1.5 %collective-permute-start = (bf16[1536,512]{1,0:T(8,128)(2,1)S(1)}, bf16[1536,512]{1,0:T(8,128)(2,1)S(1)}, u32[]{:S(2)}, u32[]{:S(2)}) collective-permute-start(bf16[1536,512]{1,0:T(8,128)(2,1)S(1)} %get-tuple-element.37.mixed), channel_id=1, source_target_pairs={{0,1},{1,0},{2,3},{3,2},{4,5},{5,4},{6,7},{7,6},{8,9},{9,8},{10,11... | collective-permute-start | bytes 4718600 | tf_op jit(solution)/shard_map/ppermute | solution.py:59
  7.8 3.9 %collective-permute-start.8 = (bf16[160,768]{1,0:T(8,128)(2,1)S(1)}, bf16[160,768]{1,0:T(8,128)(2,1)S(1)}, u32[]{:S(2)}, u32[]{:S(2)}) collective-permute-start(bf16[160,768]{1,0:T(8,128)(2,1)S(1)} %get-tuple-element.44.k0.w0), channel_id=1, source_target_pairs={{0,24},{1,97},{2,26},{3,99},{4,28},{5,101},{6,30},{7,103},{8,0},{9... | collective-permute-start | bytes 737288 | tf_op jit(solution)/shard_map/ppermute | solution.py:59
  11.6 3.1 %collective-permute-done.8.k3.w3 = bf16[160,768]{1,0:T(8,128)(2,1)S(1)} collective-permute-done((bf16[160,768]{1,0:T(8,128)(2,1)S(1)}, bf16[160,768]{1,0:T(8,128)(2,1)S(1)}, u32[]{:S(2)}, u32[]{:S(2)}) %collective-permute-start.8) | collective-permute-done | bytes 245792 | tf_op jit(solution)/shard_map/ppermute | solution.py:59
  14.8 3.1 %collective-permute-start.9 = (bf16[160,768]{1,0:T(8,128)(2,1)S(1)}, bf16[160,768]{1,0:T(8,128)(2,1)S(1)}, u32[]{:S(2)}, u32[]{:S(2)}) collective-permute-start(bf16[160,768]{1,0:T(8,128)(2,1)S(1)} %collective-permute-done.8.k3.w3), channel_id=1, source_target_pairs={{0,24},{1,97},{2,26},{3,99},{4,28},{5,101},{6,30},{7,103},{8,0},{9... | collective-permute-start | bytes 737288 | tf_op jit(solution)/shard_map/ppermute | solution.py:59
  17.9 1.5 %shard_map.186 = (f32[64,768]{1,0:T(8,128)S(1)}, bf16[64,768]{1,0:T(8,128)(2,1)S(1)}, bf16[64,768]{1,0:T(8,128)(2,1)S(1)}, bf16[64,768]{1,0:T(8,128)(2,1)S(1)}) custom-call(bf16[1536,512]{1,0:T(8,128)(2,1)S(1)} %get-tuple-element.37.mixed, bf16[1536,512]{1,0:T(8,128)(2,1)S(1)} %collective-permute-done.swapped, bf16[3072,256]{1,0:T(8,128)(2,1)S(1)} %get-tuple-element.38.cq, ...), custom_call_target="tpu_custom_call" | custom-call | flops 1207959552 | bytes 1000000 | tf_op jit(solution)/shard_map/pallas_call | solution.py:216
  19.4 1.6 %collective-permute-done.9.k2.w2 = bf16[160,768]{1,0:T(8,128)(2,1)S(1)} collective-permute-done((bf16[160,768]{1,0:T(8,128)(2,1)S(1)}, bf16[160,768]{1,0:T(8,128)(2,1)S(1)}, u32[]{:S(2)}, u32[]{:S(2)}) %collective-permute-start.9) | collective-permute-done | bytes 245792 | tf_op jit(solution)/shard_map/ppermute | solution.py:59
  21.1 3.1 %collective-permute-start.18 = (bf16[512,768]{1,0:T(8,128)(2,1)S(1)}, bf16[512,768]{1,0:T(8,128)(2,1)S(1)}, u32[]{:S(2)}, u32[]{:S(2)}) collective-permute-start(bf16[512,768]{1,0:T(8,128)(2,1)S(1)} %shard_map.190.g0), channel_id=1, source_target_pairs={{0,96},{1,25},{2,98},{3,27},{4,100},{5,29},{6,102},{7,31},{8,104},... | collective-permute-start | bytes 2359304 | tf_op jit(solution)/shard_map/ppermute | solution.py:59
  24.2 8.9 %collective-permute-done.18.g3 = bf16[512,768]{1,0:T(8,128)(2,1)S(1)} collective-permute-done((bf16[512,768]{1,0:T(8,128)(2,1)S(1)}, bf16[512,768]{1,0:T(8,128)(2,1)S(1)}, u32[]{:S(2)}, u32[]{:S(2)}) %collective-permute-start.18) | collective-permute-done | bytes 786464 | tf_op jit(solution)/shard_map/ppermute | solution.py:59
  33.1 3.4 %collective-permute-start.19 = (bf16[512,768]{1,0:T(8,128)(2,1)S(1)}, bf16[512,768]{1,0:T(8,128)(2,1)S(1)}, u32[]{:S(2)}, u32[]{:S(2)}) collective-permute-start(bf16[512,768]{1,0:T(8,128)(2,1)S(1)} %collective-permute-done.18.g3), channel_id=1, source_target_pairs={{0,96},{1,25},{2,98},{3,27},{4,100},{5,29},{6,102},{7,31},{8,104},... | collective-permute-start | bytes 2359304 | tf_op jit(solution)/shard_map/ppermute | solution.py:59
  36.6 1.2 %collective-permute-start.2 = (bf16[64,768]{1,0:T(8,128)(2,1)S(1)}, bf16[64,768]{1,0:T(8,128)(2,1)S(1)}, u32[]{:S(2)}, u32[]{:S(2)}) collective-permute-start(bf16[64,768]{1,0:T(8,128)(2,1)S(1)} %get-tuple-element.42), channel_id=1, source_target_pairs={{0,64},{1,17},{2,66},{3,19},{4,68},{5,21},{6,70},{7,23},{8,72},{9,... | collective-permute-start | bytes 294920 | tf_op jit(solution)/shard_map/ppermute | solution.py:59
  37.7 1.5 %collective-permute-start.3 = (bf16[64,768]{1,0:T(8,128)(2,1)S(1)}, bf16[64,768]{1,0:T(8,128)(2,1)S(1)}, u32[]{:S(2)}, u32[]{:S(2)}) collective-permute-start(bf16[64,768]{1,0:T(8,128)(2,1)S(1)} %get-tuple-element.43), channel_id=1, source_target_pairs={{0,96},{1,25},{2,98},{3,27},{4,100},{5,29},{6,102},{7,31},{8,104},... | collective-permute-start | bytes 294920 | tf_op jit(solution)/shard_map/ppermute | solution.py:59
  39.2 3.1 %collective-permute-done.1.r1 = bf16[64,768]{1,0:T(8,128)(2,1)S(1)} collective-permute-done((bf16[64,768]{1,0:T(8,128)(2,1)S(1)}, bf16[64,768]{1,0:T(8,128)(2,1)S(1)}, u32[]{:S(2)}, u32[]{:S(2)}) %collective-permute-start.1) | collective-permute-done | bytes 98336 | tf_op jit(solution)/shard_map/ppermute | solution.py:59
  42.3 5.3 %collective-permute-done.3.r3 = bf16[64,768]{1,0:T(8,128)(2,1)S(1)} collective-permute-done((bf16[64,768]{1,0:T(8,128)(2,1)S(1)}, bf16[64,768]{1,0:T(8,128)(2,1)S(1)}, u32[]{:S(2)}, u32[]{:S(2)}) %collective-permute-start.3) | collective-permute-done | bytes 98336 | tf_op jit(solution)/shard_map/ppermute | solution.py:59
  47.7 4.6 %collective-permute-start.5 = (bf16[64,768]{1,0:T(8,128)(2,1)S(1)}, bf16[64,768]{1,0:T(8,128)(2,1)S(1)}, u32[]{:S(2)}, u32[]{:S(2)}) collective-permute-start(bf16[64,768]{1,0:T(8,128)(2,1)S(1)} %shard_map.187.own), channel_id=1, source_target_pairs={{0,16},{1,65},{2,18},{3,67},{4,20},{5,69},{6,22},{7,71},{8,24},{9,... | collective-permute-start | bytes 294920 | tf_op jit(solution)/shard_map/ppermute | solution.py:59
  52.3 0.8 collective-permute-done.4.r1
  53.1 2.2 %collective-permute-done.5.r2 = bf16[64,768]{1,0:T(8,128)(2,1)S(1)} collective-permute-done((bf16[64,768]{1,0:T(8,128)(2,1)S(1)}, bf16[64,768]{1,0:T(8,128)(2,1)S(1)}, u32[]{:S(2)}, u32[]{:S(2)}) %collective-permute-start.5) | collective-permute-done | bytes 98336 | tf_op jit(solution)/shard_map/ppermute | solution.py:59
  55.4 0.7 collective-permute-done.6.r3
  56.1 0.2 shard_map.188
  56.3 0.1 collective-permute-start.10
  56.4 4.6 %collective-permute-start.11 = (bf16[64,768]{1,0:T(8,128)(2,1)S(1)}, bf16[64,768]{1,0:T(8,128)(2,1)S(1)}, u32[]{:S(2)}, u32[]{:S(2)}) collective-permute-start(bf16[64,768]{1,0:T(8,128)(2,1)S(1)} %get-tuple-element.45.own), channel_id=1, source_target_pairs={{0,64},{1,17},{2,66},{3,19},{4,68},{5,21},{6,70},{7,23},{8,72},{9,... | collective-permute-start | bytes 294920 | tf_op jit(solution)/shard_map/ppermute | solution.py:59
  61.0 0.8 collective-permute-done.10.r1
  61.8 2.2 %collective-permute-done.11.r2 = bf16[64,768]{1,0:T(8,128)(2,1)S(1)} collective-permute-done((bf16[64,768]{1,0:T(8,128)(2,1)S(1)}, bf16[64,768]{1,0:T(8,128)(2,1)S(1)}, u32[]{:S(2)}, u32[]{:S(2)}) %collective-permute-start.11) | collective-permute-done | bytes 98336 | tf_op jit(solution)/shard_map/ppermute | solution.py:59
  64.0 0.4 collective-permute-done.12.r3
  64.4 0.1 shard_map.189
  64.5 2.8 %collective-permute-start.13 = (f32[8,128]{1,0:T(8,128)S(1)}, f32[8,128]{1,0:T(8,128)S(1)}, u32[]{:S(2)}, u32[]{:S(2)}) collective-permute-start(f32[8,128]{1,0:T(8,128)S(1)} %get-tuple-element.46), channel_id=1, source_target_pairs={{0,4},{1,5},{2,6},{3,7},{4,0},{5,1},{6,2},{7,3},{8,12},{9,13},{10,... | collective-permute-start | bytes 12296 | tf_op jit(solution)/shard_map/ppermute | solution.py:59
  67.3 0.3 collective-permute-start.14
  67.7 2.4 %collective-permute-start.15 = (f32[8,128]{1,0:T(8,128)S(1)}, f32[8,128]{1,0:T(8,128)S(1)}, u32[]{:S(2)}, u32[]{:S(2)}) collective-permute-start(f32[8,128]{1,0:T(8,128)S(1)} %get-tuple-element.46), channel_id=1, source_target_pairs={{0,6},{1,7},{2,0},{3,1},{4,2},{5,3},{6,4},{7,5},{8,14},{9,15},{10,... | collective-permute-start | bytes 12296 | tf_op jit(solution)/shard_map/ppermute | solution.py:59
  70.0 1.0 %collective-permute-done.14 = f32[8,128]{1,0:T(8,128)S(1)} collective-permute-done((f32[8,128]{1,0:T(8,128)S(1)}, f32[8,128]{1,0:T(8,128)S(1)}, u32[]{:S(2)}, u32[]{:S(2)}) %collective-permute-start.14) | collective-permute-done | bytes 4128 | tf_op jit(solution)/shard_map/ppermute | solution.py:59
  71.0 9.2 %collective-permute-start.16 = (f32[8,128]{1,0:T(8,128)S(1)}, f32[8,128]{1,0:T(8,128)S(1)}, u32[]{:S(2)}, u32[]{:S(2)}) collective-permute-start(f32[8,128]{1,0:T(8,128)S(1)} %add_add_fusion.s_own), channel_id=1, source_target_pairs={{0,1},{1,0},{2,3},{3,2},{4,5},{5,4},{6,7},{7,6},{8,9},{9,8},{10,11... | collective-permute-start | bytes 12296 | tf_op jit(solution)/shard_map/ppermute | solution.py:59
  80.2 0.8 collective-permute-done.16.s_other
  81.1 3.0 %weights.1 = (f32[128,256]{1,0:T(8,128)}, f32[128,512]{1,0:T(8,128)}, f32[128,256]{1,0:T(8,128)}, f32[128,512]{1,0:T(8,128)}, bf16[2048,256]{1,0:T(8,128)(2,1)},...) custom-call(f32[8,128]{1,0:T(8,128)S(1)} %add_add_fusion.s_own, ...), custom_call_target="tpu_custom_call" | custom-call | flops 805306368 | bytes 12000000 | tf_op jit(solution)/shard_map/weights/pallas_call | solution.py:332
  (28 shorter events, 0.2 us)
Async XLA Ops:
  6.3 11.6 %collective-permute-start = (bf16[1536,512]{1,0:T(8,128)(2,1)S(1)}, bf16[1536,512]{1,0:T(8,128)(2,1)S(1)}, u32[]{:S(2)}, u32[]{:S(2)}) collective-permute-start(bf16[1536,512]{1,0:T(8,128)(2,1)S(1)} %get-tuple-element.37.mixed), channel_id=1, source_target_pairs={{0,1},{1,0},{2,3},{3,2},{4,5},{5,4},{6,7},{7,6},{8,9},{9,8},{10,11... | collective-permute-start | bytes 4718600 | tf_op jit(solution)/shard_map/ppermute | solution.py:59
  7.8 7.0 %collective-permute-start.8 = (bf16[160,768]{1,0:T(8,128)(2,1)S(1)}, bf16[160,768]{1,0:T(8,128)(2,1)S(1)}, u32[]{:S(2)}, u32[]{:S(2)}) collective-permute-start(bf16[160,768]{1,0:T(8,128)(2,1)S(1)} %get-tuple-element.44.k0.w0), channel_id=1, source_target_pairs={{0,24},{1,97},{2,26},{3,99},{4,28},{5,101},{6,30},{7,103},{8,0},{9... | collective-permute-start | bytes 737288 | tf_op jit(solution)/shard_map/ppermute | solution.py:59
  11.6 7.8 %collective-permute-start.7 = (bf16[160,768]{1,0:T(8,128)(2,1)S(1)}, bf16[160,768]{1,0:T(8,128)(2,1)S(1)}, u32[]{:S(2)}, u32[]{:S(2)}) collective-permute-start(bf16[160,768]{1,0:T(8,128)(2,1)S(1)} %get-tuple-element.44.k0.w0), channel_id=1, source_target_pairs={{0,8},{1,33},{2,10},{3,35},{4,12},{5,37},{6,14},{7,39},{8,16},{9,4... | collective-permute-start | bytes 737288 | tf_op jit(solution)/shard_map/ppermute | solution.py:59
  14.8 6.3 %collective-permute-start.9 = (bf16[160,768]{1,0:T(8,128)(2,1)S(1)}, bf16[160,768]{1,0:T(8,128)(2,1)S(1)}, u32[]{:S(2)}, u32[]{:S(2)}) collective-permute-start(bf16[160,768]{1,0:T(8,128)(2,1)S(1)} %collective-permute-done.8.k3.w3), channel_id=1, source_target_pairs={{0,24},{1,97},{2,26},{3,99},{4,28},{5,101},{6,30},{7,103},{8,0},{9... | collective-permute-start | bytes 737288 | tf_op jit(solution)/shard_map/ppermute | solution.py:59
  19.4 36.7 %copy-start.2 = (f32[16,512]{1,0:T(8,128)S(1)}, f32[16,512]{1,0:T(8,128)}, u32[]{:S(2)}) copy-start(f32[16,512]{1,0:T(8,128)} %mv.3) | copy-start | bytes 98308
  19.4 36.7 %copy-start.3 = (f32[16,512]{1,0:T(8,128)S(1)}, f32[16,512]{1,0:T(8,128)}, u32[]{:S(2)}) copy-start(f32[16,512]{1,0:T(8,128)} %vv.3) | copy-start | bytes 98308
  19.4 36.7 %copy-start.4 = (f32[16,256]{1,0:T(8,128)S(1)}, f32[16,256]{1,0:T(8,128)}, u32[]{:S(2)}) copy-start(f32[16,256]{1,0:T(8,128)} %mq.3) | copy-start | bytes 49156
  19.4 36.7 %copy-start.5 = (f32[16,256]{1,0:T(8,128)S(1)}, f32[16,256]{1,0:T(8,128)}, u32[]{:S(2)}) copy-start(f32[16,256]{1,0:T(8,128)} %vq.3) | copy-start | bytes 49156
  21.0 60.0 %copy-start = (f32[128,512]{1,0:T(8,128)S(1)}, f32[128,512]{1,0:T(8,128)}, u32[]{:S(2)}) copy-start(f32[128,512]{1,0:T(8,128)} %wv.3) | copy-start | bytes 786436
  21.0 60.0 %copy-start.1 = (f32[128,256]{1,0:T(8,128)S(1)}, f32[128,256]{1,0:T(8,128)}, u32[]{:S(2)}) copy-start(f32[128,256]{1,0:T(8,128)} %wq.3) | copy-start | bytes 393220
  21.1 12.0 %collective-permute-start.18 = (bf16[512,768]{1,0:T(8,128)(2,1)S(1)}, bf16[512,768]{1,0:T(8,128)(2,1)S(1)}, u32[]{:S(2)}, u32[]{:S(2)}) collective-permute-start(bf16[512,768]{1,0:T(8,128)(2,1)S(1)} %shard_map.190.g0), channel_id=1, source_target_pairs={{0,96},{1,25},{2,98},{3,27},{4,100},{5,29},{6,102},{7,31},{8,104},... | collective-permute-start | bytes 2359304 | tf_op jit(solution)/shard_map/ppermute | solution.py:59
  24.2 56.8 %collective-permute-start.17 = (bf16[512,768]{1,0:T(8,128)(2,1)S(1)}, bf16[512,768]{1,0:T(8,128)(2,1)S(1)}, u32[]{:S(2)}, u32[]{:S(2)}) collective-permute-start(bf16[512,768]{1,0:T(8,128)(2,1)S(1)} %shard_map.190.g0), channel_id=1, source_target_pairs={{0,32},{1,9},{2,34},{3,11},{4,36},{5,13},{6,38},{7,15},{8,40},{9,1... | collective-permute-start | bytes 2359304 | tf_op jit(solution)/shard_map/ppermute | solution.py:59
  33.1 47.9 %collective-permute-start.19 = (bf16[512,768]{1,0:T(8,128)(2,1)S(1)}, bf16[512,768]{1,0:T(8,128)(2,1)S(1)}, u32[]{:S(2)}, u32[]{:S(2)}) collective-permute-start(bf16[512,768]{1,0:T(8,128)(2,1)S(1)} %collective-permute-done.18.g3), channel_id=1, source_target_pairs={{0,96},{1,25},{2,98},{3,27},{4,100},{5,29},{6,102},{7,31},{8,104},... | collective-permute-start | bytes 2359304 | tf_op jit(solution)/shard_map/ppermute | solution.py:59
  36.5 5.7 %collective-permute-start.1 = (bf16[64,768]{1,0:T(8,128)(2,1)S(1)}, bf16[64,768]{1,0:T(8,128)(2,1)S(1)}, u32[]{:S(2)}, u32[]{:S(2)}) collective-permute-start(bf16[64,768]{1,0:T(8,128)(2,1)S(1)} %get-tuple-element.41), channel_id=1, source_target_pairs={{0,32},{1,9},{2,34},{3,11},{4,36},{5,13},{6,38},{7,15},{8,40},{9,1... | collective-permute-start | bytes 294920 | tf_op jit(solution)/shard_map/ppermute | solution.py:59
  36.6 5.7 %collective-permute-start.2 = (bf16[64,768]{1,0:T(8,128)(2,1)S(1)}, bf16[64,768]{1,0:T(8,128)(2,1)S(1)}, u32[]{:S(2)}, u32[]{:S(2)}) collective-permute-start(bf16[64,768]{1,0:T(8,128)(2,1)S(1)} %get-tuple-element.42), channel_id=1, source_target_pairs={{0,64},{1,17},{2,66},{3,19},{4,68},{5,21},{6,70},{7,23},{8,72},{9,... | collective-permute-start | bytes 294920 | tf_op jit(solution)/shard_map/ppermute | solution.py:59
  37.7 9.9 %collective-permute-start.3 = (bf16[64,768]{1,0:T(8,128)(2,1)S(1)}, bf16[64,768]{1,0:T(8,128)(2,1)S(1)}, u32[]{:S(2)}, u32[]{:S(2)}) collective-permute-start(bf16[64,768]{1,0:T(8,128)(2,1)S(1)} %get-tuple-element.43), channel_id=1, source_target_pairs={{0,96},{1,25},{2,98},{3,27},{4,100},{5,29},{6,102},{7,31},{8,104},... | collective-permute-start | bytes 294920 | tf_op jit(solution)/shard_map/ppermute | solution.py:59
  47.6 5.5 %collective-permute-start.4 = (bf16[64,768]{1,0:T(8,128)(2,1)S(1)}, bf16[64,768]{1,0:T(8,128)(2,1)S(1)}, u32[]{:S(2)}, u32[]{:S(2)}) collective-permute-start(bf16[64,768]{1,0:T(8,128)(2,1)S(1)} %shard_map.187.own), channel_id=1, source_target_pairs={{0,8},{1,33},{2,10},{3,35},{4,12},{5,37},{6,14},{7,39},{8,16},{9,4... | collective-permute-start | bytes 294920 | tf_op jit(solution)/shard_map/ppermute | solution.py:59
  47.7 7.6 %collective-permute-start.5 = (bf16[64,768]{1,0:T(8,128)(2,1)S(1)}, bf16[64,768]{1,0:T(8,128)(2,1)S(1)}, u32[]{:S(2)}, u32[]{:S(2)}) collective-permute-start(bf16[64,768]{1,0:T(8,128)(2,1)S(1)} %shard_map.187.own), channel_id=1, source_target_pairs={{0,16},{1,65},{2,18},{3,67},{4,20},{5,69},{6,22},{7,71},{8,24},{9,... | collective-permute-start | bytes 294920 | tf_op jit(solution)/shard_map/ppermute | solution.py:59
  52.3 3.8 %collective-permute-start.6 = (bf16[64,768]{1,0:T(8,128)(2,1)S(1)}, bf16[64,768]{1,0:T(8,128)(2,1)S(1)}, u32[]{:S(2)}, u32[]{:S(2)}) collective-permute-start(bf16[64,768]{1,0:T(8,128)(2,1)S(1)} %shard_map.187.own), channel_id=1, source_target_pairs={{0,24},{1,97},{2,26},{3,99},{4,28},{5,101},{6,30},{7,103},{8,0},{9... | collective-permute-start | bytes 294920 | tf_op jit(solution)/shard_map/ppermute | solution.py:59
  56.3 5.5 %collective-permute-start.10 = (bf16[64,768]{1,0:T(8,128)(2,1)S(1)}, bf16[64,768]{1,0:T(8,128)(2,1)S(1)}, u32[]{:S(2)}, u32[]{:S(2)}) collective-permute-start(bf16[64,768]{1,0:T(8,128)(2,1)S(1)} %get-tuple-element.45.own), channel_id=1, source_target_pairs={{0,32},{1,9},{2,34},{3,11},{4,36},{5,13},{6,38},{7,15},{8,40},{9,1... | collective-permute-start | bytes 294920 | tf_op jit(solution)/shard_map/ppermute | solution.py:59
  56.4 7.6 %collective-permute-start.11 = (bf16[64,768]{1,0:T(8,128)(2,1)S(1)}, bf16[64,768]{1,0:T(8,128)(2,1)S(1)}, u32[]{:S(2)}, u32[]{:S(2)}) collective-permute-start(bf16[64,768]{1,0:T(8,128)(2,1)S(1)} %get-tuple-element.45.own), channel_id=1, source_target_pairs={{0,64},{1,17},{2,66},{3,19},{4,68},{5,21},{6,70},{7,23},{8,72},{9,... | collective-permute-start | bytes 294920 | tf_op jit(solution)/shard_map/ppermute | solution.py:59
  61.0 3.5 %collective-permute-start.12 = (bf16[64,768]{1,0:T(8,128)(2,1)S(1)}, bf16[64,768]{1,0:T(8,128)(2,1)S(1)}, u32[]{:S(2)}, u32[]{:S(2)}) collective-permute-start(bf16[64,768]{1,0:T(8,128)(2,1)S(1)} %get-tuple-element.45.own), channel_id=1, source_target_pairs={{0,96},{1,25},{2,98},{3,27},{4,100},{5,29},{6,102},{7,31},{8,104},... | collective-permute-start | bytes 294920 | tf_op jit(solution)/shard_map/ppermute | solution.py:59
  64.5 5.5 %collective-permute-start.13 = (f32[8,128]{1,0:T(8,128)S(1)}, f32[8,128]{1,0:T(8,128)S(1)}, u32[]{:S(2)}, u32[]{:S(2)}) collective-permute-start(f32[8,128]{1,0:T(8,128)S(1)} %get-tuple-element.46), channel_id=1, source_target_pairs={{0,4},{1,5},{2,6},{3,7},{4,0},{5,1},{6,2},{7,3},{8,12},{9,13},{10,... | collective-permute-start | bytes 12296 | tf_op jit(solution)/shard_map/ppermute | solution.py:59
  67.3 3.7 %collective-permute-start.14 = (f32[8,128]{1,0:T(8,128)S(1)}, f32[8,128]{1,0:T(8,128)S(1)}, u32[]{:S(2)}, u32[]{:S(2)}) collective-permute-start(f32[8,128]{1,0:T(8,128)S(1)} %get-tuple-element.46), channel_id=1, source_target_pairs={{0,2},{1,3},{2,4},{3,5},{4,6},{5,7},{6,0},{7,1},{8,10},{9,11},{10,... | collective-permute-start | bytes 12296 | tf_op jit(solution)/shard_map/ppermute | solution.py:59
  67.7 3.4 %collective-permute-start.15 = (f32[8,128]{1,0:T(8,128)S(1)}, f32[8,128]{1,0:T(8,128)S(1)}, u32[]{:S(2)}, u32[]{:S(2)}) collective-permute-start(f32[8,128]{1,0:T(8,128)S(1)} %get-tuple-element.46), channel_id=1, source_target_pairs={{0,6},{1,7},{2,0},{3,1},{4,2},{5,3},{6,4},{7,5},{8,14},{9,15},{10,... | collective-permute-start | bytes 12296 | tf_op jit(solution)/shard_map/ppermute | solution.py:59
  71.0 10.0 %collective-permute-start.16 = (f32[8,128]{1,0:T(8,128)S(1)}, f32[8,128]{1,0:T(8,128)S(1)}, u32[]{:S(2)}, u32[]{:S(2)}) collective-permute-start(f32[8,128]{1,0:T(8,128)S(1)} %add_add_fusion.s_own), channel_id=1, source_target_pairs={{0,1},{1,0},{2,3},{3,2},{4,5},{5,4},{6,7},{7,6},{8,9},{9,8},{10,11... | collective-permute-start | bytes 12296 | tf_op jit(solution)/shard_map/ppermute | solution.py:59
